TPU v7x, 256 devices: a 8x8x2 block of a 8x8x16 slice. The times are simulated.
256 devices in a mesh: grp: 2 (over z), ep: 16 (over y, core), tp: 8 (over x).
Axes of the slice: x: 8, y: 8, z: 2, core: 2. Of those that a mesh axis runs over, the one named last changes fastest.
The devices are a block of a 8x8x16 slice.
Arguments:
- tokens: bfloat16 [4096, 4096], P(('grp', 'ep'), 'tp'), parts along dimension 0, may hold values from -6 to 6
- routes: int32 [4096, 4], P(('grp', 'ep')), parts along dimension 0, may hold values from 0 to 15, all different within a row; in each aligned block of 128 rows (0 to 127, 128 to 255, ...) at most 64 rows name the same one
- route_weights: float32 [4096, 4], P(('grp', 'ep')), parts along dimension 0, may hold values from 0.1 to 1
- norm_gain: float32 [4096], replicated, may hold values from 0.1 to 1.9
- expert_gate: bfloat16 [16, 4096, 1024], P('ep', 'tp'), may hold values from -0.09375 to 0.09375
- expert_up: bfloat16 [16, 4096, 1024], P('ep', 'tp'), may hold values from -0.09375 to 0.09375
- expert_down: bfloat16 [16, 1024, 4096], P('ep', None, 'tp')
- shared_gate: bfloat16 [4096, 1024], P('tp'), may hold values from -0.09375 to 0.09375
- shared_up: bfloat16 [4096, 1024], P('tp'), may hold values from -0.09375 to 0.09375
- shared_down: bfloat16 [1024, 4096], P(None, 'tp')
- out_gain: float32 [4096], P('tp'), may hold values from 0.1 to 1.9
Outputs:
- layer_out: bfloat16 [4096, 4096], P(('grp', 'ep'), 'tp'), parts along dimension 0
There are 2 independent parts, one for each index of `grp`. A program takes and returns all parts, laid end to end along the dimension named above; an argument that names none is the same for every part. Nothing has to cross between parts.
Inputs may be any that keep to these rules, and one draw needn't show every extreme that they name: `routes`: each row names 4 different experts; among the rows of one index of ep no expert is named more than 64 times, and in some such block some expert is named exactly 64 times.
All inputs are finite; a program needn't handle non-finite values.
Results may differ from a plain program's by a relative error of at most 0.023.
Values may be sent and summed in bfloat16 or wider, within the bound.
No kernel may reach another device: no remote copies, remote signals or barrier semaphores. Data moves between devices by JAX's collectives and lax.ppermute only.
A program may use at most 64 MiB of HBM per device.

v0:
```python
import jax
import jax.numpy as jnp
from jax import lax
from jax.experimental import pallas as pl
from jax.experimental.pallas import tpu as pltpu
from jax.sharding import PartitionSpec as P


epsilon = 1e-06
f32 = jnp.float32
bf16 = jnp.bfloat16


def dot(a, b):
    return jnp.dot(a, b, preferred_element_type=f32)


def ring(count, step):
    return [(i, (i + step) % count) for i in range(count)]


def added(own, came):
    return own if came is None else (own.astype(f32) + came.astype(f32)).astype(bf16)


def reduce_scatter(piece, size, long_way, axis):
    half = size // 2
    ahead, back = ring(size, 1), ring(size, -1)
    f_len, b_len = (half, size - 1 - half) if long_way > 0 else (size - 1 - half, half)
    f = b = None
    for d in range(half, 0, -1):
        if d <= f_len:
            f = lax.ppermute(added(piece[d], f), axis, ahead)
        if d <= b_len:
            b = lax.ppermute(added(piece[size - d], b), axis, back)
    return piece[0].astype(f32) + f.astype(f32) + b.astype(f32)


def all_gather(block, size, long_way, axis):
    half = size // 2
    ahead, back = ring(size, 1), ring(size, -1)
    f_len, b_len = (half, size - 1 - half) if long_way > 0 else (size - 1 - half, half)
    out = {0: block}
    f = b = block
    for d in range(1, half + 1):
        if d <= f_len:
            f = lax.ppermute(f, axis, ahead)
            out[size - d] = f
        if d <= b_len:
            b = lax.ppermute(b, axis, back)
            out[d] = b
    return [out[d] for d in range(size)]


LANES = 128
TILE = 256
IN_VMEM = pl.BlockSpec()
IN_SMEM = pl.BlockSpec(memory_space=pltpu.SMEM)


def block_row(me, d, size, rows):
    return pl.multiple_of(lax.rem(me + d, size) * rows, 16)


def project(me, gain, rows, gate, up, size, streams):
    height, width = rows.shape
    units = gate.shape[1]
    part = height // streams
    count = part // size

    def body(me_ref, gain_ref, rows_ref, gate_ref, up_ref, *refs):
        outs, turned_ref = refs[:-1], refs[-1]
        for k in range(streams * size):
            at = pl.multiple_of(k // size * part + block_row(me_ref[0], k % size, size, count), 16)
            block = rows_ref[pl.ds(at, count), :].astype(f32)
            squares = jnp.sum(block * block, axis=1, keepdims=True)
            outs[k][:, 2 * units :] = jnp.broadcast_to(squares, (count, LANES)).astype(bf16)
            turned_ref[k * count : (k + 1) * count, :] = (block * gain_ref[...]).astype(bf16)

        def columns(n, _):
            at = pl.multiple_of(n * TILE, TILE)
            for ref, base in ((gate_ref, 0), (up_ref, units)):
                value = dot(turned_ref[...], ref[:, pl.ds(at, TILE)]).astype(bf16)
                for k in range(streams * size):
                    outs[k][:, pl.ds(pl.multiple_of(base + at, TILE), TILE)] = value[k * count : (k + 1) * count]
            return 0

        lax.fori_loop(0, units // TILE, columns, 0)

    out = pl.pallas_call(
        body,
        out_shape=[jax.ShapeDtypeStruct((count, 2 * units + LANES), bf16)] * (streams * size),
        in_specs=[IN_SMEM] + [IN_VMEM] * 4,
        out_specs=[IN_VMEM] * (streams * size),
        scratch_shapes=[pltpu.VMEM((height, width), bf16)],
        compiler_params=pltpu.CompilerParams(vmem_limit_bytes=16 << 20),
        name="project",
    )(me, gain, rows, gate, up)
    return [out[k * size : (k + 1) * size] for k in range(streams)]


def lower_down(me, blocks_a, blocks_b, matrix, shared_matrix):
    size = len(blocks_a)
    count, units = blocks_a[0].shape
    shared = blocks_b[0].shape[0] - count
    width = matrix.shape[1]
    part = size * count

    def body(me_ref, *refs):
        ins_a, ins_b = refs[:size], refs[size : 2 * size]
        matrix_ref, shared_ref, out_ref, shared_out_ref, rows_ref, shared_rows_ref = refs[2 * size :]
        for d in range(size):
            at = block_row(me_ref[0], d, size, count)
            rows_ref[pl.ds(at, count), :] = ins_a[d][...]
            rows_ref[pl.ds(pl.multiple_of(part + at, 16), count), :] = ins_b[d][:count, :]
            shared_rows_ref[pl.ds(block_row(me_ref[0], d, size, shared), shared), :] = ins_b[d][count:, :]

        def columns(n, _):
            at = pl.multiple_of(n * TILE, TILE)
            out_ref[:, pl.ds(at, TILE)] = dot(rows_ref[...], matrix_ref[:, pl.ds(at, TILE)]).astype(bf16)
            shared_out_ref[:, pl.ds(at, TILE)] = dot(shared_rows_ref[...], shared_ref[:, pl.ds(at, TILE)])
            return 0

        lax.fori_loop(0, width // TILE, columns, 0)

    return pl.pallas_call(
        body,
        out_shape=[jax.ShapeDtypeStruct((2 * part, width), bf16), jax.ShapeDtypeStruct((size * shared, width), f32)],
        in_specs=[IN_SMEM] + [IN_VMEM] * (2 * size + 2),
        out_specs=[IN_VMEM] * 2,
        scratch_shapes=[pltpu.VMEM((2 * part, units), bf16), pltpu.VMEM((size * shared, units), bf16)],
        compiler_params=pltpu.CompilerParams(vmem_limit_bytes=14 << 20),
        name="lower_down",
    )(me, *blocks_a, *blocks_b, matrix, shared_matrix)


def layer(
    tokens,
    routes,
    route_weights,
    norm_gain,
    expert_gate,
    expert_up,
    expert_down,
    shared_gate,
    shared_up,
    shared_down,
    out_gain,
):
    tok_count, width = tokens.shape
    tp = lax.axis_size("tp")
    experts = lax.axis_size("ep")
    full_width = width * tp
    me_tp = lax.axis_index("tp")
    top_count = routes.shape[1]
    capacity = min(tok_count, 2 * tok_count * top_count // experts)
    gain = lax.dynamic_slice_in_dim(norm_gain, me_tp * width, width, 0)
    gate_matrix, up_matrix, down_matrix = expert_gate[0], expert_up[0], expert_down[0]
    hidden_units = gate_matrix.shape[1]

    expert_ids = lax.broadcasted_iota(jnp.int32, (1, 1, experts), 2)
    hit = routes[:, :, None] == expert_ids
    routed = jnp.any(hit, axis=1)
    weight = jnp.sum(jnp.where(hit, route_weights[:, :, None], 0.0), axis=1)
    lower = (
        lax.broadcasted_iota(jnp.int32, (tok_count, tok_count), 0)
        >= lax.broadcasted_iota(jnp.int32, (tok_count, tok_count), 1)
    ).astype(bf16)
    place = jnp.where(routed, dot(lower, routed.astype(bf16)) - 1.0, -1.0).astype(bf16)
    weight_high = weight.astype(bf16)
    weight_low = (weight - weight_high.astype(f32)).astype(bf16)

    columns = experts * capacity
    column = lax.broadcasted_iota(jnp.int32, (experts, columns), 1)
    expand = (column // capacity == lax.broadcasted_iota(jnp.int32, (experts, columns), 0)).astype(bf16)
    slot = (lax.broadcasted_iota(jnp.int32, (1, columns), 1) % capacity).astype(f32)
    pick = dot(place, expand) == slot
    high = jnp.where(pick, dot(weight_high, expand), 0.0).astype(bf16)
    low = jnp.where(pick, dot(weight_low, expand), 0.0).astype(bf16)

    def swapped(rows):
        return lax.all_to_all(rows.reshape(experts, capacity, width), "ep", 0, 0, tiled=True).reshape(columns, width)

    def hidden_of(total):
        scale = lax.rsqrt(total[:, 2 * hidden_units : 2 * hidden_units + 1] / full_width + epsilon)
        gate_value = total[:, :hidden_units] * scale
        up_value = total[:, hidden_units : 2 * hidden_units] * scale
        return (jax.nn.silu(gate_value) * up_value).astype(bf16)

    me = me_tp.reshape(1)
    gain = gain[None]
    leaving = lax.dot_general(pick.astype(bf16), tokens, (((0,), (0,)), ((), ())), preferred_element_type=f32)
    rows = swapped(leaving.astype(bf16))

    (pieces_s,) = project(me, gain, tokens, shared_gate, shared_up, tp, 1)
    hidden_s = hidden_of(reduce_scatter(pieces_s, tp, 1, "tp"))
    rows, hidden_s = lax.optimization_barrier((rows, hidden_s))

    pieces_a, pieces_b = project(me, gain, rows, gate_matrix, up_matrix, tp, 2)
    total_a = reduce_scatter(pieces_a, tp, -1, "tp")
    total_b = reduce_scatter(pieces_b, tp, 1, "tp")
    blocks_a = all_gather(hidden_of(total_a), tp, 1, "tp")
    blocks_b = all_gather(jnp.concatenate([hidden_of(total_b), hidden_s], 0), tp, -1, "tp")
    down, shared_out = lower_down(me, blocks_a, blocks_b, down_matrix, shared_down)
    came = swapped(down)
    mixture = shared_out + dot(high, came) + dot(low, came)

    square_sum = jnp.sum(mixture * mixture, axis=-1, keepdims=True)
    copies = jnp.broadcast_to(square_sum[None], (tp, *square_sum.shape))
    square_sum = lax.all_to_all(copies, "tp", 0, 0, tiled=True).sum(axis=0)
    scale = lax.rsqrt(square_sum / full_width + epsilon)
    return (mixture * scale * out_gain).astype(bf16)


def solution(mesh):
    return jax.shard_map(
        layer,
        mesh=mesh,
        in_specs=(
            P(("grp", "ep"), "tp"),
            P(("grp", "ep"), None),
            P(("grp", "ep"), None),
            P(),
            P("ep", "tp", None),
            P("ep", "tp", None),
            P("ep", None, "tp"),
            P("tp", None),
            P("tp", None),
            P(None, "tp"),
            P("tp"),
        ),
        out_specs=P(("grp", "ep"), "tp"),
        check_vma=False,
    )
```

profile of v0, /device:TPU:513, one launch (start us, length us, event | category | flops | bytes accessed | tf_op | source)
XLA Modules:
  0.0 192.2 jit_solution(1040017106208128679)
XLA Ops:
  0.0 0.8 dynamic_slice.3
  0.8 1.2 copy-done.4
  2.0 1.2 copy-done.5
  3.2 0.9 copy-done.6
  4.1 1.8 project.2
  5.9 2.2 %collective-permute-start = (bf16[16,2176]{1,0:T(8,128)(2,1)}, bf16[16,2176]{1,0:T(8,128)(2,1)}, u32[]{:S(2)}, u32[]{:S(2)}) collective-permute-start(bf16[16,2176]{1,0:T(8,128)(2,1)} %get-tuple-element.37), channel_id=1, source_target_pairs={{0,1},{1,2},{2,3},{3,4},{4,5},{5,6},{6,7},{7,0},{8,9},{9,10},{10,1... | collective-permute-start | bytes 208904 | tf_op jit(solution)/shard_map/ppermute | solution.py:33
  8.0 2.2 %collective-permute-start.4 = (bf16[16,2176]{1,0:T(8,128)(2,1)}, bf16[16,2176]{1,0:T(8,128)(2,1)}, u32[]{:S(2)}, u32[]{:S(2)}) collective-permute-start(bf16[16,2176]{1,0:T(8,128)(2,1)} %get-tuple-element.40), channel_id=1, source_target_pairs={{0,7},{1,0},{2,1},{3,2},{4,3},{5,4},{6,5},{7,6},{8,15},{9,8},{10,9... | collective-permute-start | bytes 208904 | tf_op jit(solution)/shard_map/ppermute | solution.py:35
  10.7 1.5 convolution_convert_fusion
  12.2 22.9 %all-to-all-start = ((bf16[16,64,512]{2,1,0:T(8,128)(2,1)}), bf16[16,64,512]{2,1,0:T(8,128)(2,1)S(1)}, u32[]{:S(2)}, u32[]{:S(2)}) async-start(bf16[16,64,512]{2,1,0:T(8,128)(2,1)} %bitcast.22), calls=%async_computation | async-start | bytes 2097152 | tf_op jit(solution)/shard_map/all_to_all | solution.py:182
  35.1 1.0 add_convert_fusion.14
  36.3 0.9 add_convert_fusion.11
  37.2 2.8 %collective-permute-start.5 = (bf16[16,2176]{1,0:T(8,128)(2,1)S(1)}, bf16[16,2176]{1,0:T(8,128)(2,1)S(1)}, u32[]{:S(2)}, u32[]{:S(2)}) collective-permute-start(bf16[16,2176]{1,0:T(8,128)(2,1)S(1)} %add_convert_fusion.11), channel_id=1, source_target_pairs={{0,7},{1,0},{2,1},{3,2},{4,3},{5,4},{6,5},{7,6},{8,15},{9,8},{10,9... | collective-permute-start | bytes 208904 | tf_op jit(solution)/shard_map/ppermute | solution.py:35
  39.9 1.0 collective-permute-done.1
  41.3 3.4 %collective-permute-start.6 = (bf16[16,2176]{1,0:T(8,128)(2,1)S(1)}, bf16[16,2176]{1,0:T(8,128)(2,1)S(1)}, u32[]{:S(2)}, u32[]{:S(2)}) collective-permute-start(bf16[16,2176]{1,0:T(8,128)(2,1)S(1)} %add_convert_fusion.10), channel_id=1, source_target_pairs={{0,7},{1,0},{2,1},{3,2},{4,3},{5,4},{6,5},{7,6},{8,15},{9,8},{10,9... | collective-permute-start | bytes 208904 | tf_op jit(solution)/shard_map/ppermute | solution.py:35
  44.7 1.0 collective-permute-done.2
  46.1 4.4 %collective-permute-done.3 = bf16[16,2176]{1,0:T(8,128)(2,1)S(1)} collective-permute-done((bf16[16,2176]{1,0:T(8,128)(2,1)S(1)}, bf16[16,2176]{1,0:T(8,128)(2,1)S(1)}, u32[]{:S(2)}, u32[]{:S(2)}) %collective-permute-start.3) | collective-permute-done | bytes 69664 | tf_op jit(solution)/shard_map/ppermute | solution.py:33
  50.8 12.4 %all-to-all-done = bf16[16,64,512]{2,1,0:T(8,128)(2,1)S(1)} async-done(((bf16[16,64,512]{2,1,0:T(8,128)(2,1)}), bf16[16,64,512]{2,1,0:T(8,128)(2,1)S(1)}, u32[]{:S(2)}, u32[]{:S(2)}) %all-to-all-start) | async-done | bytes 1048608 | tf_op jit(solution)/shard_map/all_to_all | solution.py:182
  63.2 3.2 %project.3 = (bf16[64,2176]{1,0:T(8,128)(2,1)S(1)}, bf16[64,2176]{1,0:T(8,128)(2,1)S(1)}, bf16[64,2176]{1,0:T(8,128)(2,1)S(1)}, bf16[64,2176]{1,0:T(8,128)(2,1)S...) custom-call(s32[1]{0:T(128)} %bitcast.me_ref, ...), custom_call_target="tpu_custom_call" | custom-call | tf_op jit(solution)/shard_map/project/pallas_call | solution.py:90
  66.6 2.6 %collective-permute-start.25 = (bf16[64,2176]{1,0:T(8,128)(2,1)S(1)}, bf16[64,2176]{1,0:T(8,128)(2,1)S(1)}, u32[]{:S(2)}, u32[]{:S(2)}) collective-permute-start(bf16[64,2176]{1,0:T(8,128)(2,1)S(1)} %get-tuple-element.57), channel_id=1, source_target_pairs={{0,7},{1,0},{2,1},{3,2},{4,3},{5,4},{6,5},{7,6},{8,15},{9,8},{10,9... | collective-permute-start | bytes 835592 | tf_op jit(solution)/shard_map/ppermute | solution.py:35
  69.3 2.7 %collective-permute-start.10 = (bf16[64,2176]{1,0:T(8,128)(2,1)S(1)}, bf16[64,2176]{1,0:T(8,128)(2,1)S(1)}, u32[]{:S(2)}, u32[]{:S(2)}) collective-permute-start(bf16[64,2176]{1,0:T(8,128)(2,1)S(1)} %get-tuple-element.49), channel_id=1, source_target_pairs={{0,7},{1,0},{2,1},{3,2},{4,3},{5,4},{6,5},{7,6},{8,15},{9,8},{10,9... | collective-permute-start | bytes 835592 | tf_op jit(solution)/shard_map/ppermute | solution.py:35
  71.9 4.5 %collective-permute-done.21 = bf16[64,2176]{1,0:T(8,128)(2,1)S(1)} collective-permute-done((bf16[64,2176]{1,0:T(8,128)(2,1)S(1)}, bf16[64,2176]{1,0:T(8,128)(2,1)S(1)}, u32[]{:S(2)}, u32[]{:S(2)}) %collective-permute-start.21) | collective-permute-done | bytes 278560 | tf_op jit(solution)/shard_map/ppermute | solution.py:33
  76.9 2.8 %collective-permute-start.26 = (bf16[64,2176]{1,0:T(8,128)(2,1)S(1)}, bf16[64,2176]{1,0:T(8,128)(2,1)S(1)}, u32[]{:S(2)}, u32[]{:S(2)}) collective-permute-start(bf16[64,2176]{1,0:T(8,128)(2,1)S(1)} %add_convert_fusion.1), channel_id=1, source_target_pairs={{0,7},{1,0},{2,1},{3,2},{4,3},{5,4},{6,5},{7,6},{8,15},{9,8},{10,9... | collective-permute-start | bytes 835592 | tf_op jit(solution)/shard_map/ppermute | solution.py:35
  79.7 2.7 %collective-permute-done.7 = bf16[64,2176]{1,0:T(8,128)(2,1)S(1)} collective-permute-done((bf16[64,2176]{1,0:T(8,128)(2,1)S(1)}, bf16[64,2176]{1,0:T(8,128)(2,1)S(1)}, u32[]{:S(2)}, u32[]{:S(2)}) %collective-permute-start.7) | collective-permute-done | bytes 278560 | tf_op jit(solution)/shard_map/ppermute | solution.py:33
  82.7 2.8 %collective-permute-start.11 = (bf16[64,2176]{1,0:T(8,128)(2,1)S(1)}, bf16[64,2176]{1,0:T(8,128)(2,1)S(1)}, u32[]{:S(2)}, u32[]{:S(2)}) collective-permute-start(bf16[64,2176]{1,0:T(8,128)(2,1)S(1)} %add_convert_fusion.7), channel_id=1, source_target_pairs={{0,7},{1,0},{2,1},{3,2},{4,3},{5,4},{6,5},{7,6},{8,15},{9,8},{10,9... | collective-permute-start | bytes 835592 | tf_op jit(solution)/shard_map/ppermute | solution.py:35
  85.5 2.9 %collective-permute-done.22 = bf16[64,2176]{1,0:T(8,128)(2,1)S(1)} collective-permute-done((bf16[64,2176]{1,0:T(8,128)(2,1)S(1)}, bf16[64,2176]{1,0:T(8,128)(2,1)S(1)}, u32[]{:S(2)}, u32[]{:S(2)}) %collective-permute-start.22) | collective-permute-done | bytes 278560 | tf_op jit(solution)/shard_map/ppermute | solution.py:33
  88.7 2.8 %collective-permute-start.27 = (bf16[64,2176]{1,0:T(8,128)(2,1)S(1)}, bf16[64,2176]{1,0:T(8,128)(2,1)S(1)}, u32[]{:S(2)}, u32[]{:S(2)}) collective-permute-start(bf16[64,2176]{1,0:T(8,128)(2,1)S(1)} %add_convert_fusion), channel_id=1, source_target_pairs={{0,7},{1,0},{2,1},{3,2},{4,3},{5,4},{6,5},{7,6},{8,15},{9,8},{10,9... | collective-permute-start | bytes 835592 | tf_op jit(solution)/shard_map/ppermute | solution.py:35
  91.4 2.9 %collective-permute-done.8 = bf16[64,2176]{1,0:T(8,128)(2,1)S(1)} collective-permute-done((bf16[64,2176]{1,0:T(8,128)(2,1)S(1)}, bf16[64,2176]{1,0:T(8,128)(2,1)S(1)}, u32[]{:S(2)}, u32[]{:S(2)}) %collective-permute-start.8) | collective-permute-done | bytes 278560 | tf_op jit(solution)/shard_map/ppermute | solution.py:33
  94.7 2.8 %collective-permute-start.12 = (bf16[64,2176]{1,0:T(8,128)(2,1)S(1)}, bf16[64,2176]{1,0:T(8,128)(2,1)S(1)}, u32[]{:S(2)}, u32[]{:S(2)}) collective-permute-start(bf16[64,2176]{1,0:T(8,128)(2,1)S(1)} %add_convert_fusion.6), channel_id=1, source_target_pairs={{0,7},{1,0},{2,1},{3,2},{4,3},{5,4},{6,5},{7,6},{8,15},{9,8},{10,9... | collective-permute-start | bytes 835592 | tf_op jit(solution)/shard_map/ppermute | solution.py:35
  97.4 2.9 %collective-permute-done.23 = bf16[64,2176]{1,0:T(8,128)(2,1)S(1)} collective-permute-done((bf16[64,2176]{1,0:T(8,128)(2,1)S(1)}, bf16[64,2176]{1,0:T(8,128)(2,1)S(1)}, u32[]{:S(2)}, u32[]{:S(2)}) %collective-permute-start.23) | collective-permute-done | bytes 278560 | tf_op jit(solution)/shard_map/ppermute | solution.py:33
  100.5 4.5 %collective-permute-done.12 = bf16[64,2176]{1,0:T(8,128)(2,1)S(1)} collective-permute-done((bf16[64,2176]{1,0:T(8,128)(2,1)S(1)}, bf16[64,2176]{1,0:T(8,128)(2,1)S(1)}, u32[]{:S(2)}, u32[]{:S(2)}) %collective-permute-start.12) | collective-permute-done | bytes 278560 | tf_op jit(solution)/shard_map/ppermute | solution.py:35
  105.1 3.2 %collective-permute-start.13 = (bf16[64,2176]{1,0:T(8,128)(2,1)S(1)}, bf16[64,2176]{1,0:T(8,128)(2,1)S(1)}, u32[]{:S(2)}, u32[]{:S(2)}) collective-permute-start(bf16[64,2176]{1,0:T(8,128)(2,1)S(1)} %add_convert_fusion.5), channel_id=1, source_target_pairs={{0,7},{1,0},{2,1},{3,2},{4,3},{5,4},{6,5},{7,6},{8,15},{9,8},{10,9... | collective-permute-start | bytes 835592 | tf_op jit(solution)/shard_map/ppermute | solution.py:35
  108.4 2.8 %collective-permute-done.24 = bf16[64,2176]{1,0:T(8,128)(2,1)S(1)} collective-permute-done((bf16[64,2176]{1,0:T(8,128)(2,1)S(1)}, bf16[64,2176]{1,0:T(8,128)(2,1)S(1)}, u32[]{:S(2)}, u32[]{:S(2)}) %collective-permute-start.24) | collective-permute-done | bytes 278560 | tf_op jit(solution)/shard_map/ppermute | solution.py:33
  111.8 2.4 %collective-permute-done.13 = bf16[64,2176]{1,0:T(8,128)(2,1)S(1)} collective-permute-done((bf16[64,2176]{1,0:T(8,128)(2,1)S(1)}, bf16[64,2176]{1,0:T(8,128)(2,1)S(1)}, u32[]{:S(2)}, u32[]{:S(2)}) %collective-permute-start.13) | collective-permute-done | bytes 278560 | tf_op jit(solution)/shard_map/ppermute | solution.py:35
  114.9 2.8 %collective-permute-done.28.refs_9_ = bf16[80,1024]{1,0:T(8,128)(2,1)S(1)} collective-permute-done((bf16[80,1024]{1,0:T(8,128)(2,1)S(1)}, bf16[80,1024]{1,0:T(8,128)(2,1)S(1)}, u32[]{:S(2)}, u32[]{:S(2)}) %collective-permute-start.28) | collective-permute-done | bytes 163872 | tf_op jit(solution)/shard_map/ppermute | solution.py:50
  117.7 3.4 %collective-permute-start.29 = (bf16[80,1024]{1,0:T(8,128)(2,1)S(1)}, bf16[80,1024]{1,0:T(8,128)(2,1)S(1)}, u32[]{:S(2)}, u32[]{:S(2)}) collective-permute-start(bf16[80,1024]{1,0:T(8,128)(2,1)S(1)} %collective-permute-done.28.refs_9_), channel_id=1, source_target_pairs={{0,7},{1,0},{2,1},{3,2},{4,3},{5,4},{6,5},{7,6},{8,15},{9,8},{10,9... | collective-permute-start | bytes 491528 | tf_op jit(solution)/shard_map/ppermute | solution.py:50
  121.1 1.4 collective-permute-start.18
  122.6 1.2 collective-permute-done.32.refs_15_
  123.8 3.2 %collective-permute-start.30 = (bf16[80,1024]{1,0:T(8,128)(2,1)S(1)}, bf16[80,1024]{1,0:T(8,128)(2,1)S(1)}, u32[]{:S(2)}, u32[]{:S(2)}) collective-permute-start(bf16[80,1024]{1,0:T(8,128)(2,1)S(1)} %collective-permute-done.29.refs_10_), channel_id=1, source_target_pairs={{0,7},{1,0},{2,1},{3,2},{4,3},{5,4},{6,5},{7,6},{8,15},{9,8},{10,9... | collective-permute-start | bytes 491528 | tf_op jit(solution)/shard_map/ppermute | solution.py:50
  127.0 2.8 %collective-permute-start.15 = (bf16[64,1024]{1,0:T(8,128)(2,1)S(1)}, bf16[64,1024]{1,0:T(8,128)(2,1)S(1)}, u32[]{:S(2)}, u32[]{:S(2)}) collective-permute-start(bf16[64,1024]{1,0:T(8,128)(2,1)S(1)} %collective-permute-done.14.refs_1_), channel_id=1, source_target_pairs={{0,7},{1,0},{2,1},{3,2},{4,3},{5,4},{6,5},{7,6},{8,15},{9,8},{10,9... | collective-permute-start | bytes 393224 | tf_op jit(solution)/shard_map/ppermute | solution.py:50
  130.3 2.7 %collective-permute-start.31 = (bf16[80,1024]{1,0:T(8,128)(2,1)S(1)}, bf16[80,1024]{1,0:T(8,128)(2,1)S(1)}, u32[]{:S(2)}, u32[]{:S(2)}) collective-permute-start(bf16[80,1024]{1,0:T(8,128)(2,1)S(1)} %collective-permute-done.30.refs_11_), channel_id=1, source_target_pairs={{0,7},{1,0},{2,1},{3,2},{4,3},{5,4},{6,5},{7,6},{8,15},{9,8},{10,9... | collective-permute-start | bytes 491528 | tf_op jit(solution)/shard_map/ppermute | solution.py:50
  133.0 2.7 %collective-permute-start.16 = (bf16[64,1024]{1,0:T(8,128)(2,1)S(1)}, bf16[64,1024]{1,0:T(8,128)(2,1)S(1)}, u32[]{:S(2)}, u32[]{:S(2)}) collective-permute-start(bf16[64,1024]{1,0:T(8,128)(2,1)S(1)} %collective-permute-done.15.refs_2_), channel_id=1, source_target_pairs={{0,7},{1,0},{2,1},{3,2},{4,3},{5,4},{6,5},{7,6},{8,15},{9,8},{10,9... | collective-permute-start | bytes 393224 | tf_op jit(solution)/shard_map/ppermute | solution.py:50
  135.6 2.5 %collective-permute-done.16.refs_3_ = bf16[64,1024]{1,0:T(8,128)(2,1)S(1)} collective-permute-done((bf16[64,1024]{1,0:T(8,128)(2,1)S(1)}, bf16[64,1024]{1,0:T(8,128)(2,1)S(1)}, u32[]{:S(2)}, u32[]{:S(2)}) %collective-permute-start.16) | collective-permute-done | bytes 131104 | tf_op jit(solution)/shard_map/ppermute | solution.py:50
  138.1 3.1 %collective-permute-done.20.refs_4_ = bf16[64,1024]{1,0:T(8,128)(2,1)S(1)} collective-permute-done((bf16[64,1024]{1,0:T(8,128)(2,1)S(1)}, bf16[64,1024]{1,0:T(8,128)(2,1)S(1)}, u32[]{:S(2)}, u32[]{:S(2)}) %collective-permute-start.20) | collective-permute-done | bytes 131104 | tf_op jit(solution)/shard_map/ppermute | solution.py:47
  141.2 2.7 %lower_down.1 = (bf16[1024,512]{1,0:T(8,128)(2,1)}, f32[128,512]{1,0:T(8,128)S(1)}) custom-call(s32[1]{0:T(128)} %bitcast.me_ref, bf16[64,1024]{1,0:T(8,128)(2,1)S(1)} %fusion.9.refs_0_, bf16[64,1024]{1,0:T(8,128)(2,1)S(1)} %collective-permute-done.14.refs_1_, bf16[64,1024]{1,0:T(8,128)(2,1)S(1)} %collective-permute-done.15.refs_2_, ...), custom_call_target="tpu_custom_call" | custom-call | tf_op jit(solution)/shard_map/lower_down/pallas_call | solution.py:126
  144.0 9.5 %all-to-all-start.1 = ((bf16[16,64,512]{2,1,0:T(8,128)(2,1)}), bf16[16,64,512]{2,1,0:T(8,128)(2,1)S(1)}, u32[]{:S(2)}, u32[]{:S(2)}) async-start(bf16[16,64,512]{2,1,0:T(8,128)(2,1)} %bitcast.7), calls=%async_computation.1 | async-start | bytes 2097152 | tf_op jit(solution)/shard_map/all_to_all | solution.py:182
  153.5 28.0 %all-to-all-done.1 = bf16[16,64,512]{2,1,0:T(8,128)(2,1)S(1)} async-done(((bf16[16,64,512]{2,1,0:T(8,128)(2,1)}), bf16[16,64,512]{2,1,0:T(8,128)(2,1)S(1)}, u32[]{:S(2)}, u32[]{:S(2)}) %all-to-all-start.1) | async-done | bytes 1048608 | tf_op jit(solution)/shard_map/all_to_all | solution.py:182
  182.4 9.0 %all_to_all.15 = f32[8,128,1]{1,2,0:T(1,128)S(1)} all-to-all(f32[8,128,1]{1,2,0:T(1,128)S(1)} %broadcast_in_dim.34), channel_id=1, replica_groups=mesh['grp'=2,'ep'=16,'tp'=8] {'tp'}, dimensions={0} | all-to-all | bytes 8192 | tf_op jit(solution)/shard_map/all_to_all | solution.py:210
  191.5 0.8 multiply_convert_fusion
  (97 shorter events, 6.1 us)
Async XLA Ops:
  4.1 6.1 %copy-start.11 = (s32[128,4]{0,1:T(4,128)S(1)}, s32[128,4]{0,1:T(4,128)}, u32[]{:S(2)}) copy-start(s32[128,4]{0,1:T(4,128)} %param.12) | copy-start | bytes 6148
  4.1 6.6 %copy-start.7 = (bf16[128,512]{1,0:T(8,128)(2,1)S(1)}, bf16[128,512]{1,0:T(8,128)(2,1)}, u32[]{:S(2)}) copy-start(bf16[128,512]{1,0:T(8,128)(2,1)} %rows_ref.1) | copy-start | bytes 393220
  5.9 6.3 %copy-start.8 = (bf16[16,2176]{1,0:T(8,128)(2,1)}, bf16[16,2176]{1,0:T(8,128)(2,1)S(1)}, u32[]{:S(2)}) copy-start(bf16[16,2176]{1,0:T(8,128)(2,1)S(1)} %get-tuple-element.36) | copy-start | bytes 208900
  5.9 29.2 %collective-permute-start = (bf16[16,2176]{1,0:T(8,128)(2,1)}, bf16[16,2176]{1,0:T(8,128)(2,1)}, u32[]{:S(2)}, u32[]{:S(2)}) collective-permute-start(bf16[16,2176]{1,0:T(8,128)(2,1)} %get-tuple-element.37), channel_id=1, source_target_pairs={{0,1},{1,2},{2,3},{3,4},{4,5},{5,6},{6,7},{7,0},{8,9},{9,10},{10,1... | collective-permute-start | bytes 208904 | tf_op jit(solution)/shard_map/ppermute | solution.py:33
  8.0 28.2 %collective-permute-start.4 = (bf16[16,2176]{1,0:T(8,128)(2,1)}, bf16[16,2176]{1,0:T(8,128)(2,1)}, u32[]{:S(2)}, u32[]{:S(2)}) collective-permute-start(bf16[16,2176]{1,0:T(8,128)(2,1)} %get-tuple-element.40), channel_id=1, source_target_pairs={{0,7},{1,0},{2,1},{3,2},{4,3},{5,4},{6,5},{7,6},{8,15},{9,8},{10,9... | collective-permute-start | bytes 208904 | tf_op jit(solution)/shard_map/ppermute | solution.py:35
  10.7 1.5 copy-start.9
  12.2 51.0 %copy-start.1 = (bf16[1,512,1024]{2,1,0:T(8,128)(2,1)S(1)}, bf16[1,512,1024]{2,1,0:T(8,128)(2,1)}, u32[]{:S(2)}) copy-start(bf16[1,512,1024]{2,1,0:T(8,128)(2,1)} %param.16) | copy-start | bytes 3145732
  12.2 51.0 %all-to-all-start = ((bf16[16,64,512]{2,1,0:T(8,128)(2,1)}), bf16[16,64,512]{2,1,0:T(8,128)(2,1)S(1)}, u32[]{:S(2)}, u32[]{:S(2)}) async-start(bf16[16,64,512]{2,1,0:T(8,128)(2,1)} %bitcast.22), calls=%async_computation | async-start | bytes 2097152 | tf_op jit(solution)/shard_map/all_to_all | solution.py:182
  35.1 28.1 %copy-start = (bf16[1,512,1024]{2,1,0:T(8,128)(2,1)S(1)}, bf16[1,512,1024]{2,1,0:T(8,128)(2,1)}, u32[]{:S(2)}) copy-start(bf16[1,512,1024]{2,1,0:T(8,128)(2,1)} %param.15) | copy-start | bytes 3145732
  36.1 4.8 %collective-permute-start.1 = (bf16[16,2176]{1,0:T(8,128)(2,1)S(1)}, bf16[16,2176]{1,0:T(8,128)(2,1)S(1)}, u32[]{:S(2)}, u32[]{:S(2)}) collective-permute-start(bf16[16,2176]{1,0:T(8,128)(2,1)S(1)} %add_convert_fusion.14), channel_id=1, source_target_pairs={{0,1},{1,2},{2,3},{3,4},{4,5},{5,6},{6,7},{7,0},{8,9},{9,10},{10,1... | collective-permute-start | bytes 208904 | tf_op jit(solution)/shard_map/ppermute | solution.py:33
  37.2 4.1 %collective-permute-start.5 = (bf16[16,2176]{1,0:T(8,128)(2,1)S(1)}, bf16[16,2176]{1,0:T(8,128)(2,1)S(1)}, u32[]{:S(2)}, u32[]{:S(2)}) collective-permute-start(bf16[16,2176]{1,0:T(8,128)(2,1)S(1)} %add_convert_fusion.11), channel_id=1, source_target_pairs={{0,7},{1,0},{2,1},{3,2},{4,3},{5,4},{6,5},{7,6},{8,15},{9,8},{10,9... | collective-permute-start | bytes 208904 | tf_op jit(solution)/shard_map/ppermute | solution.py:35
  40.9 4.8 %collective-permute-start.2 = (bf16[16,2176]{1,0:T(8,128)(2,1)S(1)}, bf16[16,2176]{1,0:T(8,128)(2,1)S(1)}, u32[]{:S(2)}, u32[]{:S(2)}) collective-permute-start(bf16[16,2176]{1,0:T(8,128)(2,1)S(1)} %add_convert_fusion.13), channel_id=1, source_target_pairs={{0,1},{1,2},{2,3},{3,4},{4,5},{5,6},{6,7},{7,0},{8,9},{9,10},{10,1... | collective-permute-start | bytes 208904 | tf_op jit(solution)/shard_map/ppermute | solution.py:33
  41.3 4.8 %collective-permute-start.6 = (bf16[16,2176]{1,0:T(8,128)(2,1)S(1)}, bf16[16,2176]{1,0:T(8,128)(2,1)S(1)}, u32[]{:S(2)}, u32[]{:S(2)}) collective-permute-start(bf16[16,2176]{1,0:T(8,128)(2,1)S(1)} %add_convert_fusion.10), channel_id=1, source_target_pairs={{0,7},{1,0},{2,1},{3,2},{4,3},{5,4},{6,5},{7,6},{8,15},{9,8},{10,9... | collective-permute-start | bytes 208904 | tf_op jit(solution)/shard_map/ppermute | solution.py:35
  45.7 4.8 %collective-permute-start.3 = (bf16[16,2176]{1,0:T(8,128)(2,1)S(1)}, bf16[16,2176]{1,0:T(8,128)(2,1)S(1)}, u32[]{:S(2)}, u32[]{:S(2)}) collective-permute-start(bf16[16,2176]{1,0:T(8,128)(2,1)S(1)} %add_convert_fusion.12), channel_id=1, source_target_pairs={{0,1},{1,2},{2,3},{3,4},{4,5},{5,6},{6,7},{7,0},{8,9},{9,10},{10,1... | collective-permute-start | bytes 208904 | tf_op jit(solution)/shard_map/ppermute | solution.py:33
  66.5 10.0 %collective-permute-start.21 = (bf16[64,2176]{1,0:T(8,128)(2,1)S(1)}, bf16[64,2176]{1,0:T(8,128)(2,1)S(1)}, u32[]{:S(2)}, u32[]{:S(2)}) collective-permute-start(bf16[64,2176]{1,0:T(8,128)(2,1)S(1)} %get-tuple-element.54), channel_id=1, source_target_pairs={{0,1},{1,2},{2,3},{3,4},{4,5},{5,6},{6,7},{7,0},{8,9},{9,10},{10,1... | collective-permute-start | bytes 835592 | tf_op jit(solution)/shard_map/ppermute | solution.py:33
  66.6 10.3 %collective-permute-start.25 = (bf16[64,2176]{1,0:T(8,128)(2,1)S(1)}, bf16[64,2176]{1,0:T(8,128)(2,1)S(1)}, u32[]{:S(2)}, u32[]{:S(2)}) collective-permute-start(bf16[64,2176]{1,0:T(8,128)(2,1)S(1)} %get-tuple-element.57), channel_id=1, source_target_pairs={{0,7},{1,0},{2,1},{3,2},{4,3},{5,4},{6,5},{7,6},{8,15},{9,8},{10,9... | collective-permute-start | bytes 835592 | tf_op jit(solution)/shard_map/ppermute | solution.py:35
  69.2 13.2 %collective-permute-start.7 = (bf16[64,2176]{1,0:T(8,128)(2,1)S(1)}, bf16[64,2176]{1,0:T(8,128)(2,1)S(1)}, u32[]{:S(2)}, u32[]{:S(2)}) collective-permute-start(bf16[64,2176]{1,0:T(8,128)(2,1)S(1)} %get-tuple-element.45), channel_id=1, source_target_pairs={{0,1},{1,2},{2,3},{3,4},{4,5},{5,6},{6,7},{7,0},{8,9},{9,10},{10,1... | collective-permute-start | bytes 835592 | tf_op jit(solution)/shard_map/ppermute | solution.py:33
  69.3 13.4 %collective-permute-start.10 = (bf16[64,2176]{1,0:T(8,128)(2,1)S(1)}, bf16[64,2176]{1,0:T(8,128)(2,1)S(1)}, u32[]{:S(2)}, u32[]{:S(2)}) collective-permute-start(bf16[64,2176]{1,0:T(8,128)(2,1)S(1)} %get-tuple-element.49), channel_id=1, source_target_pairs={{0,7},{1,0},{2,1},{3,2},{4,3},{5,4},{6,5},{7,6},{8,15},{9,8},{10,9... | collective-permute-start | bytes 835592 | tf_op jit(solution)/shard_map/ppermute | solution.py:35
  76.5 11.9 %collective-permute-start.22 = (bf16[64,2176]{1,0:T(8,128)(2,1)S(1)}, bf16[64,2176]{1,0:T(8,128)(2,1)S(1)}, u32[]{:S(2)}, u32[]{:S(2)}) collective-permute-start(bf16[64,2176]{1,0:T(8,128)(2,1)S(1)} %add_convert_fusion.4), channel_id=1, source_target_pairs={{0,1},{1,2},{2,3},{3,4},{4,5},{5,6},{6,7},{7,0},{8,9},{9,10},{10,1... | collective-permute-start | bytes 835592 | tf_op jit(solution)/shard_map/ppermute | solution.py:33
  76.9 11.7 %collective-permute-start.26 = (bf16[64,2176]{1,0:T(8,128)(2,1)S(1)}, bf16[64,2176]{1,0:T(8,128)(2,1)S(1)}, u32[]{:S(2)}, u32[]{:S(2)}) collective-permute-start(bf16[64,2176]{1,0:T(8,128)(2,1)S(1)} %add_convert_fusion.1), channel_id=1, source_target_pairs={{0,7},{1,0},{2,1},{3,2},{4,3},{5,4},{6,5},{7,6},{8,15},{9,8},{10,9... | collective-permute-start | bytes 835592 | tf_op jit(solution)/shard_map/ppermute | solution.py:35
  82.5 11.9 %collective-permute-start.8 = (bf16[64,2176]{1,0:T(8,128)(2,1)S(1)}, bf16[64,2176]{1,0:T(8,128)(2,1)S(1)}, u32[]{:S(2)}, u32[]{:S(2)}) collective-permute-start(bf16[64,2176]{1,0:T(8,128)(2,1)S(1)} %add_convert_fusion.9), channel_id=1, source_target_pairs={{0,1},{1,2},{2,3},{3,4},{4,5},{5,6},{6,7},{7,0},{8,9},{9,10},{10,1... | collective-permute-start | bytes 835592 | tf_op jit(solution)/shard_map/ppermute | solution.py:33
  82.7 11.9 %collective-permute-start.11 = (bf16[64,2176]{1,0:T(8,128)(2,1)S(1)}, bf16[64,2176]{1,0:T(8,128)(2,1)S(1)}, u32[]{:S(2)}, u32[]{:S(2)}) collective-permute-start(bf16[64,2176]{1,0:T(8,128)(2,1)S(1)} %add_convert_fusion.7), channel_id=1, source_target_pairs={{0,7},{1,0},{2,1},{3,2},{4,3},{5,4},{6,5},{7,6},{8,15},{9,8},{10,9... | collective-permute-start | bytes 835592 | tf_op jit(solution)/shard_map/ppermute | solution.py:35
  88.5 11.9 %collective-permute-start.23 = (bf16[64,2176]{1,0:T(8,128)(2,1)S(1)}, bf16[64,2176]{1,0:T(8,128)(2,1)S(1)}, u32[]{:S(2)}, u32[]{:S(2)}) collective-permute-start(bf16[64,2176]{1,0:T(8,128)(2,1)S(1)} %add_convert_fusion.3), channel_id=1, source_target_pairs={{0,1},{1,2},{2,3},{3,4},{4,5},{5,6},{6,7},{7,0},{8,9},{9,10},{10,1... | collective-permute-start | bytes 835592 | tf_op jit(solution)/shard_map/ppermute | solution.py:33
  88.7 19.7 %collective-permute-start.27 = (bf16[64,2176]{1,0:T(8,128)(2,1)S(1)}, bf16[64,2176]{1,0:T(8,128)(2,1)S(1)}, u32[]{:S(2)}, u32[]{:S(2)}) collective-permute-start(bf16[64,2176]{1,0:T(8,128)(2,1)S(1)} %add_convert_fusion), channel_id=1, source_target_pairs={{0,7},{1,0},{2,1},{3,2},{4,3},{5,4},{6,5},{7,6},{8,15},{9,8},{10,9... | collective-permute-start | bytes 835592 | tf_op jit(solution)/shard_map/ppermute | solution.py:35
  94.4 17.3 %collective-permute-start.9 = (bf16[64,2176]{1,0:T(8,128)(2,1)S(1)}, bf16[64,2176]{1,0:T(8,128)(2,1)S(1)}, u32[]{:S(2)}, u32[]{:S(2)}) collective-permute-start(bf16[64,2176]{1,0:T(8,128)(2,1)S(1)} %add_convert_fusion.8), channel_id=1, source_target_pairs={{0,1},{1,2},{2,3},{3,4},{4,5},{5,6},{6,7},{7,0},{8,9},{9,10},{10,1... | collective-permute-start | bytes 835592 | tf_op jit(solution)/shard_map/ppermute | solution.py:33
  94.7 10.4 %collective-permute-start.12 = (bf16[64,2176]{1,0:T(8,128)(2,1)S(1)}, bf16[64,2176]{1,0:T(8,128)(2,1)S(1)}, u32[]{:S(2)}, u32[]{:S(2)}) collective-permute-start(bf16[64,2176]{1,0:T(8,128)(2,1)S(1)} %add_convert_fusion.6), channel_id=1, source_target_pairs={{0,7},{1,0},{2,1},{3,2},{4,3},{5,4},{6,5},{7,6},{8,15},{9,8},{10,9... | collective-permute-start | bytes 835592 | tf_op jit(solution)/shard_map/ppermute | solution.py:35
  100.4 10.8 %collective-permute-start.24 = (bf16[64,2176]{1,0:T(8,128)(2,1)S(1)}, bf16[64,2176]{1,0:T(8,128)(2,1)S(1)}, u32[]{:S(2)}, u32[]{:S(2)}) collective-permute-start(bf16[64,2176]{1,0:T(8,128)(2,1)S(1)} %add_convert_fusion.2), channel_id=1, source_target_pairs={{0,1},{1,2},{2,3},{3,4},{4,5},{5,6},{6,7},{7,0},{8,9},{9,10},{10,1... | collective-permute-start | bytes 835592 | tf_op jit(solution)/shard_map/ppermute | solution.py:33
  105.1 9.1 %collective-permute-start.13 = (bf16[64,2176]{1,0:T(8,128)(2,1)S(1)}, bf16[64,2176]{1,0:T(8,128)(2,1)S(1)}, u32[]{:S(2)}, u32[]{:S(2)}) collective-permute-start(bf16[64,2176]{1,0:T(8,128)(2,1)S(1)} %add_convert_fusion.5), channel_id=1, source_target_pairs={{0,7},{1,0},{2,1},{3,2},{4,3},{5,4},{6,5},{7,6},{8,15},{9,8},{10,9... | collective-permute-start | bytes 835592 | tf_op jit(solution)/shard_map/ppermute | solution.py:35
  111.6 29.6 %copy-start.3 = (bf16[1024,512]{1,0:T(8,128)(2,1)S(1)}, bf16[1024,512]{1,0:T(8,128)(2,1)}, u32[]{:S(2)}) copy-start(bf16[1024,512]{1,0:T(8,128)(2,1)} %refs_17_.1) | copy-start | bytes 3145732
  111.6 29.6 %copy-start.2 = (bf16[1,1024,512]{2,1,0:T(8,128)(2,1)S(1)}, bf16[1,1024,512]{2,1,0:T(8,128)(2,1)}, u32[]{:S(2)}) copy-start(bf16[1,1024,512]{2,1,0:T(8,128)(2,1)} %param.17) | copy-start | bytes 3145732
  111.6 6.1 %collective-permute-start.28 = (bf16[80,1024]{1,0:T(8,128)(2,1)S(1)}, bf16[80,1024]{1,0:T(8,128)(2,1)S(1)}, u32[]{:S(2)}, u32[]{:S(2)}) collective-permute-start(bf16[80,1024]{1,0:T(8,128)(2,1)S(1)} %pad_maximum_fusion.refs_8_), channel_id=1, source_target_pairs={{0,7},{1,0},{2,1},{3,2},{4,3},{5,4},{6,5},{7,6},{8,15},{9,8},{10,9... | collective-permute-start | bytes 491528 | tf_op jit(solution)/shard_map/ppermute | solution.py:50
  114.6 6.6 %collective-permute-start.17 = (bf16[64,1024]{1,0:T(8,128)(2,1)S(1)}, bf16[64,1024]{1,0:T(8,128)(2,1)S(1)}, u32[]{:S(2)}, u32[]{:S(2)}) collective-permute-start(bf16[64,1024]{1,0:T(8,128)(2,1)S(1)} %fusion.9.refs_0_), channel_id=1, source_target_pairs={{0,1},{1,2},{2,3},{3,4},{4,5},{5,6},{6,7},{7,0},{8,9},{9,10},{10,1... | collective-permute-start | bytes 393224 | tf_op jit(solution)/shard_map/ppermute | solution.py:47
  114.7 9.1 %collective-permute-start.32 = (bf16[80,1024]{1,0:T(8,128)(2,1)S(1)}, bf16[80,1024]{1,0:T(8,128)(2,1)S(1)}, u32[]{:S(2)}, u32[]{:S(2)}) collective-permute-start(bf16[80,1024]{1,0:T(8,128)(2,1)S(1)} %pad_maximum_fusion.refs_8_), channel_id=1, source_target_pairs={{0,1},{1,2},{2,3},{3,4},{4,5},{5,6},{6,7},{7,0},{8,9},{9,10},{10,1... | collective-permute-start | bytes 491528 | tf_op jit(solution)/shard_map/ppermute | solution.py:47
  117.7 6.1 %collective-permute-start.29 = (bf16[80,1024]{1,0:T(8,128)(2,1)S(1)}, bf16[80,1024]{1,0:T(8,128)(2,1)S(1)}, u32[]{:S(2)}, u32[]{:S(2)}) collective-permute-start(bf16[80,1024]{1,0:T(8,128)(2,1)S(1)} %collective-permute-done.28.refs_9_), channel_id=1, source_target_pairs={{0,7},{1,0},{2,1},{3,2},{4,3},{5,4},{6,5},{7,6},{8,15},{9,8},{10,9... | collective-permute-start | bytes 491528 | tf_op jit(solution)/shard_map/ppermute | solution.py:50
  121.1 5.9 %collective-permute-start.14 = (bf16[64,1024]{1,0:T(8,128)(2,1)S(1)}, bf16[64,1024]{1,0:T(8,128)(2,1)S(1)}, u32[]{:S(2)}, u32[]{:S(2)}) collective-permute-start(bf16[64,1024]{1,0:T(8,128)(2,1)S(1)} %fusion.9.refs_0_), channel_id=1, source_target_pairs={{0,7},{1,0},{2,1},{3,2},{4,3},{5,4},{6,5},{7,6},{8,15},{9,8},{10,9... | collective-permute-start | bytes 393224 | tf_op jit(solution)/shard_map/ppermute | solution.py:50
  121.1 8.7 %collective-permute-start.18 = (bf16[64,1024]{1,0:T(8,128)(2,1)S(1)}, bf16[64,1024]{1,0:T(8,128)(2,1)S(1)}, u32[]{:S(2)}, u32[]{:S(2)}) collective-permute-start(bf16[64,1024]{1,0:T(8,128)(2,1)S(1)} %collective-permute-done.17.refs_7_), channel_id=1, source_target_pairs={{0,1},{1,2},{2,3},{3,4},{4,5},{5,6},{6,7},{7,0},{8,9},{9,10},{10,1... | collective-permute-start | bytes 393224 | tf_op jit(solution)/shard_map/ppermute | solution.py:47
  123.8 6.5 %collective-permute-start.33 = (bf16[80,1024]{1,0:T(8,128)(2,1)S(1)}, bf16[80,1024]{1,0:T(8,128)(2,1)S(1)}, u32[]{:S(2)}, u32[]{:S(2)}) collective-permute-start(bf16[80,1024]{1,0:T(8,128)(2,1)S(1)} %collective-permute-done.32.refs_15_), channel_id=1, source_target_pairs={{0,1},{1,2},{2,3},{3,4},{4,5},{5,6},{6,7},{7,0},{8,9},{9,10},{10,1... | collective-permute-start | bytes 491528 | tf_op jit(solution)/shard_map/ppermute | solution.py:47
  123.8 6.5 %collective-permute-start.30 = (bf16[80,1024]{1,0:T(8,128)(2,1)S(1)}, bf16[80,1024]{1,0:T(8,128)(2,1)S(1)}, u32[]{:S(2)}, u32[]{:S(2)}) collective-permute-start(bf16[80,1024]{1,0:T(8,128)(2,1)S(1)} %collective-permute-done.29.refs_10_), channel_id=1, source_target_pairs={{0,7},{1,0},{2,1},{3,2},{4,3},{5,4},{6,5},{7,6},{8,15},{9,8},{10,9... | collective-permute-start | bytes 491528 | tf_op jit(solution)/shard_map/ppermute | solution.py:50
  127.0 5.9 %collective-permute-start.15 = (bf16[64,1024]{1,0:T(8,128)(2,1)S(1)}, bf16[64,1024]{1,0:T(8,128)(2,1)S(1)}, u32[]{:S(2)}, u32[]{:S(2)}) collective-permute-start(bf16[64,1024]{1,0:T(8,128)(2,1)S(1)} %collective-permute-done.14.refs_1_), channel_id=1, source_target_pairs={{0,7},{1,0},{2,1},{3,2},{4,3},{5,4},{6,5},{7,6},{8,15},{9,8},{10,9... | collective-permute-start | bytes 393224 | tf_op jit(solution)/shard_map/ppermute | solution.py:50
  129.9 5.8 %collective-permute-start.19 = (bf16[64,1024]{1,0:T(8,128)(2,1)S(1)}, bf16[64,1024]{1,0:T(8,128)(2,1)S(1)}, u32[]{:S(2)}, u32[]{:S(2)}) collective-permute-start(bf16[64,1024]{1,0:T(8,128)(2,1)S(1)} %collective-permute-done.18.refs_6_), channel_id=1, source_target_pairs={{0,1},{1,2},{2,3},{3,4},{4,5},{5,6},{6,7},{7,0},{8,9},{9,10},{10,1... | collective-permute-start | bytes 393224 | tf_op jit(solution)/shard_map/ppermute | solution.py:47
  130.3 7.8 %collective-permute-start.34 = (bf16[80,1024]{1,0:T(8,128)(2,1)S(1)}, bf16[80,1024]{1,0:T(8,128)(2,1)S(1)}, u32[]{:S(2)}, u32[]{:S(2)}) collective-permute-start(bf16[80,1024]{1,0:T(8,128)(2,1)S(1)} %collective-permute-done.33.refs_14_), channel_id=1, source_target_pairs={{0,1},{1,2},{2,3},{3,4},{4,5},{5,6},{6,7},{7,0},{8,9},{9,10},{10,1... | collective-permute-start | bytes 491528 | tf_op jit(solution)/shard_map/ppermute | solution.py:47
  130.3 10.9 %collective-permute-start.31 = (bf16[80,1024]{1,0:T(8,128)(2,1)S(1)}, bf16[80,1024]{1,0:T(8,128)(2,1)S(1)}, u32[]{:S(2)}, u32[]{:S(2)}) collective-permute-start(bf16[80,1024]{1,0:T(8,128)(2,1)S(1)} %collective-permute-done.30.refs_11_), channel_id=1, source_target_pairs={{0,7},{1,0},{2,1},{3,2},{4,3},{5,4},{6,5},{7,6},{8,15},{9,8},{10,9... | collective-permute-start | bytes 491528 | tf_op jit(solution)/shard_map/ppermute | solution.py:50
  133.0 5.1 %collective-permute-start.16 = (bf16[64,1024]{1,0:T(8,128)(2,1)S(1)}, bf16[64,1024]{1,0:T(8,128)(2,1)S(1)}, u32[]{:S(2)}, u32[]{:S(2)}) collective-permute-start(bf16[64,1024]{1,0:T(8,128)(2,1)S(1)} %collective-permute-done.15.refs_2_), channel_id=1, source_target_pairs={{0,7},{1,0},{2,1},{3,2},{4,3},{5,4},{6,5},{7,6},{8,15},{9,8},{10,9... | collective-permute-start | bytes 393224 | tf_op jit(solution)/shard_map/ppermute | solution.py:50
  135.6 5.6 %collective-permute-start.20 = (bf16[64,1024]{1,0:T(8,128)(2,1)S(1)}, bf16[64,1024]{1,0:T(8,128)(2,1)S(1)}, u32[]{:S(2)}, u32[]{:S(2)}) collective-permute-start(bf16[64,1024]{1,0:T(8,128)(2,1)S(1)} %collective-permute-done.19.refs_5_), channel_id=1, source_target_pairs={{0,1},{1,2},{2,3},{3,4},{4,5},{5,6},{6,7},{7,0},{8,9},{9,10},{10,1... | collective-permute-start | bytes 393224 | tf_op jit(solution)/shard_map/ppermute | solution.py:47
  144.0 9.5 %copy-start.13 = (f32[128,4]{0,1:T(4,128)S(1)}, f32[128,4]{0,1:T(4,128)}, u32[]{:S(2)}) copy-start(f32[128,4]{0,1:T(4,128)} %param.13) | copy-start | bytes 6148
  144.0 37.5 %copy-start.10 = (pred[128,1024]{1,0:T(32,128)(4,1)S(1)}, pred[128,1024]{1,0:T(32,128)(4,1)}, u32[]{:S(2)}) copy-start(pred[128,1024]{1,0:T(32,128)(4,1)} %copy-done.9) | copy-start | bytes 393220
  144.0 37.5 %all-to-all-start.1 = ((bf16[16,64,512]{2,1,0:T(8,128)(2,1)}), bf16[16,64,512]{2,1,0:T(8,128)(2,1)S(1)}, u32[]{:S(2)}, u32[]{:S(2)}) async-start(bf16[16,64,512]{2,1,0:T(8,128)(2,1)} %bitcast.7), calls=%async_computation.1 | async-start | bytes 2097152 | tf_op jit(solution)/shard_map/all_to_all | solution.py:182
  181.9 9.6 %copy-start.12 = (f32[512]{0:T(512)S(1)}, f32[512]{0:T(512)}, u32[]{:S(2)}) copy-start(f32[512]{0:T(512)} %param.21) | copy-start | bytes 6148
  (3 other events, 3.4 us)
where the time goes:
time: 193 us; the launch traced here: 192 us
  waiting for transfers between devices  83.1 us (43%)
  starting transfers between devices  80.4 us (42%)
  blocking collectives  8.97 us (5%)
  Pallas kernels  7.75 us (4%)
  other arithmetic  4.54 us (2%)
  local copies, waits for them, and re-layouts  4.17 us (2%)
  matrix products  2.87 us (1%)
    all_to_all x2, waiting for transfers between devices, swapped(): lax.all_to_all(rows.reshape(experts, capacity, width), 'ep', 0, 0, tiled=...  40.4 us
    all_to_all x2, starting transfers between devices, swapped(): lax.all_to_all(rows.reshape(experts, capacity, width), 'ep', 0, 0, tiled=...  32.3 us
    ppermute x10, starting transfers between devices, reduce_scatter(): b = lax.ppermute(added(piece[size - d], b), axis, back)  27.9 us
    ppermute x11, waiting for transfers between devices, reduce_scatter(): f = lax.ppermute(added(piece[d], f), axis, ahead)  25.2 us
    ppermute x7, starting transfers between devices, all_gather(): b = lax.ppermute(b, axis, back)  14.9 us
    all_to_all x1, blocking collectives, layer(): square_sum = lax.all_to_all(copies, 'tp', 0, 0, tiled=True).sum(axis=0)  8.97 us
    ppermute x10, waiting for transfers between devices, reduce_scatter(): b = lax.ppermute(added(piece[size - d], b), axis, back)  7.44 us
    ppermute x7, waiting for transfers between devices, all_gather(): b = lax.ppermute(b, axis, back)  5.31 us
  transfers between devices with their start and end apart: 37, of which 20 were waited for; matrix products, arithmetic and copies ran while one was open for 3% of the time, Pallas kernels for 0%

commit v1 on v0

v1 whole, which is shorter than its diff:
```python
import jax
import jax.numpy as jnp
from jax import lax
from jax.experimental import pallas as pl
from jax.experimental.pallas import tpu as pltpu
from jax.sharding import PartitionSpec as P


epsilon = 1e-06
f32 = jnp.float32
bf16 = jnp.bfloat16


def dot(a, b):
    return jnp.dot(a, b, preferred_element_type=f32)


def ring(count, step):
    return [(i, (i + step) % count) for i in range(count)]


def added(own, came):
    return own if came is None else (own.astype(f32) + came.astype(f32)).astype(bf16)


def held(values, waited):
    if not waited:
        return values
    return lax.optimization_barrier((tuple(values), tuple(waited)))[0]


class Stream:
    def __init__(self, pieces, size, axis, long_way):
        self.pieces, self.size, self.axis = pieces, size, axis
        self.ways = (ring(size, 1), ring(size, -1))
        half = size // 2
        self.lengths = (half, size - 1 - half) if long_way > 0 else (size - 1 - half, half)
        self.came = [None, None]

    def sent(self, values, waited):
        came = [None, None]
        for i in (0, 1):
            if values[i] is not None:
                value = values[i] if waited[i] is None else held([values[i]], [waited[i]])[0]
                came[i] = self.came[i] = lax.ppermute(value, self.axis, self.ways[i])
        return came

    def scatter(self, step, waited):
        d = self.size // 2 - step
        places = (d, self.size - d)
        values = [added(self.pieces[places[i]], self.came[i]) if d <= self.lengths[i] else None for i in (0, 1)]
        return self.sent(values, waited)

    def total(self):
        return sum((v.astype(f32) for v in self.came), self.pieces[0].astype(f32))

    def open(self, block):
        self.blocks = {0: block}
        self.came = [block, block]
        self.lengths = self.lengths[::-1]

    def gather(self, step, waited):
        d = step + 1
        came = self.sent([self.came[i] if d <= self.lengths[i] else None for i in (0, 1)], waited)
        for i, place in ((0, self.size - d), (1, d)):
            if d <= self.lengths[i]:
                self.blocks[place] = self.came[i]
        return came

    def gathered(self):
        return [self.blocks[d] for d in range(self.size)]


LANES = 128
TILE = 256
IN_VMEM = pl.BlockSpec()
IN_SMEM = pl.BlockSpec(memory_space=pltpu.SMEM)


def block_row(me, d, size, rows):
    return pl.multiple_of(lax.rem(me + d, size) * rows, 16)


def project(me, gain, rows, gate, up, size, space):
    height, width = rows.shape
    units = gate.shape[1]
    count = height // size

    def body(me_ref, gain_ref, rows_ref, gate_ref, up_ref, *refs):
        outs, turned_ref = refs[:-1], refs[-1]
        for d in range(size):
            block = rows_ref[pl.ds(block_row(me_ref[0], d, size, count), count), :].astype(f32)
            squares = jnp.sum(block * block, axis=1, keepdims=True)
            outs[d][:, 2 * units :] = jnp.broadcast_to(squares, (count, LANES)).astype(bf16)
            turned_ref[d * count : (d + 1) * count, :] = (block * gain_ref[...]).astype(bf16)

        def columns(n, _):
            at = pl.multiple_of(n * TILE, TILE)
            for ref, base in ((gate_ref, 0), (up_ref, units)):
                value = dot(turned_ref[...], ref[:, pl.ds(at, TILE)]).astype(bf16)
                for d in range(size):
                    outs[d][:, pl.ds(pl.multiple_of(base + at, TILE), TILE)] = value[d * count : (d + 1) * count]
            return 0

        lax.fori_loop(0, units // TILE, columns, 0)

    return pl.pallas_call(
        body,
        out_shape=[space((count, 2 * units + LANES), bf16)] * size,
        in_specs=[IN_SMEM] + [IN_VMEM] * 4,
        out_specs=[IN_VMEM] * size,
        scratch_shapes=[pltpu.VMEM((height, width), bf16)],
        compiler_params=pltpu.CompilerParams(vmem_limit_bytes=12 << 20),
        name="project",
    )(me, gain, rows, gate, up)


def lower_down(me, blocks, sinks):
    size = len(blocks)
    units = blocks[0].shape[1]
    counts = [count for count, _, _ in sinks]
    width = sinks[0][1].shape[1]

    def body(me_ref, *refs):
        ins, mats = refs[:size], refs[size : size + len(counts)]
        outs, scratch = refs[size + len(counts) : size + 2 * len(counts)], refs[size + 2 * len(counts) :]
        first = 0
        for i, count in enumerate(counts):
            for d in range(size):
                scratch[i][pl.ds(block_row(me_ref[0], d, size, count), count), :] = ins[d][first : first + count, :]

            def columns(n, _, i=i):
                at = pl.multiple_of(n * TILE, TILE)
                outs[i][:, pl.ds(at, TILE)] = dot(scratch[i][...], mats[i][:, pl.ds(at, TILE)]).astype(outs[i].dtype)
                return 0

            lax.fori_loop(0, width // TILE, columns, 0)
            first += count

    return pl.pallas_call(
        body,
        out_shape=[jax.ShapeDtypeStruct((size * count, width), kind) for count, _, kind in sinks],
        in_specs=[IN_SMEM] + [IN_VMEM] * (size + len(counts)),
        out_specs=[IN_VMEM] * len(counts),
        scratch_shapes=[pltpu.VMEM((size * count, units), bf16) for count in counts],
        compiler_params=pltpu.CompilerParams(vmem_limit_bytes=12 << 20),
        name="lower_down",
    )(me, *blocks, *[matrix for _, matrix, _ in sinks])


def layer(
    tokens,
    routes,
    route_weights,
    norm_gain,
    expert_gate,
    expert_up,
    expert_down,
    shared_gate,
    shared_up,
    shared_down,
    out_gain,
):
    tok_count, width = tokens.shape
    tp = lax.axis_size("tp")
    experts = lax.axis_size("ep")
    full_width = width * tp
    me_tp = lax.axis_index("tp")
    top_count = routes.shape[1]
    capacity = min(tok_count, 2 * tok_count * top_count // experts)
    gain = lax.dynamic_slice_in_dim(norm_gain, me_tp * width, width, 0)
    gate_matrix, up_matrix, down_matrix = expert_gate[0], expert_up[0], expert_down[0]
    hidden_units = gate_matrix.shape[1]

    expert_ids = lax.broadcasted_iota(jnp.int32, (1, 1, experts), 2)
    hit = routes[:, :, None] == expert_ids
    routed = jnp.any(hit, axis=1)
    weight = jnp.sum(jnp.where(hit, route_weights[:, :, None], 0.0), axis=1)
    lower = (
        lax.broadcasted_iota(jnp.int32, (tok_count, tok_count), 0)
        >= lax.broadcasted_iota(jnp.int32, (tok_count, tok_count), 1)
    ).astype(bf16)
    place = jnp.where(routed, dot(lower, routed.astype(bf16)) - 1.0, -1.0).astype(bf16)
    weight_high = weight.astype(bf16)
    weight_low = (weight - weight_high.astype(f32)).astype(bf16)

    part = capacity // 2
    columns = experts * part
    column = lax.broadcasted_iota(jnp.int32, (experts, 2 * columns), 1)
    expand = (column % columns // part == lax.broadcasted_iota(jnp.int32, (experts, 2 * columns), 0)).astype(bf16)
    column = lax.broadcasted_iota(jnp.int32, (1, 2 * columns), 1)
    slot = (column // columns * part + column % part).astype(f32)
    pick = dot(place, expand) == slot
    high = jnp.where(pick, dot(weight_high, expand), 0.0).astype(bf16)
    low = jnp.where(pick, dot(weight_low, expand), 0.0).astype(bf16)

    def swapped(rows):
        return lax.all_to_all(rows.reshape(experts, part, width), "ep", 0, 0, tiled=True).reshape(columns, width)

    def hidden_of(total):
        scale = lax.rsqrt(total[:, 2 * hidden_units : 2 * hidden_units + 1] / full_width + epsilon)
        gate_value = total[:, :hidden_units] * scale
        up_value = total[:, hidden_units : 2 * hidden_units] * scale
        return (jax.nn.silu(gate_value) * up_value).astype(bf16)

    me = me_tp.reshape(1)
    gain = gain[None]
    leaving = lax.dot_general(pick.astype(bf16), tokens, (((0,), (0,)), ((), ())), preferred_element_type=f32)
    leaving = leaving.astype(bf16)
    rows_a = swapped(leaving[:columns])
    (leaving_b,) = held([leaving[columns:]], [rows_a])
    rows_b = swapped(leaving_b)

    steps = tp // 2
    shared = Stream(project(me, gain, tokens, shared_gate, shared_up, tp, jax.ShapeDtypeStruct), tp, "tp", 1)
    for step in range(steps):
        shared.scatter(step, [None, None])
    hidden_s = hidden_of(shared.total())

    a = Stream(project(me, gain, rows_a, gate_matrix, up_matrix, tp, pltpu.HBM), tp, "tp", -1)
    b = Stream(project(me, gain, rows_b, gate_matrix, up_matrix, tp, jax.ShapeDtypeStruct), tp, "tp", 1)

    done = {id(a): 0, id(b): 0}
    came = []
    for stream in [a] + [a, b] * (2 * steps - 1) + [b]:
        step = done[id(stream)]
        done[id(stream)] += 1
        waited = came[-3] if len(came) > 2 else [None, None]
        if step < steps:
            came.append(stream.scatter(step, waited))
            continue
        if step == steps:
            hidden = hidden_of(stream.total())
            stream.open(jnp.concatenate([hidden, hidden_s], 0) if stream is a else hidden)
        came.append(stream.gather(step - steps, waited))

    shared_rows = tok_count // tp
    blocks_a, blocks_b = a.gathered(), b.gathered()
    down_a, shared_out = lower_down(
        me,
        blocks_a,
        [(blocks_b[0].shape[0], down_matrix, bf16), (shared_rows, shared_down, f32)],
    )
    back_a = swapped(down_a)
    (down_b,) = lower_down(me, blocks_b, [(blocks_b[0].shape[0], down_matrix, bf16)])
    (down_b,) = held([down_b], [back_a])
    back_b = swapped(down_b)
    mixture = shared_out + dot(high[:, :columns], back_a) + dot(low[:, :columns], back_a)
    mixture = mixture + dot(high[:, columns:], back_b) + dot(low[:, columns:], back_b)

    square_sum = jnp.sum(mixture * mixture, axis=-1, keepdims=True)
    copies = jnp.broadcast_to(square_sum[None], (tp, *square_sum.shape))
    square_sum = lax.all_to_all(copies, "tp", 0, 0, tiled=True).sum(axis=0)
    scale = lax.rsqrt(square_sum / full_width + epsilon)
    return (mixture * scale * out_gain).astype(bf16)


def solution(mesh):
    return jax.shard_map(
        layer,
        mesh=mesh,
        in_specs=(
            P(("grp", "ep"), "tp"),
            P(("grp", "ep"), None),
            P(("grp", "ep"), None),
            P(),
            P("ep", "tp", None),
            P("ep", "tp", None),
            P("ep", None, "tp"),
            P("tp", None),
            P("tp", None),
            P(None, "tp"),
            P("tp"),
        ),
        out_specs=P(("grp", "ep"), "tp"),
        check_vma=False,
    )
```

time: 193 us -> 217 us (1.12)
  starting transfers between devices: 80.4 us -> 96.7 us
  waiting for transfers between devices: 83.1 us -> 86.4 us
  Pallas kernels: 7.75 us -> 10.2 us
    ppermute x35, waiting for transfers between devices: 42.7 us -> 64.4 us  [sent(): came[i] = self.came[i] = lax.ppermute(value, self.axis, self.ways[i])]
    all_to_all x2 -> x4, starting transfers between devices: 32.3 us -> 53 us  [swapped(): lax.all_to_all(rows.reshape(experts, part, width), 'ep', 0, 0, tiled=True)]
    all_to_all x2 -> x4, waiting for transfers between devices: 40.4 us -> 22.1 us  [swapped(): lax.all_to_all(rows.reshape(experts, part, width), 'ep', 0, 0, tiled=True)]
    ppermute x35, starting transfers between devices: 48.1 us -> 43.7 us  [sent(): came[i] = self.came[i] = lax.ppermute(value, self.axis, self.ways[i])]
    pallas_call x3 -> x5, Pallas kernels: 7.75 us -> 10.2 us  [the longest x3 6.46 us: project(): pl.pallas_call(body, out_shape=[space((count, 2 * units + LANES), bf16)]...]
  transfers between devices with their start and end apart: 37 -> 39, of which waited for: 20 -> 24; matrix products, arithmetic and copies ran while one was open for 3% -> 3% of each run, Pallas kernels for 0% -> 2%
where the time goes in v1:
time: 217 us; the launch traced here: 216 us
  starting transfers between devices  96.7 us (45%)
  waiting for transfers between devices  86.4 us (40%)
  blocking collectives  11 us (5%)
  Pallas kernels  10.2 us (5%)
  local copies, waits for them, and re-layouts  5.25 us (2%)
  other arithmetic  3.74 us (2%)
  matrix products  2.32 us (1%)
    ppermute x35, waiting for transfers between devices, sent(): came[i] = self.came[i] = lax.ppermute(value, self.axis, self.ways[i])  64.4 us
    all_to_all x4, starting transfers between devices, swapped(): lax.all_to_all(rows.reshape(experts, part, width), 'ep', 0, 0, tiled=True)  53 us
    ppermute x35, starting transfers between devices, sent(): came[i] = self.came[i] = lax.ppermute(value, self.axis, self.ways[i])  43.7 us
    all_to_all x4, waiting for transfers between devices, swapped(): lax.all_to_all(rows.reshape(experts, part, width), 'ep', 0, 0, tiled=True)  22.1 us
    all_to_all x1, blocking collectives, layer(): square_sum = lax.all_to_all(copies, 'tp', 0, 0, tiled=True).sum(axis=0)  11 us
    pallas_call x3, Pallas kernels, project(): pl.pallas_call(body, out_shape=[space((count, 2 * units + LANES), bf16)]...  6.46 us
  transfers between devices with their start and end apart: 39, of which 24 were waited for; matrix products, arithmetic and copies ran while one was open for 3% of the time, Pallas kernels for 2%

profile of v1, /device:TPU:513, one launch (start us, length us, event | category | flops | bytes accessed | tf_op | source)
XLA Modules:
  0.0 216.2 jit_solution(157166866502775695)
XLA Ops:
  0.8 1.2 copy-done.3
  2.0 1.2 copy-done.4
  4.1 1.1 project.5
  5.2 2.3 %collective-permute-start.8 = (bf16[16,2176]{1,0:T(8,128)(2,1)S(1)}, bf16[16,2176]{1,0:T(8,128)(2,1)S(1)}, u32[]{:S(2)}, u32[]{:S(2)}) collective-permute-start(bf16[16,2176]{1,0:T(8,128)(2,1)S(1)} %get-tuple-element.71), channel_id=1, source_target_pairs={{0,1},{1,2},{2,3},{3,4},{4,5},{5,6},{6,7},{7,0},{8,9},{9,10},{10,1... | collective-permute-start | bytes 208904 | tf_op jit(solution)/shard_map/ppermute | solution.py:45
  8.5 1.1 fusion.55
  9.5 22.0 %all-to-all-start = ((bf16[16,32,512]{2,1,0:T(8,128)(2,1)}), bf16[16,32,512]{2,1,0:T(8,128)(2,1)S(1)}, u32[]{:S(2)}, u32[]{:S(2)}) async-start(bf16[16,32,512]{2,1,0:T(8,128)(2,1)} %bitcast.35), calls=%async_computation | async-start | bytes 1048576 | tf_op jit(solution)/shard_map/all_to_all | solution.py:198
  31.6 2.7 %collective-permute-start.12 = (bf16[16,2176]{1,0:T(8,128)(2,1)S(1)}, bf16[16,2176]{1,0:T(8,128)(2,1)S(1)}, u32[]{:S(2)}, u32[]{:S(2)}) collective-permute-start(bf16[16,2176]{1,0:T(8,128)(2,1)S(1)} %get-tuple-element.74), channel_id=1, source_target_pairs={{0,7},{1,0},{2,1},{3,2},{4,3},{5,4},{6,5},{7,6},{8,15},{9,8},{10,9... | collective-permute-start | bytes 208904 | tf_op jit(solution)/shard_map/ppermute | solution.py:45
  34.4 1.2 collective-permute-done.12
  35.7 3.1 %collective-permute-start.13 = (bf16[16,2176]{1,0:T(8,128)(2,1)S(1)}, bf16[16,2176]{1,0:T(8,128)(2,1)S(1)}, u32[]{:S(2)}, u32[]{:S(2)}) collective-permute-start(bf16[16,2176]{1,0:T(8,128)(2,1)S(1)} %add_convert_fusion.11), channel_id=1, source_target_pairs={{0,7},{1,0},{2,1},{3,2},{4,3},{5,4},{6,5},{7,6},{8,15},{9,8},{10,9... | collective-permute-start | bytes 208904 | tf_op jit(solution)/shard_map/ppermute | solution.py:45
  40.2 3.4 %collective-permute-start.14 = (bf16[16,2176]{1,0:T(8,128)(2,1)S(1)}, bf16[16,2176]{1,0:T(8,128)(2,1)S(1)}, u32[]{:S(2)}, u32[]{:S(2)}) collective-permute-start(bf16[16,2176]{1,0:T(8,128)(2,1)S(1)} %add_convert_fusion.10), channel_id=1, source_target_pairs={{0,7},{1,0},{2,1},{3,2},{4,3},{5,4},{6,5},{7,6},{8,15},{9,8},{10,9... | collective-permute-start | bytes 208904 | tf_op jit(solution)/shard_map/ppermute | solution.py:45
  44.9 3.4 %collective-permute-done.11 = bf16[16,2176]{1,0:T(8,128)(2,1)S(1)} collective-permute-done((bf16[16,2176]{1,0:T(8,128)(2,1)S(1)}, bf16[16,2176]{1,0:T(8,128)(2,1)S(1)}, u32[]{:S(2)}, u32[]{:S(2)}) %collective-permute-start.11) | collective-permute-done | bytes 69664 | tf_op jit(solution)/shard_map/ppermute | solution.py:45
  48.8 3.3 %project.3 = (bf16[64,2176]{1,0:T(8,128)(2,1)}, bf16[64,2176]{1,0:T(8,128)(2,1)}, bf16[64,2176]{1,0:T(8,128)(2,1)}, bf16[64,2176]{1,0:T(8,128)(2,1)}, bf16[64,21...) custom-call(s32[1]{0:T(128)} %bitcast.me_ref, ...), custom_call_target="tpu_custom_call" | custom-call | tf_op jit(solution)/shard_map/project/pallas_call | solution.py:107
  52.1 2.7 %collective-permute-start.4 = (bf16[64,2176]{1,0:T(8,128)(2,1)}, bf16[64,2176]{1,0:T(8,128)(2,1)}, u32[]{:S(2)}, u32[]{:S(2)}) collective-permute-start(bf16[64,2176]{1,0:T(8,128)(2,1)} %get-tuple-element.65), channel_id=1, source_target_pairs={{0,7},{1,0},{2,1},{3,2},{4,3},{5,4},{6,5},{7,6},{8,15},{9,8},{10,9... | collective-permute-start | bytes 835592 | tf_op jit(solution)/shard_map/ppermute | solution.py:45
  55.2 9.5 %all-to-all-start.1 = ((bf16[16,32,512]{2,1,0:T(8,128)(2,1)}), bf16[16,32,512]{2,1,0:T(8,128)(2,1)S(1)}, u32[]{:S(2)}, u32[]{:S(2)}) async-start(bf16[16,32,512]{2,1,0:T(8,128)(2,1)} %bitcast.6), calls=%async_computation.1 | async-start | bytes 1048576 | tf_op jit(solution)/shard_map/all_to_all | solution.py:198
  64.7 1.1 add_convert_fusion.7
  65.8 1.1 collective-permute-start.5
  67.6 6.2 %collective-permute-done.5 = bf16[64,2176]{1,0:T(8,128)(2,1)S(1)} collective-permute-done((bf16[64,2176]{1,0:T(8,128)(2,1)S(1)}, bf16[64,2176]{1,0:T(8,128)(2,1)S(1)}, u32[]{:S(2)}, u32[]{:S(2)}) %collective-permute-start.5) | collective-permute-done | bytes 278560 | tf_op jit(solution)/shard_map/ppermute | solution.py:45
  73.9 2.5 %collective-permute-start.6 = (bf16[64,2176]{1,0:T(8,128)(2,1)S(1)}, bf16[64,2176]{1,0:T(8,128)(2,1)S(1)}, u32[]{:S(2)}, u32[]{:S(2)}) collective-permute-start(bf16[64,2176]{1,0:T(8,128)(2,1)S(1)} %add_convert_fusion.6), channel_id=1, source_target_pairs={{0,7},{1,0},{2,1},{3,2},{4,3},{5,4},{6,5},{7,6},{8,15},{9,8},{10,9... | collective-permute-start | bytes 835592 | tf_op jit(solution)/shard_map/ppermute | solution.py:45
  76.4 5.5 %all-to-all-done.1 = bf16[16,32,512]{2,1,0:T(8,128)(2,1)S(1)} async-done(((bf16[16,32,512]{2,1,0:T(8,128)(2,1)}), bf16[16,32,512]{2,1,0:T(8,128)(2,1)S(1)}, u32[]{:S(2)}, u32[]{:S(2)}) %all-to-all-start.1) | async-done | bytes 524320 | tf_op jit(solution)/shard_map/all_to_all | solution.py:198
  81.9 2.0 project.4
  84.1 2.7 %collective-permute-start.7 = (bf16[64,2176]{1,0:T(8,128)(2,1)S(1)}, bf16[64,2176]{1,0:T(8,128)(2,1)S(1)}, u32[]{:S(2)}, u32[]{:S(2)}) collective-permute-start(bf16[64,2176]{1,0:T(8,128)(2,1)S(1)} %add_convert_fusion.5), channel_id=1, source_target_pairs={{0,7},{1,0},{2,1},{3,2},{4,3},{5,4},{6,5},{7,6},{8,15},{9,8},{10,9... | collective-permute-start | bytes 835592 | tf_op jit(solution)/shard_map/ppermute | solution.py:45
  87.0 5.9 %collective-permute-done.2 = bf16[64,2176]{1,0:T(8,128)(2,1)S(1)} collective-permute-done((bf16[64,2176]{1,0:T(8,128)(2,1)S(1)}, bf16[64,2176]{1,0:T(8,128)(2,1)S(1)}, u32[]{:S(2)}, u32[]{:S(2)}) %collective-permute-start.2) | collective-permute-done | bytes 278560 | tf_op jit(solution)/shard_map/ppermute | solution.py:45
  93.1 5.8 %collective-permute-done.15 = bf16[64,2176]{1,0:T(8,128)(2,1)S(1)} collective-permute-done((bf16[64,2176]{1,0:T(8,128)(2,1)S(1)}, bf16[64,2176]{1,0:T(8,128)(2,1)S(1)}, u32[]{:S(2)}, u32[]{:S(2)}) %collective-permute-start.15) | collective-permute-done | bytes 278560 | tf_op jit(solution)/shard_map/ppermute | solution.py:45
  99.0 3.5 %collective-permute-start.17 = (bf16[64,2176]{1,0:T(8,128)(2,1)S(1)}, bf16[64,2176]{1,0:T(8,128)(2,1)S(1)}, u32[]{:S(2)}, u32[]{:S(2)}) collective-permute-start(bf16[64,2176]{1,0:T(8,128)(2,1)S(1)} %add_convert_fusion.4), channel_id=1, source_target_pairs={{0,7},{1,0},{2,1},{3,2},{4,3},{5,4},{6,5},{7,6},{8,15},{9,8},{10,9... | collective-permute-start | bytes 835592 | tf_op jit(solution)/shard_map/ppermute | solution.py:45
  102.8 5.5 %collective-permute-done.21 = bf16[64,2176]{1,0:T(8,128)(2,1)S(1)} collective-permute-done((bf16[64,2176]{1,0:T(8,128)(2,1)S(1)}, bf16[64,2176]{1,0:T(8,128)(2,1)S(1)}, u32[]{:S(2)}, u32[]{:S(2)}) %collective-permute-start.21) | collective-permute-done | bytes 278560 | tf_op jit(solution)/shard_map/ppermute | solution.py:45
  108.8 8.2 %collective-permute-done.23 = bf16[64,2176]{1,0:T(8,128)(2,1)S(1)} collective-permute-done((bf16[64,2176]{1,0:T(8,128)(2,1)S(1)}, bf16[64,2176]{1,0:T(8,128)(2,1)S(1)}, u32[]{:S(2)}, u32[]{:S(2)}) %collective-permute-start.23) | collective-permute-done | bytes 278560 | tf_op jit(solution)/shard_map/ppermute | solution.py:45
  117.4 2.7 %collective-permute-start.19 = (bf16[64,2176]{1,0:T(8,128)(2,1)S(1)}, bf16[64,2176]{1,0:T(8,128)(2,1)S(1)}, u32[]{:S(2)}, u32[]{:S(2)}) collective-permute-start(bf16[64,2176]{1,0:T(8,128)(2,1)S(1)} %add_convert_fusion.3), channel_id=1, source_target_pairs={{0,7},{1,0},{2,1},{3,2},{4,3},{5,4},{6,5},{7,6},{8,15},{9,8},{10,9... | collective-permute-start | bytes 835592 | tf_op jit(solution)/shard_map/ppermute | solution.py:45
  120.6 1.0 collective-permute-start.24
  121.6 4.8 %collective-permute-done.16.refs_1_ = bf16[80,1024]{1,0:T(8,128)(2,1)S(1)} collective-permute-done((bf16[80,1024]{1,0:T(8,128)(2,1)S(1)}, bf16[80,1024]{1,0:T(8,128)(2,1)S(1)}, u32[]{:S(2)}, u32[]{:S(2)}) %collective-permute-start.16) | collective-permute-done | bytes 163872 | tf_op jit(solution)/shard_map/ppermute | solution.py:45
  126.4 3.4 %collective-permute-start.18 = (bf16[80,1024]{1,0:T(8,128)(2,1)S(1)}, bf16[80,1024]{1,0:T(8,128)(2,1)S(1)}, u32[]{:S(2)}, u32[]{:S(2)}) collective-permute-start(bf16[80,1024]{1,0:T(8,128)(2,1)S(1)} %collective-permute-done.16.refs_1_), channel_id=1, source_target_pairs={{0,7},{1,0},{2,1},{3,2},{4,3},{5,4},{6,5},{7,6},{8,15},{9,8},{10,9... | collective-permute-start | bytes 491528 | tf_op jit(solution)/shard_map/ppermute | solution.py:45
  130.4 1.7 collective-permute-done.18.refs_2_
  132.1 3.1 %collective-permute-start.20 = (bf16[80,1024]{1,0:T(8,128)(2,1)S(1)}, bf16[80,1024]{1,0:T(8,128)(2,1)S(1)}, u32[]{:S(2)}, u32[]{:S(2)}) collective-permute-start(bf16[80,1024]{1,0:T(8,128)(2,1)S(1)} %collective-permute-done.18.refs_2_), channel_id=1, source_target_pairs={{0,7},{1,0},{2,1},{3,2},{4,3},{5,4},{6,5},{7,6},{8,15},{9,8},{10,9... | collective-permute-start | bytes 491528 | tf_op jit(solution)/shard_map/ppermute | solution.py:45
  135.2 1.4 collective-permute-done.27.refs_7_
  136.6 1.8 collective-permute-done.20.refs_3_
  138.4 4.8 %collective-permute-done.28.refs_4_ = bf16[80,1024]{1,0:T(8,128)(2,1)S(1)} collective-permute-done((bf16[80,1024]{1,0:T(8,128)(2,1)S(1)}, bf16[80,1024]{1,0:T(8,128)(2,1)S(1)}, u32[]{:S(2)}, u32[]{:S(2)}) %collective-permute-start.28) | collective-permute-done | bytes 163872 | tf_op jit(solution)/shard_map/ppermute | solution.py:45
  143.2 2.0 lower_down.2
  145.3 10.1 %all-to-all-start.2 = ((bf16[16,32,512]{2,1,0:T(8,128)(2,1)}), bf16[16,32,512]{2,1,0:T(8,128)(2,1)S(1)}, u32[]{:S(2)}, u32[]{:S(2)}) async-start(bf16[16,32,512]{2,1,0:T(8,128)(2,1)} %bitcast.9), calls=%async_computation.2 | async-start | bytes 1048576 | tf_op jit(solution)/shard_map/all_to_all | solution.py:198
  155.4 4.3 %collective-permute-done.29.refs_1_ = bf16[64,1024]{1,0:T(8,128)(2,1)S(1)} collective-permute-done((bf16[64,1024]{1,0:T(8,128)(2,1)S(1)}, bf16[64,1024]{1,0:T(8,128)(2,1)S(1)}, u32[]{:S(2)}, u32[]{:S(2)}) %collective-permute-start.29) | collective-permute-done | bytes 131104 | tf_op jit(solution)/shard_map/ppermute | solution.py:45
  159.6 1.5 collective-permute-start.30
  161.1 2.6 %collective-permute-done.30.refs_2_ = bf16[64,1024]{1,0:T(8,128)(2,1)S(1)} collective-permute-done((bf16[64,1024]{1,0:T(8,128)(2,1)S(1)}, bf16[64,1024]{1,0:T(8,128)(2,1)S(1)}, u32[]{:S(2)}, u32[]{:S(2)}) %collective-permute-start.30) | collective-permute-done | bytes 131104 | tf_op jit(solution)/shard_map/ppermute | solution.py:45
  163.8 2.7 %collective-permute-start.31 = (bf16[64,1024]{1,0:T(8,128)(2,1)S(1)}, bf16[64,1024]{1,0:T(8,128)(2,1)S(1)}, u32[]{:S(2)}, u32[]{:S(2)}) collective-permute-start(bf16[64,1024]{1,0:T(8,128)(2,1)S(1)} %collective-permute-done.30.refs_2_), channel_id=1, source_target_pairs={{0,7},{1,0},{2,1},{3,2},{4,3},{5,4},{6,5},{7,6},{8,15},{9,8},{10,9... | collective-permute-start | bytes 393224 | tf_op jit(solution)/shard_map/ppermute | solution.py:45
  166.5 1.9 collective-permute-done.31.refs_3_
  168.4 3.1 %collective-permute-start.32 = (bf16[64,1024]{1,0:T(8,128)(2,1)S(1)}, bf16[64,1024]{1,0:T(8,128)(2,1)S(1)}, u32[]{:S(2)}, u32[]{:S(2)}) collective-permute-start(bf16[64,1024]{1,0:T(8,128)(2,1)S(1)} %collective-permute-done.31.refs_3_), channel_id=1, source_target_pairs={{0,7},{1,0},{2,1},{3,2},{4,3},{5,4},{6,5},{7,6},{8,15},{9,8},{10,9... | collective-permute-start | bytes 393224 | tf_op jit(solution)/shard_map/ppermute | solution.py:45
  171.5 1.9 collective-permute-done.32.refs_4_
  173.4 1.8 lower_down.3
  175.2 11.3 %all-to-all-start.3 = ((bf16[16,32,512]{2,1,0:T(8,128)(2,1)}), bf16[16,32,512]{2,1,0:T(8,128)(2,1)S(1)}, u32[]{:S(2)}, u32[]{:S(2)}) async-start(bf16[16,32,512]{2,1,0:T(8,128)(2,1)} %bitcast.11), calls=%async_computation.3 | async-start | bytes 1048576 | tf_op jit(solution)/shard_map/all_to_all | solution.py:198
  187.6 16.2 %all-to-all-done.3 = bf16[16,32,512]{2,1,0:T(8,128)(2,1)S(1)} async-done(((bf16[16,32,512]{2,1,0:T(8,128)(2,1)}), bf16[16,32,512]{2,1,0:T(8,128)(2,1)S(1)}, u32[]{:S(2)}, u32[]{:S(2)}) %all-to-all-start.3) | async-done | bytes 524320 | tf_op jit(solution)/shard_map/all_to_all | solution.py:198
  204.4 11.0 %all_to_all.25 = f32[8,128,1]{1,2,0:T(1,128)S(1)} all-to-all(f32[8,128,1]{1,2,0:T(1,128)S(1)} %broadcast_in_dim.34), channel_id=1, replica_groups=mesh['grp'=2,'ep'=16,'tp'=8] {'tp'}, dimensions={0} | all-to-all | bytes 8192 | tf_op jit(solution)/shard_map/all_to_all | solution.py:253
  (119 shorter events, 12.2 us)
Async XLA Ops:
  5.2 29.0 %collective-permute-start.8 = (bf16[16,2176]{1,0:T(8,128)(2,1)S(1)}, bf16[16,2176]{1,0:T(8,128)(2,1)S(1)}, u32[]{:S(2)}, u32[]{:S(2)}) collective-permute-start(bf16[16,2176]{1,0:T(8,128)(2,1)S(1)} %get-tuple-element.71), channel_id=1, source_target_pairs={{0,1},{1,2},{2,3},{3,4},{4,5},{5,6},{6,7},{7,0},{8,9},{9,10},{10,1... | collective-permute-start | bytes 208904 | tf_op jit(solution)/shard_map/ppermute | solution.py:45
  9.5 39.3 %copy-start = (bf16[1,512,1024]{2,1,0:T(8,128)(2,1)S(1)}, bf16[1,512,1024]{2,1,0:T(8,128)(2,1)}, u32[]{:S(2)}) copy-start(bf16[1,512,1024]{2,1,0:T(8,128)(2,1)} %param.15) | copy-start | bytes 3145732
  9.5 39.3 %copy-start.1 = (bf16[1,512,1024]{2,1,0:T(8,128)(2,1)S(1)}, bf16[1,512,1024]{2,1,0:T(8,128)(2,1)}, u32[]{:S(2)}) copy-start(bf16[1,512,1024]{2,1,0:T(8,128)(2,1)} %param.16) | copy-start | bytes 3145732
  9.5 39.2 %all-to-all-start = ((bf16[16,32,512]{2,1,0:T(8,128)(2,1)}), bf16[16,32,512]{2,1,0:T(8,128)(2,1)S(1)}, u32[]{:S(2)}, u32[]{:S(2)}) async-start(bf16[16,32,512]{2,1,0:T(8,128)(2,1)} %bitcast.35), calls=%async_computation | async-start | bytes 1048576 | tf_op jit(solution)/shard_map/all_to_all | solution.py:198
  31.6 4.0 %collective-permute-start.12 = (bf16[16,2176]{1,0:T(8,128)(2,1)S(1)}, bf16[16,2176]{1,0:T(8,128)(2,1)S(1)}, u32[]{:S(2)}, u32[]{:S(2)}) collective-permute-start(bf16[16,2176]{1,0:T(8,128)(2,1)S(1)} %get-tuple-element.74), channel_id=1, source_target_pairs={{0,7},{1,0},{2,1},{3,2},{4,3},{5,4},{6,5},{7,6},{8,15},{9,8},{10,9... | collective-permute-start | bytes 208904 | tf_op jit(solution)/shard_map/ppermute | solution.py:45
  34.3 4.7 %collective-permute-start.9 = (bf16[16,2176]{1,0:T(8,128)(2,1)S(1)}, bf16[16,2176]{1,0:T(8,128)(2,1)S(1)}, u32[]{:S(2)}, u32[]{:S(2)}) collective-permute-start(bf16[16,2176]{1,0:T(8,128)(2,1)S(1)} %add_convert_fusion.14), channel_id=1, source_target_pairs={{0,1},{1,2},{2,3},{3,4},{4,5},{5,6},{6,7},{7,0},{8,9},{9,10},{10,1... | collective-permute-start | bytes 208904 | tf_op jit(solution)/shard_map/ppermute | solution.py:45
  35.7 4.5 %collective-permute-start.13 = (bf16[16,2176]{1,0:T(8,128)(2,1)S(1)}, bf16[16,2176]{1,0:T(8,128)(2,1)S(1)}, u32[]{:S(2)}, u32[]{:S(2)}) collective-permute-start(bf16[16,2176]{1,0:T(8,128)(2,1)S(1)} %add_convert_fusion.11), channel_id=1, source_target_pairs={{0,7},{1,0},{2,1},{3,2},{4,3},{5,4},{6,5},{7,6},{8,15},{9,8},{10,9... | collective-permute-start | bytes 208904 | tf_op jit(solution)/shard_map/ppermute | solution.py:45
  39.1 4.8 %collective-permute-start.10 = (bf16[16,2176]{1,0:T(8,128)(2,1)S(1)}, bf16[16,2176]{1,0:T(8,128)(2,1)S(1)}, u32[]{:S(2)}, u32[]{:S(2)}) collective-permute-start(bf16[16,2176]{1,0:T(8,128)(2,1)S(1)} %add_convert_fusion.13), channel_id=1, source_target_pairs={{0,1},{1,2},{2,3},{3,4},{4,5},{5,6},{6,7},{7,0},{8,9},{9,10},{10,1... | collective-permute-start | bytes 208904 | tf_op jit(solution)/shard_map/ppermute | solution.py:45
  40.2 4.8 %collective-permute-start.14 = (bf16[16,2176]{1,0:T(8,128)(2,1)S(1)}, bf16[16,2176]{1,0:T(8,128)(2,1)S(1)}, u32[]{:S(2)}, u32[]{:S(2)}) collective-permute-start(bf16[16,2176]{1,0:T(8,128)(2,1)S(1)} %add_convert_fusion.10), channel_id=1, source_target_pairs={{0,7},{1,0},{2,1},{3,2},{4,3},{5,4},{6,5},{7,6},{8,15},{9,8},{10,9... | collective-permute-start | bytes 208904 | tf_op jit(solution)/shard_map/ppermute | solution.py:45
  43.9 4.5 %collective-permute-start.11 = (bf16[16,2176]{1,0:T(8,128)(2,1)S(1)}, bf16[16,2176]{1,0:T(8,128)(2,1)S(1)}, u32[]{:S(2)}, u32[]{:S(2)}) collective-permute-start(bf16[16,2176]{1,0:T(8,128)(2,1)S(1)} %add_convert_fusion.12), channel_id=1, source_target_pairs={{0,1},{1,2},{2,3},{3,4},{4,5},{5,6},{6,7},{7,0},{8,9},{9,10},{10,1... | collective-permute-start | bytes 208904 | tf_op jit(solution)/shard_map/ppermute | solution.py:45
  52.1 12.5 %copy-start.13 = (bf16[64,2176]{1,0:T(8,128)(2,1)S(1)}, bf16[64,2176]{1,0:T(8,128)(2,1)}, u32[]{:S(2)}) copy-start(bf16[64,2176]{1,0:T(8,128)(2,1)} %get-tuple-element.64) | copy-start | bytes 835588
  52.1 14.7 %copy-start.12 = (bf16[64,2176]{1,0:T(8,128)(2,1)S(1)}, bf16[64,2176]{1,0:T(8,128)(2,1)}, u32[]{:S(2)}) copy-start(bf16[64,2176]{1,0:T(8,128)(2,1)} %get-tuple-element.57) | copy-start | bytes 835588
  52.1 12.5 %collective-permute-start.4 = (bf16[64,2176]{1,0:T(8,128)(2,1)}, bf16[64,2176]{1,0:T(8,128)(2,1)}, u32[]{:S(2)}, u32[]{:S(2)}) collective-permute-start(bf16[64,2176]{1,0:T(8,128)(2,1)} %get-tuple-element.65), channel_id=1, source_target_pairs={{0,7},{1,0},{2,1},{3,2},{4,3},{5,4},{6,5},{7,6},{8,15},{9,8},{10,9... | collective-permute-start | bytes 835592 | tf_op jit(solution)/shard_map/ppermute | solution.py:45
  55.0 11.8 %collective-permute-start = (bf16[64,2176]{1,0:T(8,128)(2,1)}, bf16[64,2176]{1,0:T(8,128)(2,1)S(1)}, u32[]{:S(2)}, u32[]{:S(2)}) collective-permute-start(bf16[64,2176]{1,0:T(8,128)(2,1)} %get-tuple-element.58), channel_id=1, source_target_pairs={{0,1},{1,2},{2,3},{3,4},{4,5},{5,6},{6,7},{7,0},{8,9},{9,10},{10,1... | collective-permute-start | bytes 835592 | tf_op jit(solution)/shard_map/ppermute | solution.py:45
  55.2 26.7 %all-to-all-start.1 = ((bf16[16,32,512]{2,1,0:T(8,128)(2,1)}), bf16[16,32,512]{2,1,0:T(8,128)(2,1)S(1)}, u32[]{:S(2)}, u32[]{:S(2)}) async-start(bf16[16,32,512]{2,1,0:T(8,128)(2,1)} %bitcast.6), calls=%async_computation.1 | async-start | bytes 1048576 | tf_op jit(solution)/shard_map/all_to_all | solution.py:198
  64.7 11.6 %copy-start.10 = (bf16[64,2176]{1,0:T(8,128)(2,1)S(1)}, bf16[64,2176]{1,0:T(8,128)(2,1)}, u32[]{:S(2)}) copy-start(bf16[64,2176]{1,0:T(8,128)(2,1)} %get-tuple-element.56) | copy-start | bytes 835588
  65.8 8.0 %collective-permute-start.5 = (bf16[64,2176]{1,0:T(8,128)(2,1)S(1)}, bf16[64,2176]{1,0:T(8,128)(2,1)S(1)}, u32[]{:S(2)}, u32[]{:S(2)}) collective-permute-start(bf16[64,2176]{1,0:T(8,128)(2,1)S(1)} %add_convert_fusion.7), channel_id=1, source_target_pairs={{0,7},{1,0},{2,1},{3,2},{4,3},{5,4},{6,5},{7,6},{8,15},{9,8},{10,9... | collective-permute-start | bytes 835592 | tf_op jit(solution)/shard_map/ppermute | solution.py:45
  66.9 9.4 %collective-permute-start.1 = (bf16[64,2176]{1,0:T(8,128)(2,1)S(1)}, bf16[64,2176]{1,0:T(8,128)(2,1)S(1)}, u32[]{:S(2)}, u32[]{:S(2)}) collective-permute-start(bf16[64,2176]{1,0:T(8,128)(2,1)S(1)} %add_convert_fusion.9), channel_id=1, source_target_pairs={{0,1},{1,2},{2,3},{3,4},{4,5},{5,6},{6,7},{7,0},{8,9},{9,10},{10,1... | collective-permute-start | bytes 835592 | tf_op jit(solution)/shard_map/ppermute | solution.py:45
  73.9 10.2 %collective-permute-start.6 = (bf16[64,2176]{1,0:T(8,128)(2,1)S(1)}, bf16[64,2176]{1,0:T(8,128)(2,1)S(1)}, u32[]{:S(2)}, u32[]{:S(2)}) collective-permute-start(bf16[64,2176]{1,0:T(8,128)(2,1)S(1)} %add_convert_fusion.6), channel_id=1, source_target_pairs={{0,7},{1,0},{2,1},{3,2},{4,3},{5,4},{6,5},{7,6},{8,15},{9,8},{10,9... | collective-permute-start | bytes 835592 | tf_op jit(solution)/shard_map/ppermute | solution.py:45
  83.9 9.0 %collective-permute-start.2 = (bf16[64,2176]{1,0:T(8,128)(2,1)S(1)}, bf16[64,2176]{1,0:T(8,128)(2,1)S(1)}, u32[]{:S(2)}, u32[]{:S(2)}) collective-permute-start(bf16[64,2176]{1,0:T(8,128)(2,1)S(1)} %get-tuple-element.60), channel_id=1, source_target_pairs={{0,1},{1,2},{2,3},{3,4},{4,5},{5,6},{6,7},{7,0},{8,9},{9,10},{10,1... | collective-permute-start | bytes 835592 | tf_op jit(solution)/shard_map/ppermute | solution.py:45
  84.1 18.5 %copy-start.8 = (bf16[64,2176]{1,0:T(8,128)(2,1)S(1)}, bf16[64,2176]{1,0:T(8,128)(2,1)}, u32[]{:S(2)}) copy-start(bf16[64,2176]{1,0:T(8,128)(2,1)} %get-tuple-element.55) | copy-start | bytes 835588
  84.1 18.4 %collective-permute-start.7 = (bf16[64,2176]{1,0:T(8,128)(2,1)S(1)}, bf16[64,2176]{1,0:T(8,128)(2,1)S(1)}, u32[]{:S(2)}, u32[]{:S(2)}) collective-permute-start(bf16[64,2176]{1,0:T(8,128)(2,1)S(1)} %add_convert_fusion.5), channel_id=1, source_target_pairs={{0,7},{1,0},{2,1},{3,2},{4,3},{5,4},{6,5},{7,6},{8,15},{9,8},{10,9... | collective-permute-start | bytes 835592 | tf_op jit(solution)/shard_map/ppermute | solution.py:45
  86.9 12.1 %collective-permute-start.15 = (bf16[64,2176]{1,0:T(8,128)(2,1)S(1)}, bf16[64,2176]{1,0:T(8,128)(2,1)S(1)}, u32[]{:S(2)}, u32[]{:S(2)}) collective-permute-start(bf16[64,2176]{1,0:T(8,128)(2,1)S(1)} %get-tuple-element.76), channel_id=1, source_target_pairs={{0,7},{1,0},{2,1},{3,2},{4,3},{5,4},{6,5},{7,6},{8,15},{9,8},{10,9... | collective-permute-start | bytes 835592 | tf_op jit(solution)/shard_map/ppermute | solution.py:45
  92.9 9.6 %collective-permute-start.3 = (bf16[64,2176]{1,0:T(8,128)(2,1)S(1)}, bf16[64,2176]{1,0:T(8,128)(2,1)S(1)}, u32[]{:S(2)}, u32[]{:S(2)}) collective-permute-start(bf16[64,2176]{1,0:T(8,128)(2,1)S(1)} %add_convert_fusion.8), channel_id=1, source_target_pairs={{0,1},{1,2},{2,3},{3,4},{4,5},{5,6},{6,7},{7,0},{8,9},{9,10},{10,1... | collective-permute-start | bytes 835592 | tf_op jit(solution)/shard_map/ppermute | solution.py:45
  93.0 15.3 %collective-permute-start.21 = (bf16[64,2176]{1,0:T(8,128)(2,1)S(1)}, bf16[64,2176]{1,0:T(8,128)(2,1)S(1)}, u32[]{:S(2)}, u32[]{:S(2)}) collective-permute-start(bf16[64,2176]{1,0:T(8,128)(2,1)S(1)} %add_convert_fusion.2), channel_id=1, source_target_pairs={{0,1},{1,2},{2,3},{3,4},{4,5},{5,6},{6,7},{7,0},{8,9},{9,10},{10,1... | collective-permute-start | bytes 835592 | tf_op jit(solution)/shard_map/ppermute | solution.py:45
  99.0 18.3 %collective-permute-start.17 = (bf16[64,2176]{1,0:T(8,128)(2,1)S(1)}, bf16[64,2176]{1,0:T(8,128)(2,1)S(1)}, u32[]{:S(2)}, u32[]{:S(2)}) collective-permute-start(bf16[64,2176]{1,0:T(8,128)(2,1)S(1)} %add_convert_fusion.4), channel_id=1, source_target_pairs={{0,7},{1,0},{2,1},{3,2},{4,3},{5,4},{6,5},{7,6},{8,15},{9,8},{10,9... | collective-permute-start | bytes 835592 | tf_op jit(solution)/shard_map/ppermute | solution.py:45
  108.4 8.7 %collective-permute-start.23 = (bf16[64,2176]{1,0:T(8,128)(2,1)S(1)}, bf16[64,2176]{1,0:T(8,128)(2,1)S(1)}, u32[]{:S(2)}, u32[]{:S(2)}) collective-permute-start(bf16[64,2176]{1,0:T(8,128)(2,1)S(1)} %add_convert_fusion.1), channel_id=1, source_target_pairs={{0,1},{1,2},{2,3},{3,4},{4,5},{5,6},{6,7},{7,0},{8,9},{9,10},{10,1... | collective-permute-start | bytes 835592 | tf_op jit(solution)/shard_map/ppermute | solution.py:45
  108.7 11.9 %collective-permute-start.22 = (bf16[80,1024]{1,0:T(8,128)(2,1)S(1)}, bf16[80,1024]{1,0:T(8,128)(2,1)S(1)}, u32[]{:S(2)}, u32[]{:S(2)}) collective-permute-start(bf16[80,1024]{1,0:T(8,128)(2,1)S(1)} %pad_maximum_fusion.refs_0_), channel_id=1, source_target_pairs={{0,1},{1,2},{2,3},{3,4},{4,5},{5,6},{6,7},{7,0},{8,9},{9,10},{10,1... | collective-permute-start | bytes 491528 | tf_op jit(solution)/shard_map/ppermute | solution.py:45
  117.1 12.7 %collective-permute-start.25 = (bf16[64,2176]{1,0:T(8,128)(2,1)S(1)}, bf16[64,2176]{1,0:T(8,128)(2,1)S(1)}, u32[]{:S(2)}, u32[]{:S(2)}) collective-permute-start(bf16[64,2176]{1,0:T(8,128)(2,1)S(1)} %add_convert_fusion), channel_id=1, source_target_pairs={{0,1},{1,2},{2,3},{3,4},{4,5},{5,6},{6,7},{7,0},{8,9},{9,10},{10,1... | collective-permute-start | bytes 835592 | tf_op jit(solution)/shard_map/ppermute | solution.py:45
  117.3 25.9 %copy-start.5 = (bf16[1024,512]{1,0:T(8,128)(2,1)S(1)}, bf16[1024,512]{1,0:T(8,128)(2,1)}, u32[]{:S(2)}) copy-start(bf16[1024,512]{1,0:T(8,128)(2,1)} %refs_9_.1) | copy-start | bytes 3145732
  117.4 25.8 %copy-start.2 = (bf16[1,1024,512]{2,1,0:T(8,128)(2,1)S(1)}, bf16[1,1024,512]{2,1,0:T(8,128)(2,1)}, u32[]{:S(2)}) copy-start(bf16[1,1024,512]{2,1,0:T(8,128)(2,1)} %param.17) | copy-start | bytes 3145732
  117.4 12.4 %collective-permute-start.19 = (bf16[64,2176]{1,0:T(8,128)(2,1)S(1)}, bf16[64,2176]{1,0:T(8,128)(2,1)S(1)}, u32[]{:S(2)}, u32[]{:S(2)}) collective-permute-start(bf16[64,2176]{1,0:T(8,128)(2,1)S(1)} %add_convert_fusion.3), channel_id=1, source_target_pairs={{0,7},{1,0},{2,1},{3,2},{4,3},{5,4},{6,5},{7,6},{8,15},{9,8},{10,9... | collective-permute-start | bytes 835592 | tf_op jit(solution)/shard_map/ppermute | solution.py:45
  120.1 6.2 %collective-permute-start.16 = (bf16[80,1024]{1,0:T(8,128)(2,1)S(1)}, bf16[80,1024]{1,0:T(8,128)(2,1)S(1)}, u32[]{:S(2)}, u32[]{:S(2)}) collective-permute-start(bf16[80,1024]{1,0:T(8,128)(2,1)S(1)} %pad_maximum_fusion.refs_0_), channel_id=1, source_target_pairs={{0,7},{1,0},{2,1},{3,2},{4,3},{5,4},{6,5},{7,6},{8,15},{9,8},{10,9... | collective-permute-start | bytes 491528 | tf_op jit(solution)/shard_map/ppermute | solution.py:45
  120.6 9.2 %collective-permute-start.24 = (bf16[80,1024]{1,0:T(8,128)(2,1)S(1)}, bf16[80,1024]{1,0:T(8,128)(2,1)S(1)}, u32[]{:S(2)}, u32[]{:S(2)}) collective-permute-start(bf16[80,1024]{1,0:T(8,128)(2,1)S(1)} %collective-permute-done.22.refs_7_), channel_id=1, source_target_pairs={{0,1},{1,2},{2,3},{3,4},{4,5},{5,6},{6,7},{7,0},{8,9},{9,10},{10,1... | collective-permute-start | bytes 491528 | tf_op jit(solution)/shard_map/ppermute | solution.py:45
  126.4 5.7 %collective-permute-start.18 = (bf16[80,1024]{1,0:T(8,128)(2,1)S(1)}, bf16[80,1024]{1,0:T(8,128)(2,1)S(1)}, u32[]{:S(2)}, u32[]{:S(2)}) collective-permute-start(bf16[80,1024]{1,0:T(8,128)(2,1)S(1)} %collective-permute-done.16.refs_1_), channel_id=1, source_target_pairs={{0,7},{1,0},{2,1},{3,2},{4,3},{5,4},{6,5},{7,6},{8,15},{9,8},{10,9... | collective-permute-start | bytes 491528 | tf_op jit(solution)/shard_map/ppermute | solution.py:45
  129.8 6.8 %collective-permute-start.26 = (bf16[80,1024]{1,0:T(8,128)(2,1)S(1)}, bf16[80,1024]{1,0:T(8,128)(2,1)S(1)}, u32[]{:S(2)}, u32[]{:S(2)}) collective-permute-start(bf16[80,1024]{1,0:T(8,128)(2,1)S(1)} %collective-permute-done.24.refs_6_), channel_id=1, source_target_pairs={{0,1},{1,2},{2,3},{3,4},{4,5},{5,6},{6,7},{7,0},{8,9},{9,10},{10,1... | collective-permute-start | bytes 491528 | tf_op jit(solution)/shard_map/ppermute | solution.py:45
  130.2 6.4 %collective-permute-start.27 = (bf16[64,1024]{1,0:T(8,128)(2,1)S(1)}, bf16[64,1024]{1,0:T(8,128)(2,1)S(1)}, u32[]{:S(2)}, u32[]{:S(2)}) collective-permute-start(bf16[64,1024]{1,0:T(8,128)(2,1)S(1)} %fusion.5.refs_0_), channel_id=1, source_target_pairs={{0,1},{1,2},{2,3},{3,4},{4,5},{5,6},{6,7},{7,0},{8,9},{9,10},{10,1... | collective-permute-start | bytes 393224 | tf_op jit(solution)/shard_map/ppermute | solution.py:45
  132.1 6.4 %collective-permute-start.20 = (bf16[80,1024]{1,0:T(8,128)(2,1)S(1)}, bf16[80,1024]{1,0:T(8,128)(2,1)S(1)}, u32[]{:S(2)}, u32[]{:S(2)}) collective-permute-start(bf16[80,1024]{1,0:T(8,128)(2,1)S(1)} %collective-permute-done.18.refs_2_), channel_id=1, source_target_pairs={{0,7},{1,0},{2,1},{3,2},{4,3},{5,4},{6,5},{7,6},{8,15},{9,8},{10,9... | collective-permute-start | bytes 491528 | tf_op jit(solution)/shard_map/ppermute | solution.py:45
  136.6 6.6 %collective-permute-start.28 = (bf16[80,1024]{1,0:T(8,128)(2,1)S(1)}, bf16[80,1024]{1,0:T(8,128)(2,1)S(1)}, u32[]{:S(2)}, u32[]{:S(2)}) collective-permute-start(bf16[80,1024]{1,0:T(8,128)(2,1)S(1)} %collective-permute-done.26.refs_5_), channel_id=1, source_target_pairs={{0,1},{1,2},{2,3},{3,4},{4,5},{5,6},{6,7},{7,0},{8,9},{9,10},{10,1... | collective-permute-start | bytes 491528 | tf_op jit(solution)/shard_map/ppermute | solution.py:45
  145.3 29.9 %all-to-all-start.2 = ((bf16[16,32,512]{2,1,0:T(8,128)(2,1)}), bf16[16,32,512]{2,1,0:T(8,128)(2,1)S(1)}, u32[]{:S(2)}, u32[]{:S(2)}) async-start(bf16[16,32,512]{2,1,0:T(8,128)(2,1)} %bitcast.9), calls=%async_computation.2 | async-start | bytes 1048576 | tf_op jit(solution)/shard_map/all_to_all | solution.py:198
  155.4 4.3 %collective-permute-start.29 = (bf16[64,1024]{1,0:T(8,128)(2,1)S(1)}, bf16[64,1024]{1,0:T(8,128)(2,1)S(1)}, u32[]{:S(2)}, u32[]{:S(2)}) collective-permute-start(bf16[64,1024]{1,0:T(8,128)(2,1)S(1)} %fusion.5.refs_0_), channel_id=1, source_target_pairs={{0,7},{1,0},{2,1},{3,2},{4,3},{5,4},{6,5},{7,6},{8,15},{9,8},{10,9... | collective-permute-start | bytes 393224 | tf_op jit(solution)/shard_map/ppermute | solution.py:45
  159.6 4.1 %collective-permute-start.30 = (bf16[64,1024]{1,0:T(8,128)(2,1)S(1)}, bf16[64,1024]{1,0:T(8,128)(2,1)S(1)}, u32[]{:S(2)}, u32[]{:S(2)}) collective-permute-start(bf16[64,1024]{1,0:T(8,128)(2,1)S(1)} %collective-permute-done.29.refs_1_), channel_id=1, source_target_pairs={{0,7},{1,0},{2,1},{3,2},{4,3},{5,4},{6,5},{7,6},{8,15},{9,8},{10,9... | collective-permute-start | bytes 393224 | tf_op jit(solution)/shard_map/ppermute | solution.py:45
  161.1 5.3 %collective-permute-start.33 = (bf16[64,1024]{1,0:T(8,128)(2,1)S(1)}, bf16[64,1024]{1,0:T(8,128)(2,1)S(1)}, u32[]{:S(2)}, u32[]{:S(2)}) collective-permute-start(bf16[64,1024]{1,0:T(8,128)(2,1)S(1)} %collective-permute-done.27.refs_7_), channel_id=1, source_target_pairs={{0,1},{1,2},{2,3},{3,4},{4,5},{5,6},{6,7},{7,0},{8,9},{9,10},{10,1... | collective-permute-start | bytes 393224 | tf_op jit(solution)/shard_map/ppermute | solution.py:45
  163.8 4.7 %collective-permute-start.31 = (bf16[64,1024]{1,0:T(8,128)(2,1)S(1)}, bf16[64,1024]{1,0:T(8,128)(2,1)S(1)}, u32[]{:S(2)}, u32[]{:S(2)}) collective-permute-start(bf16[64,1024]{1,0:T(8,128)(2,1)S(1)} %collective-permute-done.30.refs_2_), channel_id=1, source_target_pairs={{0,7},{1,0},{2,1},{3,2},{4,3},{5,4},{6,5},{7,6},{8,15},{9,8},{10,9... | collective-permute-start | bytes 393224 | tf_op jit(solution)/shard_map/ppermute | solution.py:45
  166.5 5.0 %collective-permute-start.34 = (bf16[64,1024]{1,0:T(8,128)(2,1)S(1)}, bf16[64,1024]{1,0:T(8,128)(2,1)S(1)}, u32[]{:S(2)}, u32[]{:S(2)}) collective-permute-start(bf16[64,1024]{1,0:T(8,128)(2,1)S(1)} %collective-permute-done.33.refs_6_), channel_id=1, source_target_pairs={{0,1},{1,2},{2,3},{3,4},{4,5},{5,6},{6,7},{7,0},{8,9},{9,10},{10,1... | collective-permute-start | bytes 393224 | tf_op jit(solution)/shard_map/ppermute | solution.py:45
  168.4 5.0 %collective-permute-start.32 = (bf16[64,1024]{1,0:T(8,128)(2,1)S(1)}, bf16[64,1024]{1,0:T(8,128)(2,1)S(1)}, u32[]{:S(2)}, u32[]{:S(2)}) collective-permute-start(bf16[64,1024]{1,0:T(8,128)(2,1)S(1)} %collective-permute-done.31.refs_3_), channel_id=1, source_target_pairs={{0,7},{1,0},{2,1},{3,2},{4,3},{5,4},{6,5},{7,6},{8,15},{9,8},{10,9... | collective-permute-start | bytes 393224 | tf_op jit(solution)/shard_map/ppermute | solution.py:45
  175.2 28.5 %all-to-all-start.3 = ((bf16[16,32,512]{2,1,0:T(8,128)(2,1)}), bf16[16,32,512]{2,1,0:T(8,128)(2,1)S(1)}, u32[]{:S(2)}, u32[]{:S(2)}) async-start(bf16[16,32,512]{2,1,0:T(8,128)(2,1)} %bitcast.11), calls=%async_computation.3 | async-start | bytes 1048576 | tf_op jit(solution)/shard_map/all_to_all | solution.py:198
  204.0 11.5 %copy-start.17 = (f32[512]{0:T(512)S(1)}, f32[512]{0:T(512)}, u32[]{:S(2)}) copy-start(f32[512]{0:T(512)} %param.21) | copy-start | bytes 6148
  (10 other events, 45.1 us)

commit v2 on v0

--- a/solution.py
+++ b/solution.py
@@ -15,40 +15,37 @@
     return jnp.dot(a, b, preferred_element_type=f32)
 
 
-def ring(count, step):
-    return [(i, (i + step) % count) for i in range(count)]
+def exchanges(size, flip):
+    pairs = [[(i, (i + (1 if i % 2 == way else -1)) % size) for i in range(size)] for way in (0, 1)]
+    return pairs[::-1] if flip else pairs
 
 
 def added(own, came):
-    return own if came is None else (own.astype(f32) + came.astype(f32)).astype(bf16)
-
-
-def reduce_scatter(piece, size, long_way, axis):
+    return (own.astype(f32) + came.astype(f32)).astype(bf16)
+
+
+def reduce_scatter(piece, size, flip, axis):
+    one, two = exchanges(size, flip)
     half = size // 2
-    ahead, back = ring(size, 1), ring(size, -1)
-    f_len, b_len = (half, size - 1 - half) if long_way > 0 else (size - 1 - half, half)
-    f = b = None
-    for d in range(half, 0, -1):
-        if d <= f_len:
-            f = lax.ppermute(added(piece[d], f), axis, ahead)
-        if d <= b_len:
-            b = lax.ppermute(added(piece[size - d], b), axis, back)
-    return piece[0].astype(f32) + f.astype(f32) + b.astype(f32)
-
-
-def all_gather(block, size, long_way, axis):
-    half = size // 2
-    ahead, back = ring(size, 1), ring(size, -1)
-    f_len, b_len = (half, size - 1 - half) if long_way > 0 else (size - 1 - half, half)
+    x = lax.ppermute(piece[half], axis, one)
+    y = None
+    for d in range(half - 1, 0, -1):
+        x, y = (
+            lax.ppermute(added(piece[size - d], x), axis, two),
+            lax.ppermute(piece[d] if y is None else added(piece[d], y), axis, one),
+        )
+        x, y = y, x
+    return piece[0].astype(f32) + x.astype(f32) + y.astype(f32)
+
+
+def all_gather(block, size, flip, axis):
+    one, two = exchanges(size, flip)
     out = {0: block}
-    f = b = block
-    for d in range(1, half + 1):
-        if d <= f_len:
-            f = lax.ppermute(f, axis, ahead)
-            out[size - d] = f
-        if d <= b_len:
-            b = lax.ppermute(b, axis, back)
-            out[d] = b
+    x = y = block
+    for d in range(1, size // 2):
+        x, y = lax.ppermute(y, axis, one), lax.ppermute(x, axis, two)
+        out[d], out[size - d] = x, y
+    out[size // 2] = lax.ppermute(y, axis, one)
     return [out[d] for d in range(size)]
 
 
@@ -58,45 +55,44 @@
 IN_SMEM = pl.BlockSpec(memory_space=pltpu.SMEM)
 
 
-def block_row(me, d, size, rows):
-    return pl.multiple_of(lax.rem(me + d, size) * rows, 16)
-
-
-def project(me, gain, rows, gate, up, size, streams):
-    height, width = rows.shape
+def block_row(me, d, size, rows, flip):
+    along = 1 - 2 * lax.rem(me, 2)
+    return pl.multiple_of(lax.rem(me + size + (-d if flip else d) * along, size) * rows, 16)
+
+
+def project(me, gain, rows, first, height, gate, up, size, flip):
+    width = rows.shape[1]
     units = gate.shape[1]
-    part = height // streams
-    count = part // size
+    count = height // size
 
     def body(me_ref, gain_ref, rows_ref, gate_ref, up_ref, *refs):
         outs, turned_ref = refs[:-1], refs[-1]
-        for k in range(streams * size):
-            at = pl.multiple_of(k // size * part + block_row(me_ref[0], k % size, size, count), 16)
+        for d in range(size):
+            at = pl.multiple_of(first + block_row(me_ref[0], d, size, count, flip), 16)
             block = rows_ref[pl.ds(at, count), :].astype(f32)
             squares = jnp.sum(block * block, axis=1, keepdims=True)
-            outs[k][:, 2 * units :] = jnp.broadcast_to(squares, (count, LANES)).astype(bf16)
-            turned_ref[k * count : (k + 1) * count, :] = (block * gain_ref[...]).astype(bf16)
+            outs[d][:, 2 * units :] = jnp.broadcast_to(squares, (count, LANES)).astype(bf16)
+            turned_ref[d * count : (d + 1) * count, :] = (block * gain_ref[...]).astype(bf16)
 
         def columns(n, _):
             at = pl.multiple_of(n * TILE, TILE)
             for ref, base in ((gate_ref, 0), (up_ref, units)):
                 value = dot(turned_ref[...], ref[:, pl.ds(at, TILE)]).astype(bf16)
-                for k in range(streams * size):
-                    outs[k][:, pl.ds(pl.multiple_of(base + at, TILE), TILE)] = value[k * count : (k + 1) * count]
+                for d in range(size):
+                    outs[d][:, pl.ds(pl.multiple_of(base + at, TILE), TILE)] = value[d * count : (d + 1) * count]
             return 0
 
         lax.fori_loop(0, units // TILE, columns, 0)
 
-    out = pl.pallas_call(
+    return pl.pallas_call(
         body,
-        out_shape=[jax.ShapeDtypeStruct((count, 2 * units + LANES), bf16)] * (streams * size),
+        out_shape=[jax.ShapeDtypeStruct((count, 2 * units + LANES), bf16)] * size,
         in_specs=[IN_SMEM] + [IN_VMEM] * 4,
-        out_specs=[IN_VMEM] * (streams * size),
+        out_specs=[IN_VMEM] * size,
         scratch_shapes=[pltpu.VMEM((height, width), bf16)],
-        compiler_params=pltpu.CompilerParams(vmem_limit_bytes=16 << 20),
+        compiler_params=pltpu.CompilerParams(vmem_limit_bytes=12 << 20),
         name="project",
     )(me, gain, rows, gate, up)
-    return [out[k * size : (k + 1) * size] for k in range(streams)]
 
 
 def lower_down(me, blocks_a, blocks_b, matrix, shared_matrix):
@@ -110,10 +106,12 @@
         ins_a, ins_b = refs[:size], refs[size : 2 * size]
         matrix_ref, shared_ref, out_ref, shared_out_ref, rows_ref, shared_rows_ref = refs[2 * size :]
         for d in range(size):
-            at = block_row(me_ref[0], d, size, count)
-            rows_ref[pl.ds(at, count), :] = ins_a[d][...]
-            rows_ref[pl.ds(pl.multiple_of(part + at, 16), count), :] = ins_b[d][:count, :]
-            shared_rows_ref[pl.ds(block_row(me_ref[0], d, size, shared), shared), :] = ins_b[d][count:, :]
+            at_a = block_row(me_ref[0], d, size, count, False)
+            at_b = pl.multiple_of(part + block_row(me_ref[0], d, size, count, True), 16)
+            at_s = block_row(me_ref[0], d, size, shared, True)
+            rows_ref[pl.ds(at_a, count), :] = ins_a[d][...]
+            rows_ref[pl.ds(at_b, count), :] = ins_b[d][:count, :]
+            shared_rows_ref[pl.ds(at_s, shared), :] = ins_b[d][count:, :]
 
         def columns(n, _):
             at = pl.multiple_of(n * TILE, TILE)
@@ -192,15 +190,17 @@
     leaving = lax.dot_general(pick.astype(bf16), tokens, (((0,), (0,)), ((), ())), preferred_element_type=f32)
     rows = swapped(leaving.astype(bf16))
 
-    (pieces_s,) = project(me, gain, tokens, shared_gate, shared_up, tp, 1)
-    hidden_s = hidden_of(reduce_scatter(pieces_s, tp, 1, "tp"))
+    pieces_s = project(me, gain, tokens, 0, tok_count, shared_gate, shared_up, tp, False)
+    hidden_s = hidden_of(reduce_scatter(pieces_s, tp, False, "tp"))
     rows, hidden_s = lax.optimization_barrier((rows, hidden_s))
 
-    pieces_a, pieces_b = project(me, gain, rows, gate_matrix, up_matrix, tp, 2)
-    total_a = reduce_scatter(pieces_a, tp, -1, "tp")
-    total_b = reduce_scatter(pieces_b, tp, 1, "tp")
-    blocks_a = all_gather(hidden_of(total_a), tp, 1, "tp")
-    blocks_b = all_gather(jnp.concatenate([hidden_of(total_b), hidden_s], 0), tp, -1, "tp")
+    part = columns // 2
+    pieces_a = project(me, gain, rows, 0, part, gate_matrix, up_matrix, tp, False)
+    pieces_b = project(me, gain, rows, part, part, gate_matrix, up_matrix, tp, True)
+    total_a = reduce_scatter(pieces_a, tp, False, "tp")
+    total_b = reduce_scatter(pieces_b, tp, True, "tp")
+    blocks_a = all_gather(hidden_of(total_a), tp, False, "tp")
+    blocks_b = all_gather(jnp.concatenate([hidden_of(total_b), hidden_s], 0), tp, True, "tp")
     down, shared_out = lower_down(me, blocks_a, blocks_b, down_matrix, shared_down)
     came = swapped(down)
     mixture = shared_out + dot(high, came) + dot(low, came)

time: 193 us -> 192 us (level)
  starting transfers between devices: 80.4 us -> 61.7 us
  waiting for transfers between devices: 83.1 us -> 101 us
    ppermute x35, waiting for transfers between devices: 42.7 us -> 61.5 us  [the longest x9 28.6 us: reduce_scatter(): lax.ppermute(added(piece[size - d], x), axis, two)]
    ppermute x35, starting transfers between devices: 48.1 us -> 31.6 us  [the longest x9 9.31 us: reduce_scatter(): lax.ppermute(piece[d] if y is None else added(piece[d], y), axis, one)]
    all_to_all x2, starting transfers between devices: 32.3 us -> 30.1 us  [swapped(): lax.all_to_all(rows.reshape(experts, capacity, width), 'ep', 0, 0, tiled=...]
    pallas_call x2 -> x3, Pallas kernels: 5 us -> 5.75 us  [project(): pl.pallas_call(body, out_shape=[jax.ShapeDtypeStruct((count, 2 * units +...]
  transfers between devices with their start and end apart: 37 -> 37, of which waited for: 20 -> 24; matrix products, arithmetic and copies ran while one was open for 3% -> 2% of each run, Pallas kernels for 0% -> 1%
where the time goes in v2:
time: 192 us
  waiting for transfers between devices  101 us (53%)
  starting transfers between devices  61.7 us (32%)
  blocking collectives  9.24 us (5%)
  Pallas kernels  8.49 us (4%)
  local copies, waits for them, and re-layouts  4.17 us (2%)
  other arithmetic  3.5 us (2%)
  matrix products  2.88 us (2%)
    all_to_all x2, waiting for transfers between devices, swapped(): lax.all_to_all(rows.reshape(experts, capacity, width), 'ep', 0, 0, tiled=...  40 us
    all_to_all x2, starting transfers between devices, swapped(): lax.all_to_all(rows.reshape(experts, capacity, width), 'ep', 0, 0, tiled=...  30.1 us
    ppermute x9, waiting for transfers between devices, reduce_scatter(): lax.ppermute(added(piece[size - d], x), axis, two)  28.6 us
    ppermute x9, waiting for transfers between devices, reduce_scatter(): lax.ppermute(piece[d] if y is None else added(piece[d], y), axis, one)  16 us
    ppermute x12, waiting for transfers between devices, all_gather(): x, y = (lax.ppermute(y, axis, one), lax.ppermute(x, axis, two))  12.2 us
    ppermute x9, starting transfers between devices, reduce_scatter(): lax.ppermute(piece[d] if y is None else added(piece[d], y), axis, one)  9.31 us
    all_to_all x1, blocking collectives, layer(): square_sum = lax.all_to_all(copies, 'tp', 0, 0, tiled=True).sum(axis=0)  9.24 us
    ppermute x12, starting transfers between devices, all_gather(): x, y = (lax.ppermute(y, axis, one), lax.ppermute(x, axis, two))  8.25 us
  transfers between devices with their start and end apart: 37, of which 24 were waited for; matrix products, arithmetic and copies ran while one was open for 2% of the time, Pallas kernels for 1%

profile of v2, /device:TPU:513, one launch (start us, length us, event | category | flops | bytes accessed | tf_op | source)
XLA Modules:
  0.0 191.8 jit_solution(16751069808926847943)
XLA Ops:
  0.8 1.2 copy-done.4
  2.0 1.2 copy-done.5
  3.2 0.9 copy-done.6
  4.1 1.7 project.3
  5.8 2.2 %collective-permute-start.3 = (bf16[16,2176]{1,0:T(8,128)(2,1)}, bf16[16,2176]{1,0:T(8,128)(2,1)}, u32[]{:S(2)}, u32[]{:S(2)}) collective-permute-start(bf16[16,2176]{1,0:T(8,128)(2,1)} %get-tuple-element.40), channel_id=1, source_target_pairs={{0,1},{1,0},{2,3},{3,2},{4,5},{5,4},{6,7},{7,6},{8,9},{9,8},{10,11... | collective-permute-start | bytes 208904 | tf_op jit(solution)/shard_map/ppermute | solution.py:30
  8.5 1.5 convolution_convert_fusion
  10.0 21.9 %all-to-all-start = ((bf16[16,64,512]{2,1,0:T(8,128)(2,1)}), bf16[16,64,512]{2,1,0:T(8,128)(2,1)S(1)}, u32[]{:S(2)}, u32[]{:S(2)}) async-start(bf16[16,64,512]{2,1,0:T(8,128)(2,1)} %bitcast.2), calls=%async_computation | async-start | bytes 2097152 | tf_op jit(solution)/shard_map/all_to_all | solution.py:180
  31.8 1.9 collective-permute-start
  33.7 0.9 add_convert_fusion.12
  34.8 0.8 collective-permute-done
  35.6 1.9 %collective-permute-start.1 = (bf16[16,2176]{1,0:T(8,128)(2,1)S(1)}, bf16[16,2176]{1,0:T(8,128)(2,1)S(1)}, u32[]{:S(2)}, u32[]{:S(2)}) collective-permute-start(bf16[16,2176]{1,0:T(8,128)(2,1)S(1)} %add_convert_fusion.14), channel_id=1, source_target_pairs={{0,7},{1,2},{2,1},{3,4},{4,3},{5,6},{6,5},{7,0},{8,15},{9,10},{10,... | collective-permute-start | bytes 208904 | tf_op jit(solution)/shard_map/ppermute | solution.py:34
  37.6 1.8 collective-permute-done.4
  39.6 1.2 collective-permute-done.1
  41.2 1.8 collective-permute-done.5
  43.2 1.2 collective-permute-done.2
  44.4 3.5 %collective-permute-done.6 = bf16[16,2176]{1,0:T(8,128)(2,1)S(1)} collective-permute-done((bf16[16,2176]{1,0:T(8,128)(2,1)S(1)}, bf16[16,2176]{1,0:T(8,128)(2,1)S(1)}, u32[]{:S(2)}, u32[]{:S(2)}) %collective-permute-start.6) | collective-permute-done | bytes 69664 | tf_op jit(solution)/shard_map/ppermute | solution.py:34
  48.1 11.9 %all-to-all-done = bf16[16,64,512]{2,1,0:T(8,128)(2,1)S(1)} async-done(((bf16[16,64,512]{2,1,0:T(8,128)(2,1)}), bf16[16,64,512]{2,1,0:T(8,128)(2,1)S(1)}, u32[]{:S(2)}, u32[]{:S(2)}) %all-to-all-start) | async-done | bytes 1048608 | tf_op jit(solution)/shard_map/all_to_all | solution.py:180
  60.0 2.0 %project.4 = (bf16[64,2176]{1,0:T(8,128)(2,1)S(1)}, bf16[64,2176]{1,0:T(8,128)(2,1)S(1)}, bf16[64,2176]{1,0:T(8,128)(2,1)S(1)}, bf16[64,2176]{1,0:T(8,128)(2,1)S...) custom-call(s32[1]{0:T(128)} %bitcast.me_ref, ...), custom_call_target="tpu_custom_call" | custom-call | tf_op jit(solution)/shard_map/project/pallas_call | solution.py:87
  62.0 1.9 collective-permute-start.10
  63.9 2.0 %project.5 = (bf16[64,2176]{1,0:T(8,128)(2,1)S(1)}, bf16[64,2176]{1,0:T(8,128)(2,1)S(1)}, bf16[64,2176]{1,0:T(8,128)(2,1)S(1)}, bf16[64,2176]{1,0:T(8,128)(2,1)S...) custom-call(s32[1]{0:T(128)} %bitcast.me_ref, ...), custom_call_target="tpu_custom_call" | custom-call | tf_op jit(solution)/shard_map/project/pallas_call | solution.py:87
  66.2 2.6 %collective-permute-start.21 = (bf16[64,2176]{1,0:T(8,128)(2,1)S(1)}, bf16[64,2176]{1,0:T(8,128)(2,1)S(1)}, u32[]{:S(2)}, u32[]{:S(2)}) collective-permute-start(bf16[64,2176]{1,0:T(8,128)(2,1)S(1)} %get-tuple-element.53), channel_id=1, source_target_pairs={{0,7},{1,2},{2,1},{3,4},{4,3},{5,6},{6,5},{7,0},{8,15},{9,10},{10,... | collective-permute-start | bytes 835592 | tf_op jit(solution)/shard_map/ppermute | solution.py:35
  68.8 2.3 %collective-permute-done.10 = bf16[64,2176]{1,0:T(8,128)(2,1)S(1)} collective-permute-done((bf16[64,2176]{1,0:T(8,128)(2,1)S(1)}, bf16[64,2176]{1,0:T(8,128)(2,1)S(1)}, u32[]{:S(2)}, u32[]{:S(2)}) %collective-permute-start.10) | collective-permute-done | bytes 278560 | tf_op jit(solution)/shard_map/ppermute | solution.py:30
  71.3 4.7 %collective-permute-done.7 = bf16[64,2176]{1,0:T(8,128)(2,1)S(1)} collective-permute-done((bf16[64,2176]{1,0:T(8,128)(2,1)S(1)}, bf16[64,2176]{1,0:T(8,128)(2,1)S(1)}, u32[]{:S(2)}, u32[]{:S(2)}) %collective-permute-start.7) | collective-permute-done | bytes 278560 | tf_op jit(solution)/shard_map/ppermute | solution.py:35
  76.3 1.8 collective-permute-start.25
  78.2 3.9 %collective-permute-done.21 = bf16[64,2176]{1,0:T(8,128)(2,1)S(1)} collective-permute-done((bf16[64,2176]{1,0:T(8,128)(2,1)S(1)}, bf16[64,2176]{1,0:T(8,128)(2,1)S(1)}, u32[]{:S(2)}, u32[]{:S(2)}) %collective-permute-start.21) | collective-permute-done | bytes 278560 | tf_op jit(solution)/shard_map/ppermute | solution.py:35
  82.3 5.7 %collective-permute-done.11 = bf16[64,2176]{1,0:T(8,128)(2,1)S(1)} collective-permute-done((bf16[64,2176]{1,0:T(8,128)(2,1)S(1)}, bf16[64,2176]{1,0:T(8,128)(2,1)S(1)}, u32[]{:S(2)}, u32[]{:S(2)}) %collective-permute-start.11) | collective-permute-done | bytes 278560 | tf_op jit(solution)/shard_map/ppermute | solution.py:34
  88.5 4.7 %collective-permute-done.8 = bf16[64,2176]{1,0:T(8,128)(2,1)S(1)} collective-permute-done((bf16[64,2176]{1,0:T(8,128)(2,1)S(1)}, bf16[64,2176]{1,0:T(8,128)(2,1)S(1)}, u32[]{:S(2)}, u32[]{:S(2)}) %collective-permute-start.8) | collective-permute-done | bytes 278560 | tf_op jit(solution)/shard_map/ppermute | solution.py:34
  94.3 2.8 %collective-permute-start.23 = (bf16[64,2176]{1,0:T(8,128)(2,1)S(1)}, bf16[64,2176]{1,0:T(8,128)(2,1)S(1)}, u32[]{:S(2)}, u32[]{:S(2)}) collective-permute-start(bf16[64,2176]{1,0:T(8,128)(2,1)S(1)} %add_convert_fusion.3), channel_id=1, source_target_pairs={{0,7},{1,2},{2,1},{3,4},{4,3},{5,6},{6,5},{7,0},{8,15},{9,10},{10,... | collective-permute-start | bytes 835592 | tf_op jit(solution)/shard_map/ppermute | solution.py:35
  97.4 2.4 %collective-permute-start.13 = (bf16[64,2176]{1,0:T(8,128)(2,1)S(1)}, bf16[64,2176]{1,0:T(8,128)(2,1)S(1)}, u32[]{:S(2)}, u32[]{:S(2)}) collective-permute-start(bf16[64,2176]{1,0:T(8,128)(2,1)S(1)} %add_convert_fusion.5), channel_id=1, source_target_pairs={{0,7},{1,2},{2,1},{3,4},{4,3},{5,6},{6,5},{7,0},{8,15},{9,10},{10,... | collective-permute-start | bytes 835592 | tf_op jit(solution)/shard_map/ppermute | solution.py:34
  99.8 3.4 %collective-permute-done.26 = bf16[64,2176]{1,0:T(8,128)(2,1)S(1)} collective-permute-done((bf16[64,2176]{1,0:T(8,128)(2,1)S(1)}, bf16[64,2176]{1,0:T(8,128)(2,1)S(1)}, u32[]{:S(2)}, u32[]{:S(2)}) %collective-permute-start.26) | collective-permute-done | bytes 278560 | tf_op jit(solution)/shard_map/ppermute | solution.py:35
  103.4 11.7 %collective-permute-done.13 = bf16[64,2176]{1,0:T(8,128)(2,1)S(1)} collective-permute-done((bf16[64,2176]{1,0:T(8,128)(2,1)S(1)}, bf16[64,2176]{1,0:T(8,128)(2,1)S(1)}, u32[]{:S(2)}, u32[]{:S(2)}) %collective-permute-start.13) | collective-permute-done | bytes 278560 | tf_op jit(solution)/shard_map/ppermute | solution.py:34
  116.5 2.4 %collective-permute-start.28 = (bf16[80,1024]{1,0:T(8,128)(2,1)S(1)}, bf16[80,1024]{1,0:T(8,128)(2,1)S(1)}, u32[]{:S(2)}, u32[]{:S(2)}) collective-permute-start(bf16[80,1024]{1,0:T(8,128)(2,1)S(1)} %pad_maximum_fusion.refs_8_), channel_id=1, source_target_pairs={{0,7},{1,2},{2,1},{3,4},{4,3},{5,6},{6,5},{7,0},{8,15},{9,10},{10,... | collective-permute-start | bytes 491528 | tf_op jit(solution)/shard_map/ppermute | solution.py:46
  118.9 1.2 collective-permute-done.29.refs_15_
  120.1 0.9 collective-permute-start.30
  121.3 1.2 collective-permute-start.16
  122.4 2.3 %collective-permute-done.28.refs_9_ = bf16[80,1024]{1,0:T(8,128)(2,1)S(1)} collective-permute-done((bf16[80,1024]{1,0:T(8,128)(2,1)S(1)}, bf16[80,1024]{1,0:T(8,128)(2,1)S(1)}, u32[]{:S(2)}, u32[]{:S(2)}) %collective-permute-start.28) | collective-permute-done | bytes 163872 | tf_op jit(solution)/shard_map/ppermute | solution.py:46
  124.7 3.5 %collective-permute-done.30.refs_10_ = bf16[80,1024]{1,0:T(8,128)(2,1)S(1)} collective-permute-done((bf16[80,1024]{1,0:T(8,128)(2,1)S(1)}, bf16[80,1024]{1,0:T(8,128)(2,1)S(1)}, u32[]{:S(2)}, u32[]{:S(2)}) %collective-permute-start.30) | collective-permute-done | bytes 163872 | tf_op jit(solution)/shard_map/ppermute | solution.py:46
  128.9 2.0 %collective-permute-start.19 = (bf16[64,1024]{1,0:T(8,128)(2,1)S(1)}, bf16[64,1024]{1,0:T(8,128)(2,1)S(1)}, u32[]{:S(2)}, u32[]{:S(2)}) collective-permute-start(bf16[64,1024]{1,0:T(8,128)(2,1)S(1)} %collective-permute-done.16.refs_2_), channel_id=1, source_target_pairs={{0,7},{1,2},{2,1},{3,4},{4,3},{5,6},{6,5},{7,0},{8,15},{9,10},{10,... | collective-permute-start | bytes 393224 | tf_op jit(solution)/shard_map/ppermute | solution.py:46
  131.5 2.2 %collective-permute-done.33.refs_13_ = bf16[80,1024]{1,0:T(8,128)(2,1)S(1)} collective-permute-done((bf16[80,1024]{1,0:T(8,128)(2,1)S(1)}, bf16[80,1024]{1,0:T(8,128)(2,1)S(1)}, u32[]{:S(2)}, u32[]{:S(2)}) %collective-permute-start.33) | collective-permute-done | bytes 163872 | tf_op jit(solution)/shard_map/ppermute | solution.py:46
  133.8 1.3 collective-permute-start.34
  135.1 1.5 collective-permute-start.20
  136.5 2.6 %collective-permute-done.18.refs_3_ = bf16[64,1024]{1,0:T(8,128)(2,1)S(1)} collective-permute-done((bf16[64,1024]{1,0:T(8,128)(2,1)S(1)}, bf16[64,1024]{1,0:T(8,128)(2,1)S(1)}, u32[]{:S(2)}, u32[]{:S(2)}) %collective-permute-start.18) | collective-permute-done | bytes 131104 | tf_op jit(solution)/shard_map/ppermute | solution.py:46
  139.2 1.4 collective-permute-done.20.refs_4_
  140.6 1.1 collective-permute-done.34.refs_12_
  141.6 2.7 %lower_down.1 = (bf16[1024,512]{1,0:T(8,128)(2,1)}, f32[128,512]{1,0:T(8,128)S(1)}) custom-call(s32[1]{0:T(128)} %bitcast.me_ref, bf16[64,1024]{1,0:T(8,128)(2,1)S(1)} %fusion.9.refs_0_, bf16[64,1024]{1,0:T(8,128)(2,1)S(1)} %collective-permute-done.14.refs_1_, bf16[64,1024]{1,0:T(8,128)(2,1)S(1)} %collective-permute-done.16.refs_2_, ...), custom_call_target="tpu_custom_call" | custom-call | tf_op jit(solution)/shard_map/lower_down/pallas_call | solution.py:124
  144.4 8.2 %all-to-all-start.1 = ((bf16[16,64,512]{2,1,0:T(8,128)(2,1)}), bf16[16,64,512]{2,1,0:T(8,128)(2,1)S(1)}, u32[]{:S(2)}, u32[]{:S(2)}) async-start(bf16[16,64,512]{2,1,0:T(8,128)(2,1)} %bitcast.7), calls=%async_computation.1 | async-start | bytes 2097152 | tf_op jit(solution)/shard_map/all_to_all | solution.py:180
  152.6 28.1 %all-to-all-done.1 = bf16[16,64,512]{2,1,0:T(8,128)(2,1)S(1)} async-done(((bf16[16,64,512]{2,1,0:T(8,128)(2,1)}), bf16[16,64,512]{2,1,0:T(8,128)(2,1)S(1)}, u32[]{:S(2)}, u32[]{:S(2)}) %all-to-all-start.1) | async-done | bytes 1048608 | tf_op jit(solution)/shard_map/all_to_all | solution.py:180
  181.8 9.2 %all_to_all.15 = f32[8,128,1]{1,2,0:T(1,128)S(1)} all-to-all(f32[8,128,1]{1,2,0:T(1,128)S(1)} %broadcast_in_dim.34), channel_id=1, replica_groups=mesh['grp'=2,'ep'=16,'tp'=8] {'tp'}, dimensions={0} | all-to-all | bytes 8192 | tf_op jit(solution)/shard_map/all_to_all | solution.py:210
  (100 shorter events, 10.3 us)
Async XLA Ops:
  4.1 3.9 %copy-start.12 = (s32[128,4]{0,1:T(4,128)S(1)}, s32[128,4]{0,1:T(4,128)}, u32[]{:S(2)}) copy-start(s32[128,4]{0,1:T(4,128)} %param.12) | copy-start | bytes 6148
  4.1 4.4 %copy-start.7 = (bf16[128,512]{1,0:T(8,128)(2,1)S(1)}, bf16[128,512]{1,0:T(8,128)(2,1)}, u32[]{:S(2)}) copy-start(bf16[128,512]{1,0:T(8,128)(2,1)} %rows_ref.1) | copy-start | bytes 393220
  5.8 4.1 %copy-start.8 = (bf16[16,2176]{1,0:T(8,128)(2,1)}, bf16[16,2176]{1,0:T(8,128)(2,1)S(1)}, u32[]{:S(2)}) copy-start(bf16[16,2176]{1,0:T(8,128)(2,1)S(1)} %get-tuple-element.39) | copy-start | bytes 208900
  5.8 4.1 %copy-start.9 = (bf16[16,2176]{1,0:T(8,128)(2,1)}, bf16[16,2176]{1,0:T(8,128)(2,1)S(1)}, u32[]{:S(2)}) copy-start(bf16[16,2176]{1,0:T(8,128)(2,1)S(1)} %get-tuple-element.36) | copy-start | bytes 208900
  5.8 27.9 %collective-permute-start.3 = (bf16[16,2176]{1,0:T(8,128)(2,1)}, bf16[16,2176]{1,0:T(8,128)(2,1)}, u32[]{:S(2)}, u32[]{:S(2)}) collective-permute-start(bf16[16,2176]{1,0:T(8,128)(2,1)} %get-tuple-element.40), channel_id=1, source_target_pairs={{0,1},{1,0},{2,3},{3,2},{4,5},{5,4},{6,7},{7,6},{8,9},{9,8},{10,11... | collective-permute-start | bytes 208904 | tf_op jit(solution)/shard_map/ppermute | solution.py:30
  10.0 50.0 %copy-start.1 = (bf16[1,512,1024]{2,1,0:T(8,128)(2,1)S(1)}, bf16[1,512,1024]{2,1,0:T(8,128)(2,1)}, u32[]{:S(2)}) copy-start(bf16[1,512,1024]{2,1,0:T(8,128)(2,1)} %param.16) | copy-start | bytes 3145732
  10.0 50.0 %all-to-all-start = ((bf16[16,64,512]{2,1,0:T(8,128)(2,1)}), bf16[16,64,512]{2,1,0:T(8,128)(2,1)S(1)}, u32[]{:S(2)}, u32[]{:S(2)}) async-start(bf16[16,64,512]{2,1,0:T(8,128)(2,1)} %bitcast.2), calls=%async_computation | async-start | bytes 2097152 | tf_op jit(solution)/shard_map/all_to_all | solution.py:180
  31.8 28.1 %copy-start = (bf16[1,512,1024]{2,1,0:T(8,128)(2,1)S(1)}, bf16[1,512,1024]{2,1,0:T(8,128)(2,1)}, u32[]{:S(2)}) copy-start(bf16[1,512,1024]{2,1,0:T(8,128)(2,1)} %param.15) | copy-start | bytes 3145732
  31.8 3.8 %collective-permute-start = (bf16[16,2176]{1,0:T(8,128)(2,1)}, bf16[16,2176]{1,0:T(8,128)(2,1)S(1)}, u32[]{:S(2)}, u32[]{:S(2)}) collective-permute-start(bf16[16,2176]{1,0:T(8,128)(2,1)} %copy-done.9), channel_id=1, source_target_pairs={{0,1},{1,0},{2,3},{3,2},{4,5},{5,4},{6,7},{7,6},{8,9},{9,8},{10,11... | collective-permute-start | bytes 208904 | tf_op jit(solution)/shard_map/ppermute | solution.py:35
  34.6 4.8 %collective-permute-start.4 = (bf16[16,2176]{1,0:T(8,128)(2,1)S(1)}, bf16[16,2176]{1,0:T(8,128)(2,1)S(1)}, u32[]{:S(2)}, u32[]{:S(2)}) collective-permute-start(bf16[16,2176]{1,0:T(8,128)(2,1)S(1)} %add_convert_fusion.12), channel_id=1, source_target_pairs={{0,7},{1,2},{2,1},{3,4},{4,3},{5,6},{6,5},{7,0},{8,15},{9,10},{10,... | collective-permute-start | bytes 208904 | tf_op jit(solution)/shard_map/ppermute | solution.py:34
  35.6 5.1 %collective-permute-start.1 = (bf16[16,2176]{1,0:T(8,128)(2,1)S(1)}, bf16[16,2176]{1,0:T(8,128)(2,1)S(1)}, u32[]{:S(2)}, u32[]{:S(2)}) collective-permute-start(bf16[16,2176]{1,0:T(8,128)(2,1)S(1)} %add_convert_fusion.14), channel_id=1, source_target_pairs={{0,7},{1,2},{2,1},{3,4},{4,3},{5,6},{6,5},{7,0},{8,15},{9,10},{10,... | collective-permute-start | bytes 208904 | tf_op jit(solution)/shard_map/ppermute | solution.py:34
  39.5 3.6 %collective-permute-start.5 = (bf16[16,2176]{1,0:T(8,128)(2,1)S(1)}, bf16[16,2176]{1,0:T(8,128)(2,1)S(1)}, u32[]{:S(2)}, u32[]{:S(2)}) collective-permute-start(bf16[16,2176]{1,0:T(8,128)(2,1)S(1)} %add_convert_fusion.11), channel_id=1, source_target_pairs={{0,1},{1,0},{2,3},{3,2},{4,5},{5,4},{6,7},{7,6},{8,9},{9,8},{10,11... | collective-permute-start | bytes 208904 | tf_op jit(solution)/shard_map/ppermute | solution.py:35
  40.8 3.6 %collective-permute-start.2 = (bf16[16,2176]{1,0:T(8,128)(2,1)S(1)}, bf16[16,2176]{1,0:T(8,128)(2,1)S(1)}, u32[]{:S(2)}, u32[]{:S(2)}) collective-permute-start(bf16[16,2176]{1,0:T(8,128)(2,1)S(1)} %add_convert_fusion.13), channel_id=1, source_target_pairs={{0,1},{1,0},{2,3},{3,2},{4,5},{5,4},{6,7},{7,6},{8,9},{9,8},{10,11... | collective-permute-start | bytes 208904 | tf_op jit(solution)/shard_map/ppermute | solution.py:35
  43.1 4.8 %collective-permute-start.6 = (bf16[16,2176]{1,0:T(8,128)(2,1)S(1)}, bf16[16,2176]{1,0:T(8,128)(2,1)S(1)}, u32[]{:S(2)}, u32[]{:S(2)}) collective-permute-start(bf16[16,2176]{1,0:T(8,128)(2,1)S(1)} %add_convert_fusion.10), channel_id=1, source_target_pairs={{0,7},{1,2},{2,1},{3,4},{4,3},{5,6},{6,5},{7,0},{8,15},{9,10},{10,... | collective-permute-start | bytes 208904 | tf_op jit(solution)/shard_map/ppermute | solution.py:34
  62.0 9.1 %collective-permute-start.10 = (bf16[64,2176]{1,0:T(8,128)(2,1)S(1)}, bf16[64,2176]{1,0:T(8,128)(2,1)S(1)}, u32[]{:S(2)}, u32[]{:S(2)}) collective-permute-start(bf16[64,2176]{1,0:T(8,128)(2,1)S(1)} %get-tuple-element.49), channel_id=1, source_target_pairs={{0,1},{1,0},{2,3},{3,2},{4,5},{5,4},{6,7},{7,6},{8,9},{9,8},{10,11... | collective-permute-start | bytes 835592 | tf_op jit(solution)/shard_map/ppermute | solution.py:30
  65.9 10.1 %collective-permute-start.7 = (bf16[64,2176]{1,0:T(8,128)(2,1)S(1)}, bf16[64,2176]{1,0:T(8,128)(2,1)S(1)}, u32[]{:S(2)}, u32[]{:S(2)}) collective-permute-start(bf16[64,2176]{1,0:T(8,128)(2,1)S(1)} %get-tuple-element.45), channel_id=1, source_target_pairs={{0,1},{1,0},{2,3},{3,2},{4,5},{5,4},{6,7},{7,6},{8,9},{9,8},{10,11... | collective-permute-start | bytes 835592 | tf_op jit(solution)/shard_map/ppermute | solution.py:35
  66.1 10.2 %collective-permute-start.24 = (bf16[64,2176]{1,0:T(8,128)(2,1)S(1)}, bf16[64,2176]{1,0:T(8,128)(2,1)S(1)}, u32[]{:S(2)}, u32[]{:S(2)}) collective-permute-start(bf16[64,2176]{1,0:T(8,128)(2,1)S(1)} %get-tuple-element.57), channel_id=1, source_target_pairs={{0,7},{1,2},{2,1},{3,4},{4,3},{5,6},{6,5},{7,0},{8,15},{9,10},{10,... | collective-permute-start | bytes 835592 | tf_op jit(solution)/shard_map/ppermute | solution.py:30
  66.2 15.8 %collective-permute-start.21 = (bf16[64,2176]{1,0:T(8,128)(2,1)S(1)}, bf16[64,2176]{1,0:T(8,128)(2,1)S(1)}, u32[]{:S(2)}, u32[]{:S(2)}) collective-permute-start(bf16[64,2176]{1,0:T(8,128)(2,1)S(1)} %get-tuple-element.53), channel_id=1, source_target_pairs={{0,7},{1,2},{2,1},{3,4},{4,3},{5,6},{6,5},{7,0},{8,15},{9,10},{10,... | collective-permute-start | bytes 835592 | tf_op jit(solution)/shard_map/ppermute | solution.py:35
  71.2 16.8 %collective-permute-start.11 = (bf16[64,2176]{1,0:T(8,128)(2,1)S(1)}, bf16[64,2176]{1,0:T(8,128)(2,1)S(1)}, u32[]{:S(2)}, u32[]{:S(2)}) collective-permute-start(bf16[64,2176]{1,0:T(8,128)(2,1)S(1)} %add_convert_fusion.7), channel_id=1, source_target_pairs={{0,7},{1,2},{2,1},{3,4},{4,3},{5,6},{6,5},{7,0},{8,15},{9,10},{10,... | collective-permute-start | bytes 835592 | tf_op jit(solution)/shard_map/ppermute | solution.py:34
  76.1 17.1 %collective-permute-start.8 = (bf16[64,2176]{1,0:T(8,128)(2,1)S(1)}, bf16[64,2176]{1,0:T(8,128)(2,1)S(1)}, u32[]{:S(2)}, u32[]{:S(2)}) collective-permute-start(bf16[64,2176]{1,0:T(8,128)(2,1)S(1)} %add_convert_fusion.9), channel_id=1, source_target_pairs={{0,7},{1,2},{2,1},{3,4},{4,3},{5,6},{6,5},{7,0},{8,15},{9,10},{10,... | collective-permute-start | bytes 835592 | tf_op jit(solution)/shard_map/ppermute | solution.py:34
  76.3 17.7 %collective-permute-start.25 = (bf16[64,2176]{1,0:T(8,128)(2,1)S(1)}, bf16[64,2176]{1,0:T(8,128)(2,1)S(1)}, u32[]{:S(2)}, u32[]{:S(2)}) collective-permute-start(bf16[64,2176]{1,0:T(8,128)(2,1)S(1)} %add_convert_fusion.2), channel_id=1, source_target_pairs={{0,1},{1,0},{2,3},{3,2},{4,5},{5,4},{6,7},{7,6},{8,9},{9,8},{10,11... | collective-permute-start | bytes 835592 | tf_op jit(solution)/shard_map/ppermute | solution.py:34
  82.1 12.2 %collective-permute-start.22 = (bf16[64,2176]{1,0:T(8,128)(2,1)S(1)}, bf16[64,2176]{1,0:T(8,128)(2,1)S(1)}, u32[]{:S(2)}, u32[]{:S(2)}) collective-permute-start(bf16[64,2176]{1,0:T(8,128)(2,1)S(1)} %add_convert_fusion.4), channel_id=1, source_target_pairs={{0,1},{1,0},{2,3},{3,2},{4,5},{5,4},{6,7},{7,6},{8,9},{9,8},{10,11... | collective-permute-start | bytes 835592 | tf_op jit(solution)/shard_map/ppermute | solution.py:34
  88.0 9.3 %collective-permute-start.12 = (bf16[64,2176]{1,0:T(8,128)(2,1)S(1)}, bf16[64,2176]{1,0:T(8,128)(2,1)S(1)}, u32[]{:S(2)}, u32[]{:S(2)}) collective-permute-start(bf16[64,2176]{1,0:T(8,128)(2,1)S(1)} %add_convert_fusion.6), channel_id=1, source_target_pairs={{0,1},{1,0},{2,3},{3,2},{4,5},{5,4},{6,7},{7,6},{8,9},{9,8},{10,11... | collective-permute-start | bytes 835592 | tf_op jit(solution)/shard_map/ppermute | solution.py:35
  93.2 10.2 %collective-permute-start.9 = (bf16[64,2176]{1,0:T(8,128)(2,1)S(1)}, bf16[64,2176]{1,0:T(8,128)(2,1)S(1)}, u32[]{:S(2)}, u32[]{:S(2)}) collective-permute-start(bf16[64,2176]{1,0:T(8,128)(2,1)S(1)} %add_convert_fusion.8), channel_id=1, source_target_pairs={{0,1},{1,0},{2,3},{3,2},{4,5},{5,4},{6,7},{7,6},{8,9},{9,8},{10,11... | collective-permute-start | bytes 835592 | tf_op jit(solution)/shard_map/ppermute | solution.py:35
  94.1 9.1 %collective-permute-start.26 = (bf16[64,2176]{1,0:T(8,128)(2,1)S(1)}, bf16[64,2176]{1,0:T(8,128)(2,1)S(1)}, u32[]{:S(2)}, u32[]{:S(2)}) collective-permute-start(bf16[64,2176]{1,0:T(8,128)(2,1)S(1)} %add_convert_fusion.1), channel_id=1, source_target_pairs={{0,7},{1,2},{2,1},{3,4},{4,3},{5,6},{6,5},{7,0},{8,15},{9,10},{10,... | collective-permute-start | bytes 835592 | tf_op jit(solution)/shard_map/ppermute | solution.py:35
  94.3 21.0 %collective-permute-start.23 = (bf16[64,2176]{1,0:T(8,128)(2,1)S(1)}, bf16[64,2176]{1,0:T(8,128)(2,1)S(1)}, u32[]{:S(2)}, u32[]{:S(2)}) collective-permute-start(bf16[64,2176]{1,0:T(8,128)(2,1)S(1)} %add_convert_fusion.3), channel_id=1, source_target_pairs={{0,7},{1,2},{2,1},{3,4},{4,3},{5,6},{6,5},{7,0},{8,15},{9,10},{10,... | collective-permute-start | bytes 835592 | tf_op jit(solution)/shard_map/ppermute | solution.py:35
  97.4 17.8 %collective-permute-start.13 = (bf16[64,2176]{1,0:T(8,128)(2,1)S(1)}, bf16[64,2176]{1,0:T(8,128)(2,1)S(1)}, u32[]{:S(2)}, u32[]{:S(2)}) collective-permute-start(bf16[64,2176]{1,0:T(8,128)(2,1)S(1)} %add_convert_fusion.5), channel_id=1, source_target_pairs={{0,7},{1,2},{2,1},{3,4},{4,3},{5,6},{6,5},{7,0},{8,15},{9,10},{10,... | collective-permute-start | bytes 835592 | tf_op jit(solution)/shard_map/ppermute | solution.py:34
  103.3 12.1 %collective-permute-start.27 = (bf16[64,2176]{1,0:T(8,128)(2,1)S(1)}, bf16[64,2176]{1,0:T(8,128)(2,1)S(1)}, u32[]{:S(2)}, u32[]{:S(2)}) collective-permute-start(bf16[64,2176]{1,0:T(8,128)(2,1)S(1)} %add_convert_fusion), channel_id=1, source_target_pairs={{0,1},{1,0},{2,3},{3,2},{4,5},{5,4},{6,7},{7,6},{8,9},{9,8},{10,11... | collective-permute-start | bytes 835592 | tf_op jit(solution)/shard_map/ppermute | solution.py:34
  115.4 26.3 %copy-start.3 = (bf16[1024,512]{1,0:T(8,128)(2,1)S(1)}, bf16[1024,512]{1,0:T(8,128)(2,1)}, u32[]{:S(2)}) copy-start(bf16[1024,512]{1,0:T(8,128)(2,1)} %refs_17_.1) | copy-start | bytes 3145732
  115.5 26.2 %copy-start.2 = (bf16[1,1024,512]{2,1,0:T(8,128)(2,1)S(1)}, bf16[1,1024,512]{2,1,0:T(8,128)(2,1)}, u32[]{:S(2)}) copy-start(bf16[1,1024,512]{2,1,0:T(8,128)(2,1)} %param.17) | copy-start | bytes 3145732
  115.8 4.3 %collective-permute-start.29 = (bf16[80,1024]{1,0:T(8,128)(2,1)S(1)}, bf16[80,1024]{1,0:T(8,128)(2,1)S(1)}, u32[]{:S(2)}, u32[]{:S(2)}) collective-permute-start(bf16[80,1024]{1,0:T(8,128)(2,1)S(1)} %pad_maximum_fusion.refs_8_), channel_id=1, source_target_pairs={{0,1},{1,0},{2,3},{3,2},{4,5},{5,4},{6,7},{7,6},{8,9},{9,8},{10,11... | collective-permute-start | bytes 491528 | tf_op jit(solution)/shard_map/ppermute | solution.py:46
  116.1 5.2 %collective-permute-start.15 = (bf16[64,1024]{1,0:T(8,128)(2,1)S(1)}, bf16[64,1024]{1,0:T(8,128)(2,1)S(1)}, u32[]{:S(2)}, u32[]{:S(2)}) collective-permute-start(bf16[64,1024]{1,0:T(8,128)(2,1)S(1)} %fusion.9.refs_0_), channel_id=1, source_target_pairs={{0,7},{1,2},{2,1},{3,4},{4,3},{5,6},{6,5},{7,0},{8,15},{9,10},{10,... | collective-permute-start | bytes 393224 | tf_op jit(solution)/shard_map/ppermute | solution.py:46
  116.5 8.2 %collective-permute-start.28 = (bf16[80,1024]{1,0:T(8,128)(2,1)S(1)}, bf16[80,1024]{1,0:T(8,128)(2,1)S(1)}, u32[]{:S(2)}, u32[]{:S(2)}) collective-permute-start(bf16[80,1024]{1,0:T(8,128)(2,1)S(1)} %pad_maximum_fusion.refs_8_), channel_id=1, source_target_pairs={{0,7},{1,2},{2,1},{3,4},{4,3},{5,6},{6,5},{7,0},{8,15},{9,10},{10,... | collective-permute-start | bytes 491528 | tf_op jit(solution)/shard_map/ppermute | solution.py:46
  120.1 8.1 %collective-permute-start.30 = (bf16[80,1024]{1,0:T(8,128)(2,1)S(1)}, bf16[80,1024]{1,0:T(8,128)(2,1)S(1)}, u32[]{:S(2)}, u32[]{:S(2)}) collective-permute-start(bf16[80,1024]{1,0:T(8,128)(2,1)S(1)} %collective-permute-done.29.refs_15_), channel_id=1, source_target_pairs={{0,7},{1,2},{2,1},{3,4},{4,3},{5,6},{6,5},{7,0},{8,15},{9,10},{10,... | collective-permute-start | bytes 491528 | tf_op jit(solution)/shard_map/ppermute | solution.py:46
  121.0 7.3 %collective-permute-start.14 = (bf16[64,1024]{1,0:T(8,128)(2,1)S(1)}, bf16[64,1024]{1,0:T(8,128)(2,1)S(1)}, u32[]{:S(2)}, u32[]{:S(2)}) collective-permute-start(bf16[64,1024]{1,0:T(8,128)(2,1)S(1)} %fusion.9.refs_0_), channel_id=1, source_target_pairs={{0,1},{1,0},{2,3},{3,2},{4,5},{5,4},{6,7},{7,6},{8,9},{9,8},{10,11... | collective-permute-start | bytes 393224 | tf_op jit(solution)/shard_map/ppermute | solution.py:46
  121.3 7.6 %collective-permute-start.16 = (bf16[64,1024]{1,0:T(8,128)(2,1)S(1)}, bf16[64,1024]{1,0:T(8,128)(2,1)S(1)}, u32[]{:S(2)}, u32[]{:S(2)}) collective-permute-start(bf16[64,1024]{1,0:T(8,128)(2,1)S(1)} %collective-permute-done.15.refs_7_), channel_id=1, source_target_pairs={{0,1},{1,0},{2,3},{3,2},{4,5},{5,4},{6,7},{7,6},{8,9},{9,8},{10,11... | collective-permute-start | bytes 393224 | tf_op jit(solution)/shard_map/ppermute | solution.py:46
  124.7 6.2 %collective-permute-start.31 = (bf16[80,1024]{1,0:T(8,128)(2,1)S(1)}, bf16[80,1024]{1,0:T(8,128)(2,1)S(1)}, u32[]{:S(2)}, u32[]{:S(2)}) collective-permute-start(bf16[80,1024]{1,0:T(8,128)(2,1)S(1)} %collective-permute-done.28.refs_9_), channel_id=1, source_target_pairs={{0,1},{1,0},{2,3},{3,2},{4,5},{5,4},{6,7},{7,6},{8,9},{9,8},{10,11... | collective-permute-start | bytes 491528 | tf_op jit(solution)/shard_map/ppermute | solution.py:46
  128.2 5.6 %collective-permute-start.33 = (bf16[80,1024]{1,0:T(8,128)(2,1)S(1)}, bf16[80,1024]{1,0:T(8,128)(2,1)S(1)}, u32[]{:S(2)}, u32[]{:S(2)}) collective-permute-start(bf16[80,1024]{1,0:T(8,128)(2,1)S(1)} %collective-permute-done.30.refs_10_), channel_id=1, source_target_pairs={{0,1},{1,0},{2,3},{3,2},{4,5},{5,4},{6,7},{7,6},{8,9},{9,8},{10,11... | collective-permute-start | bytes 491528 | tf_op jit(solution)/shard_map/ppermute | solution.py:46
  128.2 6.8 %collective-permute-start.17 = (bf16[64,1024]{1,0:T(8,128)(2,1)S(1)}, bf16[64,1024]{1,0:T(8,128)(2,1)S(1)}, u32[]{:S(2)}, u32[]{:S(2)}) collective-permute-start(bf16[64,1024]{1,0:T(8,128)(2,1)S(1)} %collective-permute-done.14.refs_1_), channel_id=1, source_target_pairs={{0,7},{1,2},{2,1},{3,4},{4,3},{5,6},{6,5},{7,0},{8,15},{9,10},{10,... | collective-permute-start | bytes 393224 | tf_op jit(solution)/shard_map/ppermute | solution.py:46
  128.9 6.2 %collective-permute-start.19 = (bf16[64,1024]{1,0:T(8,128)(2,1)S(1)}, bf16[64,1024]{1,0:T(8,128)(2,1)S(1)}, u32[]{:S(2)}, u32[]{:S(2)}) collective-permute-start(bf16[64,1024]{1,0:T(8,128)(2,1)S(1)} %collective-permute-done.16.refs_2_), channel_id=1, source_target_pairs={{0,7},{1,2},{2,1},{3,4},{4,3},{5,6},{6,5},{7,0},{8,15},{9,10},{10,... | collective-permute-start | bytes 393224 | tf_op jit(solution)/shard_map/ppermute | solution.py:46
  130.9 8.3 %collective-permute-start.32 = (bf16[80,1024]{1,0:T(8,128)(2,1)S(1)}, bf16[80,1024]{1,0:T(8,128)(2,1)S(1)}, u32[]{:S(2)}, u32[]{:S(2)}) collective-permute-start(bf16[80,1024]{1,0:T(8,128)(2,1)S(1)} %collective-permute-done.31.refs_14_), channel_id=1, source_target_pairs={{0,7},{1,2},{2,1},{3,4},{4,3},{5,6},{6,5},{7,0},{8,15},{9,10},{10,... | collective-permute-start | bytes 491528 | tf_op jit(solution)/shard_map/ppermute | solution.py:46
  133.8 7.9 %collective-permute-start.34 = (bf16[80,1024]{1,0:T(8,128)(2,1)S(1)}, bf16[80,1024]{1,0:T(8,128)(2,1)S(1)}, u32[]{:S(2)}, u32[]{:S(2)}) collective-permute-start(bf16[80,1024]{1,0:T(8,128)(2,1)S(1)} %collective-permute-done.33.refs_13_), channel_id=1, source_target_pairs={{0,7},{1,2},{2,1},{3,4},{4,3},{5,6},{6,5},{7,0},{8,15},{9,10},{10,... | collective-permute-start | bytes 491528 | tf_op jit(solution)/shard_map/ppermute | solution.py:48
  135.1 4.1 %collective-permute-start.18 = (bf16[64,1024]{1,0:T(8,128)(2,1)S(1)}, bf16[64,1024]{1,0:T(8,128)(2,1)S(1)}, u32[]{:S(2)}, u32[]{:S(2)}) collective-permute-start(bf16[64,1024]{1,0:T(8,128)(2,1)S(1)} %collective-permute-done.17.refs_6_), channel_id=1, source_target_pairs={{0,1},{1,0},{2,3},{3,2},{4,5},{5,4},{6,7},{7,6},{8,9},{9,8},{10,11... | collective-permute-start | bytes 393224 | tf_op jit(solution)/shard_map/ppermute | solution.py:46
  135.1 5.5 %collective-permute-start.20 = (bf16[64,1024]{1,0:T(8,128)(2,1)S(1)}, bf16[64,1024]{1,0:T(8,128)(2,1)S(1)}, u32[]{:S(2)}, u32[]{:S(2)}) collective-permute-start(bf16[64,1024]{1,0:T(8,128)(2,1)S(1)} %collective-permute-done.19.refs_5_), channel_id=1, source_target_pairs={{0,1},{1,0},{2,3},{3,2},{4,5},{5,4},{6,7},{7,6},{8,9},{9,8},{10,11... | collective-permute-start | bytes 393224 | tf_op jit(solution)/shard_map/ppermute | solution.py:48
  144.4 8.2 %copy-start.14 = (f32[128,4]{0,1:T(4,128)S(1)}, f32[128,4]{0,1:T(4,128)}, u32[]{:S(2)}) copy-start(f32[128,4]{0,1:T(4,128)} %param.13) | copy-start | bytes 6148
  144.4 36.4 %copy-start.11 = (pred[128,1024]{1,0:T(32,128)(4,1)S(1)}, pred[128,1024]{1,0:T(32,128)(4,1)}, u32[]{:S(2)}) copy-start(pred[128,1024]{1,0:T(32,128)(4,1)} %copy-done.10) | copy-start | bytes 393220
  144.4 36.4 %all-to-all-start.1 = ((bf16[16,64,512]{2,1,0:T(8,128)(2,1)}), bf16[16,64,512]{2,1,0:T(8,128)(2,1)S(1)}, u32[]{:S(2)}, u32[]{:S(2)}) async-start(bf16[16,64,512]{2,1,0:T(8,128)(2,1)} %bitcast.7), calls=%async_computation.1 | async-start | bytes 2097152 | tf_op jit(solution)/shard_map/all_to_all | solution.py:180
  181.2 9.8 %copy-start.13 = (f32[512]{0:T(512)S(1)}, f32[512]{0:T(512)}, u32[]{:S(2)}) copy-start(f32[512]{0:T(512)} %param.21) | copy-start | bytes 6148
  (4 other events, 4.8 us)

commit v3 on v2

--- a/solution.py
+++ b/solution.py
@@ -51,6 +51,7 @@
 
 LANES = 128
 TILE = 256
+STREAMS = 3
 IN_VMEM = pl.BlockSpec()
 IN_SMEM = pl.BlockSpec(memory_space=pltpu.SMEM)
 
@@ -95,23 +96,26 @@
     )(me, gain, rows, gate, up)
 
 
-def lower_down(me, blocks_a, blocks_b, matrix, shared_matrix):
-    size = len(blocks_a)
-    count, units = blocks_a[0].shape
-    shared = blocks_b[0].shape[0] - count
+def lower_down(me, streams, matrix, shared, shared_matrix):
+    size = len(streams[0][0])
+    units = streams[0][0][0].shape[1]
+    counts = [blocks[0].shape[0] for blocks, _ in streams]
+    counts[-1] -= shared
+    height = size * sum(counts)
     width = matrix.shape[1]
-    part = size * count
 
     def body(me_ref, *refs):
-        ins_a, ins_b = refs[:size], refs[size : 2 * size]
-        matrix_ref, shared_ref, out_ref, shared_out_ref, rows_ref, shared_rows_ref = refs[2 * size :]
-        for d in range(size):
-            at_a = block_row(me_ref[0], d, size, count, False)
-            at_b = pl.multiple_of(part + block_row(me_ref[0], d, size, count, True), 16)
-            at_s = block_row(me_ref[0], d, size, shared, True)
-            rows_ref[pl.ds(at_a, count), :] = ins_a[d][...]
-            rows_ref[pl.ds(at_b, count), :] = ins_b[d][:count, :]
-            shared_rows_ref[pl.ds(at_s, shared), :] = ins_b[d][count:, :]
+        matrix_ref, shared_ref, out_ref, shared_out_ref, rows_ref, shared_rows_ref = refs[size * len(counts) :]
+        first = 0
+        for i, count in enumerate(counts):
+            flip = streams[i][1]
+            for d in range(size):
+                in_ref = refs[i * size + d]
+                at = pl.multiple_of(first + block_row(me_ref[0], d, size, count, flip), 16)
+                rows_ref[pl.ds(at, count), :] = in_ref[:count, :]
+                if i == len(counts) - 1:
+                    shared_rows_ref[pl.ds(block_row(me_ref[0], d, size, shared, flip), shared), :] = in_ref[count:, :]
+            first += size * count
 
         def columns(n, _):
             at = pl.multiple_of(n * TILE, TILE)
@@ -123,13 +127,13 @@
 
     return pl.pallas_call(
         body,
-        out_shape=[jax.ShapeDtypeStruct((2 * part, width), bf16), jax.ShapeDtypeStruct((size * shared, width), f32)],
-        in_specs=[IN_SMEM] + [IN_VMEM] * (2 * size + 2),
+        out_shape=[jax.ShapeDtypeStruct((height, width), bf16), jax.ShapeDtypeStruct((size * shared, width), f32)],
+        in_specs=[IN_SMEM] + [IN_VMEM] * (size * len(counts) + 2),
         out_specs=[IN_VMEM] * 2,
-        scratch_shapes=[pltpu.VMEM((2 * part, units), bf16), pltpu.VMEM((size * shared, units), bf16)],
+        scratch_shapes=[pltpu.VMEM((height, units), bf16), pltpu.VMEM((size * shared, units), bf16)],
         compiler_params=pltpu.CompilerParams(vmem_limit_bytes=14 << 20),
         name="lower_down",
-    )(me, *blocks_a, *blocks_b, matrix, shared_matrix)
+    )(me, *[v for blocks, _ in streams for v in blocks], matrix, shared_matrix)
 
 
 def layer(
@@ -194,14 +198,21 @@
     hidden_s = hidden_of(reduce_scatter(pieces_s, tp, False, "tp"))
     rows, hidden_s = lax.optimization_barrier((rows, hidden_s))
 
-    part = columns // 2
-    pieces_a = project(me, gain, rows, 0, part, gate_matrix, up_matrix, tp, False)
-    pieces_b = project(me, gain, rows, part, part, gate_matrix, up_matrix, tp, True)
-    total_a = reduce_scatter(pieces_a, tp, False, "tp")
-    total_b = reduce_scatter(pieces_b, tp, True, "tp")
-    blocks_a = all_gather(hidden_of(total_a), tp, False, "tp")
-    blocks_b = all_gather(jnp.concatenate([hidden_of(total_b), hidden_s], 0), tp, True, "tp")
-    down, shared_out = lower_down(me, blocks_a, blocks_b, down_matrix, shared_down)
+    unit = 16 * tp
+    units = columns // unit
+    heights = [unit * (units * (i + 1) // STREAMS - units * i // STREAMS) for i in range(STREAMS)][::-1]
+    totals = []
+    for i, height in enumerate(heights):
+        first, flip = sum(heights[:i]), i % 2 == 1
+        pieces = project(me, gain, rows, first, height, gate_matrix, up_matrix, tp, flip)
+        totals.append((reduce_scatter(pieces, tp, flip, "tp"), flip))
+    streams = []
+    for i, (total, flip) in enumerate(totals):
+        hidden = hidden_of(total)
+        if i == STREAMS - 1:
+            hidden = jnp.concatenate([hidden, hidden_s], 0)
+        streams.append((all_gather(hidden, tp, flip, "tp"), flip))
+    down, shared_out = lower_down(me, streams, down_matrix, tok_count // tp, shared_down)
     came = swapped(down)
     mixture = shared_out + dot(high, came) + dot(low, came)
 

time: 192 us -> 200 us (1.042)
  starting transfers between devices: 61.7 us -> 76.5 us
  waiting for transfers between devices: 101 us -> 92.1 us
    ppermute x9 -> x12, starting transfers between devices: 7.15 us -> 14.1 us  [reduce_scatter(): lax.ppermute(added(piece[size - d], x), axis, two)]
    ppermute x12 -> x18, starting transfers between devices: 8.25 us -> 13.7 us  [all_gather(): x, y = (lax.ppermute(y, axis, one), lax.ppermute(x, axis, two))]
    all_to_all x2, starting transfers between devices: 30.1 us -> 33.9 us  [swapped(): lax.all_to_all(rows.reshape(experts, capacity, width), 'ep', 0, 0, tiled=...]
    ppermute x9 -> x12, waiting for transfers between devices: 28.6 us -> 24.9 us  [reduce_scatter(): lax.ppermute(added(piece[size - d], x), axis, two)]
    ppermute x3 -> x4, waiting for transfers between devices: 2.26 us -> 0.01 us  [reduce_scatter(): x = lax.ppermute(piece[half], axis, one)]
    ppermute x9 -> x12, waiting for transfers between devices: 16 us -> 13.9 us  [reduce_scatter(): lax.ppermute(piece[d] if y is None else added(piece[d], y), axis, one)]
    ppermute x12 -> x18, waiting for transfers between devices: 12.2 us -> 10.8 us  [all_gather(): x, y = (lax.ppermute(y, axis, one), lax.ppermute(x, axis, two))]
    ppermute x9 -> x12, starting transfers between devices: 9.31 us -> 8.37 us  [reduce_scatter(): lax.ppermute(piece[d] if y is None else added(piece[d], y), axis, one)]
  transfers between devices with their start and end apart: 37 -> 51, of which waited for: 24 -> 27; matrix products, arithmetic and copies ran while one was open for 2% -> 2% of each run, Pallas kernels for 1% -> 2%
where the time goes in v3:
time: 200 us
  waiting for transfers between devices  92.1 us (46%)
  starting transfers between devices  76.5 us (38%)
  blocking collectives  10.6 us (5%)
  Pallas kernels  9.34 us (5%)
  local copies, waits for them, and re-layouts  4.17 us (2%)
  other arithmetic  3.74 us (2%)
  matrix products  2.9 us (1%)
    all_to_all x2, waiting for transfers between devices, swapped(): lax.all_to_all(rows.reshape(experts, capacity, width), 'ep', 0, 0, tiled=...  40 us
    all_to_all x2, starting transfers between devices, swapped(): lax.all_to_all(rows.reshape(experts, capacity, width), 'ep', 0, 0, tiled=...  33.9 us
    ppermute x12, waiting for transfers between devices, reduce_scatter(): lax.ppermute(added(piece[size - d], x), axis, two)  24.9 us
    ppermute x12, starting transfers between devices, reduce_scatter(): lax.ppermute(added(piece[size - d], x), axis, two)  14.1 us
    ppermute x12, waiting for transfers between devices, reduce_scatter(): lax.ppermute(piece[d] if y is None else added(piece[d], y), axis, one)  13.9 us
    ppermute x18, starting transfers between devices, all_gather(): x, y = (lax.ppermute(y, axis, one), lax.ppermute(x, axis, two))  13.7 us
    ppermute x18, waiting for transfers between devices, all_gather(): x, y = (lax.ppermute(y, axis, one), lax.ppermute(x, axis, two))  10.8 us
    all_to_all x1, blocking collectives, layer(): square_sum = lax.all_to_all(copies, 'tp', 0, 0, tiled=True).sum(axis=0)  10.6 us
  transfers between devices with their start and end apart: 51, of which 27 were waited for; matrix products, arithmetic and copies ran while one was open for 2% of the time, Pallas kernels for 2%

profile of v3, /device:TPU:513, one launch (start us, length us, event | category | flops | bytes accessed | tf_op | source)
XLA Modules:
  0.0 199.7 jit_solution(690118330763030049)
XLA Ops:
  0.8 1.2 copy-done.4
  2.0 1.2 copy-done.5
  4.1 1.7 project.4
  5.8 2.2 %collective-permute-start.3 = (bf16[16,2176]{1,0:T(8,128)(2,1)}, bf16[16,2176]{1,0:T(8,128)(2,1)}, u32[]{:S(2)}, u32[]{:S(2)}) collective-permute-start(bf16[16,2176]{1,0:T(8,128)(2,1)} %get-tuple-element.48), channel_id=1, source_target_pairs={{0,1},{1,0},{2,3},{3,2},{4,5},{5,4},{6,7},{7,6},{8,9},{9,8},{10,11... | collective-permute-start | bytes 208904 | tf_op jit(solution)/shard_map/ppermute | solution.py:30
  8.5 1.5 convolution_convert_fusion
  10.0 21.9 %all-to-all-start = ((bf16[16,64,512]{2,1,0:T(8,128)(2,1)}), bf16[16,64,512]{2,1,0:T(8,128)(2,1)S(1)}, u32[]{:S(2)}, u32[]{:S(2)}) async-start(bf16[16,64,512]{2,1,0:T(8,128)(2,1)} %bitcast.2), calls=%async_computation | async-start | bytes 2097152 | tf_op jit(solution)/shard_map/all_to_all | solution.py:184
  31.9 1.9 collective-permute-start
  35.7 1.9 collective-permute-start.1
  37.6 1.8 collective-permute-done.4
  39.6 1.2 collective-permute-done.1
  41.2 1.8 collective-permute-done.5
  43.2 1.2 collective-permute-done.2
  44.4 3.5 %collective-permute-done.6 = bf16[16,2176]{1,0:T(8,128)(2,1)S(1)} collective-permute-done((bf16[16,2176]{1,0:T(8,128)(2,1)S(1)}, bf16[16,2176]{1,0:T(8,128)(2,1)S(1)}, u32[]{:S(2)}, u32[]{:S(2)}) %collective-permute-start.6) | collective-permute-done | bytes 69664 | tf_op jit(solution)/shard_map/ppermute | solution.py:34
  48.1 11.9 %all-to-all-done = bf16[16,64,512]{2,1,0:T(8,128)(2,1)S(1)} async-done(((bf16[16,64,512]{2,1,0:T(8,128)(2,1)}), bf16[16,64,512]{2,1,0:T(8,128)(2,1)S(1)}, u32[]{:S(2)}, u32[]{:S(2)}) %all-to-all-start) | async-done | bytes 1048608 | tf_op jit(solution)/shard_map/all_to_all | solution.py:184
  60.0 1.4 project.7
  61.4 1.9 collective-permute-start.38
  63.3 1.7 project.5
  65.0 1.7 project.6
  66.9 1.4 collective-permute-start.7
  68.3 2.7 %collective-permute-start.21 = (bf16[48,2176]{1,0:T(8,128)(2,1)S(1)}, bf16[48,2176]{1,0:T(8,128)(2,1)S(1)}, u32[]{:S(2)}, u32[]{:S(2)}) collective-permute-start(bf16[48,2176]{1,0:T(8,128)(2,1)S(1)} %get-tuple-element.61), channel_id=1, source_target_pairs={{0,7},{1,2},{2,1},{3,4},{4,3},{5,6},{6,5},{7,0},{8,15},{9,10},{10,... | collective-permute-start | bytes 626696 | tf_op jit(solution)/shard_map/ppermute | solution.py:35
  71.0 10.0 %collective-permute-done.35 = bf16[32,2176]{1,0:T(8,128)(2,1)S(1)} collective-permute-done((bf16[32,2176]{1,0:T(8,128)(2,1)S(1)}, bf16[32,2176]{1,0:T(8,128)(2,1)S(1)}, u32[]{:S(2)}, u32[]{:S(2)}) %collective-permute-start.35) | collective-permute-done | bytes 139296 | tf_op jit(solution)/shard_map/ppermute | solution.py:35
  81.1 2.8 %collective-permute-start.36 = (bf16[32,2176]{1,0:T(8,128)(2,1)S(1)}, bf16[32,2176]{1,0:T(8,128)(2,1)S(1)}, u32[]{:S(2)}, u32[]{:S(2)}) collective-permute-start(bf16[32,2176]{1,0:T(8,128)(2,1)S(1)} %add_convert_fusion.14), channel_id=1, source_target_pairs={{0,7},{1,2},{2,1},{3,4},{4,3},{5,6},{6,5},{7,0},{8,15},{9,10},{10,... | collective-permute-start | bytes 417800 | tf_op jit(solution)/shard_map/ppermute | solution.py:34
  84.3 2.8 %collective-permute-start.8 = (bf16[48,2176]{1,0:T(8,128)(2,1)S(1)}, bf16[48,2176]{1,0:T(8,128)(2,1)S(1)}, u32[]{:S(2)}, u32[]{:S(2)}) collective-permute-start(bf16[48,2176]{1,0:T(8,128)(2,1)S(1)} %add_convert_fusion.9), channel_id=1, source_target_pairs={{0,7},{1,2},{2,1},{3,4},{4,3},{5,6},{6,5},{7,0},{8,15},{9,10},{10,... | collective-permute-start | bytes 626696 | tf_op jit(solution)/shard_map/ppermute | solution.py:34
  87.6 1.4 collective-permute-start.22
  89.0 1.5 collective-permute-done.36
  90.6 4.4 %collective-permute-done.11 = bf16[48,2176]{1,0:T(8,128)(2,1)S(1)} collective-permute-done((bf16[48,2176]{1,0:T(8,128)(2,1)S(1)}, bf16[48,2176]{1,0:T(8,128)(2,1)S(1)}, u32[]{:S(2)}, u32[]{:S(2)}) %collective-permute-start.11) | collective-permute-done | bytes 208928 | tf_op jit(solution)/shard_map/ppermute | solution.py:34
  95.1 4.4 %collective-permute-done.8 = bf16[48,2176]{1,0:T(8,128)(2,1)S(1)} collective-permute-done((bf16[48,2176]{1,0:T(8,128)(2,1)S(1)}, bf16[48,2176]{1,0:T(8,128)(2,1)S(1)}, u32[]{:S(2)}, u32[]{:S(2)}) %collective-permute-start.8) | collective-permute-done | bytes 208928 | tf_op jit(solution)/shard_map/ppermute | solution.py:34
  99.6 1.6 collective-permute-start.9
  101.4 2.8 %collective-permute-start.41 = (bf16[32,2176]{1,0:T(8,128)(2,1)S(1)}, bf16[32,2176]{1,0:T(8,128)(2,1)S(1)}, u32[]{:S(2)}, u32[]{:S(2)}) collective-permute-start(bf16[32,2176]{1,0:T(8,128)(2,1)S(1)} %add_convert_fusion.10), channel_id=1, source_target_pairs={{0,7},{1,2},{2,1},{3,4},{4,3},{5,6},{6,5},{7,0},{8,15},{9,10},{10,... | collective-permute-start | bytes 417800 | tf_op jit(solution)/shard_map/ppermute | solution.py:34
  104.4 5.3 %collective-permute-done.41 = bf16[32,2176]{1,0:T(8,128)(2,1)S(1)} collective-permute-done((bf16[32,2176]{1,0:T(8,128)(2,1)S(1)}, bf16[32,2176]{1,0:T(8,128)(2,1)S(1)}, u32[]{:S(2)}, u32[]{:S(2)}) %collective-permute-start.41) | collective-permute-done | bytes 139296 | tf_op jit(solution)/shard_map/ppermute | solution.py:34
  110.2 1.5 collective-permute-start.43
  111.7 1.5 collective-permute-start.13
  113.5 2.9 %collective-permute-done.43.refs_23_ = bf16[48,1024]{1,0:T(8,128)(2,1)S(1)} collective-permute-done((bf16[48,1024]{1,0:T(8,128)(2,1)S(1)}, bf16[48,1024]{1,0:T(8,128)(2,1)S(1)}, u32[]{:S(2)}, u32[]{:S(2)}) %collective-permute-start.43) | collective-permute-done | bytes 98336 | tf_op jit(solution)/shard_map/ppermute | solution.py:46
  116.5 1.2 collective-permute-start.45
  117.7 2.5 %collective-permute-done.13 = bf16[48,2176]{1,0:T(8,128)(2,1)S(1)} collective-permute-done((bf16[48,2176]{1,0:T(8,128)(2,1)S(1)}, bf16[48,2176]{1,0:T(8,128)(2,1)S(1)}, u32[]{:S(2)}, u32[]{:S(2)}) %collective-permute-start.13) | collective-permute-done | bytes 208928 | tf_op jit(solution)/shard_map/ppermute | solution.py:34
  122.2 1.4 collective-permute-start.46
  124.0 1.7 collective-permute-start.28
  125.7 1.3 collective-permute-done.29.refs_15_
  129.9 1.6 collective-permute-start.17
  131.5 1.2 collective-permute-start.19
  135.0 1.4 collective-permute-done.31.refs_14_
  139.6 1.3 collective-permute-done.18.refs_3_
  140.9 1.4 collective-permute-done.32.refs_11_
  142.3 2.1 %collective-permute-done.34.refs_12_ = bf16[48,1024]{1,0:T(8,128)(2,1)S(1)} collective-permute-done((bf16[48,1024]{1,0:T(8,128)(2,1)S(1)}, bf16[48,1024]{1,0:T(8,128)(2,1)S(1)}, u32[]{:S(2)}, u32[]{:S(2)}) %collective-permute-start.34) | collective-permute-done | bytes 98336 | tf_op jit(solution)/shard_map/ppermute | solution.py:48
  144.4 2.8 %lower_down.1 = (bf16[1024,512]{1,0:T(8,128)(2,1)}, f32[128,512]{1,0:T(8,128)S(1)}) custom-call(s32[1]{0:T(128)} %bitcast.me_ref, bf16[48,1024]{1,0:T(8,128)(2,1)S(1)} %fusion.11.refs_0_, bf16[48,1024]{1,0:T(8,128)(2,1)S(1)} %collective-permute-done.14.refs_1_, bf16[48,1024]{1,0:T(8,128)(2,1)S(1)} %collective-permute-done.16.refs_2_, ...), custom_call_target="tpu_custom_call" | custom-call | tf_op jit(solution)/shard_map/lower_down/pallas_call | solution.py:128
  147.2 12.0 %all-to-all-start.1 = ((bf16[16,64,512]{2,1,0:T(8,128)(2,1)}), bf16[16,64,512]{2,1,0:T(8,128)(2,1)S(1)}, u32[]{:S(2)}, u32[]{:S(2)}) async-start(bf16[16,64,512]{2,1,0:T(8,128)(2,1)} %bitcast.7), calls=%async_computation.1 | async-start | bytes 2097152 | tf_op jit(solution)/shard_map/all_to_all | solution.py:184
  159.2 28.1 %all-to-all-done.1 = bf16[16,64,512]{2,1,0:T(8,128)(2,1)S(1)} async-done(((bf16[16,64,512]{2,1,0:T(8,128)(2,1)}), bf16[16,64,512]{2,1,0:T(8,128)(2,1)S(1)}, u32[]{:S(2)}, u32[]{:S(2)}) %all-to-all-start.1) | async-done | bytes 1048608 | tf_op jit(solution)/shard_map/all_to_all | solution.py:184
  188.3 10.6 %all_to_all.15 = f32[8,128,1]{1,2,0:T(1,128)S(1)} all-to-all(f32[8,128,1]{1,2,0:T(1,128)S(1)} %broadcast_in_dim.34), channel_id=1, replica_groups=mesh['grp'=2,'ep'=16,'tp'=8] {'tp'}, dimensions={0} | all-to-all | bytes 8192 | tf_op jit(solution)/shard_map/all_to_all | solution.py:221
  (137 shorter events, 20.3 us)
Async XLA Ops:
  5.8 27.9 %collective-permute-start.3 = (bf16[16,2176]{1,0:T(8,128)(2,1)}, bf16[16,2176]{1,0:T(8,128)(2,1)}, u32[]{:S(2)}, u32[]{:S(2)}) collective-permute-start(bf16[16,2176]{1,0:T(8,128)(2,1)} %get-tuple-element.48), channel_id=1, source_target_pairs={{0,1},{1,0},{2,3},{3,2},{4,5},{5,4},{6,7},{7,6},{8,9},{9,8},{10,11... | collective-permute-start | bytes 208904 | tf_op jit(solution)/shard_map/ppermute | solution.py:30
  10.0 50.0 %all-to-all-start = ((bf16[16,64,512]{2,1,0:T(8,128)(2,1)}), bf16[16,64,512]{2,1,0:T(8,128)(2,1)S(1)}, u32[]{:S(2)}, u32[]{:S(2)}) async-start(bf16[16,64,512]{2,1,0:T(8,128)(2,1)} %bitcast.2), calls=%async_computation | async-start | bytes 2097152 | tf_op jit(solution)/shard_map/all_to_all | solution.py:184
  34.7 4.8 %collective-permute-start.4 = (bf16[16,2176]{1,0:T(8,128)(2,1)S(1)}, bf16[16,2176]{1,0:T(8,128)(2,1)S(1)}, u32[]{:S(2)}, u32[]{:S(2)}) collective-permute-start(bf16[16,2176]{1,0:T(8,128)(2,1)S(1)} %add_convert_fusion.17), channel_id=1, source_target_pairs={{0,7},{1,2},{2,1},{3,4},{4,3},{5,6},{6,5},{7,0},{8,15},{9,10},{10,... | collective-permute-start | bytes 208904 | tf_op jit(solution)/shard_map/ppermute | solution.py:34
  35.7 5.1 %collective-permute-start.1 = (bf16[16,2176]{1,0:T(8,128)(2,1)S(1)}, bf16[16,2176]{1,0:T(8,128)(2,1)S(1)}, u32[]{:S(2)}, u32[]{:S(2)}) collective-permute-start(bf16[16,2176]{1,0:T(8,128)(2,1)S(1)} %add_convert_fusion.19), channel_id=1, source_target_pairs={{0,7},{1,2},{2,1},{3,4},{4,3},{5,6},{6,5},{7,0},{8,15},{9,10},{10,... | collective-permute-start | bytes 208904 | tf_op jit(solution)/shard_map/ppermute | solution.py:34
  43.1 4.8 %collective-permute-start.6 = (bf16[16,2176]{1,0:T(8,128)(2,1)S(1)}, bf16[16,2176]{1,0:T(8,128)(2,1)S(1)}, u32[]{:S(2)}, u32[]{:S(2)}) collective-permute-start(bf16[16,2176]{1,0:T(8,128)(2,1)S(1)} %add_convert_fusion.15), channel_id=1, source_target_pairs={{0,7},{1,2},{2,1},{3,4},{4,3},{5,6},{6,5},{7,0},{8,15},{9,10},{10,... | collective-permute-start | bytes 208904 | tf_op jit(solution)/shard_map/ppermute | solution.py:34
  61.4 9.6 %collective-permute-start.38 = (bf16[32,2176]{1,0:T(8,128)(2,1)S(1)}, bf16[32,2176]{1,0:T(8,128)(2,1)S(1)}, u32[]{:S(2)}, u32[]{:S(2)}) collective-permute-start(bf16[32,2176]{1,0:T(8,128)(2,1)S(1)} %get-tuple-element.73), channel_id=1, source_target_pairs={{0,1},{1,0},{2,3},{3,2},{4,5},{5,4},{6,7},{7,6},{8,9},{9,8},{10,11... | collective-permute-start | bytes 417800 | tf_op jit(solution)/shard_map/ppermute | solution.py:30
  66.7 14.3 %collective-permute-start.10 = (bf16[48,2176]{1,0:T(8,128)(2,1)S(1)}, bf16[48,2176]{1,0:T(8,128)(2,1)S(1)}, u32[]{:S(2)}, u32[]{:S(2)}) collective-permute-start(bf16[48,2176]{1,0:T(8,128)(2,1)S(1)} %get-tuple-element.57), channel_id=1, source_target_pairs={{0,1},{1,0},{2,3},{3,2},{4,5},{5,4},{6,7},{7,6},{8,9},{9,8},{10,11... | collective-permute-start | bytes 626696 | tf_op jit(solution)/shard_map/ppermute | solution.py:30
  66.9 17.0 %collective-permute-start.7 = (bf16[48,2176]{1,0:T(8,128)(2,1)S(1)}, bf16[48,2176]{1,0:T(8,128)(2,1)S(1)}, u32[]{:S(2)}, u32[]{:S(2)}) collective-permute-start(bf16[48,2176]{1,0:T(8,128)(2,1)S(1)} %get-tuple-element.53), channel_id=1, source_target_pairs={{0,1},{1,0},{2,3},{3,2},{4,5},{5,4},{6,7},{7,6},{8,9},{9,8},{10,11... | collective-permute-start | bytes 626696 | tf_op jit(solution)/shard_map/ppermute | solution.py:35
  68.3 16.0 %collective-permute-start.24 = (bf16[48,2176]{1,0:T(8,128)(2,1)S(1)}, bf16[48,2176]{1,0:T(8,128)(2,1)S(1)}, u32[]{:S(2)}, u32[]{:S(2)}) collective-permute-start(bf16[48,2176]{1,0:T(8,128)(2,1)S(1)} %get-tuple-element.65), channel_id=1, source_target_pairs={{0,7},{1,2},{2,1},{3,4},{4,3},{5,6},{6,5},{7,0},{8,15},{9,10},{10,... | collective-permute-start | bytes 626696 | tf_op jit(solution)/shard_map/ppermute | solution.py:30
  68.3 18.8 %collective-permute-start.21 = (bf16[48,2176]{1,0:T(8,128)(2,1)S(1)}, bf16[48,2176]{1,0:T(8,128)(2,1)S(1)}, u32[]{:S(2)}, u32[]{:S(2)}) collective-permute-start(bf16[48,2176]{1,0:T(8,128)(2,1)S(1)} %get-tuple-element.61), channel_id=1, source_target_pairs={{0,7},{1,2},{2,1},{3,4},{4,3},{5,6},{6,5},{7,0},{8,15},{9,10},{10,... | collective-permute-start | bytes 626696 | tf_op jit(solution)/shard_map/ppermute | solution.py:35
  71.0 10.0 %collective-permute-start.35 = (bf16[32,2176]{1,0:T(8,128)(2,1)S(1)}, bf16[32,2176]{1,0:T(8,128)(2,1)S(1)}, u32[]{:S(2)}, u32[]{:S(2)}) collective-permute-start(bf16[32,2176]{1,0:T(8,128)(2,1)S(1)} %get-tuple-element.69), channel_id=1, source_target_pairs={{0,1},{1,0},{2,3},{3,2},{4,5},{5,4},{6,7},{7,6},{8,9},{9,8},{10,11... | collective-permute-start | bytes 417800 | tf_op jit(solution)/shard_map/ppermute | solution.py:35
  81.0 6.5 %collective-permute-start.39 = (bf16[32,2176]{1,0:T(8,128)(2,1)S(1)}, bf16[32,2176]{1,0:T(8,128)(2,1)S(1)}, u32[]{:S(2)}, u32[]{:S(2)}) collective-permute-start(bf16[32,2176]{1,0:T(8,128)(2,1)S(1)} %add_convert_fusion.12), channel_id=1, source_target_pairs={{0,7},{1,2},{2,1},{3,4},{4,3},{5,6},{6,5},{7,0},{8,15},{9,10},{10,... | collective-permute-start | bytes 417800 | tf_op jit(solution)/shard_map/ppermute | solution.py:34
  81.1 9.5 %collective-permute-start.36 = (bf16[32,2176]{1,0:T(8,128)(2,1)S(1)}, bf16[32,2176]{1,0:T(8,128)(2,1)S(1)}, u32[]{:S(2)}, u32[]{:S(2)}) collective-permute-start(bf16[32,2176]{1,0:T(8,128)(2,1)S(1)} %add_convert_fusion.14), channel_id=1, source_target_pairs={{0,7},{1,2},{2,1},{3,4},{4,3},{5,6},{6,5},{7,0},{8,15},{9,10},{10,... | collective-permute-start | bytes 417800 | tf_op jit(solution)/shard_map/ppermute | solution.py:34
  83.9 11.1 %collective-permute-start.11 = (bf16[48,2176]{1,0:T(8,128)(2,1)S(1)}, bf16[48,2176]{1,0:T(8,128)(2,1)S(1)}, u32[]{:S(2)}, u32[]{:S(2)}) collective-permute-start(bf16[48,2176]{1,0:T(8,128)(2,1)S(1)} %add_convert_fusion.7), channel_id=1, source_target_pairs={{0,7},{1,2},{2,1},{3,4},{4,3},{5,6},{6,5},{7,0},{8,15},{9,10},{10,... | collective-permute-start | bytes 626696 | tf_op jit(solution)/shard_map/ppermute | solution.py:34
  84.3 15.1 %collective-permute-start.8 = (bf16[48,2176]{1,0:T(8,128)(2,1)S(1)}, bf16[48,2176]{1,0:T(8,128)(2,1)S(1)}, u32[]{:S(2)}, u32[]{:S(2)}) collective-permute-start(bf16[48,2176]{1,0:T(8,128)(2,1)S(1)} %add_convert_fusion.9), channel_id=1, source_target_pairs={{0,7},{1,2},{2,1},{3,4},{4,3},{5,6},{6,5},{7,0},{8,15},{9,10},{10,... | collective-permute-start | bytes 626696 | tf_op jit(solution)/shard_map/ppermute | solution.py:34
  87.2 12.4 %collective-permute-start.25 = (bf16[48,2176]{1,0:T(8,128)(2,1)S(1)}, bf16[48,2176]{1,0:T(8,128)(2,1)S(1)}, u32[]{:S(2)}, u32[]{:S(2)}) collective-permute-start(bf16[48,2176]{1,0:T(8,128)(2,1)S(1)} %add_convert_fusion.2), channel_id=1, source_target_pairs={{0,1},{1,0},{2,3},{3,2},{4,5},{5,4},{6,7},{7,6},{8,9},{9,8},{10,11... | collective-permute-start | bytes 626696 | tf_op jit(solution)/shard_map/ppermute | solution.py:34
  87.6 13.9 %collective-permute-start.22 = (bf16[48,2176]{1,0:T(8,128)(2,1)S(1)}, bf16[48,2176]{1,0:T(8,128)(2,1)S(1)}, u32[]{:S(2)}, u32[]{:S(2)}) collective-permute-start(bf16[48,2176]{1,0:T(8,128)(2,1)S(1)} %add_convert_fusion.4), channel_id=1, source_target_pairs={{0,1},{1,0},{2,3},{3,2},{4,5},{5,4},{6,7},{7,6},{8,9},{9,8},{10,11... | collective-permute-start | bytes 626696 | tf_op jit(solution)/shard_map/ppermute | solution.py:34
  90.5 10.7 %collective-permute-start.40 = (bf16[32,2176]{1,0:T(8,128)(2,1)S(1)}, bf16[32,2176]{1,0:T(8,128)(2,1)S(1)}, u32[]{:S(2)}, u32[]{:S(2)}) collective-permute-start(bf16[32,2176]{1,0:T(8,128)(2,1)S(1)} %add_convert_fusion.11), channel_id=1, source_target_pairs={{0,1},{1,0},{2,3},{3,2},{4,5},{5,4},{6,7},{7,6},{8,9},{9,8},{10,11... | collective-permute-start | bytes 417800 | tf_op jit(solution)/shard_map/ppermute | solution.py:35
  95.0 9.2 %collective-permute-start.37 = (bf16[32,2176]{1,0:T(8,128)(2,1)S(1)}, bf16[32,2176]{1,0:T(8,128)(2,1)S(1)}, u32[]{:S(2)}, u32[]{:S(2)}) collective-permute-start(bf16[32,2176]{1,0:T(8,128)(2,1)S(1)} %add_convert_fusion.13), channel_id=1, source_target_pairs={{0,1},{1,0},{2,3},{3,2},{4,5},{5,4},{6,7},{7,6},{8,9},{9,8},{10,11... | collective-permute-start | bytes 417800 | tf_op jit(solution)/shard_map/ppermute | solution.py:35
  99.5 10.7 %collective-permute-start.12 = (bf16[48,2176]{1,0:T(8,128)(2,1)S(1)}, bf16[48,2176]{1,0:T(8,128)(2,1)S(1)}, u32[]{:S(2)}, u32[]{:S(2)}) collective-permute-start(bf16[48,2176]{1,0:T(8,128)(2,1)S(1)} %add_convert_fusion.6), channel_id=1, source_target_pairs={{0,1},{1,0},{2,3},{3,2},{4,5},{5,4},{6,7},{7,6},{8,9},{9,8},{10,11... | collective-permute-start | bytes 626696 | tf_op jit(solution)/shard_map/ppermute | solution.py:35
  99.6 13.7 %collective-permute-start.9 = (bf16[48,2176]{1,0:T(8,128)(2,1)S(1)}, bf16[48,2176]{1,0:T(8,128)(2,1)S(1)}, u32[]{:S(2)}, u32[]{:S(2)}) collective-permute-start(bf16[48,2176]{1,0:T(8,128)(2,1)S(1)} %add_convert_fusion.8), channel_id=1, source_target_pairs={{0,1},{1,0},{2,3},{3,2},{4,5},{5,4},{6,7},{7,6},{8,9},{9,8},{10,11... | collective-permute-start | bytes 626696 | tf_op jit(solution)/shard_map/ppermute | solution.py:35
  101.2 10.5 %collective-permute-start.26 = (bf16[48,2176]{1,0:T(8,128)(2,1)S(1)}, bf16[48,2176]{1,0:T(8,128)(2,1)S(1)}, u32[]{:S(2)}, u32[]{:S(2)}) collective-permute-start(bf16[48,2176]{1,0:T(8,128)(2,1)S(1)} %add_convert_fusion.1), channel_id=1, source_target_pairs={{0,7},{1,2},{2,1},{3,4},{4,3},{5,6},{6,5},{7,0},{8,15},{9,10},{10,... | collective-permute-start | bytes 626696 | tf_op jit(solution)/shard_map/ppermute | solution.py:35
  101.4 8.3 %collective-permute-start.41 = (bf16[32,2176]{1,0:T(8,128)(2,1)S(1)}, bf16[32,2176]{1,0:T(8,128)(2,1)S(1)}, u32[]{:S(2)}, u32[]{:S(2)}) collective-permute-start(bf16[32,2176]{1,0:T(8,128)(2,1)S(1)} %add_convert_fusion.10), channel_id=1, source_target_pairs={{0,7},{1,2},{2,1},{3,4},{4,3},{5,6},{6,5},{7,0},{8,15},{9,10},{10,... | collective-permute-start | bytes 417800 | tf_op jit(solution)/shard_map/ppermute | solution.py:34
  104.2 17.4 %collective-permute-start.23 = (bf16[48,2176]{1,0:T(8,128)(2,1)S(1)}, bf16[48,2176]{1,0:T(8,128)(2,1)S(1)}, u32[]{:S(2)}, u32[]{:S(2)}) collective-permute-start(bf16[48,2176]{1,0:T(8,128)(2,1)S(1)} %add_convert_fusion.3), channel_id=1, source_target_pairs={{0,7},{1,2},{2,1},{3,4},{4,3},{5,6},{6,5},{7,0},{8,15},{9,10},{10,... | collective-permute-start | bytes 626696 | tf_op jit(solution)/shard_map/ppermute | solution.py:35
  110.1 6.4 %collective-permute-start.42 = (bf16[48,1024]{1,0:T(8,128)(2,1)S(1)}, bf16[48,1024]{1,0:T(8,128)(2,1)S(1)}, u32[]{:S(2)}, u32[]{:S(2)}) collective-permute-start(bf16[48,1024]{1,0:T(8,128)(2,1)S(1)} %pad_maximum_fusion.refs_16_), channel_id=1, source_target_pairs={{0,1},{1,0},{2,3},{3,2},{4,5},{5,4},{6,7},{7,6},{8,9},{9,8},{10,11... | collective-permute-start | bytes 294920 | tf_op jit(solution)/shard_map/ppermute | solution.py:46
  110.2 6.1 %collective-permute-start.43 = (bf16[48,1024]{1,0:T(8,128)(2,1)S(1)}, bf16[48,1024]{1,0:T(8,128)(2,1)S(1)}, u32[]{:S(2)}, u32[]{:S(2)}) collective-permute-start(bf16[48,1024]{1,0:T(8,128)(2,1)S(1)} %pad_maximum_fusion.refs_16_), channel_id=1, source_target_pairs={{0,7},{1,2},{2,1},{3,4},{4,3},{5,6},{6,5},{7,0},{8,15},{9,10},{10,... | collective-permute-start | bytes 294920 | tf_op jit(solution)/shard_map/ppermute | solution.py:46
  111.7 8.4 %collective-permute-start.13 = (bf16[48,2176]{1,0:T(8,128)(2,1)S(1)}, bf16[48,2176]{1,0:T(8,128)(2,1)S(1)}, u32[]{:S(2)}, u32[]{:S(2)}) collective-permute-start(bf16[48,2176]{1,0:T(8,128)(2,1)S(1)} %add_convert_fusion.5), channel_id=1, source_target_pairs={{0,7},{1,2},{2,1},{3,4},{4,3},{5,6},{6,5},{7,0},{8,15},{9,10},{10,... | collective-permute-start | bytes 626696 | tf_op jit(solution)/shard_map/ppermute | solution.py:34
  113.3 8.4 %collective-permute-start.27 = (bf16[48,2176]{1,0:T(8,128)(2,1)S(1)}, bf16[48,2176]{1,0:T(8,128)(2,1)S(1)}, u32[]{:S(2)}, u32[]{:S(2)}) collective-permute-start(bf16[48,2176]{1,0:T(8,128)(2,1)S(1)} %add_convert_fusion), channel_id=1, source_target_pairs={{0,1},{1,0},{2,3},{3,2},{4,5},{5,4},{6,7},{7,6},{8,9},{9,8},{10,11... | collective-permute-start | bytes 626696 | tf_op jit(solution)/shard_map/ppermute | solution.py:34
  116.4 7.6 %collective-permute-start.44 = (bf16[48,1024]{1,0:T(8,128)(2,1)S(1)}, bf16[48,1024]{1,0:T(8,128)(2,1)S(1)}, u32[]{:S(2)}, u32[]{:S(2)}) collective-permute-start(bf16[48,1024]{1,0:T(8,128)(2,1)S(1)} %collective-permute-done.43.refs_23_), channel_id=1, source_target_pairs={{0,1},{1,0},{2,3},{3,2},{4,5},{5,4},{6,7},{7,6},{8,9},{9,8},{10,11... | collective-permute-start | bytes 294920 | tf_op jit(solution)/shard_map/ppermute | solution.py:46
  116.5 5.7 %collective-permute-start.45 = (bf16[48,1024]{1,0:T(8,128)(2,1)S(1)}, bf16[48,1024]{1,0:T(8,128)(2,1)S(1)}, u32[]{:S(2)}, u32[]{:S(2)}) collective-permute-start(bf16[48,1024]{1,0:T(8,128)(2,1)S(1)} %collective-permute-done.42.refs_17_), channel_id=1, source_target_pairs={{0,7},{1,2},{2,1},{3,4},{4,3},{5,6},{6,5},{7,0},{8,15},{9,10},{10,... | collective-permute-start | bytes 294920 | tf_op jit(solution)/shard_map/ppermute | solution.py:46
  120.5 5.1 %collective-permute-start.15 = (bf16[48,1024]{1,0:T(8,128)(2,1)S(1)}, bf16[48,1024]{1,0:T(8,128)(2,1)S(1)}, u32[]{:S(2)}, u32[]{:S(2)}) collective-permute-start(bf16[48,1024]{1,0:T(8,128)(2,1)S(1)} %fusion.11.refs_0_), channel_id=1, source_target_pairs={{0,7},{1,2},{2,1},{3,4},{4,3},{5,6},{6,5},{7,0},{8,15},{9,10},{10,... | collective-permute-start | bytes 294920 | tf_op jit(solution)/shard_map/ppermute | solution.py:46
  122.0 4.9 %collective-permute-start.29 = (bf16[48,1024]{1,0:T(8,128)(2,1)S(1)}, bf16[48,1024]{1,0:T(8,128)(2,1)S(1)}, u32[]{:S(2)}, u32[]{:S(2)}) collective-permute-start(bf16[48,1024]{1,0:T(8,128)(2,1)S(1)} %fusion.9.refs_8_), channel_id=1, source_target_pairs={{0,1},{1,0},{2,3},{3,2},{4,5},{5,4},{6,7},{7,6},{8,9},{9,8},{10,11... | collective-permute-start | bytes 294920 | tf_op jit(solution)/shard_map/ppermute | solution.py:46
  122.2 6.7 %collective-permute-start.46 = (bf16[48,1024]{1,0:T(8,128)(2,1)S(1)}, bf16[48,1024]{1,0:T(8,128)(2,1)S(1)}, u32[]{:S(2)}, u32[]{:S(2)}) collective-permute-start(bf16[48,1024]{1,0:T(8,128)(2,1)S(1)} %collective-permute-done.45.refs_22_), channel_id=1, source_target_pairs={{0,1},{1,0},{2,3},{3,2},{4,5},{5,4},{6,7},{7,6},{8,9},{9,8},{10,11... | collective-permute-start | bytes 294920 | tf_op jit(solution)/shard_map/ppermute | solution.py:46
  123.6 6.3 %collective-permute-start.14 = (bf16[48,1024]{1,0:T(8,128)(2,1)S(1)}, bf16[48,1024]{1,0:T(8,128)(2,1)S(1)}, u32[]{:S(2)}, u32[]{:S(2)}) collective-permute-start(bf16[48,1024]{1,0:T(8,128)(2,1)S(1)} %fusion.11.refs_0_), channel_id=1, source_target_pairs={{0,1},{1,0},{2,3},{3,2},{4,5},{5,4},{6,7},{7,6},{8,9},{9,8},{10,11... | collective-permute-start | bytes 294920 | tf_op jit(solution)/shard_map/ppermute | solution.py:46
  124.0 7.5 %collective-permute-start.28 = (bf16[48,1024]{1,0:T(8,128)(2,1)S(1)}, bf16[48,1024]{1,0:T(8,128)(2,1)S(1)}, u32[]{:S(2)}, u32[]{:S(2)}) collective-permute-start(bf16[48,1024]{1,0:T(8,128)(2,1)S(1)} %fusion.9.refs_8_), channel_id=1, source_target_pairs={{0,7},{1,2},{2,1},{3,4},{4,3},{5,6},{6,5},{7,0},{8,15},{9,10},{10,... | collective-permute-start | bytes 294920 | tf_op jit(solution)/shard_map/ppermute | solution.py:46
  125.7 5.8 %collective-permute-start.16 = (bf16[48,1024]{1,0:T(8,128)(2,1)S(1)}, bf16[48,1024]{1,0:T(8,128)(2,1)S(1)}, u32[]{:S(2)}, u32[]{:S(2)}) collective-permute-start(bf16[48,1024]{1,0:T(8,128)(2,1)S(1)} %collective-permute-done.15.refs_7_), channel_id=1, source_target_pairs={{0,1},{1,0},{2,3},{3,2},{4,5},{5,4},{6,7},{7,6},{8,9},{9,8},{10,11... | collective-permute-start | bytes 294920 | tf_op jit(solution)/shard_map/ppermute | solution.py:46
  126.9 5.7 %collective-permute-start.30 = (bf16[48,1024]{1,0:T(8,128)(2,1)S(1)}, bf16[48,1024]{1,0:T(8,128)(2,1)S(1)}, u32[]{:S(2)}, u32[]{:S(2)}) collective-permute-start(bf16[48,1024]{1,0:T(8,128)(2,1)S(1)} %collective-permute-done.29.refs_15_), channel_id=1, source_target_pairs={{0,7},{1,2},{2,1},{3,4},{4,3},{5,6},{6,5},{7,0},{8,15},{9,10},{10,... | collective-permute-start | bytes 294920 | tf_op jit(solution)/shard_map/ppermute | solution.py:46
  128.8 4.7 %collective-permute-start.47 = (bf16[48,1024]{1,0:T(8,128)(2,1)S(1)}, bf16[48,1024]{1,0:T(8,128)(2,1)S(1)}, u32[]{:S(2)}, u32[]{:S(2)}) collective-permute-start(bf16[48,1024]{1,0:T(8,128)(2,1)S(1)} %collective-permute-done.44.refs_18_), channel_id=1, source_target_pairs={{0,7},{1,2},{2,1},{3,4},{4,3},{5,6},{6,5},{7,0},{8,15},{9,10},{10,... | collective-permute-start | bytes 294920 | tf_op jit(solution)/shard_map/ppermute | solution.py:46
  129.9 4.7 %collective-permute-start.17 = (bf16[48,1024]{1,0:T(8,128)(2,1)S(1)}, bf16[48,1024]{1,0:T(8,128)(2,1)S(1)}, u32[]{:S(2)}, u32[]{:S(2)}) collective-permute-start(bf16[48,1024]{1,0:T(8,128)(2,1)S(1)} %collective-permute-done.14.refs_1_), channel_id=1, source_target_pairs={{0,7},{1,2},{2,1},{3,4},{4,3},{5,6},{6,5},{7,0},{8,15},{9,10},{10,... | collective-permute-start | bytes 294920 | tf_op jit(solution)/shard_map/ppermute | solution.py:46
  131.5 4.8 %collective-permute-start.31 = (bf16[48,1024]{1,0:T(8,128)(2,1)S(1)}, bf16[48,1024]{1,0:T(8,128)(2,1)S(1)}, u32[]{:S(2)}, u32[]{:S(2)}) collective-permute-start(bf16[48,1024]{1,0:T(8,128)(2,1)S(1)} %collective-permute-done.28.refs_9_), channel_id=1, source_target_pairs={{0,1},{1,0},{2,3},{3,2},{4,5},{5,4},{6,7},{7,6},{8,9},{9,8},{10,11... | collective-permute-start | bytes 294920 | tf_op jit(solution)/shard_map/ppermute | solution.py:46
  131.5 5.3 %collective-permute-start.19 = (bf16[48,1024]{1,0:T(8,128)(2,1)S(1)}, bf16[48,1024]{1,0:T(8,128)(2,1)S(1)}, u32[]{:S(2)}, u32[]{:S(2)}) collective-permute-start(bf16[48,1024]{1,0:T(8,128)(2,1)S(1)} %collective-permute-done.16.refs_2_), channel_id=1, source_target_pairs={{0,7},{1,2},{2,1},{3,4},{4,3},{5,6},{6,5},{7,0},{8,15},{9,10},{10,... | collective-permute-start | bytes 294920 | tf_op jit(solution)/shard_map/ppermute | solution.py:46
  132.7 5.7 %collective-permute-start.33 = (bf16[48,1024]{1,0:T(8,128)(2,1)S(1)}, bf16[48,1024]{1,0:T(8,128)(2,1)S(1)}, u32[]{:S(2)}, u32[]{:S(2)}) collective-permute-start(bf16[48,1024]{1,0:T(8,128)(2,1)S(1)} %collective-permute-done.30.refs_10_), channel_id=1, source_target_pairs={{0,1},{1,0},{2,3},{3,2},{4,5},{5,4},{6,7},{7,6},{8,9},{9,8},{10,11... | collective-permute-start | bytes 294920 | tf_op jit(solution)/shard_map/ppermute | solution.py:46
  133.5 6.1 %collective-permute-start.48 = (bf16[48,1024]{1,0:T(8,128)(2,1)S(1)}, bf16[48,1024]{1,0:T(8,128)(2,1)S(1)}, u32[]{:S(2)}, u32[]{:S(2)}) collective-permute-start(bf16[48,1024]{1,0:T(8,128)(2,1)S(1)} %collective-permute-done.47.refs_21_), channel_id=1, source_target_pairs={{0,1},{1,0},{2,3},{3,2},{4,5},{5,4},{6,7},{7,6},{8,9},{9,8},{10,11... | collective-permute-start | bytes 294920 | tf_op jit(solution)/shard_map/ppermute | solution.py:48
  134.5 6.4 %collective-permute-start.18 = (bf16[48,1024]{1,0:T(8,128)(2,1)S(1)}, bf16[48,1024]{1,0:T(8,128)(2,1)S(1)}, u32[]{:S(2)}, u32[]{:S(2)}) collective-permute-start(bf16[48,1024]{1,0:T(8,128)(2,1)S(1)} %collective-permute-done.17.refs_6_), channel_id=1, source_target_pairs={{0,1},{1,0},{2,3},{3,2},{4,5},{5,4},{6,7},{7,6},{8,9},{9,8},{10,11... | collective-permute-start | bytes 294920 | tf_op jit(solution)/shard_map/ppermute | solution.py:46
  136.3 6.0 %collective-permute-start.32 = (bf16[48,1024]{1,0:T(8,128)(2,1)S(1)}, bf16[48,1024]{1,0:T(8,128)(2,1)S(1)}, u32[]{:S(2)}, u32[]{:S(2)}) collective-permute-start(bf16[48,1024]{1,0:T(8,128)(2,1)S(1)} %collective-permute-done.31.refs_14_), channel_id=1, source_target_pairs={{0,7},{1,2},{2,1},{3,4},{4,3},{5,6},{6,5},{7,0},{8,15},{9,10},{10,... | collective-permute-start | bytes 294920 | tf_op jit(solution)/shard_map/ppermute | solution.py:46
  136.8 5.6 %collective-permute-start.20 = (bf16[48,1024]{1,0:T(8,128)(2,1)S(1)}, bf16[48,1024]{1,0:T(8,128)(2,1)S(1)}, u32[]{:S(2)}, u32[]{:S(2)}) collective-permute-start(bf16[48,1024]{1,0:T(8,128)(2,1)S(1)} %collective-permute-done.19.refs_5_), channel_id=1, source_target_pairs={{0,1},{1,0},{2,3},{3,2},{4,5},{5,4},{6,7},{7,6},{8,9},{9,8},{10,11... | collective-permute-start | bytes 294920 | tf_op jit(solution)/shard_map/ppermute | solution.py:48
  138.4 6.0 %collective-permute-start.34 = (bf16[48,1024]{1,0:T(8,128)(2,1)S(1)}, bf16[48,1024]{1,0:T(8,128)(2,1)S(1)}, u32[]{:S(2)}, u32[]{:S(2)}) collective-permute-start(bf16[48,1024]{1,0:T(8,128)(2,1)S(1)} %collective-permute-done.33.refs_13_), channel_id=1, source_target_pairs={{0,7},{1,2},{2,1},{3,4},{4,3},{5,6},{6,5},{7,0},{8,15},{9,10},{10,... | collective-permute-start | bytes 294920 | tf_op jit(solution)/shard_map/ppermute | solution.py:48
  147.2 40.1 %all-to-all-start.1 = ((bf16[16,64,512]{2,1,0:T(8,128)(2,1)}), bf16[16,64,512]{2,1,0:T(8,128)(2,1)S(1)}, u32[]{:S(2)}, u32[]{:S(2)}) async-start(bf16[16,64,512]{2,1,0:T(8,128)(2,1)} %bitcast.7), calls=%async_computation.1 | async-start | bytes 2097152 | tf_op jit(solution)/shard_map/all_to_all | solution.py:184
  (18 other events, 222.2 us)

commit v4 on v2

--- a/solution.py
+++ b/solution.py
@@ -30,22 +30,25 @@
     x = lax.ppermute(piece[half], axis, one)
     y = None
     for d in range(half - 1, 0, -1):
-        x, y = (
-            lax.ppermute(added(piece[size - d], x), axis, two),
-            lax.ppermute(piece[d] if y is None else added(piece[d], y), axis, one),
-        )
-        x, y = y, x
+        x_next = added(piece[size - d] if (half - d) % 2 else piece[d], x)
+        y_next = piece[d] if (half - d) % 2 else piece[size - d]
+        y_next = y_next if y is None else added(y_next, y)
+        x = lax.ppermute(x_next, axis, two if (half - d) % 2 else one)
+        y = lax.ppermute(y_next, axis, one if (half - d) % 2 else two)
     return piece[0].astype(f32) + x.astype(f32) + y.astype(f32)
 
 
 def all_gather(block, size, flip, axis):
     one, two = exchanges(size, flip)
+    half = size // 2
     out = {0: block}
     x = y = block
-    for d in range(1, size // 2):
-        x, y = lax.ppermute(y, axis, one), lax.ppermute(x, axis, two)
-        out[d], out[size - d] = x, y
-    out[size // 2] = lax.ppermute(y, axis, one)
+    for d in range(1, half + 1):
+        x = lax.ppermute(x, axis, two if d % 2 else one)
+        out[size - d if d % 2 else d] = x
+        if d < half:
+            y = lax.ppermute(y, axis, one if d % 2 else two)
+            out[d if d % 2 else size - d] = y
     return [out[d] for d in range(size)]
 
 

time: 192 us -> 195 us (1.016)
  starting transfers between devices: 61.7 us -> 67.6 us
  waiting for transfers between devices: 101 us -> 99 us
    ppermute x32, waiting for transfers between devices: 59.2 us -> 50.6 us  [the longest x9 26.9 us: reduce_scatter(): x = lax.ppermute(x_next, axis, two if (half - d) % 2 else one)]
    ppermute x3, waiting for transfers between devices: 2.26 us -> 8.55 us  [reduce_scatter(): x = lax.ppermute(piece[half], axis, one)]
    all_to_all x2, starting transfers between devices: 30.1 us -> 34.2 us  [swapped(): lax.all_to_all(rows.reshape(experts, capacity, width), 'ep', 0, 0, tiled=...]
where the time goes in v4:
time: 195 us
  waiting for transfers between devices  99 us (51%)
  starting transfers between devices  67.6 us (35%)
  blocking collectives  8.97 us (5%)
  Pallas kernels  8.49 us (4%)
  local copies, waits for them, and re-layouts  4.17 us (2%)
  other arithmetic  3.5 us (2%)
  matrix products  2.89 us (1%)
    all_to_all x2, waiting for transfers between devices, swapped(): lax.all_to_all(rows.reshape(experts, capacity, width), 'ep', 0, 0, tiled=...  39.8 us
    all_to_all x2, starting transfers between devices, swapped(): lax.all_to_all(rows.reshape(experts, capacity, width), 'ep', 0, 0, tiled=...  34.2 us
    ppermute x9, waiting for transfers between devices, reduce_scatter(): x = lax.ppermute(x_next, axis, two if (half - d) % 2 else one)  26.9 us
    ppermute x9, waiting for transfers between devices, reduce_scatter(): y = lax.ppermute(y_next, axis, one if (half - d) % 2 else two)  11.1 us
    ppermute x8, waiting for transfers between devices, all_gather(): x = lax.ppermute(x, axis, two if d % 2 else one)  9.22 us
    all_to_all x1, blocking collectives, layer(): square_sum = lax.all_to_all(copies, 'tp', 0, 0, tiled=True).sum(axis=0)  8.97 us
    ppermute x9, starting transfers between devices, reduce_scatter(): y = lax.ppermute(y_next, axis, one if (half - d) % 2 else two)  8.69 us
    ppermute x3, waiting for transfers between devices, reduce_scatter(): x = lax.ppermute(piece[half], axis, one)  8.55 us
  transfers between devices with their start and end apart: 37, of which 24 were waited for; matrix products, arithmetic and copies ran while one was open for 2% of the time, Pallas kernels for 1%

profile of v4, /device:TPU:513, one launch (start us, length us, event | category | flops | bytes accessed | tf_op | source)
XLA Modules:
  0.0 194.9 jit_solution(9441190911601260455)
XLA Ops:
  0.8 1.2 copy-done.4
  2.0 1.2 copy-done.5
  4.1 1.7 project.3
  5.8 2.2 %collective-permute-start = (bf16[16,2176]{1,0:T(8,128)(2,1)}, bf16[16,2176]{1,0:T(8,128)(2,1)}, u32[]{:S(2)}, u32[]{:S(2)}) collective-permute-start(bf16[16,2176]{1,0:T(8,128)(2,1)} %get-tuple-element.37), channel_id=1, source_target_pairs={{0,1},{1,0},{2,3},{3,2},{4,5},{5,4},{6,7},{7,6},{8,9},{9,8},{10,11... | collective-permute-start | bytes 208904 | tf_op jit(solution)/shard_map/ppermute | solution.py:30
  8.5 1.5 convolution_convert_fusion
  10.0 21.9 %all-to-all-start = ((bf16[16,64,512]{2,1,0:T(8,128)(2,1)}), bf16[16,64,512]{2,1,0:T(8,128)(2,1)S(1)}, u32[]{:S(2)}, u32[]{:S(2)}) async-start(bf16[16,64,512]{2,1,0:T(8,128)(2,1)} %bitcast.2), calls=%async_computation | async-start | bytes 2097152 | tf_op jit(solution)/shard_map/all_to_all | solution.py:183
  31.8 1.9 collective-permute-start.4
  33.7 0.9 add_convert_fusion.14
  35.6 1.9 collective-permute-start.5
  37.6 1.8 collective-permute-done.1
  39.6 1.2 collective-permute-done.5
  41.2 1.8 collective-permute-done.2
  43.2 1.2 collective-permute-done.6
  44.4 3.5 %collective-permute-done.3 = bf16[16,2176]{1,0:T(8,128)(2,1)S(1)} collective-permute-done((bf16[16,2176]{1,0:T(8,128)(2,1)S(1)}, bf16[16,2176]{1,0:T(8,128)(2,1)S(1)}, u32[]{:S(2)}, u32[]{:S(2)}) %collective-permute-start.3) | collective-permute-done | bytes 69664 | tf_op jit(solution)/shard_map/ppermute | solution.py:36
  48.1 11.9 %all-to-all-done = bf16[16,64,512]{2,1,0:T(8,128)(2,1)S(1)} async-done(((bf16[16,64,512]{2,1,0:T(8,128)(2,1)}), bf16[16,64,512]{2,1,0:T(8,128)(2,1)S(1)}, u32[]{:S(2)}, u32[]{:S(2)}) %all-to-all-start) | async-done | bytes 1048608 | tf_op jit(solution)/shard_map/all_to_all | solution.py:183
  60.0 2.0 %project.4 = (bf16[64,2176]{1,0:T(8,128)(2,1)S(1)}, bf16[64,2176]{1,0:T(8,128)(2,1)S(1)}, bf16[64,2176]{1,0:T(8,128)(2,1)S(1)}, bf16[64,2176]{1,0:T(8,128)(2,1)S...) custom-call(s32[1]{0:T(128)} %bitcast.me_ref, ...), custom_call_target="tpu_custom_call" | custom-call | tf_op jit(solution)/shard_map/project/pallas_call | solution.py:90
  62.0 1.9 collective-permute-start.11
  63.9 2.0 %project.5 = (bf16[64,2176]{1,0:T(8,128)(2,1)S(1)}, bf16[64,2176]{1,0:T(8,128)(2,1)S(1)}, bf16[64,2176]{1,0:T(8,128)(2,1)S(1)}, bf16[64,2176]{1,0:T(8,128)(2,1)S...) custom-call(s32[1]{0:T(128)} %bitcast.me_ref, ...), custom_call_target="tpu_custom_call" | custom-call | tf_op jit(solution)/shard_map/project/pallas_call | solution.py:90
  66.2 2.6 %collective-permute-start.21 = (bf16[64,2176]{1,0:T(8,128)(2,1)S(1)}, bf16[64,2176]{1,0:T(8,128)(2,1)S(1)}, u32[]{:S(2)}, u32[]{:S(2)}) collective-permute-start(bf16[64,2176]{1,0:T(8,128)(2,1)S(1)} %get-tuple-element.54), channel_id=1, source_target_pairs={{0,7},{1,2},{2,1},{3,4},{4,3},{5,6},{6,5},{7,0},{8,15},{9,10},{10,... | collective-permute-start | bytes 835592 | tf_op jit(solution)/shard_map/ppermute | solution.py:30
  68.8 2.3 %collective-permute-done.11 = bf16[64,2176]{1,0:T(8,128)(2,1)S(1)} collective-permute-done((bf16[64,2176]{1,0:T(8,128)(2,1)S(1)}, bf16[64,2176]{1,0:T(8,128)(2,1)S(1)}, u32[]{:S(2)}, u32[]{:S(2)}) %collective-permute-start.11) | collective-permute-done | bytes 278560 | tf_op jit(solution)/shard_map/ppermute | solution.py:37
  71.3 4.7 %collective-permute-done.7 = bf16[64,2176]{1,0:T(8,128)(2,1)S(1)} collective-permute-done((bf16[64,2176]{1,0:T(8,128)(2,1)S(1)}, bf16[64,2176]{1,0:T(8,128)(2,1)S(1)}, u32[]{:S(2)}, u32[]{:S(2)}) %collective-permute-start.7) | collective-permute-done | bytes 278560 | tf_op jit(solution)/shard_map/ppermute | solution.py:30
  76.3 1.8 collective-permute-start.26
  78.2 3.9 %collective-permute-done.21 = bf16[64,2176]{1,0:T(8,128)(2,1)S(1)} collective-permute-done((bf16[64,2176]{1,0:T(8,128)(2,1)S(1)}, bf16[64,2176]{1,0:T(8,128)(2,1)S(1)}, u32[]{:S(2)}, u32[]{:S(2)}) %collective-permute-start.21) | collective-permute-done | bytes 278560 | tf_op jit(solution)/shard_map/ppermute | solution.py:30
  82.3 5.7 %collective-permute-done.12 = bf16[64,2176]{1,0:T(8,128)(2,1)S(1)} collective-permute-done((bf16[64,2176]{1,0:T(8,128)(2,1)S(1)}, bf16[64,2176]{1,0:T(8,128)(2,1)S(1)}, u32[]{:S(2)}, u32[]{:S(2)}) %collective-permute-start.12) | collective-permute-done | bytes 278560 | tf_op jit(solution)/shard_map/ppermute | solution.py:37
  88.5 4.7 %collective-permute-done.8 = bf16[64,2176]{1,0:T(8,128)(2,1)S(1)} collective-permute-done((bf16[64,2176]{1,0:T(8,128)(2,1)S(1)}, bf16[64,2176]{1,0:T(8,128)(2,1)S(1)}, u32[]{:S(2)}, u32[]{:S(2)}) %collective-permute-start.8) | collective-permute-done | bytes 278560 | tf_op jit(solution)/shard_map/ppermute | solution.py:36
  94.3 2.8 %collective-permute-start.23 = (bf16[64,2176]{1,0:T(8,128)(2,1)S(1)}, bf16[64,2176]{1,0:T(8,128)(2,1)S(1)}, u32[]{:S(2)}, u32[]{:S(2)}) collective-permute-start(bf16[64,2176]{1,0:T(8,128)(2,1)S(1)} %add_convert_fusion.3), channel_id=1, source_target_pairs={{0,7},{1,2},{2,1},{3,4},{4,3},{5,6},{6,5},{7,0},{8,15},{9,10},{10,... | collective-permute-start | bytes 835592 | tf_op jit(solution)/shard_map/ppermute | solution.py:36
  97.1 6.0 %collective-permute-done.9 = bf16[64,2176]{1,0:T(8,128)(2,1)S(1)} collective-permute-done((bf16[64,2176]{1,0:T(8,128)(2,1)S(1)}, bf16[64,2176]{1,0:T(8,128)(2,1)S(1)}, u32[]{:S(2)}, u32[]{:S(2)}) %collective-permute-start.9) | collective-permute-done | bytes 278560 | tf_op jit(solution)/shard_map/ppermute | solution.py:36
  103.1 2.6 %collective-permute-start.10 = (bf16[64,2176]{1,0:T(8,128)(2,1)S(1)}, bf16[64,2176]{1,0:T(8,128)(2,1)S(1)}, u32[]{:S(2)}, u32[]{:S(2)}) collective-permute-start(bf16[64,2176]{1,0:T(8,128)(2,1)S(1)} %add_convert_fusion.7), channel_id=1, source_target_pairs={{0,7},{1,2},{2,1},{3,4},{4,3},{5,6},{6,5},{7,0},{8,15},{9,10},{10,... | collective-permute-start | bytes 835592 | tf_op jit(solution)/shard_map/ppermute | solution.py:36
  105.8 3.4 %collective-permute-done.23 = bf16[64,2176]{1,0:T(8,128)(2,1)S(1)} collective-permute-done((bf16[64,2176]{1,0:T(8,128)(2,1)S(1)}, bf16[64,2176]{1,0:T(8,128)(2,1)S(1)}, u32[]{:S(2)}, u32[]{:S(2)}) %collective-permute-start.23) | collective-permute-done | bytes 278560 | tf_op jit(solution)/shard_map/ppermute | solution.py:36
  109.4 5.7 %collective-permute-done.10 = bf16[64,2176]{1,0:T(8,128)(2,1)S(1)} collective-permute-done((bf16[64,2176]{1,0:T(8,128)(2,1)S(1)}, bf16[64,2176]{1,0:T(8,128)(2,1)S(1)}, u32[]{:S(2)}, u32[]{:S(2)}) %collective-permute-start.10) | collective-permute-done | bytes 278560 | tf_op jit(solution)/shard_map/ppermute | solution.py:36
  116.3 1.2 collective-permute-start.15
  117.5 1.6 collective-permute-start.28
  119.1 0.9 collective-permute-done.29.refs_15_
  120.1 1.0 collective-permute-start.30
  121.5 1.1 collective-permute-start.16
  123.5 4.0 %collective-permute-done.30.refs_10_ = bf16[80,1024]{1,0:T(8,128)(2,1)S(1)} collective-permute-done((bf16[80,1024]{1,0:T(8,128)(2,1)S(1)}, bf16[80,1024]{1,0:T(8,128)(2,1)S(1)}, u32[]{:S(2)}, u32[]{:S(2)}) %collective-permute-start.30) | collective-permute-done | bytes 163872 | tf_op jit(solution)/shard_map/ppermute | solution.py:47
  127.5 1.4 collective-permute-start.17
  128.9 1.3 collective-permute-start.19
  130.2 1.4 collective-permute-start.32
  131.6 2.1 %collective-permute-done.33.refs_13_ = bf16[80,1024]{1,0:T(8,128)(2,1)S(1)} collective-permute-done((bf16[80,1024]{1,0:T(8,128)(2,1)S(1)}, bf16[80,1024]{1,0:T(8,128)(2,1)S(1)}, u32[]{:S(2)}, u32[]{:S(2)}) %collective-permute-start.33) | collective-permute-done | bytes 163872 | tf_op jit(solution)/shard_map/ppermute | solution.py:47
  133.7 1.4 collective-permute-start.34
  135.1 1.5 collective-permute-start.20
  136.6 2.6 %collective-permute-done.18.refs_3_ = bf16[64,1024]{1,0:T(8,128)(2,1)S(1)} collective-permute-done((bf16[64,1024]{1,0:T(8,128)(2,1)S(1)}, bf16[64,1024]{1,0:T(8,128)(2,1)S(1)}, u32[]{:S(2)}, u32[]{:S(2)}) %collective-permute-start.18) | collective-permute-done | bytes 131104 | tf_op jit(solution)/shard_map/ppermute | solution.py:50
  139.3 1.4 collective-permute-done.20.refs_4_
  141.0 2.7 %lower_down.1 = (bf16[1024,512]{1,0:T(8,128)(2,1)}, f32[128,512]{1,0:T(8,128)S(1)}) custom-call(s32[1]{0:T(128)} %bitcast.me_ref, bf16[64,1024]{1,0:T(8,128)(2,1)S(1)} %fusion.9.refs_0_, bf16[64,1024]{1,0:T(8,128)(2,1)S(1)} %collective-permute-done.14.refs_1_, bf16[64,1024]{1,0:T(8,128)(2,1)S(1)} %collective-permute-done.16.refs_2_, ...), custom_call_target="tpu_custom_call" | custom-call | tf_op jit(solution)/shard_map/lower_down/pallas_call | solution.py:127
  143.8 12.4 %all-to-all-start.1 = ((bf16[16,64,512]{2,1,0:T(8,128)(2,1)}), bf16[16,64,512]{2,1,0:T(8,128)(2,1)S(1)}, u32[]{:S(2)}, u32[]{:S(2)}) async-start(bf16[16,64,512]{2,1,0:T(8,128)(2,1)} %bitcast.7), calls=%async_computation.1 | async-start | bytes 2097152 | tf_op jit(solution)/shard_map/all_to_all | solution.py:183
  156.2 28.0 %all-to-all-done.1 = bf16[16,64,512]{2,1,0:T(8,128)(2,1)S(1)} async-done(((bf16[16,64,512]{2,1,0:T(8,128)(2,1)}), bf16[16,64,512]{2,1,0:T(8,128)(2,1)S(1)}, u32[]{:S(2)}, u32[]{:S(2)}) %all-to-all-start.1) | async-done | bytes 1048608 | tf_op jit(solution)/shard_map/all_to_all | solution.py:183
  185.2 9.0 %all_to_all.15 = f32[8,128,1]{1,2,0:T(1,128)S(1)} all-to-all(f32[8,128,1]{1,2,0:T(1,128)S(1)} %broadcast_in_dim.34), channel_id=1, replica_groups=mesh['grp'=2,'ep'=16,'tp'=8] {'tp'}, dimensions={0} | all-to-all | bytes 8192 | tf_op jit(solution)/shard_map/all_to_all | solution.py:213
  (100 shorter events, 11.8 us)
Async XLA Ops:
  4.1 3.9 %copy-start.12 = (s32[128,4]{0,1:T(4,128)S(1)}, s32[128,4]{0,1:T(4,128)}, u32[]{:S(2)}) copy-start(s32[128,4]{0,1:T(4,128)} %param.12) | copy-start | bytes 6148
  4.1 4.4 %copy-start.7 = (bf16[128,512]{1,0:T(8,128)(2,1)S(1)}, bf16[128,512]{1,0:T(8,128)(2,1)}, u32[]{:S(2)}) copy-start(bf16[128,512]{1,0:T(8,128)(2,1)} %rows_ref.1) | copy-start | bytes 393220
  5.8 4.1 %copy-start.8 = (bf16[16,2176]{1,0:T(8,128)(2,1)}, bf16[16,2176]{1,0:T(8,128)(2,1)S(1)}, u32[]{:S(2)}) copy-start(bf16[16,2176]{1,0:T(8,128)(2,1)S(1)} %get-tuple-element.36) | copy-start | bytes 208900
  5.8 4.1 %copy-start.9 = (bf16[16,2176]{1,0:T(8,128)(2,1)}, bf16[16,2176]{1,0:T(8,128)(2,1)S(1)}, u32[]{:S(2)}) copy-start(bf16[16,2176]{1,0:T(8,128)(2,1)S(1)} %get-tuple-element.40) | copy-start | bytes 208900
  5.8 27.9 %collective-permute-start = (bf16[16,2176]{1,0:T(8,128)(2,1)}, bf16[16,2176]{1,0:T(8,128)(2,1)}, u32[]{:S(2)}, u32[]{:S(2)}) collective-permute-start(bf16[16,2176]{1,0:T(8,128)(2,1)} %get-tuple-element.37), channel_id=1, source_target_pairs={{0,1},{1,0},{2,3},{3,2},{4,5},{5,4},{6,7},{7,6},{8,9},{9,8},{10,11... | collective-permute-start | bytes 208904 | tf_op jit(solution)/shard_map/ppermute | solution.py:30
  10.0 50.0 %copy-start.1 = (bf16[1,512,1024]{2,1,0:T(8,128)(2,1)S(1)}, bf16[1,512,1024]{2,1,0:T(8,128)(2,1)}, u32[]{:S(2)}) copy-start(bf16[1,512,1024]{2,1,0:T(8,128)(2,1)} %param.16) | copy-start | bytes 3145732
  10.0 50.0 %all-to-all-start = ((bf16[16,64,512]{2,1,0:T(8,128)(2,1)}), bf16[16,64,512]{2,1,0:T(8,128)(2,1)S(1)}, u32[]{:S(2)}, u32[]{:S(2)}) async-start(bf16[16,64,512]{2,1,0:T(8,128)(2,1)} %bitcast.2), calls=%async_computation | async-start | bytes 2097152 | tf_op jit(solution)/shard_map/all_to_all | solution.py:183
  31.8 28.1 %copy-start = (bf16[1,512,1024]{2,1,0:T(8,128)(2,1)S(1)}, bf16[1,512,1024]{2,1,0:T(8,128)(2,1)}, u32[]{:S(2)}) copy-start(bf16[1,512,1024]{2,1,0:T(8,128)(2,1)} %param.15) | copy-start | bytes 3145732
  31.8 3.8 %collective-permute-start.4 = (bf16[16,2176]{1,0:T(8,128)(2,1)}, bf16[16,2176]{1,0:T(8,128)(2,1)S(1)}, u32[]{:S(2)}, u32[]{:S(2)}) collective-permute-start(bf16[16,2176]{1,0:T(8,128)(2,1)} %copy-done.9), channel_id=1, source_target_pairs={{0,1},{1,0},{2,3},{3,2},{4,5},{5,4},{6,7},{7,6},{8,9},{9,8},{10,11... | collective-permute-start | bytes 208904 | tf_op jit(solution)/shard_map/ppermute | solution.py:37
  34.6 4.8 %collective-permute-start.1 = (bf16[16,2176]{1,0:T(8,128)(2,1)S(1)}, bf16[16,2176]{1,0:T(8,128)(2,1)S(1)}, u32[]{:S(2)}, u32[]{:S(2)}) collective-permute-start(bf16[16,2176]{1,0:T(8,128)(2,1)S(1)} %add_convert_fusion.14), channel_id=1, source_target_pairs={{0,7},{1,2},{2,1},{3,4},{4,3},{5,6},{6,5},{7,0},{8,15},{9,10},{10,... | collective-permute-start | bytes 208904 | tf_op jit(solution)/shard_map/ppermute | solution.py:36
  35.6 5.1 %collective-permute-start.5 = (bf16[16,2176]{1,0:T(8,128)(2,1)S(1)}, bf16[16,2176]{1,0:T(8,128)(2,1)S(1)}, u32[]{:S(2)}, u32[]{:S(2)}) collective-permute-start(bf16[16,2176]{1,0:T(8,128)(2,1)S(1)} %add_convert_fusion.11), channel_id=1, source_target_pairs={{0,7},{1,2},{2,1},{3,4},{4,3},{5,6},{6,5},{7,0},{8,15},{9,10},{10,... | collective-permute-start | bytes 208904 | tf_op jit(solution)/shard_map/ppermute | solution.py:37
  39.5 3.6 %collective-permute-start.2 = (bf16[16,2176]{1,0:T(8,128)(2,1)S(1)}, bf16[16,2176]{1,0:T(8,128)(2,1)S(1)}, u32[]{:S(2)}, u32[]{:S(2)}) collective-permute-start(bf16[16,2176]{1,0:T(8,128)(2,1)S(1)} %add_convert_fusion.13), channel_id=1, source_target_pairs={{0,1},{1,0},{2,3},{3,2},{4,5},{5,4},{6,7},{7,6},{8,9},{9,8},{10,11... | collective-permute-start | bytes 208904 | tf_op jit(solution)/shard_map/ppermute | solution.py:36
  40.8 3.6 %collective-permute-start.6 = (bf16[16,2176]{1,0:T(8,128)(2,1)S(1)}, bf16[16,2176]{1,0:T(8,128)(2,1)S(1)}, u32[]{:S(2)}, u32[]{:S(2)}) collective-permute-start(bf16[16,2176]{1,0:T(8,128)(2,1)S(1)} %add_convert_fusion.10), channel_id=1, source_target_pairs={{0,1},{1,0},{2,3},{3,2},{4,5},{5,4},{6,7},{7,6},{8,9},{9,8},{10,11... | collective-permute-start | bytes 208904 | tf_op jit(solution)/shard_map/ppermute | solution.py:37
  43.1 4.8 %collective-permute-start.3 = (bf16[16,2176]{1,0:T(8,128)(2,1)S(1)}, bf16[16,2176]{1,0:T(8,128)(2,1)S(1)}, u32[]{:S(2)}, u32[]{:S(2)}) collective-permute-start(bf16[16,2176]{1,0:T(8,128)(2,1)S(1)} %add_convert_fusion.12), channel_id=1, source_target_pairs={{0,7},{1,2},{2,1},{3,4},{4,3},{5,6},{6,5},{7,0},{8,15},{9,10},{10,... | collective-permute-start | bytes 208904 | tf_op jit(solution)/shard_map/ppermute | solution.py:36
  62.0 9.1 %collective-permute-start.11 = (bf16[64,2176]{1,0:T(8,128)(2,1)S(1)}, bf16[64,2176]{1,0:T(8,128)(2,1)S(1)}, u32[]{:S(2)}, u32[]{:S(2)}) collective-permute-start(bf16[64,2176]{1,0:T(8,128)(2,1)S(1)} %get-tuple-element.49), channel_id=1, source_target_pairs={{0,1},{1,0},{2,3},{3,2},{4,5},{5,4},{6,7},{7,6},{8,9},{9,8},{10,11... | collective-permute-start | bytes 835592 | tf_op jit(solution)/shard_map/ppermute | solution.py:37
  65.9 10.1 %collective-permute-start.7 = (bf16[64,2176]{1,0:T(8,128)(2,1)S(1)}, bf16[64,2176]{1,0:T(8,128)(2,1)S(1)}, u32[]{:S(2)}, u32[]{:S(2)}) collective-permute-start(bf16[64,2176]{1,0:T(8,128)(2,1)S(1)} %get-tuple-element.46), channel_id=1, source_target_pairs={{0,1},{1,0},{2,3},{3,2},{4,5},{5,4},{6,7},{7,6},{8,9},{9,8},{10,11... | collective-permute-start | bytes 835592 | tf_op jit(solution)/shard_map/ppermute | solution.py:30
  66.1 10.2 %collective-permute-start.25 = (bf16[64,2176]{1,0:T(8,128)(2,1)S(1)}, bf16[64,2176]{1,0:T(8,128)(2,1)S(1)}, u32[]{:S(2)}, u32[]{:S(2)}) collective-permute-start(bf16[64,2176]{1,0:T(8,128)(2,1)S(1)} %get-tuple-element.57), channel_id=1, source_target_pairs={{0,7},{1,2},{2,1},{3,4},{4,3},{5,6},{6,5},{7,0},{8,15},{9,10},{10,... | collective-permute-start | bytes 835592 | tf_op jit(solution)/shard_map/ppermute | solution.py:37
  66.2 15.8 %collective-permute-start.21 = (bf16[64,2176]{1,0:T(8,128)(2,1)S(1)}, bf16[64,2176]{1,0:T(8,128)(2,1)S(1)}, u32[]{:S(2)}, u32[]{:S(2)}) collective-permute-start(bf16[64,2176]{1,0:T(8,128)(2,1)S(1)} %get-tuple-element.54), channel_id=1, source_target_pairs={{0,7},{1,2},{2,1},{3,4},{4,3},{5,6},{6,5},{7,0},{8,15},{9,10},{10,... | collective-permute-start | bytes 835592 | tf_op jit(solution)/shard_map/ppermute | solution.py:30
  71.2 16.8 %collective-permute-start.12 = (bf16[64,2176]{1,0:T(8,128)(2,1)S(1)}, bf16[64,2176]{1,0:T(8,128)(2,1)S(1)}, u32[]{:S(2)}, u32[]{:S(2)}) collective-permute-start(bf16[64,2176]{1,0:T(8,128)(2,1)S(1)} %add_convert_fusion.6), channel_id=1, source_target_pairs={{0,7},{1,2},{2,1},{3,4},{4,3},{5,6},{6,5},{7,0},{8,15},{9,10},{10,... | collective-permute-start | bytes 835592 | tf_op jit(solution)/shard_map/ppermute | solution.py:37
  76.1 17.1 %collective-permute-start.8 = (bf16[64,2176]{1,0:T(8,128)(2,1)S(1)}, bf16[64,2176]{1,0:T(8,128)(2,1)S(1)}, u32[]{:S(2)}, u32[]{:S(2)}) collective-permute-start(bf16[64,2176]{1,0:T(8,128)(2,1)S(1)} %add_convert_fusion.9), channel_id=1, source_target_pairs={{0,7},{1,2},{2,1},{3,4},{4,3},{5,6},{6,5},{7,0},{8,15},{9,10},{10,... | collective-permute-start | bytes 835592 | tf_op jit(solution)/shard_map/ppermute | solution.py:36
  76.3 17.7 %collective-permute-start.26 = (bf16[64,2176]{1,0:T(8,128)(2,1)S(1)}, bf16[64,2176]{1,0:T(8,128)(2,1)S(1)}, u32[]{:S(2)}, u32[]{:S(2)}) collective-permute-start(bf16[64,2176]{1,0:T(8,128)(2,1)S(1)} %add_convert_fusion.1), channel_id=1, source_target_pairs={{0,1},{1,0},{2,3},{3,2},{4,5},{5,4},{6,7},{7,6},{8,9},{9,8},{10,11... | collective-permute-start | bytes 835592 | tf_op jit(solution)/shard_map/ppermute | solution.py:37
  82.1 12.2 %collective-permute-start.22 = (bf16[64,2176]{1,0:T(8,128)(2,1)S(1)}, bf16[64,2176]{1,0:T(8,128)(2,1)S(1)}, u32[]{:S(2)}, u32[]{:S(2)}) collective-permute-start(bf16[64,2176]{1,0:T(8,128)(2,1)S(1)} %add_convert_fusion.4), channel_id=1, source_target_pairs={{0,1},{1,0},{2,3},{3,2},{4,5},{5,4},{6,7},{7,6},{8,9},{9,8},{10,11... | collective-permute-start | bytes 835592 | tf_op jit(solution)/shard_map/ppermute | solution.py:36
  88.0 21.3 %collective-permute-start.13 = (bf16[64,2176]{1,0:T(8,128)(2,1)S(1)}, bf16[64,2176]{1,0:T(8,128)(2,1)S(1)}, u32[]{:S(2)}, u32[]{:S(2)}) collective-permute-start(bf16[64,2176]{1,0:T(8,128)(2,1)S(1)} %add_convert_fusion.5), channel_id=1, source_target_pairs={{0,1},{1,0},{2,3},{3,2},{4,5},{5,4},{6,7},{7,6},{8,9},{9,8},{10,11... | collective-permute-start | bytes 835592 | tf_op jit(solution)/shard_map/ppermute | solution.py:37
  93.2 9.8 %collective-permute-start.9 = (bf16[64,2176]{1,0:T(8,128)(2,1)S(1)}, bf16[64,2176]{1,0:T(8,128)(2,1)S(1)}, u32[]{:S(2)}, u32[]{:S(2)}) collective-permute-start(bf16[64,2176]{1,0:T(8,128)(2,1)S(1)} %add_convert_fusion.8), channel_id=1, source_target_pairs={{0,1},{1,0},{2,3},{3,2},{4,5},{5,4},{6,7},{7,6},{8,9},{9,8},{10,11... | collective-permute-start | bytes 835592 | tf_op jit(solution)/shard_map/ppermute | solution.py:36
  94.1 21.2 %collective-permute-start.27 = (bf16[64,2176]{1,0:T(8,128)(2,1)S(1)}, bf16[64,2176]{1,0:T(8,128)(2,1)S(1)}, u32[]{:S(2)}, u32[]{:S(2)}) collective-permute-start(bf16[64,2176]{1,0:T(8,128)(2,1)S(1)} %add_convert_fusion), channel_id=1, source_target_pairs={{0,7},{1,2},{2,1},{3,4},{4,3},{5,6},{6,5},{7,0},{8,15},{9,10},{10,... | collective-permute-start | bytes 835592 | tf_op jit(solution)/shard_map/ppermute | solution.py:37
  94.3 14.8 %collective-permute-start.23 = (bf16[64,2176]{1,0:T(8,128)(2,1)S(1)}, bf16[64,2176]{1,0:T(8,128)(2,1)S(1)}, u32[]{:S(2)}, u32[]{:S(2)}) collective-permute-start(bf16[64,2176]{1,0:T(8,128)(2,1)S(1)} %add_convert_fusion.3), channel_id=1, source_target_pairs={{0,7},{1,2},{2,1},{3,4},{4,3},{5,6},{6,5},{7,0},{8,15},{9,10},{10,... | collective-permute-start | bytes 835592 | tf_op jit(solution)/shard_map/ppermute | solution.py:36
  103.1 12.0 %collective-permute-start.10 = (bf16[64,2176]{1,0:T(8,128)(2,1)S(1)}, bf16[64,2176]{1,0:T(8,128)(2,1)S(1)}, u32[]{:S(2)}, u32[]{:S(2)}) collective-permute-start(bf16[64,2176]{1,0:T(8,128)(2,1)S(1)} %add_convert_fusion.7), channel_id=1, source_target_pairs={{0,7},{1,2},{2,1},{3,4},{4,3},{5,6},{6,5},{7,0},{8,15},{9,10},{10,... | collective-permute-start | bytes 835592 | tf_op jit(solution)/shard_map/ppermute | solution.py:36
  109.2 6.1 %collective-permute-start.24 = (bf16[64,2176]{1,0:T(8,128)(2,1)S(1)}, bf16[64,2176]{1,0:T(8,128)(2,1)S(1)}, u32[]{:S(2)}, u32[]{:S(2)}) collective-permute-start(bf16[64,2176]{1,0:T(8,128)(2,1)S(1)} %add_convert_fusion.2), channel_id=1, source_target_pairs={{0,1},{1,0},{2,3},{3,2},{4,5},{5,4},{6,7},{7,6},{8,9},{9,8},{10,11... | collective-permute-start | bytes 835592 | tf_op jit(solution)/shard_map/ppermute | solution.py:36
  115.4 25.7 %copy-start.3 = (bf16[1024,512]{1,0:T(8,128)(2,1)S(1)}, bf16[1024,512]{1,0:T(8,128)(2,1)}, u32[]{:S(2)}) copy-start(bf16[1024,512]{1,0:T(8,128)(2,1)} %refs_17_.1) | copy-start | bytes 3145732
  115.5 25.6 %copy-start.2 = (bf16[1,1024,512]{2,1,0:T(8,128)(2,1)S(1)}, bf16[1,1024,512]{2,1,0:T(8,128)(2,1)}, u32[]{:S(2)}) copy-start(bf16[1,1024,512]{2,1,0:T(8,128)(2,1)} %param.17) | copy-start | bytes 3145732
  115.8 4.3 %collective-permute-start.29 = (bf16[80,1024]{1,0:T(8,128)(2,1)S(1)}, bf16[80,1024]{1,0:T(8,128)(2,1)S(1)}, u32[]{:S(2)}, u32[]{:S(2)}) collective-permute-start(bf16[80,1024]{1,0:T(8,128)(2,1)S(1)} %pad_maximum_fusion.refs_8_), channel_id=1, source_target_pairs={{0,1},{1,0},{2,3},{3,2},{4,5},{5,4},{6,7},{7,6},{8,9},{9,8},{10,11... | collective-permute-start | bytes 491528 | tf_op jit(solution)/shard_map/ppermute | solution.py:47
  116.3 5.2 %collective-permute-start.15 = (bf16[64,1024]{1,0:T(8,128)(2,1)S(1)}, bf16[64,1024]{1,0:T(8,128)(2,1)S(1)}, u32[]{:S(2)}, u32[]{:S(2)}) collective-permute-start(bf16[64,1024]{1,0:T(8,128)(2,1)S(1)} %fusion.9.refs_0_), channel_id=1, source_target_pairs={{0,7},{1,2},{2,1},{3,4},{4,3},{5,6},{6,5},{7,0},{8,15},{9,10},{10,... | collective-permute-start | bytes 393224 | tf_op jit(solution)/shard_map/ppermute | solution.py:47
  117.5 5.7 %collective-permute-start.28 = (bf16[80,1024]{1,0:T(8,128)(2,1)S(1)}, bf16[80,1024]{1,0:T(8,128)(2,1)S(1)}, u32[]{:S(2)}, u32[]{:S(2)}) collective-permute-start(bf16[80,1024]{1,0:T(8,128)(2,1)S(1)} %pad_maximum_fusion.refs_8_), channel_id=1, source_target_pairs={{0,7},{1,2},{2,1},{3,4},{4,3},{5,6},{6,5},{7,0},{8,15},{9,10},{10,... | collective-permute-start | bytes 491528 | tf_op jit(solution)/shard_map/ppermute | solution.py:50
  120.1 7.4 %collective-permute-start.30 = (bf16[80,1024]{1,0:T(8,128)(2,1)S(1)}, bf16[80,1024]{1,0:T(8,128)(2,1)S(1)}, u32[]{:S(2)}, u32[]{:S(2)}) collective-permute-start(bf16[80,1024]{1,0:T(8,128)(2,1)S(1)} %collective-permute-done.29.refs_15_), channel_id=1, source_target_pairs={{0,7},{1,2},{2,1},{3,4},{4,3},{5,6},{6,5},{7,0},{8,15},{9,10},{10,... | collective-permute-start | bytes 491528 | tf_op jit(solution)/shard_map/ppermute | solution.py:47
  121.1 6.4 %collective-permute-start.14 = (bf16[64,1024]{1,0:T(8,128)(2,1)S(1)}, bf16[64,1024]{1,0:T(8,128)(2,1)S(1)}, u32[]{:S(2)}, u32[]{:S(2)}) collective-permute-start(bf16[64,1024]{1,0:T(8,128)(2,1)S(1)} %fusion.9.refs_0_), channel_id=1, source_target_pairs={{0,1},{1,0},{2,3},{3,2},{4,5},{5,4},{6,7},{7,6},{8,9},{9,8},{10,11... | collective-permute-start | bytes 393224 | tf_op jit(solution)/shard_map/ppermute | solution.py:50
  121.5 7.4 %collective-permute-start.16 = (bf16[64,1024]{1,0:T(8,128)(2,1)S(1)}, bf16[64,1024]{1,0:T(8,128)(2,1)S(1)}, u32[]{:S(2)}, u32[]{:S(2)}) collective-permute-start(bf16[64,1024]{1,0:T(8,128)(2,1)S(1)} %collective-permute-done.15.refs_7_), channel_id=1, source_target_pairs={{0,1},{1,0},{2,3},{3,2},{4,5},{5,4},{6,7},{7,6},{8,9},{9,8},{10,11... | collective-permute-start | bytes 393224 | tf_op jit(solution)/shard_map/ppermute | solution.py:47
  123.3 7.0 %collective-permute-start.31 = (bf16[80,1024]{1,0:T(8,128)(2,1)S(1)}, bf16[80,1024]{1,0:T(8,128)(2,1)S(1)}, u32[]{:S(2)}, u32[]{:S(2)}) collective-permute-start(bf16[80,1024]{1,0:T(8,128)(2,1)S(1)} %collective-permute-done.28.refs_9_), channel_id=1, source_target_pairs={{0,1},{1,0},{2,3},{3,2},{4,5},{5,4},{6,7},{7,6},{8,9},{9,8},{10,11... | collective-permute-start | bytes 491528 | tf_op jit(solution)/shard_map/ppermute | solution.py:50
  127.5 6.2 %collective-permute-start.33 = (bf16[80,1024]{1,0:T(8,128)(2,1)S(1)}, bf16[80,1024]{1,0:T(8,128)(2,1)S(1)}, u32[]{:S(2)}, u32[]{:S(2)}) collective-permute-start(bf16[80,1024]{1,0:T(8,128)(2,1)S(1)} %collective-permute-done.30.refs_10_), channel_id=1, source_target_pairs={{0,1},{1,0},{2,3},{3,2},{4,5},{5,4},{6,7},{7,6},{8,9},{9,8},{10,11... | collective-permute-start | bytes 491528 | tf_op jit(solution)/shard_map/ppermute | solution.py:47
  127.5 7.6 %collective-permute-start.17 = (bf16[64,1024]{1,0:T(8,128)(2,1)S(1)}, bf16[64,1024]{1,0:T(8,128)(2,1)S(1)}, u32[]{:S(2)}, u32[]{:S(2)}) collective-permute-start(bf16[64,1024]{1,0:T(8,128)(2,1)S(1)} %collective-permute-done.14.refs_1_), channel_id=1, source_target_pairs={{0,7},{1,2},{2,1},{3,4},{4,3},{5,6},{6,5},{7,0},{8,15},{9,10},{10,... | collective-permute-start | bytes 393224 | tf_op jit(solution)/shard_map/ppermute | solution.py:50
  128.9 6.2 %collective-permute-start.19 = (bf16[64,1024]{1,0:T(8,128)(2,1)S(1)}, bf16[64,1024]{1,0:T(8,128)(2,1)S(1)}, u32[]{:S(2)}, u32[]{:S(2)}) collective-permute-start(bf16[64,1024]{1,0:T(8,128)(2,1)S(1)} %collective-permute-done.16.refs_2_), channel_id=1, source_target_pairs={{0,7},{1,2},{2,1},{3,4},{4,3},{5,6},{6,5},{7,0},{8,15},{9,10},{10,... | collective-permute-start | bytes 393224 | tf_op jit(solution)/shard_map/ppermute | solution.py:47
  130.2 9.0 %collective-permute-start.32 = (bf16[80,1024]{1,0:T(8,128)(2,1)S(1)}, bf16[80,1024]{1,0:T(8,128)(2,1)S(1)}, u32[]{:S(2)}, u32[]{:S(2)}) collective-permute-start(bf16[80,1024]{1,0:T(8,128)(2,1)S(1)} %collective-permute-done.31.refs_14_), channel_id=1, source_target_pairs={{0,7},{1,2},{2,1},{3,4},{4,3},{5,6},{6,5},{7,0},{8,15},{9,10},{10,... | collective-permute-start | bytes 491528 | tf_op jit(solution)/shard_map/ppermute | solution.py:50
  133.7 7.3 %collective-permute-start.34 = (bf16[80,1024]{1,0:T(8,128)(2,1)S(1)}, bf16[80,1024]{1,0:T(8,128)(2,1)S(1)}, u32[]{:S(2)}, u32[]{:S(2)}) collective-permute-start(bf16[80,1024]{1,0:T(8,128)(2,1)S(1)} %collective-permute-done.33.refs_13_), channel_id=1, source_target_pairs={{0,7},{1,2},{2,1},{3,4},{4,3},{5,6},{6,5},{7,0},{8,15},{9,10},{10,... | collective-permute-start | bytes 491528 | tf_op jit(solution)/shard_map/ppermute | solution.py:47
  135.1 4.1 %collective-permute-start.18 = (bf16[64,1024]{1,0:T(8,128)(2,1)S(1)}, bf16[64,1024]{1,0:T(8,128)(2,1)S(1)}, u32[]{:S(2)}, u32[]{:S(2)}) collective-permute-start(bf16[64,1024]{1,0:T(8,128)(2,1)S(1)} %collective-permute-done.17.refs_6_), channel_id=1, source_target_pairs={{0,1},{1,0},{2,3},{3,2},{4,5},{5,4},{6,7},{7,6},{8,9},{9,8},{10,11... | collective-permute-start | bytes 393224 | tf_op jit(solution)/shard_map/ppermute | solution.py:50
  135.1 5.5 %collective-permute-start.20 = (bf16[64,1024]{1,0:T(8,128)(2,1)S(1)}, bf16[64,1024]{1,0:T(8,128)(2,1)S(1)}, u32[]{:S(2)}, u32[]{:S(2)}) collective-permute-start(bf16[64,1024]{1,0:T(8,128)(2,1)S(1)} %collective-permute-done.19.refs_5_), channel_id=1, source_target_pairs={{0,1},{1,0},{2,3},{3,2},{4,5},{5,4},{6,7},{7,6},{8,9},{9,8},{10,11... | collective-permute-start | bytes 393224 | tf_op jit(solution)/shard_map/ppermute | solution.py:47
  143.8 12.4 %copy-start.14 = (f32[128,4]{0,1:T(4,128)S(1)}, f32[128,4]{0,1:T(4,128)}, u32[]{:S(2)}) copy-start(f32[128,4]{0,1:T(4,128)} %param.13) | copy-start | bytes 6148
  143.8 40.4 %copy-start.11 = (pred[128,1024]{1,0:T(32,128)(4,1)S(1)}, pred[128,1024]{1,0:T(32,128)(4,1)}, u32[]{:S(2)}) copy-start(pred[128,1024]{1,0:T(32,128)(4,1)} %copy-done.10) | copy-start | bytes 393220
  143.8 40.4 %all-to-all-start.1 = ((bf16[16,64,512]{2,1,0:T(8,128)(2,1)}), bf16[16,64,512]{2,1,0:T(8,128)(2,1)S(1)}, u32[]{:S(2)}, u32[]{:S(2)}) async-start(bf16[16,64,512]{2,1,0:T(8,128)(2,1)} %bitcast.7), calls=%async_computation.1 | async-start | bytes 2097152 | tf_op jit(solution)/shard_map/all_to_all | solution.py:183
  184.6 9.6 %copy-start.13 = (f32[512]{0:T(512)S(1)}, f32[512]{0:T(512)}, u32[]{:S(2)}) copy-start(f32[512]{0:T(512)} %param.21) | copy-start | bytes 6148
  (4 other events, 4.8 us)

commit v5 on v4

--- a/solution.py
+++ b/solution.py
@@ -98,41 +98,36 @@
     )(me, gain, rows, gate, up)
 
 
-def lower_down(me, blocks_a, blocks_b, matrix, shared_matrix):
-    size = len(blocks_a)
-    count, units = blocks_a[0].shape
-    shared = blocks_b[0].shape[0] - count
+def lower_down(me, streams, matrix, kind):
+    size = len(streams[0][0])
+    count, units = streams[0][0][0].shape
+    part = size * count
+    height = part * len(streams)
     width = matrix.shape[1]
-    part = size * count
 
     def body(me_ref, *refs):
-        ins_a, ins_b = refs[:size], refs[size : 2 * size]
-        matrix_ref, shared_ref, out_ref, shared_out_ref, rows_ref, shared_rows_ref = refs[2 * size :]
-        for d in range(size):
-            at_a = block_row(me_ref[0], d, size, count, False)
-            at_b = pl.multiple_of(part + block_row(me_ref[0], d, size, count, True), 16)
-            at_s = block_row(me_ref[0], d, size, shared, True)
-            rows_ref[pl.ds(at_a, count), :] = ins_a[d][...]
-            rows_ref[pl.ds(at_b, count), :] = ins_b[d][:count, :]
-            shared_rows_ref[pl.ds(at_s, shared), :] = ins_b[d][count:, :]
+        ins, (matrix_ref, out_ref, rows_ref) = refs[:-3], refs[-3:]
+        for i, (_, flip) in enumerate(streams):
+            for d in range(size):
+                at = pl.multiple_of(i * part + block_row(me_ref[0], d, size, count, flip), 16)
+                rows_ref[pl.ds(at, count), :] = ins[i * size + d][...]
 
         def columns(n, _):
             at = pl.multiple_of(n * TILE, TILE)
-            out_ref[:, pl.ds(at, TILE)] = dot(rows_ref[...], matrix_ref[:, pl.ds(at, TILE)]).astype(bf16)
-            shared_out_ref[:, pl.ds(at, TILE)] = dot(shared_rows_ref[...], shared_ref[:, pl.ds(at, TILE)])
+            out_ref[:, pl.ds(at, TILE)] = dot(rows_ref[...], matrix_ref[:, pl.ds(at, TILE)]).astype(kind)
             return 0
 
         lax.fori_loop(0, width // TILE, columns, 0)
 
     return pl.pallas_call(
         body,
-        out_shape=[jax.ShapeDtypeStruct((2 * part, width), bf16), jax.ShapeDtypeStruct((size * shared, width), f32)],
-        in_specs=[IN_SMEM] + [IN_VMEM] * (2 * size + 2),
-        out_specs=[IN_VMEM] * 2,
-        scratch_shapes=[pltpu.VMEM((2 * part, units), bf16), pltpu.VMEM((size * shared, units), bf16)],
+        out_shape=jax.ShapeDtypeStruct((height, width), kind),
+        in_specs=[IN_SMEM] + [IN_VMEM] * (size * len(streams) + 1),
+        out_specs=IN_VMEM,
+        scratch_shapes=[pltpu.VMEM((height, units), bf16)],
         compiler_params=pltpu.CompilerParams(vmem_limit_bytes=14 << 20),
         name="lower_down",
-    )(me, *blocks_a, *blocks_b, matrix, shared_matrix)
+    )(me, *[v for blocks, _ in streams for v in blocks], matrix)
 
 
 def layer(
@@ -203,9 +198,11 @@
     total_a = reduce_scatter(pieces_a, tp, False, "tp")
     total_b = reduce_scatter(pieces_b, tp, True, "tp")
     blocks_a = all_gather(hidden_of(total_a), tp, False, "tp")
-    blocks_b = all_gather(jnp.concatenate([hidden_of(total_b), hidden_s], 0), tp, True, "tp")
-    down, shared_out = lower_down(me, blocks_a, blocks_b, down_matrix, shared_down)
+    blocks_b = all_gather(hidden_of(total_b), tp, True, "tp")
+    down = lower_down(me, [(blocks_a, False), (blocks_b, True)], down_matrix, bf16)
     came = swapped(down)
+    blocks_s = all_gather(hidden_s, tp, False, "tp")
+    shared_out = lower_down(me, [(blocks_s, False)], shared_down, f32)
     mixture = shared_out + dot(high, came) + dot(low, came)
 
     square_sum = jnp.sum(mixture * mixture, axis=-1, keepdims=True)

time: 195 us -> 191 us (0.979)
  waiting for transfers between devices: 99 us -> 88.8 us
  starting transfers between devices: 67.6 us -> 71.8 us
    all_to_all x2, waiting for transfers between devices: 39.8 us -> 24.7 us  [swapped(): lax.all_to_all(rows.reshape(experts, capacity, width), 'ep', 0, 0, tiled=...]
    ppermute x6 -> x9, starting transfers between devices: 4.68 us -> 8.25 us  [all_gather(): y = lax.ppermute(y, axis, one if d % 2 else two)]
    ppermute x8 -> x12, starting transfers between devices: 7.86 us -> 10.7 us  [all_gather(): x = lax.ppermute(x, axis, two if d % 2 else one)]
    ppermute x8 -> x12, waiting for transfers between devices: 9.22 us -> 11.8 us  [all_gather(): x = lax.ppermute(x, axis, two if d % 2 else one)]
    ppermute x6 -> x9, waiting for transfers between devices: 3.3 us -> 5.68 us  [all_gather(): y = lax.ppermute(y, axis, one if d % 2 else two)]
    all_to_all x2, starting transfers between devices: 34.2 us -> 32 us  [swapped(): lax.all_to_all(rows.reshape(experts, capacity, width), 'ep', 0, 0, tiled=...]
  transfers between devices with their start and end apart: 37 -> 44, of which waited for: 24 -> 31; matrix products, arithmetic and copies ran while one was open for 2% -> 2% of each run, Pallas kernels for 1% -> 1%
where the time goes in v5:
time: 191 us
  waiting for transfers between devices  88.8 us (46%)
  starting transfers between devices  71.8 us (38%)
  blocking collectives  10.2 us (5%)
  Pallas kernels  8.82 us (5%)
  local copies, waits for them, and re-layouts  4.17 us (2%)
  other arithmetic  3.49 us (2%)
  matrix products  2.91 us (2%)
    all_to_all x2, starting transfers between devices, swapped(): lax.all_to_all(rows.reshape(experts, capacity, width), 'ep', 0, 0, tiled=...  32 us
    ppermute x9, waiting for transfers between devices, reduce_scatter(): x = lax.ppermute(x_next, axis, two if (half - d) % 2 else one)  27 us
    all_to_all x2, waiting for transfers between devices, swapped(): lax.all_to_all(rows.reshape(experts, capacity, width), 'ep', 0, 0, tiled=...  24.7 us
    ppermute x12, waiting for transfers between devices, all_gather(): x = lax.ppermute(x, axis, two if d % 2 else one)  11.8 us
    ppermute x9, waiting for transfers between devices, reduce_scatter(): y = lax.ppermute(y_next, axis, one if (half - d) % 2 else two)  11.1 us
    ppermute x12, starting transfers between devices, all_gather(): x = lax.ppermute(x, axis, two if d % 2 else one)  10.7 us
    all_to_all x1, blocking collectives, layer(): square_sum = lax.all_to_all(copies, 'tp', 0, 0, tiled=True).sum(axis=0)  10.2 us
    ppermute x9, starting transfers between devices, reduce_scatter(): y = lax.ppermute(y_next, axis, one if (half - d) % 2 else two)  8.71 us
  transfers between devices with their start and end apart: 44, of which 31 were waited for; matrix products, arithmetic and copies ran while one was open for 2% of the time, Pallas kernels for 1%

profile of v5, /device:TPU:513, one launch (start us, length us, event | category | flops | bytes accessed | tf_op | source)
XLA Modules:
  0.0 190.6 jit_solution(14180921169308757065)
XLA Ops:
  0.8 1.2 copy-done.3
  2.0 1.2 copy-done.4
  4.1 1.7 project.3
  5.8 2.2 %collective-permute-start = (bf16[16,2176]{1,0:T(8,128)(2,1)}, bf16[16,2176]{1,0:T(8,128)(2,1)}, u32[]{:S(2)}, u32[]{:S(2)}) collective-permute-start(bf16[16,2176]{1,0:T(8,128)(2,1)} %get-tuple-element.35), channel_id=1, source_target_pairs={{0,1},{1,0},{2,3},{3,2},{4,5},{5,4},{6,7},{7,6},{8,9},{9,8},{10,11... | collective-permute-start | bytes 208904 | tf_op jit(solution)/shard_map/ppermute | solution.py:30
  8.5 1.5 convolution_convert_fusion
  10.0 21.9 %all-to-all-start = ((bf16[16,64,512]{2,1,0:T(8,128)(2,1)}), bf16[16,64,512]{2,1,0:T(8,128)(2,1)S(1)}, u32[]{:S(2)}, u32[]{:S(2)}) async-start(bf16[16,64,512]{2,1,0:T(8,128)(2,1)} %bitcast.1), calls=%async_computation | async-start | bytes 2097152 | tf_op jit(solution)/shard_map/all_to_all | solution.py:178
  31.9 1.9 collective-permute-start.4
  35.7 1.9 %collective-permute-start.5 = (bf16[16,2176]{1,0:T(8,128)(2,1)S(1)}, bf16[16,2176]{1,0:T(8,128)(2,1)S(1)}, u32[]{:S(2)}, u32[]{:S(2)}) collective-permute-start(bf16[16,2176]{1,0:T(8,128)(2,1)S(1)} %add_convert_fusion.11), channel_id=1, source_target_pairs={{0,7},{1,2},{2,1},{3,4},{4,3},{5,6},{6,5},{7,0},{8,15},{9,10},{10,... | collective-permute-start | bytes 208904 | tf_op jit(solution)/shard_map/ppermute | solution.py:37
  37.6 1.8 collective-permute-done.1
  39.6 1.2 collective-permute-done.5
  41.2 1.8 collective-permute-done.2
  43.2 1.2 collective-permute-done.6
  44.4 3.5 %collective-permute-done.3 = bf16[16,2176]{1,0:T(8,128)(2,1)S(1)} collective-permute-done((bf16[16,2176]{1,0:T(8,128)(2,1)S(1)}, bf16[16,2176]{1,0:T(8,128)(2,1)S(1)}, u32[]{:S(2)}, u32[]{:S(2)}) %collective-permute-start.3) | collective-permute-done | bytes 69664 | tf_op jit(solution)/shard_map/ppermute | solution.py:36
  48.1 11.9 %all-to-all-done = bf16[16,64,512]{2,1,0:T(8,128)(2,1)S(1)} async-done(((bf16[16,64,512]{2,1,0:T(8,128)(2,1)}), bf16[16,64,512]{2,1,0:T(8,128)(2,1)S(1)}, u32[]{:S(2)}, u32[]{:S(2)}) %all-to-all-start) | async-done | bytes 1048608 | tf_op jit(solution)/shard_map/all_to_all | solution.py:178
  60.0 2.0 %project.4 = (bf16[64,2176]{1,0:T(8,128)(2,1)S(1)}, bf16[64,2176]{1,0:T(8,128)(2,1)S(1)}, bf16[64,2176]{1,0:T(8,128)(2,1)S(1)}, bf16[64,2176]{1,0:T(8,128)(2,1)S...) custom-call(s32[1]{0:T(128)} %bitcast.me_ref, ...), custom_call_target="tpu_custom_call" | custom-call | tf_op jit(solution)/shard_map/project/pallas_call | solution.py:90
  62.0 1.9 collective-permute-start.18
  63.9 2.0 %project.5 = (bf16[64,2176]{1,0:T(8,128)(2,1)S(1)}, bf16[64,2176]{1,0:T(8,128)(2,1)S(1)}, bf16[64,2176]{1,0:T(8,128)(2,1)S(1)}, bf16[64,2176]{1,0:T(8,128)(2,1)S...) custom-call(s32[1]{0:T(128)} %bitcast.me_ref, ...), custom_call_target="tpu_custom_call" | custom-call | tf_op jit(solution)/shard_map/project/pallas_call | solution.py:90
  66.2 2.6 %collective-permute-start.28 = (bf16[64,2176]{1,0:T(8,128)(2,1)S(1)}, bf16[64,2176]{1,0:T(8,128)(2,1)S(1)}, u32[]{:S(2)}, u32[]{:S(2)}) collective-permute-start(bf16[64,2176]{1,0:T(8,128)(2,1)S(1)} %get-tuple-element.53), channel_id=1, source_target_pairs={{0,7},{1,2},{2,1},{3,4},{4,3},{5,6},{6,5},{7,0},{8,15},{9,10},{10,... | collective-permute-start | bytes 835592 | tf_op jit(solution)/shard_map/ppermute | solution.py:30
  68.9 2.2 %collective-permute-done.18 = bf16[64,2176]{1,0:T(8,128)(2,1)S(1)} collective-permute-done((bf16[64,2176]{1,0:T(8,128)(2,1)S(1)}, bf16[64,2176]{1,0:T(8,128)(2,1)S(1)}, u32[]{:S(2)}, u32[]{:S(2)}) %collective-permute-start.18) | collective-permute-done | bytes 278560 | tf_op jit(solution)/shard_map/ppermute | solution.py:37
  71.3 4.7 %collective-permute-done.14 = bf16[64,2176]{1,0:T(8,128)(2,1)S(1)} collective-permute-done((bf16[64,2176]{1,0:T(8,128)(2,1)S(1)}, bf16[64,2176]{1,0:T(8,128)(2,1)S(1)}, u32[]{:S(2)}, u32[]{:S(2)}) %collective-permute-start.14) | collective-permute-done | bytes 278560 | tf_op jit(solution)/shard_map/ppermute | solution.py:30
  76.3 1.8 collective-permute-start.33
  78.2 3.9 %collective-permute-done.28 = bf16[64,2176]{1,0:T(8,128)(2,1)S(1)} collective-permute-done((bf16[64,2176]{1,0:T(8,128)(2,1)S(1)}, bf16[64,2176]{1,0:T(8,128)(2,1)S(1)}, u32[]{:S(2)}, u32[]{:S(2)}) %collective-permute-start.28) | collective-permute-done | bytes 278560 | tf_op jit(solution)/shard_map/ppermute | solution.py:30
  82.3 5.7 %collective-permute-done.19 = bf16[64,2176]{1,0:T(8,128)(2,1)S(1)} collective-permute-done((bf16[64,2176]{1,0:T(8,128)(2,1)S(1)}, bf16[64,2176]{1,0:T(8,128)(2,1)S(1)}, u32[]{:S(2)}, u32[]{:S(2)}) %collective-permute-start.19) | collective-permute-done | bytes 278560 | tf_op jit(solution)/shard_map/ppermute | solution.py:37
  88.5 4.7 %collective-permute-done.15 = bf16[64,2176]{1,0:T(8,128)(2,1)S(1)} collective-permute-done((bf16[64,2176]{1,0:T(8,128)(2,1)S(1)}, bf16[64,2176]{1,0:T(8,128)(2,1)S(1)}, u32[]{:S(2)}, u32[]{:S(2)}) %collective-permute-start.15) | collective-permute-done | bytes 278560 | tf_op jit(solution)/shard_map/ppermute | solution.py:36
  94.4 2.8 %collective-permute-start.30 = (bf16[64,2176]{1,0:T(8,128)(2,1)S(1)}, bf16[64,2176]{1,0:T(8,128)(2,1)S(1)}, u32[]{:S(2)}, u32[]{:S(2)}) collective-permute-start(bf16[64,2176]{1,0:T(8,128)(2,1)S(1)} %add_convert_fusion.3), channel_id=1, source_target_pairs={{0,7},{1,2},{2,1},{3,4},{4,3},{5,6},{6,5},{7,0},{8,15},{9,10},{10,... | collective-permute-start | bytes 835592 | tf_op jit(solution)/shard_map/ppermute | solution.py:36
  97.1 6.0 %collective-permute-done.16 = bf16[64,2176]{1,0:T(8,128)(2,1)S(1)} collective-permute-done((bf16[64,2176]{1,0:T(8,128)(2,1)S(1)}, bf16[64,2176]{1,0:T(8,128)(2,1)S(1)}, u32[]{:S(2)}, u32[]{:S(2)}) %collective-permute-start.16) | collective-permute-done | bytes 278560 | tf_op jit(solution)/shard_map/ppermute | solution.py:36
  103.2 2.6 %collective-permute-start.17 = (bf16[64,2176]{1,0:T(8,128)(2,1)S(1)}, bf16[64,2176]{1,0:T(8,128)(2,1)S(1)}, u32[]{:S(2)}, u32[]{:S(2)}) collective-permute-start(bf16[64,2176]{1,0:T(8,128)(2,1)S(1)} %add_convert_fusion.7), channel_id=1, source_target_pairs={{0,7},{1,2},{2,1},{3,4},{4,3},{5,6},{6,5},{7,0},{8,15},{9,10},{10,... | collective-permute-start | bytes 835592 | tf_op jit(solution)/shard_map/ppermute | solution.py:36
  105.8 3.4 %collective-permute-done.30 = bf16[64,2176]{1,0:T(8,128)(2,1)S(1)} collective-permute-done((bf16[64,2176]{1,0:T(8,128)(2,1)S(1)}, bf16[64,2176]{1,0:T(8,128)(2,1)S(1)}, u32[]{:S(2)}, u32[]{:S(2)}) %collective-permute-start.30) | collective-permute-done | bytes 278560 | tf_op jit(solution)/shard_map/ppermute | solution.py:36
  109.4 5.7 %collective-permute-done.17 = bf16[64,2176]{1,0:T(8,128)(2,1)S(1)} collective-permute-done((bf16[64,2176]{1,0:T(8,128)(2,1)S(1)}, bf16[64,2176]{1,0:T(8,128)(2,1)S(1)}, u32[]{:S(2)}, u32[]{:S(2)}) %collective-permute-start.17) | collective-permute-done | bytes 278560 | tf_op jit(solution)/shard_map/ppermute | solution.py:36
  116.6 1.4 collective-permute-start.21
  118.1 2.3 %collective-permute-start.35 = (bf16[64,1024]{1,0:T(8,128)(2,1)S(1)}, bf16[64,1024]{1,0:T(8,128)(2,1)S(1)}, u32[]{:S(2)}, u32[]{:S(2)}) collective-permute-start(bf16[64,1024]{1,0:T(8,128)(2,1)S(1)} %fusion.7.refs_8_), channel_id=1, source_target_pairs={{0,7},{1,2},{2,1},{3,4},{4,3},{5,6},{6,5},{7,0},{8,15},{9,10},{10,... | collective-permute-start | bytes 393224 | tf_op jit(solution)/shard_map/ppermute | solution.py:50
  120.7 2.1 %collective-permute-start.37 = (bf16[64,1024]{1,0:T(8,128)(2,1)S(1)}, bf16[64,1024]{1,0:T(8,128)(2,1)S(1)}, u32[]{:S(2)}, u32[]{:S(2)}) collective-permute-start(bf16[64,1024]{1,0:T(8,128)(2,1)S(1)} %collective-permute-done.36.refs_15_), channel_id=1, source_target_pairs={{0,7},{1,2},{2,1},{3,4},{4,3},{5,6},{6,5},{7,0},{8,15},{9,10},{10,... | collective-permute-start | bytes 393224 | tf_op jit(solution)/shard_map/ppermute | solution.py:47
  122.8 2.3 %collective-permute-start.24 = (bf16[64,1024]{1,0:T(8,128)(2,1)S(1)}, bf16[64,1024]{1,0:T(8,128)(2,1)S(1)}, u32[]{:S(2)}, u32[]{:S(2)}) collective-permute-start(bf16[64,1024]{1,0:T(8,128)(2,1)S(1)} %collective-permute-done.21.refs_1_), channel_id=1, source_target_pairs={{0,7},{1,2},{2,1},{3,4},{4,3},{5,6},{6,5},{7,0},{8,15},{9,10},{10,... | collective-permute-start | bytes 393224 | tf_op jit(solution)/shard_map/ppermute | solution.py:50
  126.2 1.7 collective-permute-start.26
  128.0 1.3 collective-permute-done.24.refs_6_
  129.9 1.1 collective-permute-start.39
  132.2 2.1 %collective-permute-start.41 = (bf16[64,1024]{1,0:T(8,128)(2,1)S(1)}, bf16[64,1024]{1,0:T(8,128)(2,1)S(1)}, u32[]{:S(2)}, u32[]{:S(2)}) collective-permute-start(bf16[64,1024]{1,0:T(8,128)(2,1)S(1)} %collective-permute-done.40.refs_13_), channel_id=1, source_target_pairs={{0,7},{1,2},{2,1},{3,4},{4,3},{5,6},{6,5},{7,0},{8,15},{9,10},{10,... | collective-permute-start | bytes 393224 | tf_op jit(solution)/shard_map/ppermute | solution.py:47
  134.3 2.0 %collective-permute-done.39.refs_11_ = bf16[64,1024]{1,0:T(8,128)(2,1)S(1)} collective-permute-done((bf16[64,1024]{1,0:T(8,128)(2,1)S(1)}, bf16[64,1024]{1,0:T(8,128)(2,1)S(1)}, u32[]{:S(2)}, u32[]{:S(2)}) %collective-permute-start.39) | collective-permute-done | bytes 131104 | tf_op jit(solution)/shard_map/ppermute | solution.py:50
  137.8 2.6 %lower_down.3 = bf16[1024,512]{1,0:T(8,128)(2,1)} custom-call(s32[1]{0:T(128)} %bitcast.me_ref, bf16[64,1024]{1,0:T(8,128)(2,1)S(1)} %fusion.9.refs_0_, bf16[64,1024]{1,0:T(8,128)(2,1)S(1)} %collective-permute-done.21.refs_1_, bf16[64,1024]{1,0:T(8,128)(2,1)S(1)} %collective-permute-done.23.refs_2_, bf16[64,1024]{1,0:T(8,128)(2,1)S(1)} %collective-permute-done.25.refs_3_, ...), custom_call_target="tpu_custom_call" | custom-call | tf_op jit(solution)/shard_map/lower_down/pallas_call | solution.py:122
  140.3 10.2 %all-to-all-start.1 = ((bf16[16,64,512]{2,1,0:T(8,128)(2,1)}), bf16[16,64,512]{2,1,0:T(8,128)(2,1)S(1)}, u32[]{:S(2)}, u32[]{:S(2)}) async-start(bf16[16,64,512]{2,1,0:T(8,128)(2,1)} %bitcast.7), calls=%async_computation.1 | async-start | bytes 2097152 | tf_op jit(solution)/shard_map/all_to_all | solution.py:178
  150.5 2.0 %collective-permute-start.8 = (bf16[16,1024]{1,0:T(8,128)(2,1)S(1)}, bf16[16,1024]{1,0:T(8,128)(2,1)S(1)}, u32[]{:S(2)}, u32[]{:S(2)}) collective-permute-start(bf16[16,1024]{1,0:T(8,128)(2,1)S(1)} %fusion.13.refs_0_), channel_id=1, source_target_pairs={{0,7},{1,2},{2,1},{3,4},{4,3},{5,6},{6,5},{7,0},{8,15},{9,10},{10,... | collective-permute-start | bytes 98312 | tf_op jit(solution)/shard_map/ppermute | solution.py:47
  152.5 2.1 %collective-permute-done.8.refs_7_ = bf16[16,1024]{1,0:T(8,128)(2,1)S(1)} collective-permute-done((bf16[16,1024]{1,0:T(8,128)(2,1)S(1)}, bf16[16,1024]{1,0:T(8,128)(2,1)S(1)}, u32[]{:S(2)}, u32[]{:S(2)}) %collective-permute-start.8) | collective-permute-done | bytes 32800 | tf_op jit(solution)/shard_map/ppermute | solution.py:47
  156.5 1.2 collective-permute-done.9.refs_2_
  157.7 1.8 collective-permute-start.12
  159.8 2.4 %collective-permute-done.12.refs_5_ = bf16[16,1024]{1,0:T(8,128)(2,1)S(1)} collective-permute-done((bf16[16,1024]{1,0:T(8,128)(2,1)S(1)}, bf16[16,1024]{1,0:T(8,128)(2,1)S(1)}, u32[]{:S(2)}, u32[]{:S(2)}) %collective-permute-start.12) | collective-permute-done | bytes 32800 | tf_op jit(solution)/shard_map/ppermute | solution.py:47
  162.9 2.4 %collective-permute-done.13.refs_4_ = bf16[16,1024]{1,0:T(8,128)(2,1)S(1)} collective-permute-done((bf16[16,1024]{1,0:T(8,128)(2,1)S(1)}, bf16[16,1024]{1,0:T(8,128)(2,1)S(1)}, u32[]{:S(2)}, u32[]{:S(2)}) %collective-permute-start.13) | collective-permute-done | bytes 32800 | tf_op jit(solution)/shard_map/ppermute | solution.py:47
  165.8 12.8 %all-to-all-done.1 = bf16[16,64,512]{2,1,0:T(8,128)(2,1)S(1)} async-done(((bf16[16,64,512]{2,1,0:T(8,128)(2,1)}), bf16[16,64,512]{2,1,0:T(8,128)(2,1)S(1)}, u32[]{:S(2)}, u32[]{:S(2)}) %all-to-all-start.1) | async-done | bytes 1048608 | tf_op jit(solution)/shard_map/all_to_all | solution.py:178
  179.6 10.2 %all_to_all.15 = f32[8,128,1]{1,2,0:T(1,128)S(1)} all-to-all(f32[8,128,1]{1,2,0:T(1,128)S(1)} %broadcast_in_dim.34), channel_id=1, replica_groups=mesh['grp'=2,'ep'=16,'tp'=8] {'tp'}, dimensions={0} | all-to-all | bytes 8192 | tf_op jit(solution)/shard_map/all_to_all | solution.py:210
  (114 shorter events, 19.2 us)
Async XLA Ops:
  5.8 27.9 %collective-permute-start = (bf16[16,2176]{1,0:T(8,128)(2,1)}, bf16[16,2176]{1,0:T(8,128)(2,1)}, u32[]{:S(2)}, u32[]{:S(2)}) collective-permute-start(bf16[16,2176]{1,0:T(8,128)(2,1)} %get-tuple-element.35), channel_id=1, source_target_pairs={{0,1},{1,0},{2,3},{3,2},{4,5},{5,4},{6,7},{7,6},{8,9},{9,8},{10,11... | collective-permute-start | bytes 208904 | tf_op jit(solution)/shard_map/ppermute | solution.py:30
  10.0 50.0 %copy-start.1 = (bf16[1,512,1024]{2,1,0:T(8,128)(2,1)S(1)}, bf16[1,512,1024]{2,1,0:T(8,128)(2,1)}, u32[]{:S(2)}) copy-start(bf16[1,512,1024]{2,1,0:T(8,128)(2,1)} %param.16) | copy-start | bytes 3145732
  10.0 50.0 %all-to-all-start = ((bf16[16,64,512]{2,1,0:T(8,128)(2,1)}), bf16[16,64,512]{2,1,0:T(8,128)(2,1)S(1)}, u32[]{:S(2)}, u32[]{:S(2)}) async-start(bf16[16,64,512]{2,1,0:T(8,128)(2,1)} %bitcast.1), calls=%async_computation | async-start | bytes 2097152 | tf_op jit(solution)/shard_map/all_to_all | solution.py:178
  31.9 28.1 %copy-start = (bf16[1,512,1024]{2,1,0:T(8,128)(2,1)S(1)}, bf16[1,512,1024]{2,1,0:T(8,128)(2,1)}, u32[]{:S(2)}) copy-start(bf16[1,512,1024]{2,1,0:T(8,128)(2,1)} %param.15) | copy-start | bytes 3145732
  31.9 3.8 %collective-permute-start.4 = (bf16[16,2176]{1,0:T(8,128)(2,1)}, bf16[16,2176]{1,0:T(8,128)(2,1)S(1)}, u32[]{:S(2)}, u32[]{:S(2)}) collective-permute-start(bf16[16,2176]{1,0:T(8,128)(2,1)} %copy-done.9), channel_id=1, source_target_pairs={{0,1},{1,0},{2,3},{3,2},{4,5},{5,4},{6,7},{7,6},{8,9},{9,8},{10,11... | collective-permute-start | bytes 208904 | tf_op jit(solution)/shard_map/ppermute | solution.py:37
  34.7 4.8 %collective-permute-start.1 = (bf16[16,2176]{1,0:T(8,128)(2,1)S(1)}, bf16[16,2176]{1,0:T(8,128)(2,1)S(1)}, u32[]{:S(2)}, u32[]{:S(2)}) collective-permute-start(bf16[16,2176]{1,0:T(8,128)(2,1)S(1)} %add_convert_fusion.14), channel_id=1, source_target_pairs={{0,7},{1,2},{2,1},{3,4},{4,3},{5,6},{6,5},{7,0},{8,15},{9,10},{10,... | collective-permute-start | bytes 208904 | tf_op jit(solution)/shard_map/ppermute | solution.py:36
  35.7 5.1 %collective-permute-start.5 = (bf16[16,2176]{1,0:T(8,128)(2,1)S(1)}, bf16[16,2176]{1,0:T(8,128)(2,1)S(1)}, u32[]{:S(2)}, u32[]{:S(2)}) collective-permute-start(bf16[16,2176]{1,0:T(8,128)(2,1)S(1)} %add_convert_fusion.11), channel_id=1, source_target_pairs={{0,7},{1,2},{2,1},{3,4},{4,3},{5,6},{6,5},{7,0},{8,15},{9,10},{10,... | collective-permute-start | bytes 208904 | tf_op jit(solution)/shard_map/ppermute | solution.py:37
  39.5 3.6 %collective-permute-start.2 = (bf16[16,2176]{1,0:T(8,128)(2,1)S(1)}, bf16[16,2176]{1,0:T(8,128)(2,1)S(1)}, u32[]{:S(2)}, u32[]{:S(2)}) collective-permute-start(bf16[16,2176]{1,0:T(8,128)(2,1)S(1)} %add_convert_fusion.13), channel_id=1, source_target_pairs={{0,1},{1,0},{2,3},{3,2},{4,5},{5,4},{6,7},{7,6},{8,9},{9,8},{10,11... | collective-permute-start | bytes 208904 | tf_op jit(solution)/shard_map/ppermute | solution.py:36
  40.8 3.6 %collective-permute-start.6 = (bf16[16,2176]{1,0:T(8,128)(2,1)S(1)}, bf16[16,2176]{1,0:T(8,128)(2,1)S(1)}, u32[]{:S(2)}, u32[]{:S(2)}) collective-permute-start(bf16[16,2176]{1,0:T(8,128)(2,1)S(1)} %add_convert_fusion.10), channel_id=1, source_target_pairs={{0,1},{1,0},{2,3},{3,2},{4,5},{5,4},{6,7},{7,6},{8,9},{9,8},{10,11... | collective-permute-start | bytes 208904 | tf_op jit(solution)/shard_map/ppermute | solution.py:37
  43.1 4.8 %collective-permute-start.3 = (bf16[16,2176]{1,0:T(8,128)(2,1)S(1)}, bf16[16,2176]{1,0:T(8,128)(2,1)S(1)}, u32[]{:S(2)}, u32[]{:S(2)}) collective-permute-start(bf16[16,2176]{1,0:T(8,128)(2,1)S(1)} %add_convert_fusion.12), channel_id=1, source_target_pairs={{0,7},{1,2},{2,1},{3,4},{4,3},{5,6},{6,5},{7,0},{8,15},{9,10},{10,... | collective-permute-start | bytes 208904 | tf_op jit(solution)/shard_map/ppermute | solution.py:36
  62.0 9.1 %collective-permute-start.18 = (bf16[64,2176]{1,0:T(8,128)(2,1)S(1)}, bf16[64,2176]{1,0:T(8,128)(2,1)S(1)}, u32[]{:S(2)}, u32[]{:S(2)}) collective-permute-start(bf16[64,2176]{1,0:T(8,128)(2,1)S(1)} %get-tuple-element.48), channel_id=1, source_target_pairs={{0,1},{1,0},{2,3},{3,2},{4,5},{5,4},{6,7},{7,6},{8,9},{9,8},{10,11... | collective-permute-start | bytes 835592 | tf_op jit(solution)/shard_map/ppermute | solution.py:37
  65.9 10.1 %collective-permute-start.14 = (bf16[64,2176]{1,0:T(8,128)(2,1)S(1)}, bf16[64,2176]{1,0:T(8,128)(2,1)S(1)}, u32[]{:S(2)}, u32[]{:S(2)}) collective-permute-start(bf16[64,2176]{1,0:T(8,128)(2,1)S(1)} %get-tuple-element.45), channel_id=1, source_target_pairs={{0,1},{1,0},{2,3},{3,2},{4,5},{5,4},{6,7},{7,6},{8,9},{9,8},{10,11... | collective-permute-start | bytes 835592 | tf_op jit(solution)/shard_map/ppermute | solution.py:30
  66.1 10.2 %collective-permute-start.32 = (bf16[64,2176]{1,0:T(8,128)(2,1)S(1)}, bf16[64,2176]{1,0:T(8,128)(2,1)S(1)}, u32[]{:S(2)}, u32[]{:S(2)}) collective-permute-start(bf16[64,2176]{1,0:T(8,128)(2,1)S(1)} %get-tuple-element.56), channel_id=1, source_target_pairs={{0,7},{1,2},{2,1},{3,4},{4,3},{5,6},{6,5},{7,0},{8,15},{9,10},{10,... | collective-permute-start | bytes 835592 | tf_op jit(solution)/shard_map/ppermute | solution.py:37
  66.2 15.8 %collective-permute-start.28 = (bf16[64,2176]{1,0:T(8,128)(2,1)S(1)}, bf16[64,2176]{1,0:T(8,128)(2,1)S(1)}, u32[]{:S(2)}, u32[]{:S(2)}) collective-permute-start(bf16[64,2176]{1,0:T(8,128)(2,1)S(1)} %get-tuple-element.53), channel_id=1, source_target_pairs={{0,7},{1,2},{2,1},{3,4},{4,3},{5,6},{6,5},{7,0},{8,15},{9,10},{10,... | collective-permute-start | bytes 835592 | tf_op jit(solution)/shard_map/ppermute | solution.py:30
  71.2 16.8 %collective-permute-start.19 = (bf16[64,2176]{1,0:T(8,128)(2,1)S(1)}, bf16[64,2176]{1,0:T(8,128)(2,1)S(1)}, u32[]{:S(2)}, u32[]{:S(2)}) collective-permute-start(bf16[64,2176]{1,0:T(8,128)(2,1)S(1)} %add_convert_fusion.6), channel_id=1, source_target_pairs={{0,7},{1,2},{2,1},{3,4},{4,3},{5,6},{6,5},{7,0},{8,15},{9,10},{10,... | collective-permute-start | bytes 835592 | tf_op jit(solution)/shard_map/ppermute | solution.py:37
  76.1 17.1 %collective-permute-start.15 = (bf16[64,2176]{1,0:T(8,128)(2,1)S(1)}, bf16[64,2176]{1,0:T(8,128)(2,1)S(1)}, u32[]{:S(2)}, u32[]{:S(2)}) collective-permute-start(bf16[64,2176]{1,0:T(8,128)(2,1)S(1)} %add_convert_fusion.9), channel_id=1, source_target_pairs={{0,7},{1,2},{2,1},{3,4},{4,3},{5,6},{6,5},{7,0},{8,15},{9,10},{10,... | collective-permute-start | bytes 835592 | tf_op jit(solution)/shard_map/ppermute | solution.py:36
  76.3 17.7 %collective-permute-start.33 = (bf16[64,2176]{1,0:T(8,128)(2,1)S(1)}, bf16[64,2176]{1,0:T(8,128)(2,1)S(1)}, u32[]{:S(2)}, u32[]{:S(2)}) collective-permute-start(bf16[64,2176]{1,0:T(8,128)(2,1)S(1)} %add_convert_fusion.1), channel_id=1, source_target_pairs={{0,1},{1,0},{2,3},{3,2},{4,5},{5,4},{6,7},{7,6},{8,9},{9,8},{10,11... | collective-permute-start | bytes 835592 | tf_op jit(solution)/shard_map/ppermute | solution.py:37
  82.1 12.2 %collective-permute-start.29 = (bf16[64,2176]{1,0:T(8,128)(2,1)S(1)}, bf16[64,2176]{1,0:T(8,128)(2,1)S(1)}, u32[]{:S(2)}, u32[]{:S(2)}) collective-permute-start(bf16[64,2176]{1,0:T(8,128)(2,1)S(1)} %add_convert_fusion.4), channel_id=1, source_target_pairs={{0,1},{1,0},{2,3},{3,2},{4,5},{5,4},{6,7},{7,6},{8,9},{9,8},{10,11... | collective-permute-start | bytes 835592 | tf_op jit(solution)/shard_map/ppermute | solution.py:36
  88.1 21.3 %collective-permute-start.20 = (bf16[64,2176]{1,0:T(8,128)(2,1)S(1)}, bf16[64,2176]{1,0:T(8,128)(2,1)S(1)}, u32[]{:S(2)}, u32[]{:S(2)}) collective-permute-start(bf16[64,2176]{1,0:T(8,128)(2,1)S(1)} %add_convert_fusion.5), channel_id=1, source_target_pairs={{0,1},{1,0},{2,3},{3,2},{4,5},{5,4},{6,7},{7,6},{8,9},{9,8},{10,11... | collective-permute-start | bytes 835592 | tf_op jit(solution)/shard_map/ppermute | solution.py:37
  93.2 9.9 %collective-permute-start.16 = (bf16[64,2176]{1,0:T(8,128)(2,1)S(1)}, bf16[64,2176]{1,0:T(8,128)(2,1)S(1)}, u32[]{:S(2)}, u32[]{:S(2)}) collective-permute-start(bf16[64,2176]{1,0:T(8,128)(2,1)S(1)} %add_convert_fusion.8), channel_id=1, source_target_pairs={{0,1},{1,0},{2,3},{3,2},{4,5},{5,4},{6,7},{7,6},{8,9},{9,8},{10,11... | collective-permute-start | bytes 835592 | tf_op jit(solution)/shard_map/ppermute | solution.py:36
  94.1 22.0 %collective-permute-start.34 = (bf16[64,2176]{1,0:T(8,128)(2,1)S(1)}, bf16[64,2176]{1,0:T(8,128)(2,1)S(1)}, u32[]{:S(2)}, u32[]{:S(2)}) collective-permute-start(bf16[64,2176]{1,0:T(8,128)(2,1)S(1)} %add_convert_fusion), channel_id=1, source_target_pairs={{0,7},{1,2},{2,1},{3,4},{4,3},{5,6},{6,5},{7,0},{8,15},{9,10},{10,... | collective-permute-start | bytes 835592 | tf_op jit(solution)/shard_map/ppermute | solution.py:37
  94.4 14.8 %collective-permute-start.30 = (bf16[64,2176]{1,0:T(8,128)(2,1)S(1)}, bf16[64,2176]{1,0:T(8,128)(2,1)S(1)}, u32[]{:S(2)}, u32[]{:S(2)}) collective-permute-start(bf16[64,2176]{1,0:T(8,128)(2,1)S(1)} %add_convert_fusion.3), channel_id=1, source_target_pairs={{0,7},{1,2},{2,1},{3,4},{4,3},{5,6},{6,5},{7,0},{8,15},{9,10},{10,... | collective-permute-start | bytes 835592 | tf_op jit(solution)/shard_map/ppermute | solution.py:36
  103.2 12.0 %collective-permute-start.17 = (bf16[64,2176]{1,0:T(8,128)(2,1)S(1)}, bf16[64,2176]{1,0:T(8,128)(2,1)S(1)}, u32[]{:S(2)}, u32[]{:S(2)}) collective-permute-start(bf16[64,2176]{1,0:T(8,128)(2,1)S(1)} %add_convert_fusion.7), channel_id=1, source_target_pairs={{0,7},{1,2},{2,1},{3,4},{4,3},{5,6},{6,5},{7,0},{8,15},{9,10},{10,... | collective-permute-start | bytes 835592 | tf_op jit(solution)/shard_map/ppermute | solution.py:36
  109.3 6.8 %collective-permute-start.31 = (bf16[64,2176]{1,0:T(8,128)(2,1)S(1)}, bf16[64,2176]{1,0:T(8,128)(2,1)S(1)}, u32[]{:S(2)}, u32[]{:S(2)}) collective-permute-start(bf16[64,2176]{1,0:T(8,128)(2,1)S(1)} %add_convert_fusion.2), channel_id=1, source_target_pairs={{0,1},{1,0},{2,3},{3,2},{4,5},{5,4},{6,7},{7,6},{8,9},{9,8},{10,11... | collective-permute-start | bytes 835592 | tf_op jit(solution)/shard_map/ppermute | solution.py:36
  115.6 5.2 %collective-permute-start.22 = (bf16[64,1024]{1,0:T(8,128)(2,1)S(1)}, bf16[64,1024]{1,0:T(8,128)(2,1)S(1)}, u32[]{:S(2)}, u32[]{:S(2)}) collective-permute-start(bf16[64,1024]{1,0:T(8,128)(2,1)S(1)} %fusion.9.refs_0_), channel_id=1, source_target_pairs={{0,7},{1,2},{2,1},{3,4},{4,3},{5,6},{6,5},{7,0},{8,15},{9,10},{10,... | collective-permute-start | bytes 393224 | tf_op jit(solution)/shard_map/ppermute | solution.py:47
  116.5 4.2 %collective-permute-start.36 = (bf16[64,1024]{1,0:T(8,128)(2,1)S(1)}, bf16[64,1024]{1,0:T(8,128)(2,1)S(1)}, u32[]{:S(2)}, u32[]{:S(2)}) collective-permute-start(bf16[64,1024]{1,0:T(8,128)(2,1)S(1)} %fusion.7.refs_8_), channel_id=1, source_target_pairs={{0,1},{1,0},{2,3},{3,2},{4,5},{5,4},{6,7},{7,6},{8,9},{9,8},{10,11... | collective-permute-start | bytes 393224 | tf_op jit(solution)/shard_map/ppermute | solution.py:47
  116.6 6.2 %collective-permute-start.21 = (bf16[64,1024]{1,0:T(8,128)(2,1)S(1)}, bf16[64,1024]{1,0:T(8,128)(2,1)S(1)}, u32[]{:S(2)}, u32[]{:S(2)}) collective-permute-start(bf16[64,1024]{1,0:T(8,128)(2,1)S(1)} %fusion.9.refs_0_), channel_id=1, source_target_pairs={{0,1},{1,0},{2,3},{3,2},{4,5},{5,4},{6,7},{7,6},{8,9},{9,8},{10,11... | collective-permute-start | bytes 393224 | tf_op jit(solution)/shard_map/ppermute | solution.py:50
  118.1 7.1 %collective-permute-start.35 = (bf16[64,1024]{1,0:T(8,128)(2,1)S(1)}, bf16[64,1024]{1,0:T(8,128)(2,1)S(1)}, u32[]{:S(2)}, u32[]{:S(2)}) collective-permute-start(bf16[64,1024]{1,0:T(8,128)(2,1)S(1)} %fusion.7.refs_8_), channel_id=1, source_target_pairs={{0,7},{1,2},{2,1},{3,4},{4,3},{5,6},{6,5},{7,0},{8,15},{9,10},{10,... | collective-permute-start | bytes 393224 | tf_op jit(solution)/shard_map/ppermute | solution.py:50
  120.7 5.5 %collective-permute-start.23 = (bf16[64,1024]{1,0:T(8,128)(2,1)S(1)}, bf16[64,1024]{1,0:T(8,128)(2,1)S(1)}, u32[]{:S(2)}, u32[]{:S(2)}) collective-permute-start(bf16[64,1024]{1,0:T(8,128)(2,1)S(1)} %collective-permute-done.22.refs_7_), channel_id=1, source_target_pairs={{0,1},{1,0},{2,3},{3,2},{4,5},{5,4},{6,7},{7,6},{8,9},{9,8},{10,11... | collective-permute-start | bytes 393224 | tf_op jit(solution)/shard_map/ppermute | solution.py:47
  120.7 7.2 %collective-permute-start.37 = (bf16[64,1024]{1,0:T(8,128)(2,1)S(1)}, bf16[64,1024]{1,0:T(8,128)(2,1)S(1)}, u32[]{:S(2)}, u32[]{:S(2)}) collective-permute-start(bf16[64,1024]{1,0:T(8,128)(2,1)S(1)} %collective-permute-done.36.refs_15_), channel_id=1, source_target_pairs={{0,7},{1,2},{2,1},{3,4},{4,3},{5,6},{6,5},{7,0},{8,15},{9,10},{10,... | collective-permute-start | bytes 393224 | tf_op jit(solution)/shard_map/ppermute | solution.py:47
  122.8 6.4 %collective-permute-start.24 = (bf16[64,1024]{1,0:T(8,128)(2,1)S(1)}, bf16[64,1024]{1,0:T(8,128)(2,1)S(1)}, u32[]{:S(2)}, u32[]{:S(2)}) collective-permute-start(bf16[64,1024]{1,0:T(8,128)(2,1)S(1)} %collective-permute-done.21.refs_1_), channel_id=1, source_target_pairs={{0,7},{1,2},{2,1},{3,4},{4,3},{5,6},{6,5},{7,0},{8,15},{9,10},{10,... | collective-permute-start | bytes 393224 | tf_op jit(solution)/shard_map/ppermute | solution.py:50
  125.2 4.8 %collective-permute-start.38 = (bf16[64,1024]{1,0:T(8,128)(2,1)S(1)}, bf16[64,1024]{1,0:T(8,128)(2,1)S(1)}, u32[]{:S(2)}, u32[]{:S(2)}) collective-permute-start(bf16[64,1024]{1,0:T(8,128)(2,1)S(1)} %collective-permute-done.35.refs_9_), channel_id=1, source_target_pairs={{0,1},{1,0},{2,3},{3,2},{4,5},{5,4},{6,7},{7,6},{8,9},{9,8},{10,11... | collective-permute-start | bytes 393224 | tf_op jit(solution)/shard_map/ppermute | solution.py:50
  126.2 5.6 %collective-permute-start.26 = (bf16[64,1024]{1,0:T(8,128)(2,1)S(1)}, bf16[64,1024]{1,0:T(8,128)(2,1)S(1)}, u32[]{:S(2)}, u32[]{:S(2)}) collective-permute-start(bf16[64,1024]{1,0:T(8,128)(2,1)S(1)} %collective-permute-done.23.refs_2_), channel_id=1, source_target_pairs={{0,7},{1,2},{2,1},{3,4},{4,3},{5,6},{6,5},{7,0},{8,15},{9,10},{10,... | collective-permute-start | bytes 393224 | tf_op jit(solution)/shard_map/ppermute | solution.py:47
  128.0 4.2 %collective-permute-start.40 = (bf16[64,1024]{1,0:T(8,128)(2,1)S(1)}, bf16[64,1024]{1,0:T(8,128)(2,1)S(1)}, u32[]{:S(2)}, u32[]{:S(2)}) collective-permute-start(bf16[64,1024]{1,0:T(8,128)(2,1)S(1)} %collective-permute-done.37.refs_10_), channel_id=1, source_target_pairs={{0,1},{1,0},{2,3},{3,2},{4,5},{5,4},{6,7},{7,6},{8,9},{9,8},{10,11... | collective-permute-start | bytes 393224 | tf_op jit(solution)/shard_map/ppermute | solution.py:47
  129.3 5.0 %collective-permute-start.25 = (bf16[64,1024]{1,0:T(8,128)(2,1)S(1)}, bf16[64,1024]{1,0:T(8,128)(2,1)S(1)}, u32[]{:S(2)}, u32[]{:S(2)}) collective-permute-start(bf16[64,1024]{1,0:T(8,128)(2,1)S(1)} %collective-permute-done.24.refs_6_), channel_id=1, source_target_pairs={{0,1},{1,0},{2,3},{3,2},{4,5},{5,4},{6,7},{7,6},{8,9},{9,8},{10,11... | collective-permute-start | bytes 393224 | tf_op jit(solution)/shard_map/ppermute | solution.py:50
  129.9 6.4 %collective-permute-start.39 = (bf16[64,1024]{1,0:T(8,128)(2,1)S(1)}, bf16[64,1024]{1,0:T(8,128)(2,1)S(1)}, u32[]{:S(2)}, u32[]{:S(2)}) collective-permute-start(bf16[64,1024]{1,0:T(8,128)(2,1)S(1)} %collective-permute-done.38.refs_14_), channel_id=1, source_target_pairs={{0,7},{1,2},{2,1},{3,4},{4,3},{5,6},{6,5},{7,0},{8,15},{9,10},{10,... | collective-permute-start | bytes 393224 | tf_op jit(solution)/shard_map/ppermute | solution.py:50
  131.8 5.5 %collective-permute-start.27 = (bf16[64,1024]{1,0:T(8,128)(2,1)S(1)}, bf16[64,1024]{1,0:T(8,128)(2,1)S(1)}, u32[]{:S(2)}, u32[]{:S(2)}) collective-permute-start(bf16[64,1024]{1,0:T(8,128)(2,1)S(1)} %collective-permute-done.26.refs_5_), channel_id=1, source_target_pairs={{0,1},{1,0},{2,3},{3,2},{4,5},{5,4},{6,7},{7,6},{8,9},{9,8},{10,11... | collective-permute-start | bytes 393224 | tf_op jit(solution)/shard_map/ppermute | solution.py:47
  132.2 5.6 %collective-permute-start.41 = (bf16[64,1024]{1,0:T(8,128)(2,1)S(1)}, bf16[64,1024]{1,0:T(8,128)(2,1)S(1)}, u32[]{:S(2)}, u32[]{:S(2)}) collective-permute-start(bf16[64,1024]{1,0:T(8,128)(2,1)S(1)} %collective-permute-done.40.refs_13_), channel_id=1, source_target_pairs={{0,7},{1,2},{2,1},{3,4},{4,3},{5,6},{6,5},{7,0},{8,15},{9,10},{10,... | collective-permute-start | bytes 393224 | tf_op jit(solution)/shard_map/ppermute | solution.py:47
  140.3 24.9 %copy-start.5 = (bf16[1024,512]{1,0:T(8,128)(2,1)S(1)}, bf16[1024,512]{1,0:T(8,128)(2,1)}, u32[]{:S(2)}) copy-start(bf16[1024,512]{1,0:T(8,128)(2,1)} %refs_8_.1) | copy-start | bytes 3145732
  140.3 38.2 %all-to-all-start.1 = ((bf16[16,64,512]{2,1,0:T(8,128)(2,1)}), bf16[16,64,512]{2,1,0:T(8,128)(2,1)S(1)}, u32[]{:S(2)}, u32[]{:S(2)}) async-start(bf16[16,64,512]{2,1,0:T(8,128)(2,1)} %bitcast.7), calls=%async_computation.1 | async-start | bytes 2097152 | tf_op jit(solution)/shard_map/all_to_all | solution.py:178
  150.5 28.1 %copy-start.11 = (pred[128,1024]{1,0:T(32,128)(4,1)S(1)}, pred[128,1024]{1,0:T(32,128)(4,1)}, u32[]{:S(2)}) copy-start(pred[128,1024]{1,0:T(32,128)(4,1)} %copy-done.10) | copy-start | bytes 393220
  150.5 4.1 %collective-permute-start.8 = (bf16[16,1024]{1,0:T(8,128)(2,1)S(1)}, bf16[16,1024]{1,0:T(8,128)(2,1)S(1)}, u32[]{:S(2)}, u32[]{:S(2)}) collective-permute-start(bf16[16,1024]{1,0:T(8,128)(2,1)S(1)} %fusion.13.refs_0_), channel_id=1, source_target_pairs={{0,7},{1,2},{2,1},{3,4},{4,3},{5,6},{6,5},{7,0},{8,15},{9,10},{10,... | collective-permute-start | bytes 98312 | tf_op jit(solution)/shard_map/ppermute | solution.py:47
  152.5 3.1 %collective-permute-start.7 = (bf16[16,1024]{1,0:T(8,128)(2,1)S(1)}, bf16[16,1024]{1,0:T(8,128)(2,1)S(1)}, u32[]{:S(2)}, u32[]{:S(2)}) collective-permute-start(bf16[16,1024]{1,0:T(8,128)(2,1)S(1)} %fusion.13.refs_0_), channel_id=1, source_target_pairs={{0,1},{1,0},{2,3},{3,2},{4,5},{5,4},{6,7},{7,6},{8,9},{9,8},{10,11... | collective-permute-start | bytes 98312 | tf_op jit(solution)/shard_map/ppermute | solution.py:50
  154.6 3.1 %collective-permute-start.9 = (bf16[16,1024]{1,0:T(8,128)(2,1)S(1)}, bf16[16,1024]{1,0:T(8,128)(2,1)S(1)}, u32[]{:S(2)}, u32[]{:S(2)}) collective-permute-start(bf16[16,1024]{1,0:T(8,128)(2,1)S(1)} %collective-permute-done.8.refs_7_), channel_id=1, source_target_pairs={{0,1},{1,0},{2,3},{3,2},{4,5},{5,4},{6,7},{7,6},{8,9},{9,8},{10,11... | collective-permute-start | bytes 98312 | tf_op jit(solution)/shard_map/ppermute | solution.py:47
  155.5 4.3 %collective-permute-start.10 = (bf16[16,1024]{1,0:T(8,128)(2,1)S(1)}, bf16[16,1024]{1,0:T(8,128)(2,1)S(1)}, u32[]{:S(2)}, u32[]{:S(2)}) collective-permute-start(bf16[16,1024]{1,0:T(8,128)(2,1)S(1)} %collective-permute-done.7.refs_1_), channel_id=1, source_target_pairs={{0,7},{1,2},{2,1},{3,4},{4,3},{5,6},{6,5},{7,0},{8,15},{9,10},{10,... | collective-permute-start | bytes 98312 | tf_op jit(solution)/shard_map/ppermute | solution.py:50
  157.7 4.5 %collective-permute-start.12 = (bf16[16,1024]{1,0:T(8,128)(2,1)S(1)}, bf16[16,1024]{1,0:T(8,128)(2,1)S(1)}, u32[]{:S(2)}, u32[]{:S(2)}) collective-permute-start(bf16[16,1024]{1,0:T(8,128)(2,1)S(1)} %collective-permute-done.9.refs_2_), channel_id=1, source_target_pairs={{0,7},{1,2},{2,1},{3,4},{4,3},{5,6},{6,5},{7,0},{8,15},{9,10},{10,... | collective-permute-start | bytes 98312 | tf_op jit(solution)/shard_map/ppermute | solution.py:47
  159.8 3.1 %collective-permute-start.11 = (bf16[16,1024]{1,0:T(8,128)(2,1)S(1)}, bf16[16,1024]{1,0:T(8,128)(2,1)S(1)}, u32[]{:S(2)}, u32[]{:S(2)}) collective-permute-start(bf16[16,1024]{1,0:T(8,128)(2,1)S(1)} %collective-permute-done.10.refs_6_), channel_id=1, source_target_pairs={{0,1},{1,0},{2,3},{3,2},{4,5},{5,4},{6,7},{7,6},{8,9},{9,8},{10,11... | collective-permute-start | bytes 98312 | tf_op jit(solution)/shard_map/ppermute | solution.py:50
  162.2 3.1 %collective-permute-start.13 = (bf16[16,1024]{1,0:T(8,128)(2,1)S(1)}, bf16[16,1024]{1,0:T(8,128)(2,1)S(1)}, u32[]{:S(2)}, u32[]{:S(2)}) collective-permute-start(bf16[16,1024]{1,0:T(8,128)(2,1)S(1)} %collective-permute-done.12.refs_5_), channel_id=1, source_target_pairs={{0,1},{1,0},{2,3},{3,2},{4,5},{5,4},{6,7},{7,6},{8,9},{9,8},{10,11... | collective-permute-start | bytes 98312 | tf_op jit(solution)/shard_map/ppermute | solution.py:47
  (11 other events, 76.3 us)

commit v6 on v5

--- a/solution.py
+++ b/solution.py
@@ -98,36 +98,36 @@
     )(me, gain, rows, gate, up)
 
 
-def lower_down(me, streams, matrix, kind):
-    size = len(streams[0][0])
-    count, units = streams[0][0][0].shape
-    part = size * count
-    height = part * len(streams)
+def lower_down(me, blocks, flip, matrix, kind, above=()):
+    size = len(blocks)
+    count, units = blocks[0].shape
+    height = size * count
     width = matrix.shape[1]
+    first = sum(v.shape[0] for v in above)
 
     def body(me_ref, *refs):
-        ins, (matrix_ref, out_ref, rows_ref) = refs[:-3], refs[-3:]
-        for i, (_, flip) in enumerate(streams):
-            for d in range(size):
-                at = pl.multiple_of(i * part + block_row(me_ref[0], d, size, count, flip), 16)
-                rows_ref[pl.ds(at, count), :] = ins[i * size + d][...]
+        ins, matrix_ref, above_refs, (out_ref, rows_ref) = refs[:size], refs[size], refs[size + 1 : -2], refs[-2:]
+        for d in range(size):
+            rows_ref[pl.ds(block_row(me_ref[0], d, size, count, flip), count), :] = ins[d][...]
+        for ref in above_refs:
+            out_ref[:first, :] = ref[...]
 
         def columns(n, _):
             at = pl.multiple_of(n * TILE, TILE)
-            out_ref[:, pl.ds(at, TILE)] = dot(rows_ref[...], matrix_ref[:, pl.ds(at, TILE)]).astype(kind)
+            out_ref[first:, pl.ds(at, TILE)] = dot(rows_ref[...], matrix_ref[:, pl.ds(at, TILE)]).astype(kind)
             return 0
 
         lax.fori_loop(0, width // TILE, columns, 0)
 
     return pl.pallas_call(
         body,
-        out_shape=jax.ShapeDtypeStruct((height, width), kind),
-        in_specs=[IN_SMEM] + [IN_VMEM] * (size * len(streams) + 1),
+        out_shape=jax.ShapeDtypeStruct((first + height, width), kind),
+        in_specs=[IN_SMEM] + [IN_VMEM] * (size + 1 + len(above)),
         out_specs=IN_VMEM,
         scratch_shapes=[pltpu.VMEM((height, units), bf16)],
-        compiler_params=pltpu.CompilerParams(vmem_limit_bytes=14 << 20),
+        compiler_params=pltpu.CompilerParams(vmem_limit_bytes=12 << 20),
         name="lower_down",
-    )(me, *[v for blocks, _ in streams for v in blocks], matrix)
+    )(me, *blocks, matrix, *above)
 
 
 def layer(
@@ -198,11 +198,12 @@
     total_a = reduce_scatter(pieces_a, tp, False, "tp")
     total_b = reduce_scatter(pieces_b, tp, True, "tp")
     blocks_a = all_gather(hidden_of(total_a), tp, False, "tp")
-    blocks_b = all_gather(hidden_of(total_b), tp, True, "tp")
-    down = lower_down(me, [(blocks_a, False), (blocks_b, True)], down_matrix, bf16)
+    blocks_b = all_gather(hidden_of(total_b), tp, False, "tp")
+    down_a = lower_down(me, blocks_a, False, down_matrix, bf16)
+    down = lower_down(me, blocks_b, False, down_matrix, bf16, above=(down_a,))
     came = swapped(down)
     blocks_s = all_gather(hidden_s, tp, False, "tp")
-    shared_out = lower_down(me, [(blocks_s, False)], shared_down, f32)
+    shared_out = lower_down(me, blocks_s, False, shared_down, f32)
     mixture = shared_out + dot(high, came) + dot(low, came)
 
     square_sum = jnp.sum(mixture * mixture, axis=-1, keepdims=True)

time: 191 us -> 193 us (1.010)
  waiting for transfers between devices: 88.8 us -> 100 us
  starting transfers between devices: 71.8 us -> 61.7 us
    ppermute x12, waiting for transfers between devices: 11.8 us -> 23.3 us  [all_gather(): x = lax.ppermute(x, axis, two if d % 2 else one)]
    ppermute x9, waiting for transfers between devices: 11.1 us -> 18.3 us  [reduce_scatter(): y = lax.ppermute(y_next, axis, one if (half - d) % 2 else two)]
    ppermute x3, waiting for transfers between devices: 8.56 us -> 2.39 us  [reduce_scatter(): x = lax.ppermute(piece[half], axis, one)]
    ppermute x9, starting transfers between devices: 8.25 us -> 4.54 us  [all_gather(): y = lax.ppermute(y, axis, one if d % 2 else two)]
    ppermute x9, starting transfers between devices: 7.11 us -> 4.07 us  [reduce_scatter(): x = lax.ppermute(x_next, axis, two if (half - d) % 2 else one)]
    ppermute x9, waiting for transfers between devices: 5.68 us -> 2.99 us  [all_gather(): y = lax.ppermute(y, axis, one if d % 2 else two)]
    ppermute x3, starting transfers between devices: 4.98 us -> 2.3 us  [reduce_scatter(): x = lax.ppermute(piece[half], axis, one)]
    all_to_all x2, waiting for transfers between devices: 24.7 us -> 26.7 us  [swapped(): lax.all_to_all(rows.reshape(experts, capacity, width), 'ep', 0, 0, tiled=...]
  transfers between devices with their start and end apart: 44 -> 44, of which waited for: 31 -> 32; matrix products, arithmetic and copies ran while one was open for 2% -> 3% of each run, Pallas kernels for 1% -> 2%
where the time goes in v6:
time: 193 us; the launch traced here: 192 us
  waiting for transfers between devices  100 us (52%)
  starting transfers between devices  61.7 us (32%)
  Pallas kernels  9.25 us (5%)
  blocking collectives  9.02 us (5%)
  other arithmetic  4.46 us (2%)
  local copies, waits for them, and re-layouts  4.17 us (2%)
  matrix products  2.89 us (1%)
    all_to_all x2, starting transfers between devices, swapped(): lax.all_to_all(rows.reshape(experts, capacity, width), 'ep', 0, 0, tiled=...  31.3 us
    all_to_all x2, waiting for transfers between devices, swapped(): lax.all_to_all(rows.reshape(experts, capacity, width), 'ep', 0, 0, tiled=...  26.7 us
    ppermute x9, waiting for transfers between devices, reduce_scatter(): x = lax.ppermute(x_next, axis, two if (half - d) % 2 else one)  26.6 us
    ppermute x12, waiting for transfers between devices, all_gather(): x = lax.ppermute(x, axis, two if d % 2 else one)  23.3 us
    ppermute x9, waiting for transfers between devices, reduce_scatter(): y = lax.ppermute(y_next, axis, one if (half - d) % 2 else two)  18.3 us
    ppermute x9, starting transfers between devices, reduce_scatter(): y = lax.ppermute(y_next, axis, one if (half - d) % 2 else two)  10.3 us
    ppermute x12, starting transfers between devices, all_gather(): x = lax.ppermute(x, axis, two if d % 2 else one)  9.16 us
    all_to_all x1, blocking collectives, layer(): square_sum = lax.all_to_all(copies, 'tp', 0, 0, tiled=True).sum(axis=0)  9.02 us
  transfers between devices with their start and end apart: 44, of which 32 were waited for; matrix products, arithmetic and copies ran while one was open for 3% of the time, Pallas kernels for 2%

profile of v6, /device:TPU:513, one launch (start us, length us, event | category | flops | bytes accessed | tf_op | source)
XLA Modules:
  0.0 192.2 jit_solution(15664464306116059522)
XLA Ops:
  0.8 1.2 copy-done.3
  2.0 1.2 copy-done.4
  4.1 1.7 project.3
  5.9 2.2 %collective-permute-start = (bf16[16,2176]{1,0:T(8,128)(2,1)}, bf16[16,2176]{1,0:T(8,128)(2,1)}, u32[]{:S(2)}, u32[]{:S(2)}) collective-permute-start(bf16[16,2176]{1,0:T(8,128)(2,1)} %get-tuple-element.35), channel_id=1, source_target_pairs={{0,1},{1,0},{2,3},{3,2},{4,5},{5,4},{6,7},{7,6},{8,9},{9,8},{10,11... | collective-permute-start | bytes 208904 | tf_op jit(solution)/shard_map/ppermute | solution.py:30
  8.5 1.5 convolution_convert_fusion
  10.0 23.8 %all-to-all-start = ((bf16[16,64,512]{2,1,0:T(8,128)(2,1)}), bf16[16,64,512]{2,1,0:T(8,128)(2,1)S(1)}, u32[]{:S(2)}, u32[]{:S(2)}) async-start(bf16[16,64,512]{2,1,0:T(8,128)(2,1)} %bitcast.1), calls=%async_computation | async-start | bytes 2097152 | tf_op jit(solution)/shard_map/all_to_all | solution.py:178
  36.0 2.8 %collective-permute-start.5 = (bf16[16,2176]{1,0:T(8,128)(2,1)S(1)}, bf16[16,2176]{1,0:T(8,128)(2,1)S(1)}, u32[]{:S(2)}, u32[]{:S(2)}) collective-permute-start(bf16[16,2176]{1,0:T(8,128)(2,1)S(1)} %add_convert_fusion.11), channel_id=1, source_target_pairs={{0,7},{1,2},{2,1},{3,4},{4,3},{5,6},{6,5},{7,0},{8,15},{9,10},{10,... | collective-permute-start | bytes 208904 | tf_op jit(solution)/shard_map/ppermute | solution.py:37
  39.9 1.6 collective-permute-done.5
  41.6 1.7 collective-permute-done.2
  43.7 1.3 collective-permute-done.6
  45.1 3.0 %collective-permute-done.3 = bf16[16,2176]{1,0:T(8,128)(2,1)S(1)} collective-permute-done((bf16[16,2176]{1,0:T(8,128)(2,1)S(1)}, bf16[16,2176]{1,0:T(8,128)(2,1)S(1)}, u32[]{:S(2)}, u32[]{:S(2)}) %collective-permute-start.3) | collective-permute-done | bytes 69664 | tf_op jit(solution)/shard_map/ppermute | solution.py:36
  48.4 13.6 %all-to-all-done = bf16[16,64,512]{2,1,0:T(8,128)(2,1)S(1)} async-done(((bf16[16,64,512]{2,1,0:T(8,128)(2,1)}), bf16[16,64,512]{2,1,0:T(8,128)(2,1)S(1)}, u32[]{:S(2)}, u32[]{:S(2)}) %all-to-all-start) | async-done | bytes 1048608 | tf_op jit(solution)/shard_map/all_to_all | solution.py:178
  62.0 2.0 %project.5 = (bf16[64,2176]{1,0:T(8,128)(2,1)S(1)}, bf16[64,2176]{1,0:T(8,128)(2,1)S(1)}, bf16[64,2176]{1,0:T(8,128)(2,1)S(1)}, bf16[64,2176]{1,0:T(8,128)(2,1)S...) custom-call(s32[1]{0:T(128)} %bitcast.me_ref, ...), custom_call_target="tpu_custom_call" | custom-call | tf_op jit(solution)/shard_map/project/pallas_call | solution.py:90
  64.2 2.0 %project.4 = (bf16[64,2176]{1,0:T(8,128)(2,1)S(1)}, bf16[64,2176]{1,0:T(8,128)(2,1)S(1)}, bf16[64,2176]{1,0:T(8,128)(2,1)S(1)}, bf16[64,2176]{1,0:T(8,128)(2,1)S...) custom-call(s32[1]{0:T(128)} %bitcast.me_ref, ...), custom_call_target="tpu_custom_call" | custom-call | tf_op jit(solution)/shard_map/project/pallas_call | solution.py:90
  66.2 1.6 collective-permute-start.32
  67.8 2.7 %collective-permute-start.18 = (bf16[64,2176]{1,0:T(8,128)(2,1)S(1)}, bf16[64,2176]{1,0:T(8,128)(2,1)S(1)}, u32[]{:S(2)}, u32[]{:S(2)}) collective-permute-start(bf16[64,2176]{1,0:T(8,128)(2,1)S(1)} %get-tuple-element.48), channel_id=1, source_target_pairs={{0,7},{1,2},{2,1},{3,4},{4,3},{5,6},{6,5},{7,0},{8,15},{9,10},{10,... | collective-permute-start | bytes 835592 | tf_op jit(solution)/shard_map/ppermute | solution.py:37
  70.4 2.4 %collective-permute-done.28 = bf16[64,2176]{1,0:T(8,128)(2,1)S(1)} collective-permute-done((bf16[64,2176]{1,0:T(8,128)(2,1)S(1)}, bf16[64,2176]{1,0:T(8,128)(2,1)S(1)}, u32[]{:S(2)}, u32[]{:S(2)}) %collective-permute-start.28) | collective-permute-done | bytes 278560 | tf_op jit(solution)/shard_map/ppermute | solution.py:30
  73.0 5.0 %collective-permute-done.32 = bf16[64,2176]{1,0:T(8,128)(2,1)S(1)} collective-permute-done((bf16[64,2176]{1,0:T(8,128)(2,1)S(1)}, bf16[64,2176]{1,0:T(8,128)(2,1)S(1)}, u32[]{:S(2)}, u32[]{:S(2)}) %collective-permute-start.32) | collective-permute-done | bytes 278560 | tf_op jit(solution)/shard_map/ppermute | solution.py:37
  78.5 5.1 %collective-permute-done.18 = bf16[64,2176]{1,0:T(8,128)(2,1)S(1)} collective-permute-done((bf16[64,2176]{1,0:T(8,128)(2,1)S(1)}, bf16[64,2176]{1,0:T(8,128)(2,1)S(1)}, u32[]{:S(2)}, u32[]{:S(2)}) %collective-permute-start.18) | collective-permute-done | bytes 278560 | tf_op jit(solution)/shard_map/ppermute | solution.py:37
  83.8 5.7 %collective-permute-done.29 = bf16[64,2176]{1,0:T(8,128)(2,1)S(1)} collective-permute-done((bf16[64,2176]{1,0:T(8,128)(2,1)S(1)}, bf16[64,2176]{1,0:T(8,128)(2,1)S(1)}, u32[]{:S(2)}, u32[]{:S(2)}) %collective-permute-start.29) | collective-permute-done | bytes 278560 | tf_op jit(solution)/shard_map/ppermute | solution.py:36
  90.0 5.1 %collective-permute-done.33 = bf16[64,2176]{1,0:T(8,128)(2,1)S(1)} collective-permute-done((bf16[64,2176]{1,0:T(8,128)(2,1)S(1)}, bf16[64,2176]{1,0:T(8,128)(2,1)S(1)}, u32[]{:S(2)}, u32[]{:S(2)}) %collective-permute-start.33) | collective-permute-done | bytes 278560 | tf_op jit(solution)/shard_map/ppermute | solution.py:37
  95.7 2.8 %collective-permute-start.20 = (bf16[64,2176]{1,0:T(8,128)(2,1)S(1)}, bf16[64,2176]{1,0:T(8,128)(2,1)S(1)}, u32[]{:S(2)}, u32[]{:S(2)}) collective-permute-start(bf16[64,2176]{1,0:T(8,128)(2,1)S(1)} %add_convert_fusion.5), channel_id=1, source_target_pairs={{0,7},{1,2},{2,1},{3,4},{4,3},{5,6},{6,5},{7,0},{8,15},{9,10},{10,... | collective-permute-start | bytes 835592 | tf_op jit(solution)/shard_map/ppermute | solution.py:37
  99.0 2.5 %collective-permute-start.31 = (bf16[64,2176]{1,0:T(8,128)(2,1)S(1)}, bf16[64,2176]{1,0:T(8,128)(2,1)S(1)}, u32[]{:S(2)}, u32[]{:S(2)}) collective-permute-start(bf16[64,2176]{1,0:T(8,128)(2,1)S(1)} %add_convert_fusion.2), channel_id=1, source_target_pairs={{0,7},{1,2},{2,1},{3,4},{4,3},{5,6},{6,5},{7,0},{8,15},{9,10},{10,... | collective-permute-start | bytes 835592 | tf_op jit(solution)/shard_map/ppermute | solution.py:36
  101.5 3.0 %collective-permute-done.16 = bf16[64,2176]{1,0:T(8,128)(2,1)S(1)} collective-permute-done((bf16[64,2176]{1,0:T(8,128)(2,1)S(1)}, bf16[64,2176]{1,0:T(8,128)(2,1)S(1)}, u32[]{:S(2)}, u32[]{:S(2)}) %collective-permute-start.16) | collective-permute-done | bytes 278560 | tf_op jit(solution)/shard_map/ppermute | solution.py:36
  104.9 11.6 %collective-permute-done.31 = bf16[64,2176]{1,0:T(8,128)(2,1)S(1)} collective-permute-done((bf16[64,2176]{1,0:T(8,128)(2,1)S(1)}, bf16[64,2176]{1,0:T(8,128)(2,1)S(1)}, u32[]{:S(2)}, u32[]{:S(2)}) %collective-permute-start.31) | collective-permute-done | bytes 278560 | tf_op jit(solution)/shard_map/ppermute | solution.py:36
  117.7 2.5 %collective-permute-start.22 = (bf16[64,1024]{1,0:T(8,128)(2,1)S(1)}, bf16[64,1024]{1,0:T(8,128)(2,1)S(1)}, u32[]{:S(2)}, u32[]{:S(2)}) collective-permute-start(bf16[64,1024]{1,0:T(8,128)(2,1)S(1)} %fusion.9.refs_0_), channel_id=1, source_target_pairs={{0,7},{1,2},{2,1},{3,4},{4,3},{5,6},{6,5},{7,0},{8,15},{9,10},{10,... | collective-permute-start | bytes 393224 | tf_op jit(solution)/shard_map/ppermute | solution.py:47
  120.2 1.8 collective-permute-done.36.refs_7_
  122.1 1.5 collective-permute-start.21
  123.5 1.3 collective-permute-done.22.refs_7_
  125.3 1.9 collective-permute-done.37.refs_2_
  127.7 1.5 collective-permute-done.21.refs_1_
  129.2 1.3 collective-permute-start.24
  130.5 1.5 collective-permute-done.23.refs_2_
  132.0 1.3 collective-permute-start.26
  133.4 1.5 collective-permute-start.41
  135.3 3.1 %collective-permute-done.26.refs_5_ = bf16[64,1024]{1,0:T(8,128)(2,1)S(1)} collective-permute-done((bf16[64,1024]{1,0:T(8,128)(2,1)S(1)}, bf16[64,1024]{1,0:T(8,128)(2,1)S(1)}, u32[]{:S(2)}, u32[]{:S(2)}) %collective-permute-start.26) | collective-permute-done | bytes 131104 | tf_op jit(solution)/shard_map/ppermute | solution.py:47
  140.5 3.3 %collective-permute-done.27.refs_4_ = bf16[64,1024]{1,0:T(8,128)(2,1)S(1)} collective-permute-done((bf16[64,1024]{1,0:T(8,128)(2,1)S(1)}, bf16[64,1024]{1,0:T(8,128)(2,1)S(1)}, u32[]{:S(2)}, u32[]{:S(2)}) %collective-permute-start.27) | collective-permute-done | bytes 131104 | tf_op jit(solution)/shard_map/ppermute | solution.py:47
  143.8 2.0 %lower_down.5 = bf16[1024,512]{1,0:T(8,128)(2,1)} custom-call(s32[1]{0:T(128)} %bitcast.me_ref, bf16[64,1024]{1,0:T(8,128)(2,1)S(1)} %fusion.9.refs_0_, bf16[64,1024]{1,0:T(8,128)(2,1)S(1)} %collective-permute-done.21.refs_1_, bf16[64,1024]{1,0:T(8,128)(2,1)S(1)} %collective-permute-done.23.refs_2_, bf16[64,1024]{1,0:T(8,128)(2,1)S(1)} %collective-permute-done.25.refs_3_, ...), custom_call_target="tpu_custom_call" | custom-call | tf_op jit(solution)/shard_map/lower_down/pallas_call | solution.py:122
  145.8 7.5 %all-to-all-start.1 = ((bf16[16,64,512]{2,1,0:T(8,128)(2,1)}), bf16[16,64,512]{2,1,0:T(8,128)(2,1)S(1)}, u32[]{:S(2)}, u32[]{:S(2)}) async-start(bf16[16,64,512]{2,1,0:T(8,128)(2,1)} %bitcast.7), calls=%async_computation.1 | async-start | bytes 2097152 | tf_op jit(solution)/shard_map/all_to_all | solution.py:178
  153.3 1.5 collective-permute-start.8
  154.8 2.6 %collective-permute-done.8.refs_7_ = bf16[16,1024]{1,0:T(8,128)(2,1)S(1)} collective-permute-done((bf16[16,1024]{1,0:T(8,128)(2,1)S(1)}, bf16[16,1024]{1,0:T(8,128)(2,1)S(1)}, u32[]{:S(2)}, u32[]{:S(2)}) %collective-permute-start.8) | collective-permute-done | bytes 32800 | tf_op jit(solution)/shard_map/ppermute | solution.py:47
  157.5 1.3 collective-permute-start.10
  158.8 1.6 collective-permute-done.9.refs_2_
  160.4 1.4 collective-permute-start.12
  161.9 2.8 %collective-permute-done.12.refs_5_ = bf16[16,1024]{1,0:T(8,128)(2,1)S(1)} collective-permute-done((bf16[16,1024]{1,0:T(8,128)(2,1)S(1)}, bf16[16,1024]{1,0:T(8,128)(2,1)S(1)}, u32[]{:S(2)}, u32[]{:S(2)}) %collective-permute-start.12) | collective-permute-done | bytes 32800 | tf_op jit(solution)/shard_map/ppermute | solution.py:47
  164.9 2.9 %collective-permute-done.13.refs_4_ = bf16[16,1024]{1,0:T(8,128)(2,1)S(1)} collective-permute-done((bf16[16,1024]{1,0:T(8,128)(2,1)S(1)}, bf16[16,1024]{1,0:T(8,128)(2,1)S(1)}, u32[]{:S(2)}, u32[]{:S(2)}) %collective-permute-start.13) | collective-permute-done | bytes 32800 | tf_op jit(solution)/shard_map/ppermute | solution.py:47
  168.3 13.1 %all-to-all-done.1 = bf16[16,64,512]{2,1,0:T(8,128)(2,1)S(1)} async-done(((bf16[16,64,512]{2,1,0:T(8,128)(2,1)}), bf16[16,64,512]{2,1,0:T(8,128)(2,1)S(1)}, u32[]{:S(2)}, u32[]{:S(2)}) %all-to-all-start.1) | async-done | bytes 1048608 | tf_op jit(solution)/shard_map/all_to_all | solution.py:178
  182.4 9.0 %all_to_all.15 = f32[8,128,1]{1,2,0:T(1,128)S(1)} all-to-all(f32[8,128,1]{1,2,0:T(1,128)S(1)} %broadcast_in_dim.34), channel_id=1, replica_groups=mesh['grp'=2,'ep'=16,'tp'=8] {'tp'}, dimensions={0} | all-to-all | bytes 8192 | tf_op jit(solution)/shard_map/all_to_all | solution.py:211
  (113 shorter events, 16.5 us)
Async XLA Ops:
  5.9 28.0 %collective-permute-start = (bf16[16,2176]{1,0:T(8,128)(2,1)}, bf16[16,2176]{1,0:T(8,128)(2,1)}, u32[]{:S(2)}, u32[]{:S(2)}) collective-permute-start(bf16[16,2176]{1,0:T(8,128)(2,1)} %get-tuple-element.35), channel_id=1, source_target_pairs={{0,1},{1,0},{2,3},{3,2},{4,5},{5,4},{6,7},{7,6},{8,9},{9,8},{10,11... | collective-permute-start | bytes 208904 | tf_op jit(solution)/shard_map/ppermute | solution.py:30
  8.0 27.0 %collective-permute-start.4 = (bf16[16,2176]{1,0:T(8,128)(2,1)}, bf16[16,2176]{1,0:T(8,128)(2,1)}, u32[]{:S(2)}, u32[]{:S(2)}) collective-permute-start(bf16[16,2176]{1,0:T(8,128)(2,1)} %get-tuple-element.38), channel_id=1, source_target_pairs={{0,1},{1,0},{2,3},{3,2},{4,5},{5,4},{6,7},{7,6},{8,9},{9,8},{10,11... | collective-permute-start | bytes 208904 | tf_op jit(solution)/shard_map/ppermute | solution.py:37
  10.0 52.0 %copy-start.1 = (bf16[1,512,1024]{2,1,0:T(8,128)(2,1)S(1)}, bf16[1,512,1024]{2,1,0:T(8,128)(2,1)}, u32[]{:S(2)}) copy-start(bf16[1,512,1024]{2,1,0:T(8,128)(2,1)} %param.16) | copy-start | bytes 3145732
  10.0 52.0 %all-to-all-start = ((bf16[16,64,512]{2,1,0:T(8,128)(2,1)}), bf16[16,64,512]{2,1,0:T(8,128)(2,1)S(1)}, u32[]{:S(2)}, u32[]{:S(2)}) async-start(bf16[16,64,512]{2,1,0:T(8,128)(2,1)} %bitcast.1), calls=%async_computation | async-start | bytes 2097152 | tf_op jit(solution)/shard_map/all_to_all | solution.py:178
  33.9 28.1 %copy-start = (bf16[1,512,1024]{2,1,0:T(8,128)(2,1)S(1)}, bf16[1,512,1024]{2,1,0:T(8,128)(2,1)}, u32[]{:S(2)}) copy-start(bf16[1,512,1024]{2,1,0:T(8,128)(2,1)} %param.15) | copy-start | bytes 3145732
  34.9 4.8 %collective-permute-start.1 = (bf16[16,2176]{1,0:T(8,128)(2,1)S(1)}, bf16[16,2176]{1,0:T(8,128)(2,1)S(1)}, u32[]{:S(2)}, u32[]{:S(2)}) collective-permute-start(bf16[16,2176]{1,0:T(8,128)(2,1)S(1)} %add_convert_fusion.14), channel_id=1, source_target_pairs={{0,7},{1,2},{2,1},{3,4},{4,3},{5,6},{6,5},{7,0},{8,15},{9,10},{10,... | collective-permute-start | bytes 208904 | tf_op jit(solution)/shard_map/ppermute | solution.py:36
  36.0 5.5 %collective-permute-start.5 = (bf16[16,2176]{1,0:T(8,128)(2,1)S(1)}, bf16[16,2176]{1,0:T(8,128)(2,1)S(1)}, u32[]{:S(2)}, u32[]{:S(2)}) collective-permute-start(bf16[16,2176]{1,0:T(8,128)(2,1)S(1)} %add_convert_fusion.11), channel_id=1, source_target_pairs={{0,7},{1,2},{2,1},{3,4},{4,3},{5,6},{6,5},{7,0},{8,15},{9,10},{10,... | collective-permute-start | bytes 208904 | tf_op jit(solution)/shard_map/ppermute | solution.py:37
  39.7 3.6 %collective-permute-start.2 = (bf16[16,2176]{1,0:T(8,128)(2,1)S(1)}, bf16[16,2176]{1,0:T(8,128)(2,1)S(1)}, u32[]{:S(2)}, u32[]{:S(2)}) collective-permute-start(bf16[16,2176]{1,0:T(8,128)(2,1)S(1)} %add_convert_fusion.13), channel_id=1, source_target_pairs={{0,1},{1,0},{2,3},{3,2},{4,5},{5,4},{6,7},{7,6},{8,9},{9,8},{10,11... | collective-permute-start | bytes 208904 | tf_op jit(solution)/shard_map/ppermute | solution.py:36
  41.5 3.6 %collective-permute-start.6 = (bf16[16,2176]{1,0:T(8,128)(2,1)S(1)}, bf16[16,2176]{1,0:T(8,128)(2,1)S(1)}, u32[]{:S(2)}, u32[]{:S(2)}) collective-permute-start(bf16[16,2176]{1,0:T(8,128)(2,1)S(1)} %add_convert_fusion.10), channel_id=1, source_target_pairs={{0,1},{1,0},{2,3},{3,2},{4,5},{5,4},{6,7},{7,6},{8,9},{9,8},{10,11... | collective-permute-start | bytes 208904 | tf_op jit(solution)/shard_map/ppermute | solution.py:37
  43.3 4.8 %collective-permute-start.3 = (bf16[16,2176]{1,0:T(8,128)(2,1)S(1)}, bf16[16,2176]{1,0:T(8,128)(2,1)S(1)}, u32[]{:S(2)}, u32[]{:S(2)}) collective-permute-start(bf16[16,2176]{1,0:T(8,128)(2,1)S(1)} %add_convert_fusion.12), channel_id=1, source_target_pairs={{0,7},{1,2},{2,1},{3,4},{4,3},{5,6},{6,5},{7,0},{8,15},{9,10},{10,... | collective-permute-start | bytes 208904 | tf_op jit(solution)/shard_map/ppermute | solution.py:36
  64.0 8.8 %collective-permute-start.28 = (bf16[64,2176]{1,0:T(8,128)(2,1)S(1)}, bf16[64,2176]{1,0:T(8,128)(2,1)S(1)}, u32[]{:S(2)}, u32[]{:S(2)}) collective-permute-start(bf16[64,2176]{1,0:T(8,128)(2,1)S(1)} %get-tuple-element.53), channel_id=1, source_target_pairs={{0,1},{1,0},{2,3},{3,2},{4,5},{5,4},{6,7},{7,6},{8,9},{9,8},{10,11... | collective-permute-start | bytes 835592 | tf_op jit(solution)/shard_map/ppermute | solution.py:30
  66.2 11.8 %collective-permute-start.32 = (bf16[64,2176]{1,0:T(8,128)(2,1)S(1)}, bf16[64,2176]{1,0:T(8,128)(2,1)S(1)}, u32[]{:S(2)}, u32[]{:S(2)}) collective-permute-start(bf16[64,2176]{1,0:T(8,128)(2,1)S(1)} %get-tuple-element.56), channel_id=1, source_target_pairs={{0,1},{1,0},{2,3},{3,2},{4,5},{5,4},{6,7},{7,6},{8,9},{9,8},{10,11... | collective-permute-start | bytes 835592 | tf_op jit(solution)/shard_map/ppermute | solution.py:37
  67.8 10.5 %collective-permute-start.14 = (bf16[64,2176]{1,0:T(8,128)(2,1)S(1)}, bf16[64,2176]{1,0:T(8,128)(2,1)S(1)}, u32[]{:S(2)}, u32[]{:S(2)}) collective-permute-start(bf16[64,2176]{1,0:T(8,128)(2,1)S(1)} %get-tuple-element.45), channel_id=1, source_target_pairs={{0,7},{1,2},{2,1},{3,4},{4,3},{5,6},{6,5},{7,0},{8,15},{9,10},{10,... | collective-permute-start | bytes 835592 | tf_op jit(solution)/shard_map/ppermute | solution.py:30
  67.8 15.9 %collective-permute-start.18 = (bf16[64,2176]{1,0:T(8,128)(2,1)S(1)}, bf16[64,2176]{1,0:T(8,128)(2,1)S(1)}, u32[]{:S(2)}, u32[]{:S(2)}) collective-permute-start(bf16[64,2176]{1,0:T(8,128)(2,1)S(1)} %get-tuple-element.48), channel_id=1, source_target_pairs={{0,7},{1,2},{2,1},{3,4},{4,3},{5,6},{6,5},{7,0},{8,15},{9,10},{10,... | collective-permute-start | bytes 835592 | tf_op jit(solution)/shard_map/ppermute | solution.py:37
  72.9 16.7 %collective-permute-start.29 = (bf16[64,2176]{1,0:T(8,128)(2,1)S(1)}, bf16[64,2176]{1,0:T(8,128)(2,1)S(1)}, u32[]{:S(2)}, u32[]{:S(2)}) collective-permute-start(bf16[64,2176]{1,0:T(8,128)(2,1)S(1)} %add_convert_fusion.4), channel_id=1, source_target_pairs={{0,7},{1,2},{2,1},{3,4},{4,3},{5,6},{6,5},{7,0},{8,15},{9,10},{10,... | collective-permute-start | bytes 835592 | tf_op jit(solution)/shard_map/ppermute | solution.py:36
  78.1 17.0 %collective-permute-start.33 = (bf16[64,2176]{1,0:T(8,128)(2,1)S(1)}, bf16[64,2176]{1,0:T(8,128)(2,1)S(1)}, u32[]{:S(2)}, u32[]{:S(2)}) collective-permute-start(bf16[64,2176]{1,0:T(8,128)(2,1)S(1)} %add_convert_fusion.1), channel_id=1, source_target_pairs={{0,7},{1,2},{2,1},{3,4},{4,3},{5,6},{6,5},{7,0},{8,15},{9,10},{10,... | collective-permute-start | bytes 835592 | tf_op jit(solution)/shard_map/ppermute | solution.py:37
  78.3 17.0 %collective-permute-start.15 = (bf16[64,2176]{1,0:T(8,128)(2,1)S(1)}, bf16[64,2176]{1,0:T(8,128)(2,1)S(1)}, u32[]{:S(2)}, u32[]{:S(2)}) collective-permute-start(bf16[64,2176]{1,0:T(8,128)(2,1)S(1)} %add_convert_fusion.9), channel_id=1, source_target_pairs={{0,1},{1,0},{2,3},{3,2},{4,5},{5,4},{6,7},{7,6},{8,9},{9,8},{10,11... | collective-permute-start | bytes 835592 | tf_op jit(solution)/shard_map/ppermute | solution.py:36
  83.7 11.9 %collective-permute-start.19 = (bf16[64,2176]{1,0:T(8,128)(2,1)S(1)}, bf16[64,2176]{1,0:T(8,128)(2,1)S(1)}, u32[]{:S(2)}, u32[]{:S(2)}) collective-permute-start(bf16[64,2176]{1,0:T(8,128)(2,1)S(1)} %add_convert_fusion.6), channel_id=1, source_target_pairs={{0,1},{1,0},{2,3},{3,2},{4,5},{5,4},{6,7},{7,6},{8,9},{9,8},{10,11... | collective-permute-start | bytes 835592 | tf_op jit(solution)/shard_map/ppermute | solution.py:37
  89.6 9.3 %collective-permute-start.30 = (bf16[64,2176]{1,0:T(8,128)(2,1)S(1)}, bf16[64,2176]{1,0:T(8,128)(2,1)S(1)}, u32[]{:S(2)}, u32[]{:S(2)}) collective-permute-start(bf16[64,2176]{1,0:T(8,128)(2,1)S(1)} %add_convert_fusion.3), channel_id=1, source_target_pairs={{0,1},{1,0},{2,3},{3,2},{4,5},{5,4},{6,7},{7,6},{8,9},{9,8},{10,11... | collective-permute-start | bytes 835592 | tf_op jit(solution)/shard_map/ppermute | solution.py:36
  95.2 9.8 %collective-permute-start.34 = (bf16[64,2176]{1,0:T(8,128)(2,1)S(1)}, bf16[64,2176]{1,0:T(8,128)(2,1)S(1)}, u32[]{:S(2)}, u32[]{:S(2)}) collective-permute-start(bf16[64,2176]{1,0:T(8,128)(2,1)S(1)} %add_convert_fusion), channel_id=1, source_target_pairs={{0,1},{1,0},{2,3},{3,2},{4,5},{5,4},{6,7},{7,6},{8,9},{9,8},{10,11... | collective-permute-start | bytes 835592 | tf_op jit(solution)/shard_map/ppermute | solution.py:37
  95.4 9.2 %collective-permute-start.16 = (bf16[64,2176]{1,0:T(8,128)(2,1)S(1)}, bf16[64,2176]{1,0:T(8,128)(2,1)S(1)}, u32[]{:S(2)}, u32[]{:S(2)}) collective-permute-start(bf16[64,2176]{1,0:T(8,128)(2,1)S(1)} %add_convert_fusion.8), channel_id=1, source_target_pairs={{0,7},{1,2},{2,1},{3,4},{4,3},{5,6},{6,5},{7,0},{8,15},{9,10},{10,... | collective-permute-start | bytes 835592 | tf_op jit(solution)/shard_map/ppermute | solution.py:36
  95.7 21.7 %collective-permute-start.20 = (bf16[64,2176]{1,0:T(8,128)(2,1)S(1)}, bf16[64,2176]{1,0:T(8,128)(2,1)S(1)}, u32[]{:S(2)}, u32[]{:S(2)}) collective-permute-start(bf16[64,2176]{1,0:T(8,128)(2,1)S(1)} %add_convert_fusion.5), channel_id=1, source_target_pairs={{0,7},{1,2},{2,1},{3,4},{4,3},{5,6},{6,5},{7,0},{8,15},{9,10},{10,... | collective-permute-start | bytes 835592 | tf_op jit(solution)/shard_map/ppermute | solution.py:37
  99.0 17.5 %collective-permute-start.31 = (bf16[64,2176]{1,0:T(8,128)(2,1)S(1)}, bf16[64,2176]{1,0:T(8,128)(2,1)S(1)}, u32[]{:S(2)}, u32[]{:S(2)}) collective-permute-start(bf16[64,2176]{1,0:T(8,128)(2,1)S(1)} %add_convert_fusion.2), channel_id=1, source_target_pairs={{0,7},{1,2},{2,1},{3,4},{4,3},{5,6},{6,5},{7,0},{8,15},{9,10},{10,... | collective-permute-start | bytes 835592 | tf_op jit(solution)/shard_map/ppermute | solution.py:36
  104.6 12.7 %collective-permute-start.17 = (bf16[64,2176]{1,0:T(8,128)(2,1)S(1)}, bf16[64,2176]{1,0:T(8,128)(2,1)S(1)}, u32[]{:S(2)}, u32[]{:S(2)}) collective-permute-start(bf16[64,2176]{1,0:T(8,128)(2,1)S(1)} %add_convert_fusion.7), channel_id=1, source_target_pairs={{0,1},{1,0},{2,3},{3,2},{4,5},{5,4},{6,7},{7,6},{8,9},{9,8},{10,11... | collective-permute-start | bytes 835592 | tf_op jit(solution)/shard_map/ppermute | solution.py:36
  116.9 22.0 %copy-start.2 = (bf16[1,1024,512]{2,1,0:T(8,128)(2,1)S(1)}, bf16[1,1024,512]{2,1,0:T(8,128)(2,1)}, u32[]{:S(2)}) copy-start(bf16[1,1024,512]{2,1,0:T(8,128)(2,1)} %param.17) | copy-start | bytes 3145732
  116.9 5.2 %collective-permute-start.36 = (bf16[64,1024]{1,0:T(8,128)(2,1)S(1)}, bf16[64,1024]{1,0:T(8,128)(2,1)S(1)}, u32[]{:S(2)}, u32[]{:S(2)}) collective-permute-start(bf16[64,1024]{1,0:T(8,128)(2,1)S(1)} %fusion.7.refs_0_), channel_id=1, source_target_pairs={{0,7},{1,2},{2,1},{3,4},{4,3},{5,6},{6,5},{7,0},{8,15},{9,10},{10,... | collective-permute-start | bytes 393224 | tf_op jit(solution)/shard_map/ppermute | solution.py:47
  117.7 7.1 %collective-permute-start.22 = (bf16[64,1024]{1,0:T(8,128)(2,1)S(1)}, bf16[64,1024]{1,0:T(8,128)(2,1)S(1)}, u32[]{:S(2)}, u32[]{:S(2)}) collective-permute-start(bf16[64,1024]{1,0:T(8,128)(2,1)S(1)} %fusion.9.refs_0_), channel_id=1, source_target_pairs={{0,7},{1,2},{2,1},{3,4},{4,3},{5,6},{6,5},{7,0},{8,15},{9,10},{10,... | collective-permute-start | bytes 393224 | tf_op jit(solution)/shard_map/ppermute | solution.py:47
  120.2 4.6 %collective-permute-start.35 = (bf16[64,1024]{1,0:T(8,128)(2,1)S(1)}, bf16[64,1024]{1,0:T(8,128)(2,1)S(1)}, u32[]{:S(2)}, u32[]{:S(2)}) collective-permute-start(bf16[64,1024]{1,0:T(8,128)(2,1)S(1)} %fusion.7.refs_0_), channel_id=1, source_target_pairs={{0,1},{1,0},{2,3},{3,2},{4,5},{5,4},{6,7},{7,6},{8,9},{9,8},{10,11... | collective-permute-start | bytes 393224 | tf_op jit(solution)/shard_map/ppermute | solution.py:50
  122.1 5.1 %collective-permute-start.37 = (bf16[64,1024]{1,0:T(8,128)(2,1)S(1)}, bf16[64,1024]{1,0:T(8,128)(2,1)S(1)}, u32[]{:S(2)}, u32[]{:S(2)}) collective-permute-start(bf16[64,1024]{1,0:T(8,128)(2,1)S(1)} %collective-permute-done.36.refs_7_), channel_id=1, source_target_pairs={{0,1},{1,0},{2,3},{3,2},{4,5},{5,4},{6,7},{7,6},{8,9},{9,8},{10,11... | collective-permute-start | bytes 393224 | tf_op jit(solution)/shard_map/ppermute | solution.py:47
  122.1 7.2 %collective-permute-start.21 = (bf16[64,1024]{1,0:T(8,128)(2,1)S(1)}, bf16[64,1024]{1,0:T(8,128)(2,1)S(1)}, u32[]{:S(2)}, u32[]{:S(2)}) collective-permute-start(bf16[64,1024]{1,0:T(8,128)(2,1)S(1)} %fusion.9.refs_0_), channel_id=1, source_target_pairs={{0,1},{1,0},{2,3},{3,2},{4,5},{5,4},{6,7},{7,6},{8,9},{9,8},{10,11... | collective-permute-start | bytes 393224 | tf_op jit(solution)/shard_map/ppermute | solution.py:50
  124.9 7.2 %collective-permute-start.23 = (bf16[64,1024]{1,0:T(8,128)(2,1)S(1)}, bf16[64,1024]{1,0:T(8,128)(2,1)S(1)}, u32[]{:S(2)}, u32[]{:S(2)}) collective-permute-start(bf16[64,1024]{1,0:T(8,128)(2,1)S(1)} %collective-permute-done.22.refs_7_), channel_id=1, source_target_pairs={{0,1},{1,0},{2,3},{3,2},{4,5},{5,4},{6,7},{7,6},{8,9},{9,8},{10,11... | collective-permute-start | bytes 393224 | tf_op jit(solution)/shard_map/ppermute | solution.py:47
  124.9 8.5 %collective-permute-start.38 = (bf16[64,1024]{1,0:T(8,128)(2,1)S(1)}, bf16[64,1024]{1,0:T(8,128)(2,1)S(1)}, u32[]{:S(2)}, u32[]{:S(2)}) collective-permute-start(bf16[64,1024]{1,0:T(8,128)(2,1)S(1)} %collective-permute-done.35.refs_1_), channel_id=1, source_target_pairs={{0,7},{1,2},{2,1},{3,4},{4,3},{5,6},{6,5},{7,0},{8,15},{9,10},{10,... | collective-permute-start | bytes 393224 | tf_op jit(solution)/shard_map/ppermute | solution.py:50
  127.1 6.2 %collective-permute-start.40 = (bf16[64,1024]{1,0:T(8,128)(2,1)S(1)}, bf16[64,1024]{1,0:T(8,128)(2,1)S(1)}, u32[]{:S(2)}, u32[]{:S(2)}) collective-permute-start(bf16[64,1024]{1,0:T(8,128)(2,1)S(1)} %collective-permute-done.37.refs_2_), channel_id=1, source_target_pairs={{0,7},{1,2},{2,1},{3,4},{4,3},{5,6},{6,5},{7,0},{8,15},{9,10},{10,... | collective-permute-start | bytes 393224 | tf_op jit(solution)/shard_map/ppermute | solution.py:47
  129.2 6.1 %collective-permute-start.24 = (bf16[64,1024]{1,0:T(8,128)(2,1)S(1)}, bf16[64,1024]{1,0:T(8,128)(2,1)S(1)}, u32[]{:S(2)}, u32[]{:S(2)}) collective-permute-start(bf16[64,1024]{1,0:T(8,128)(2,1)S(1)} %collective-permute-done.21.refs_1_), channel_id=1, source_target_pairs={{0,7},{1,2},{2,1},{3,4},{4,3},{5,6},{6,5},{7,0},{8,15},{9,10},{10,... | collective-permute-start | bytes 393224 | tf_op jit(solution)/shard_map/ppermute | solution.py:50
  132.0 6.4 %collective-permute-start.26 = (bf16[64,1024]{1,0:T(8,128)(2,1)S(1)}, bf16[64,1024]{1,0:T(8,128)(2,1)S(1)}, u32[]{:S(2)}, u32[]{:S(2)}) collective-permute-start(bf16[64,1024]{1,0:T(8,128)(2,1)S(1)} %collective-permute-done.23.refs_2_), channel_id=1, source_target_pairs={{0,7},{1,2},{2,1},{3,4},{4,3},{5,6},{6,5},{7,0},{8,15},{9,10},{10,... | collective-permute-start | bytes 393224 | tf_op jit(solution)/shard_map/ppermute | solution.py:47
  133.3 5.1 %collective-permute-start.39 = (bf16[64,1024]{1,0:T(8,128)(2,1)S(1)}, bf16[64,1024]{1,0:T(8,128)(2,1)S(1)}, u32[]{:S(2)}, u32[]{:S(2)}) collective-permute-start(bf16[64,1024]{1,0:T(8,128)(2,1)S(1)} %collective-permute-done.38.refs_6_), channel_id=1, source_target_pairs={{0,1},{1,0},{2,3},{3,2},{4,5},{5,4},{6,7},{7,6},{8,9},{9,8},{10,11... | collective-permute-start | bytes 393224 | tf_op jit(solution)/shard_map/ppermute | solution.py:50
  133.4 5.5 %collective-permute-start.41 = (bf16[64,1024]{1,0:T(8,128)(2,1)S(1)}, bf16[64,1024]{1,0:T(8,128)(2,1)S(1)}, u32[]{:S(2)}, u32[]{:S(2)}) collective-permute-start(bf16[64,1024]{1,0:T(8,128)(2,1)S(1)} %collective-permute-done.40.refs_5_), channel_id=1, source_target_pairs={{0,1},{1,0},{2,3},{3,2},{4,5},{5,4},{6,7},{7,6},{8,9},{9,8},{10,11... | collective-permute-start | bytes 393224 | tf_op jit(solution)/shard_map/ppermute | solution.py:47
  135.3 5.2 %collective-permute-start.25 = (bf16[64,1024]{1,0:T(8,128)(2,1)S(1)}, bf16[64,1024]{1,0:T(8,128)(2,1)S(1)}, u32[]{:S(2)}, u32[]{:S(2)}) collective-permute-start(bf16[64,1024]{1,0:T(8,128)(2,1)S(1)} %collective-permute-done.24.refs_6_), channel_id=1, source_target_pairs={{0,1},{1,0},{2,3},{3,2},{4,5},{5,4},{6,7},{7,6},{8,9},{9,8},{10,11... | collective-permute-start | bytes 393224 | tf_op jit(solution)/shard_map/ppermute | solution.py:50
  138.4 5.4 %collective-permute-start.27 = (bf16[64,1024]{1,0:T(8,128)(2,1)S(1)}, bf16[64,1024]{1,0:T(8,128)(2,1)S(1)}, u32[]{:S(2)}, u32[]{:S(2)}) collective-permute-start(bf16[64,1024]{1,0:T(8,128)(2,1)S(1)} %collective-permute-done.26.refs_5_), channel_id=1, source_target_pairs={{0,1},{1,0},{2,3},{3,2},{4,5},{5,4},{6,7},{7,6},{8,9},{9,8},{10,11... | collective-permute-start | bytes 393224 | tf_op jit(solution)/shard_map/ppermute | solution.py:47
  145.8 35.6 %all-to-all-start.1 = ((bf16[16,64,512]{2,1,0:T(8,128)(2,1)}), bf16[16,64,512]{2,1,0:T(8,128)(2,1)S(1)}, u32[]{:S(2)}, u32[]{:S(2)}) async-start(bf16[16,64,512]{2,1,0:T(8,128)(2,1)} %bitcast.7), calls=%async_computation.1 | async-start | bytes 2097152 | tf_op jit(solution)/shard_map/all_to_all | solution.py:178
  153.2 28.1 %copy-start.10 = (pred[128,1024]{1,0:T(32,128)(4,1)S(1)}, pred[128,1024]{1,0:T(32,128)(4,1)}, u32[]{:S(2)}) copy-start(pred[128,1024]{1,0:T(32,128)(4,1)} %copy-done.9) | copy-start | bytes 393220
  153.3 4.1 %collective-permute-start.8 = (bf16[16,1024]{1,0:T(8,128)(2,1)S(1)}, bf16[16,1024]{1,0:T(8,128)(2,1)S(1)}, u32[]{:S(2)}, u32[]{:S(2)}) collective-permute-start(bf16[16,1024]{1,0:T(8,128)(2,1)S(1)} %fusion.13.refs_0_), channel_id=1, source_target_pairs={{0,7},{1,2},{2,1},{3,4},{4,3},{5,6},{6,5},{7,0},{8,15},{9,10},{10,... | collective-permute-start | bytes 98312 | tf_op jit(solution)/shard_map/ppermute | solution.py:47
  154.8 2.8 %collective-permute-start.7 = (bf16[16,1024]{1,0:T(8,128)(2,1)S(1)}, bf16[16,1024]{1,0:T(8,128)(2,1)S(1)}, u32[]{:S(2)}, u32[]{:S(2)}) collective-permute-start(bf16[16,1024]{1,0:T(8,128)(2,1)S(1)} %fusion.13.refs_0_), channel_id=1, source_target_pairs={{0,1},{1,0},{2,3},{3,2},{4,5},{5,4},{6,7},{7,6},{8,9},{9,8},{10,11... | collective-permute-start | bytes 98312 | tf_op jit(solution)/shard_map/ppermute | solution.py:50
  157.4 3.1 %collective-permute-start.9 = (bf16[16,1024]{1,0:T(8,128)(2,1)S(1)}, bf16[16,1024]{1,0:T(8,128)(2,1)S(1)}, u32[]{:S(2)}, u32[]{:S(2)}) collective-permute-start(bf16[16,1024]{1,0:T(8,128)(2,1)S(1)} %collective-permute-done.8.refs_7_), channel_id=1, source_target_pairs={{0,1},{1,0},{2,3},{3,2},{4,5},{5,4},{6,7},{7,6},{8,9},{9,8},{10,11... | collective-permute-start | bytes 98312 | tf_op jit(solution)/shard_map/ppermute | solution.py:47
  157.5 4.3 %collective-permute-start.10 = (bf16[16,1024]{1,0:T(8,128)(2,1)S(1)}, bf16[16,1024]{1,0:T(8,128)(2,1)S(1)}, u32[]{:S(2)}, u32[]{:S(2)}) collective-permute-start(bf16[16,1024]{1,0:T(8,128)(2,1)S(1)} %collective-permute-done.7.refs_1_), channel_id=1, source_target_pairs={{0,7},{1,2},{2,1},{3,4},{4,3},{5,6},{6,5},{7,0},{8,15},{9,10},{10,... | collective-permute-start | bytes 98312 | tf_op jit(solution)/shard_map/ppermute | solution.py:50
  160.4 4.3 %collective-permute-start.12 = (bf16[16,1024]{1,0:T(8,128)(2,1)S(1)}, bf16[16,1024]{1,0:T(8,128)(2,1)S(1)}, u32[]{:S(2)}, u32[]{:S(2)}) collective-permute-start(bf16[16,1024]{1,0:T(8,128)(2,1)S(1)} %collective-permute-done.9.refs_2_), channel_id=1, source_target_pairs={{0,7},{1,2},{2,1},{3,4},{4,3},{5,6},{6,5},{7,0},{8,15},{9,10},{10,... | collective-permute-start | bytes 98312 | tf_op jit(solution)/shard_map/ppermute | solution.py:47
  161.8 3.1 %collective-permute-start.11 = (bf16[16,1024]{1,0:T(8,128)(2,1)S(1)}, bf16[16,1024]{1,0:T(8,128)(2,1)S(1)}, u32[]{:S(2)}, u32[]{:S(2)}) collective-permute-start(bf16[16,1024]{1,0:T(8,128)(2,1)S(1)} %collective-permute-done.10.refs_6_), channel_id=1, source_target_pairs={{0,1},{1,0},{2,3},{3,2},{4,5},{5,4},{6,7},{7,6},{8,9},{9,8},{10,11... | collective-permute-start | bytes 98312 | tf_op jit(solution)/shard_map/ppermute | solution.py:50
  164.7 3.1 %collective-permute-start.13 = (bf16[16,1024]{1,0:T(8,128)(2,1)S(1)}, bf16[16,1024]{1,0:T(8,128)(2,1)S(1)}, u32[]{:S(2)}, u32[]{:S(2)}) collective-permute-start(bf16[16,1024]{1,0:T(8,128)(2,1)S(1)} %collective-permute-done.12.refs_5_), channel_id=1, source_target_pairs={{0,1},{1,0},{2,3},{3,2},{4,5},{5,4},{6,7},{7,6},{8,9},{9,8},{10,11... | collective-permute-start | bytes 98312 | tf_op jit(solution)/shard_map/ppermute | solution.py:47
  (10 other events, 67.8 us)

commit v7 on v6

--- a/solution.py
+++ b/solution.py
@@ -53,7 +53,7 @@
 
 
 LANES = 128
-TILE = 256
+TILE = 512
 IN_VMEM = pl.BlockSpec()
 IN_SMEM = pl.BlockSpec(memory_space=pltpu.SMEM)
 
@@ -185,7 +185,9 @@
 
     me = me_tp.reshape(1)
     gain = gain[None]
-    leaving = lax.dot_general(pick.astype(bf16), tokens, (((0,), (0,)), ((), ())), preferred_element_type=f32)
+    spread = lax.dot_general(expand, place, (((0,), (1,)), ((), ())), preferred_element_type=f32)
+    row_slot = (lax.broadcasted_iota(jnp.int32, (columns, 1), 0) % capacity).astype(f32)
+    leaving = dot((spread == row_slot).astype(bf16), tokens)
     rows = swapped(leaving.astype(bf16))
 
     pieces_s = project(me, gain, tokens, 0, tok_count, shared_gate, shared_up, tp, False)

time: 193 us -> 191 us (0.990)
  transfers between devices with their start and end apart: 44 -> 44, of which waited for: 32 -> 32; matrix products, arithmetic and copies ran while one was open for 3% -> 3% of each run, Pallas kernels for 2% -> 1%
where the time goes in v7:
time: 191 us
  waiting for transfers between devices  101 us (53%)
  starting transfers between devices  61.6 us (32%)
  blocking collectives  9.02 us (5%)
  Pallas kernels  7.54 us (4%)
  other arithmetic  4.46 us (2%)
  local copies, waits for them, and re-layouts  4.16 us (2%)
  matrix products  3.04 us (2%)
    all_to_all x2, starting transfers between devices, swapped(): lax.all_to_all(rows.reshape(experts, capacity, width), 'ep', 0, 0, tiled=...  31.3 us
    all_to_all x2, waiting for transfers between devices, swapped(): lax.all_to_all(rows.reshape(experts, capacity, width), 'ep', 0, 0, tiled=...  26.9 us
    ppermute x9, waiting for transfers between devices, reduce_scatter(): x = lax.ppermute(x_next, axis, two if (half - d) % 2 else one)  26.1 us
    ppermute x12, waiting for transfers between devices, all_gather(): x = lax.ppermute(x, axis, two if d % 2 else one)  22.8 us
    ppermute x9, waiting for transfers between devices, reduce_scatter(): y = lax.ppermute(y_next, axis, one if (half - d) % 2 else two)  18.5 us
    ppermute x9, starting transfers between devices, reduce_scatter(): y = lax.ppermute(y_next, axis, one if (half - d) % 2 else two)  10.5 us
    ppermute x12, starting transfers between devices, all_gather(): x = lax.ppermute(x, axis, two if d % 2 else one)  9.02 us
    all_to_all x1, blocking collectives, layer(): square_sum = lax.all_to_all(copies, 'tp', 0, 0, tiled=True).sum(axis=0)  9.02 us
  transfers between devices with their start and end apart: 44, of which 32 were waited for; matrix products, arithmetic and copies ran while one was open for 3% of the time, Pallas kernels for 1%

profile of v7, /device:TPU:513, one launch (start us, length us, event | category | flops | bytes accessed | tf_op | source)
XLA Modules:
  0.0 190.8 jit_solution(337546566393441968)
XLA Ops:
  0.8 1.2 copy-done.3
  2.0 1.2 copy-done.4
  4.1 1.4 project.3
  5.5 2.2 %collective-permute-start = (bf16[16,2176]{1,0:T(8,128)(2,1)}, bf16[16,2176]{1,0:T(8,128)(2,1)}, u32[]{:S(2)}, u32[]{:S(2)}) collective-permute-start(bf16[16,2176]{1,0:T(8,128)(2,1)} %get-tuple-element.35), channel_id=1, source_target_pairs={{0,1},{1,0},{2,3},{3,2},{4,5},{5,4},{6,7},{7,6},{8,9},{9,8},{10,11... | collective-permute-start | bytes 208904 | tf_op jit(solution)/shard_map/ppermute | solution.py:30
  7.9 1.7 convolution_convert_fusion
  9.5 23.8 %all-to-all-start = ((bf16[16,64,512]{2,1,0:T(8,128)(2,1)}), bf16[16,64,512]{2,1,0:T(8,128)(2,1)S(1)}, u32[]{:S(2)}, u32[]{:S(2)}) async-start(bf16[16,64,512]{2,1,0:T(8,128)(2,1)} %bitcast.1), calls=%async_computation | async-start | bytes 2097152 | tf_op jit(solution)/shard_map/all_to_all | solution.py:178
  35.5 2.8 %collective-permute-start.5 = (bf16[16,2176]{1,0:T(8,128)(2,1)S(1)}, bf16[16,2176]{1,0:T(8,128)(2,1)S(1)}, u32[]{:S(2)}, u32[]{:S(2)}) collective-permute-start(bf16[16,2176]{1,0:T(8,128)(2,1)S(1)} %add_convert_fusion.11), channel_id=1, source_target_pairs={{0,7},{1,2},{2,1},{3,4},{4,3},{5,6},{6,5},{7,0},{8,15},{9,10},{10,... | collective-permute-start | bytes 208904 | tf_op jit(solution)/shard_map/ppermute | solution.py:37
  39.4 1.6 collective-permute-done.5
  41.1 1.7 collective-permute-done.2
  43.3 1.3 collective-permute-done.6
  44.6 3.0 %collective-permute-done.3 = bf16[16,2176]{1,0:T(8,128)(2,1)S(1)} collective-permute-done((bf16[16,2176]{1,0:T(8,128)(2,1)S(1)}, bf16[16,2176]{1,0:T(8,128)(2,1)S(1)}, u32[]{:S(2)}, u32[]{:S(2)}) %collective-permute-start.3) | collective-permute-done | bytes 69664 | tf_op jit(solution)/shard_map/ppermute | solution.py:36
  47.9 13.6 %all-to-all-done = bf16[16,64,512]{2,1,0:T(8,128)(2,1)S(1)} async-done(((bf16[16,64,512]{2,1,0:T(8,128)(2,1)}), bf16[16,64,512]{2,1,0:T(8,128)(2,1)S(1)}, u32[]{:S(2)}, u32[]{:S(2)}) %all-to-all-start) | async-done | bytes 1048608 | tf_op jit(solution)/shard_map/all_to_all | solution.py:178
  61.5 1.7 project.5
  63.3 1.7 project.4
  65.0 1.6 collective-permute-start.32
  66.5 2.7 %collective-permute-start.18 = (bf16[64,2176]{1,0:T(8,128)(2,1)S(1)}, bf16[64,2176]{1,0:T(8,128)(2,1)S(1)}, u32[]{:S(2)}, u32[]{:S(2)}) collective-permute-start(bf16[64,2176]{1,0:T(8,128)(2,1)S(1)} %get-tuple-element.48), channel_id=1, source_target_pairs={{0,7},{1,2},{2,1},{3,4},{4,3},{5,6},{6,5},{7,0},{8,15},{9,10},{10,... | collective-permute-start | bytes 835592 | tf_op jit(solution)/shard_map/ppermute | solution.py:37
  69.2 2.7 %collective-permute-done.28 = bf16[64,2176]{1,0:T(8,128)(2,1)S(1)} collective-permute-done((bf16[64,2176]{1,0:T(8,128)(2,1)S(1)}, bf16[64,2176]{1,0:T(8,128)(2,1)S(1)}, u32[]{:S(2)}, u32[]{:S(2)}) %collective-permute-start.28) | collective-permute-done | bytes 278560 | tf_op jit(solution)/shard_map/ppermute | solution.py:30
  72.2 5.0 %collective-permute-done.32 = bf16[64,2176]{1,0:T(8,128)(2,1)S(1)} collective-permute-done((bf16[64,2176]{1,0:T(8,128)(2,1)S(1)}, bf16[64,2176]{1,0:T(8,128)(2,1)S(1)}, u32[]{:S(2)}, u32[]{:S(2)}) %collective-permute-start.32) | collective-permute-done | bytes 278560 | tf_op jit(solution)/shard_map/ppermute | solution.py:37
  77.6 4.8 %collective-permute-done.18 = bf16[64,2176]{1,0:T(8,128)(2,1)S(1)} collective-permute-done((bf16[64,2176]{1,0:T(8,128)(2,1)S(1)}, bf16[64,2176]{1,0:T(8,128)(2,1)S(1)}, u32[]{:S(2)}, u32[]{:S(2)}) %collective-permute-start.18) | collective-permute-done | bytes 278560 | tf_op jit(solution)/shard_map/ppermute | solution.py:37
  82.8 5.6 %collective-permute-done.29 = bf16[64,2176]{1,0:T(8,128)(2,1)S(1)} collective-permute-done((bf16[64,2176]{1,0:T(8,128)(2,1)S(1)}, bf16[64,2176]{1,0:T(8,128)(2,1)S(1)}, u32[]{:S(2)}, u32[]{:S(2)}) %collective-permute-start.29) | collective-permute-done | bytes 278560 | tf_op jit(solution)/shard_map/ppermute | solution.py:36
  88.6 5.3 %collective-permute-done.33 = bf16[64,2176]{1,0:T(8,128)(2,1)S(1)} collective-permute-done((bf16[64,2176]{1,0:T(8,128)(2,1)S(1)}, bf16[64,2176]{1,0:T(8,128)(2,1)S(1)}, u32[]{:S(2)}, u32[]{:S(2)}) %collective-permute-start.33) | collective-permute-done | bytes 278560 | tf_op jit(solution)/shard_map/ppermute | solution.py:37
  94.5 2.8 %collective-permute-start.20 = (bf16[64,2176]{1,0:T(8,128)(2,1)S(1)}, bf16[64,2176]{1,0:T(8,128)(2,1)S(1)}, u32[]{:S(2)}, u32[]{:S(2)}) collective-permute-start(bf16[64,2176]{1,0:T(8,128)(2,1)S(1)} %add_convert_fusion.5), channel_id=1, source_target_pairs={{0,7},{1,2},{2,1},{3,4},{4,3},{5,6},{6,5},{7,0},{8,15},{9,10},{10,... | collective-permute-start | bytes 835592 | tf_op jit(solution)/shard_map/ppermute | solution.py:37
  98.2 2.5 %collective-permute-start.31 = (bf16[64,2176]{1,0:T(8,128)(2,1)S(1)}, bf16[64,2176]{1,0:T(8,128)(2,1)S(1)}, u32[]{:S(2)}, u32[]{:S(2)}) collective-permute-start(bf16[64,2176]{1,0:T(8,128)(2,1)S(1)} %add_convert_fusion.2), channel_id=1, source_target_pairs={{0,7},{1,2},{2,1},{3,4},{4,3},{5,6},{6,5},{7,0},{8,15},{9,10},{10,... | collective-permute-start | bytes 835592 | tf_op jit(solution)/shard_map/ppermute | solution.py:36
  100.7 2.7 %collective-permute-done.16 = bf16[64,2176]{1,0:T(8,128)(2,1)S(1)} collective-permute-done((bf16[64,2176]{1,0:T(8,128)(2,1)S(1)}, bf16[64,2176]{1,0:T(8,128)(2,1)S(1)}, u32[]{:S(2)}, u32[]{:S(2)}) %collective-permute-start.16) | collective-permute-done | bytes 278560 | tf_op jit(solution)/shard_map/ppermute | solution.py:36
  104.1 11.2 %collective-permute-done.31 = bf16[64,2176]{1,0:T(8,128)(2,1)S(1)} collective-permute-done((bf16[64,2176]{1,0:T(8,128)(2,1)S(1)}, bf16[64,2176]{1,0:T(8,128)(2,1)S(1)}, u32[]{:S(2)}, u32[]{:S(2)}) %collective-permute-start.31) | collective-permute-done | bytes 278560 | tf_op jit(solution)/shard_map/ppermute | solution.py:36
  116.5 2.5 %collective-permute-start.22 = (bf16[64,1024]{1,0:T(8,128)(2,1)S(1)}, bf16[64,1024]{1,0:T(8,128)(2,1)S(1)}, u32[]{:S(2)}, u32[]{:S(2)}) collective-permute-start(bf16[64,1024]{1,0:T(8,128)(2,1)S(1)} %fusion.9.refs_0_), channel_id=1, source_target_pairs={{0,7},{1,2},{2,1},{3,4},{4,3},{5,6},{6,5},{7,0},{8,15},{9,10},{10,... | collective-permute-start | bytes 393224 | tf_op jit(solution)/shard_map/ppermute | solution.py:47
  119.0 1.8 collective-permute-done.36.refs_7_
  120.9 1.5 collective-permute-start.21
  122.3 1.3 collective-permute-done.22.refs_7_
  124.1 1.9 collective-permute-done.37.refs_2_
  126.5 1.5 collective-permute-done.21.refs_1_
  128.0 1.3 collective-permute-start.24
  129.3 1.5 collective-permute-done.23.refs_2_
  130.9 1.3 collective-permute-start.26
  132.2 1.5 collective-permute-start.41
  134.1 3.1 %collective-permute-done.26.refs_5_ = bf16[64,1024]{1,0:T(8,128)(2,1)S(1)} collective-permute-done((bf16[64,1024]{1,0:T(8,128)(2,1)S(1)}, bf16[64,1024]{1,0:T(8,128)(2,1)S(1)}, u32[]{:S(2)}, u32[]{:S(2)}) %collective-permute-start.26) | collective-permute-done | bytes 131104 | tf_op jit(solution)/shard_map/ppermute | solution.py:47
  139.3 3.3 %collective-permute-done.27.refs_4_ = bf16[64,1024]{1,0:T(8,128)(2,1)S(1)} collective-permute-done((bf16[64,1024]{1,0:T(8,128)(2,1)S(1)}, bf16[64,1024]{1,0:T(8,128)(2,1)S(1)}, u32[]{:S(2)}, u32[]{:S(2)}) %collective-permute-start.27) | collective-permute-done | bytes 131104 | tf_op jit(solution)/shard_map/ppermute | solution.py:47
  142.6 1.8 lower_down.5
  144.4 7.5 %all-to-all-start.1 = ((bf16[16,64,512]{2,1,0:T(8,128)(2,1)}), bf16[16,64,512]{2,1,0:T(8,128)(2,1)S(1)}, u32[]{:S(2)}, u32[]{:S(2)}) async-start(bf16[16,64,512]{2,1,0:T(8,128)(2,1)} %bitcast.7), calls=%async_computation.1 | async-start | bytes 2097152 | tf_op jit(solution)/shard_map/all_to_all | solution.py:178
  151.8 1.4 collective-permute-start.8
  153.2 2.6 %collective-permute-done.8.refs_7_ = bf16[16,1024]{1,0:T(8,128)(2,1)S(1)} collective-permute-done((bf16[16,1024]{1,0:T(8,128)(2,1)S(1)}, bf16[16,1024]{1,0:T(8,128)(2,1)S(1)}, u32[]{:S(2)}, u32[]{:S(2)}) %collective-permute-start.8) | collective-permute-done | bytes 32800 | tf_op jit(solution)/shard_map/ppermute | solution.py:47
  156.0 1.3 collective-permute-start.10
  157.3 1.6 collective-permute-done.9.refs_2_
  158.9 1.4 collective-permute-start.12
  160.7 2.6 %collective-permute-done.12.refs_5_ = bf16[16,1024]{1,0:T(8,128)(2,1)S(1)} collective-permute-done((bf16[16,1024]{1,0:T(8,128)(2,1)S(1)}, bf16[16,1024]{1,0:T(8,128)(2,1)S(1)}, u32[]{:S(2)}, u32[]{:S(2)}) %collective-permute-start.12) | collective-permute-done | bytes 32800 | tf_op jit(solution)/shard_map/ppermute | solution.py:47
  163.7 2.6 %collective-permute-done.13.refs_4_ = bf16[16,1024]{1,0:T(8,128)(2,1)S(1)} collective-permute-done((bf16[16,1024]{1,0:T(8,128)(2,1)S(1)}, bf16[16,1024]{1,0:T(8,128)(2,1)S(1)}, u32[]{:S(2)}, u32[]{:S(2)}) %collective-permute-start.13) | collective-permute-done | bytes 32800 | tf_op jit(solution)/shard_map/ppermute | solution.py:47
  166.7 13.3 %all-to-all-done.1 = bf16[16,64,512]{2,1,0:T(8,128)(2,1)S(1)} async-done(((bf16[16,64,512]{2,1,0:T(8,128)(2,1)}), bf16[16,64,512]{2,1,0:T(8,128)(2,1)S(1)}, u32[]{:S(2)}, u32[]{:S(2)}) %all-to-all-start.1) | async-done | bytes 1048608 | tf_op jit(solution)/shard_map/all_to_all | solution.py:178
  181.0 9.0 %all_to_all.15 = f32[8,128,1]{1,2,0:T(1,128)S(1)} all-to-all(f32[8,128,1]{1,2,0:T(1,128)S(1)} %broadcast_in_dim.34), channel_id=1, replica_groups=mesh['grp'=2,'ep'=16,'tp'=8] {'tp'}, dimensions={0} | all-to-all | bytes 8192 | tf_op jit(solution)/shard_map/all_to_all | solution.py:213
  (110 shorter events, 17.3 us)
Async XLA Ops:
  5.5 27.9 %collective-permute-start = (bf16[16,2176]{1,0:T(8,128)(2,1)}, bf16[16,2176]{1,0:T(8,128)(2,1)}, u32[]{:S(2)}, u32[]{:S(2)}) collective-permute-start(bf16[16,2176]{1,0:T(8,128)(2,1)} %get-tuple-element.35), channel_id=1, source_target_pairs={{0,1},{1,0},{2,3},{3,2},{4,5},{5,4},{6,7},{7,6},{8,9},{9,8},{10,11... | collective-permute-start | bytes 208904 | tf_op jit(solution)/shard_map/ppermute | solution.py:30
  7.7 26.9 %collective-permute-start.4 = (bf16[16,2176]{1,0:T(8,128)(2,1)}, bf16[16,2176]{1,0:T(8,128)(2,1)}, u32[]{:S(2)}, u32[]{:S(2)}) collective-permute-start(bf16[16,2176]{1,0:T(8,128)(2,1)} %get-tuple-element.38), channel_id=1, source_target_pairs={{0,1},{1,0},{2,3},{3,2},{4,5},{5,4},{6,7},{7,6},{8,9},{9,8},{10,11... | collective-permute-start | bytes 208904 | tf_op jit(solution)/shard_map/ppermute | solution.py:37
  9.5 52.0 %copy-start.1 = (bf16[1,512,1024]{2,1,0:T(8,128)(2,1)S(1)}, bf16[1,512,1024]{2,1,0:T(8,128)(2,1)}, u32[]{:S(2)}) copy-start(bf16[1,512,1024]{2,1,0:T(8,128)(2,1)} %param.16) | copy-start | bytes 3145732
  9.5 52.0 %all-to-all-start = ((bf16[16,64,512]{2,1,0:T(8,128)(2,1)}), bf16[16,64,512]{2,1,0:T(8,128)(2,1)S(1)}, u32[]{:S(2)}, u32[]{:S(2)}) async-start(bf16[16,64,512]{2,1,0:T(8,128)(2,1)} %bitcast.1), calls=%async_computation | async-start | bytes 2097152 | tf_op jit(solution)/shard_map/all_to_all | solution.py:178
  33.4 28.1 %copy-start = (bf16[1,512,1024]{2,1,0:T(8,128)(2,1)S(1)}, bf16[1,512,1024]{2,1,0:T(8,128)(2,1)}, u32[]{:S(2)}) copy-start(bf16[1,512,1024]{2,1,0:T(8,128)(2,1)} %param.15) | copy-start | bytes 3145732
  34.4 4.8 %collective-permute-start.1 = (bf16[16,2176]{1,0:T(8,128)(2,1)S(1)}, bf16[16,2176]{1,0:T(8,128)(2,1)S(1)}, u32[]{:S(2)}, u32[]{:S(2)}) collective-permute-start(bf16[16,2176]{1,0:T(8,128)(2,1)S(1)} %add_convert_fusion.14), channel_id=1, source_target_pairs={{0,7},{1,2},{2,1},{3,4},{4,3},{5,6},{6,5},{7,0},{8,15},{9,10},{10,... | collective-permute-start | bytes 208904 | tf_op jit(solution)/shard_map/ppermute | solution.py:36
  35.5 5.5 %collective-permute-start.5 = (bf16[16,2176]{1,0:T(8,128)(2,1)S(1)}, bf16[16,2176]{1,0:T(8,128)(2,1)S(1)}, u32[]{:S(2)}, u32[]{:S(2)}) collective-permute-start(bf16[16,2176]{1,0:T(8,128)(2,1)S(1)} %add_convert_fusion.11), channel_id=1, source_target_pairs={{0,7},{1,2},{2,1},{3,4},{4,3},{5,6},{6,5},{7,0},{8,15},{9,10},{10,... | collective-permute-start | bytes 208904 | tf_op jit(solution)/shard_map/ppermute | solution.py:37
  39.2 3.6 %collective-permute-start.2 = (bf16[16,2176]{1,0:T(8,128)(2,1)S(1)}, bf16[16,2176]{1,0:T(8,128)(2,1)S(1)}, u32[]{:S(2)}, u32[]{:S(2)}) collective-permute-start(bf16[16,2176]{1,0:T(8,128)(2,1)S(1)} %add_convert_fusion.13), channel_id=1, source_target_pairs={{0,1},{1,0},{2,3},{3,2},{4,5},{5,4},{6,7},{7,6},{8,9},{9,8},{10,11... | collective-permute-start | bytes 208904 | tf_op jit(solution)/shard_map/ppermute | solution.py:36
  41.0 3.6 %collective-permute-start.6 = (bf16[16,2176]{1,0:T(8,128)(2,1)S(1)}, bf16[16,2176]{1,0:T(8,128)(2,1)S(1)}, u32[]{:S(2)}, u32[]{:S(2)}) collective-permute-start(bf16[16,2176]{1,0:T(8,128)(2,1)S(1)} %add_convert_fusion.10), channel_id=1, source_target_pairs={{0,1},{1,0},{2,3},{3,2},{4,5},{5,4},{6,7},{7,6},{8,9},{9,8},{10,11... | collective-permute-start | bytes 208904 | tf_op jit(solution)/shard_map/ppermute | solution.py:37
  42.8 4.8 %collective-permute-start.3 = (bf16[16,2176]{1,0:T(8,128)(2,1)S(1)}, bf16[16,2176]{1,0:T(8,128)(2,1)S(1)}, u32[]{:S(2)}, u32[]{:S(2)}) collective-permute-start(bf16[16,2176]{1,0:T(8,128)(2,1)S(1)} %add_convert_fusion.12), channel_id=1, source_target_pairs={{0,7},{1,2},{2,1},{3,4},{4,3},{5,6},{6,5},{7,0},{8,15},{9,10},{10,... | collective-permute-start | bytes 208904 | tf_op jit(solution)/shard_map/ppermute | solution.py:36
  63.2 8.8 %collective-permute-start.28 = (bf16[64,2176]{1,0:T(8,128)(2,1)S(1)}, bf16[64,2176]{1,0:T(8,128)(2,1)S(1)}, u32[]{:S(2)}, u32[]{:S(2)}) collective-permute-start(bf16[64,2176]{1,0:T(8,128)(2,1)S(1)} %get-tuple-element.53), channel_id=1, source_target_pairs={{0,1},{1,0},{2,3},{3,2},{4,5},{5,4},{6,7},{7,6},{8,9},{9,8},{10,11... | collective-permute-start | bytes 835592 | tf_op jit(solution)/shard_map/ppermute | solution.py:30
  65.0 12.2 %collective-permute-start.32 = (bf16[64,2176]{1,0:T(8,128)(2,1)S(1)}, bf16[64,2176]{1,0:T(8,128)(2,1)S(1)}, u32[]{:S(2)}, u32[]{:S(2)}) collective-permute-start(bf16[64,2176]{1,0:T(8,128)(2,1)S(1)} %get-tuple-element.56), channel_id=1, source_target_pairs={{0,1},{1,0},{2,3},{3,2},{4,5},{5,4},{6,7},{7,6},{8,9},{9,8},{10,11... | collective-permute-start | bytes 835592 | tf_op jit(solution)/shard_map/ppermute | solution.py:37
  66.5 10.8 %collective-permute-start.14 = (bf16[64,2176]{1,0:T(8,128)(2,1)S(1)}, bf16[64,2176]{1,0:T(8,128)(2,1)S(1)}, u32[]{:S(2)}, u32[]{:S(2)}) collective-permute-start(bf16[64,2176]{1,0:T(8,128)(2,1)S(1)} %get-tuple-element.45), channel_id=1, source_target_pairs={{0,7},{1,2},{2,1},{3,4},{4,3},{5,6},{6,5},{7,0},{8,15},{9,10},{10,... | collective-permute-start | bytes 835592 | tf_op jit(solution)/shard_map/ppermute | solution.py:30
  66.5 15.8 %collective-permute-start.18 = (bf16[64,2176]{1,0:T(8,128)(2,1)S(1)}, bf16[64,2176]{1,0:T(8,128)(2,1)S(1)}, u32[]{:S(2)}, u32[]{:S(2)}) collective-permute-start(bf16[64,2176]{1,0:T(8,128)(2,1)S(1)} %get-tuple-element.48), channel_id=1, source_target_pairs={{0,7},{1,2},{2,1},{3,4},{4,3},{5,6},{6,5},{7,0},{8,15},{9,10},{10,... | collective-permute-start | bytes 835592 | tf_op jit(solution)/shard_map/ppermute | solution.py:37
  72.0 16.3 %collective-permute-start.29 = (bf16[64,2176]{1,0:T(8,128)(2,1)S(1)}, bf16[64,2176]{1,0:T(8,128)(2,1)S(1)}, u32[]{:S(2)}, u32[]{:S(2)}) collective-permute-start(bf16[64,2176]{1,0:T(8,128)(2,1)S(1)} %add_convert_fusion.4), channel_id=1, source_target_pairs={{0,7},{1,2},{2,1},{3,4},{4,3},{5,6},{6,5},{7,0},{8,15},{9,10},{10,... | collective-permute-start | bytes 835592 | tf_op jit(solution)/shard_map/ppermute | solution.py:36
  77.2 16.7 %collective-permute-start.33 = (bf16[64,2176]{1,0:T(8,128)(2,1)S(1)}, bf16[64,2176]{1,0:T(8,128)(2,1)S(1)}, u32[]{:S(2)}, u32[]{:S(2)}) collective-permute-start(bf16[64,2176]{1,0:T(8,128)(2,1)S(1)} %add_convert_fusion.1), channel_id=1, source_target_pairs={{0,7},{1,2},{2,1},{3,4},{4,3},{5,6},{6,5},{7,0},{8,15},{9,10},{10,... | collective-permute-start | bytes 835592 | tf_op jit(solution)/shard_map/ppermute | solution.py:37
  77.5 16.7 %collective-permute-start.15 = (bf16[64,2176]{1,0:T(8,128)(2,1)S(1)}, bf16[64,2176]{1,0:T(8,128)(2,1)S(1)}, u32[]{:S(2)}, u32[]{:S(2)}) collective-permute-start(bf16[64,2176]{1,0:T(8,128)(2,1)S(1)} %add_convert_fusion.9), channel_id=1, source_target_pairs={{0,1},{1,0},{2,3},{3,2},{4,5},{5,4},{6,7},{7,6},{8,9},{9,8},{10,11... | collective-permute-start | bytes 835592 | tf_op jit(solution)/shard_map/ppermute | solution.py:36
  82.5 11.9 %collective-permute-start.19 = (bf16[64,2176]{1,0:T(8,128)(2,1)S(1)}, bf16[64,2176]{1,0:T(8,128)(2,1)S(1)}, u32[]{:S(2)}, u32[]{:S(2)}) collective-permute-start(bf16[64,2176]{1,0:T(8,128)(2,1)S(1)} %add_convert_fusion.6), channel_id=1, source_target_pairs={{0,1},{1,0},{2,3},{3,2},{4,5},{5,4},{6,7},{7,6},{8,9},{9,8},{10,11... | collective-permute-start | bytes 835592 | tf_op jit(solution)/shard_map/ppermute | solution.py:37
  88.4 9.7 %collective-permute-start.30 = (bf16[64,2176]{1,0:T(8,128)(2,1)S(1)}, bf16[64,2176]{1,0:T(8,128)(2,1)S(1)}, u32[]{:S(2)}, u32[]{:S(2)}) collective-permute-start(bf16[64,2176]{1,0:T(8,128)(2,1)S(1)} %add_convert_fusion.3), channel_id=1, source_target_pairs={{0,1},{1,0},{2,3},{3,2},{4,5},{5,4},{6,7},{7,6},{8,9},{9,8},{10,11... | collective-permute-start | bytes 835592 | tf_op jit(solution)/shard_map/ppermute | solution.py:36
  94.0 10.1 %collective-permute-start.34 = (bf16[64,2176]{1,0:T(8,128)(2,1)S(1)}, bf16[64,2176]{1,0:T(8,128)(2,1)S(1)}, u32[]{:S(2)}, u32[]{:S(2)}) collective-permute-start(bf16[64,2176]{1,0:T(8,128)(2,1)S(1)} %add_convert_fusion), channel_id=1, source_target_pairs={{0,1},{1,0},{2,3},{3,2},{4,5},{5,4},{6,7},{7,6},{8,9},{9,8},{10,11... | collective-permute-start | bytes 835592 | tf_op jit(solution)/shard_map/ppermute | solution.py:37
  94.2 9.2 %collective-permute-start.16 = (bf16[64,2176]{1,0:T(8,128)(2,1)S(1)}, bf16[64,2176]{1,0:T(8,128)(2,1)S(1)}, u32[]{:S(2)}, u32[]{:S(2)}) collective-permute-start(bf16[64,2176]{1,0:T(8,128)(2,1)S(1)} %add_convert_fusion.8), channel_id=1, source_target_pairs={{0,7},{1,2},{2,1},{3,4},{4,3},{5,6},{6,5},{7,0},{8,15},{9,10},{10,... | collective-permute-start | bytes 835592 | tf_op jit(solution)/shard_map/ppermute | solution.py:36
  94.5 21.7 %collective-permute-start.20 = (bf16[64,2176]{1,0:T(8,128)(2,1)S(1)}, bf16[64,2176]{1,0:T(8,128)(2,1)S(1)}, u32[]{:S(2)}, u32[]{:S(2)}) collective-permute-start(bf16[64,2176]{1,0:T(8,128)(2,1)S(1)} %add_convert_fusion.5), channel_id=1, source_target_pairs={{0,7},{1,2},{2,1},{3,4},{4,3},{5,6},{6,5},{7,0},{8,15},{9,10},{10,... | collective-permute-start | bytes 835592 | tf_op jit(solution)/shard_map/ppermute | solution.py:37
  98.2 17.1 %collective-permute-start.31 = (bf16[64,2176]{1,0:T(8,128)(2,1)S(1)}, bf16[64,2176]{1,0:T(8,128)(2,1)S(1)}, u32[]{:S(2)}, u32[]{:S(2)}) collective-permute-start(bf16[64,2176]{1,0:T(8,128)(2,1)S(1)} %add_convert_fusion.2), channel_id=1, source_target_pairs={{0,7},{1,2},{2,1},{3,4},{4,3},{5,6},{6,5},{7,0},{8,15},{9,10},{10,... | collective-permute-start | bytes 835592 | tf_op jit(solution)/shard_map/ppermute | solution.py:36
  103.5 12.7 %collective-permute-start.17 = (bf16[64,2176]{1,0:T(8,128)(2,1)S(1)}, bf16[64,2176]{1,0:T(8,128)(2,1)S(1)}, u32[]{:S(2)}, u32[]{:S(2)}) collective-permute-start(bf16[64,2176]{1,0:T(8,128)(2,1)S(1)} %add_convert_fusion.7), channel_id=1, source_target_pairs={{0,1},{1,0},{2,3},{3,2},{4,5},{5,4},{6,7},{7,6},{8,9},{9,8},{10,11... | collective-permute-start | bytes 835592 | tf_op jit(solution)/shard_map/ppermute | solution.py:36
  115.7 22.0 %copy-start.2 = (bf16[1,1024,512]{2,1,0:T(8,128)(2,1)S(1)}, bf16[1,1024,512]{2,1,0:T(8,128)(2,1)}, u32[]{:S(2)}) copy-start(bf16[1,1024,512]{2,1,0:T(8,128)(2,1)} %param.17) | copy-start | bytes 3145732
  115.7 5.2 %collective-permute-start.36 = (bf16[64,1024]{1,0:T(8,128)(2,1)S(1)}, bf16[64,1024]{1,0:T(8,128)(2,1)S(1)}, u32[]{:S(2)}, u32[]{:S(2)}) collective-permute-start(bf16[64,1024]{1,0:T(8,128)(2,1)S(1)} %fusion.7.refs_0_), channel_id=1, source_target_pairs={{0,7},{1,2},{2,1},{3,4},{4,3},{5,6},{6,5},{7,0},{8,15},{9,10},{10,... | collective-permute-start | bytes 393224 | tf_op jit(solution)/shard_map/ppermute | solution.py:47
  116.5 7.1 %collective-permute-start.22 = (bf16[64,1024]{1,0:T(8,128)(2,1)S(1)}, bf16[64,1024]{1,0:T(8,128)(2,1)S(1)}, u32[]{:S(2)}, u32[]{:S(2)}) collective-permute-start(bf16[64,1024]{1,0:T(8,128)(2,1)S(1)} %fusion.9.refs_0_), channel_id=1, source_target_pairs={{0,7},{1,2},{2,1},{3,4},{4,3},{5,6},{6,5},{7,0},{8,15},{9,10},{10,... | collective-permute-start | bytes 393224 | tf_op jit(solution)/shard_map/ppermute | solution.py:47
  119.0 4.6 %collective-permute-start.35 = (bf16[64,1024]{1,0:T(8,128)(2,1)S(1)}, bf16[64,1024]{1,0:T(8,128)(2,1)S(1)}, u32[]{:S(2)}, u32[]{:S(2)}) collective-permute-start(bf16[64,1024]{1,0:T(8,128)(2,1)S(1)} %fusion.7.refs_0_), channel_id=1, source_target_pairs={{0,1},{1,0},{2,3},{3,2},{4,5},{5,4},{6,7},{7,6},{8,9},{9,8},{10,11... | collective-permute-start | bytes 393224 | tf_op jit(solution)/shard_map/ppermute | solution.py:50
  120.9 5.1 %collective-permute-start.37 = (bf16[64,1024]{1,0:T(8,128)(2,1)S(1)}, bf16[64,1024]{1,0:T(8,128)(2,1)S(1)}, u32[]{:S(2)}, u32[]{:S(2)}) collective-permute-start(bf16[64,1024]{1,0:T(8,128)(2,1)S(1)} %collective-permute-done.36.refs_7_), channel_id=1, source_target_pairs={{0,1},{1,0},{2,3},{3,2},{4,5},{5,4},{6,7},{7,6},{8,9},{9,8},{10,11... | collective-permute-start | bytes 393224 | tf_op jit(solution)/shard_map/ppermute | solution.py:47
  120.9 7.2 %collective-permute-start.21 = (bf16[64,1024]{1,0:T(8,128)(2,1)S(1)}, bf16[64,1024]{1,0:T(8,128)(2,1)S(1)}, u32[]{:S(2)}, u32[]{:S(2)}) collective-permute-start(bf16[64,1024]{1,0:T(8,128)(2,1)S(1)} %fusion.9.refs_0_), channel_id=1, source_target_pairs={{0,1},{1,0},{2,3},{3,2},{4,5},{5,4},{6,7},{7,6},{8,9},{9,8},{10,11... | collective-permute-start | bytes 393224 | tf_op jit(solution)/shard_map/ppermute | solution.py:50
  123.7 7.2 %collective-permute-start.23 = (bf16[64,1024]{1,0:T(8,128)(2,1)S(1)}, bf16[64,1024]{1,0:T(8,128)(2,1)S(1)}, u32[]{:S(2)}, u32[]{:S(2)}) collective-permute-start(bf16[64,1024]{1,0:T(8,128)(2,1)S(1)} %collective-permute-done.22.refs_7_), channel_id=1, source_target_pairs={{0,1},{1,0},{2,3},{3,2},{4,5},{5,4},{6,7},{7,6},{8,9},{9,8},{10,11... | collective-permute-start | bytes 393224 | tf_op jit(solution)/shard_map/ppermute | solution.py:47
  123.7 8.5 %collective-permute-start.38 = (bf16[64,1024]{1,0:T(8,128)(2,1)S(1)}, bf16[64,1024]{1,0:T(8,128)(2,1)S(1)}, u32[]{:S(2)}, u32[]{:S(2)}) collective-permute-start(bf16[64,1024]{1,0:T(8,128)(2,1)S(1)} %collective-permute-done.35.refs_1_), channel_id=1, source_target_pairs={{0,7},{1,2},{2,1},{3,4},{4,3},{5,6},{6,5},{7,0},{8,15},{9,10},{10,... | collective-permute-start | bytes 393224 | tf_op jit(solution)/shard_map/ppermute | solution.py:50
  126.0 6.2 %collective-permute-start.40 = (bf16[64,1024]{1,0:T(8,128)(2,1)S(1)}, bf16[64,1024]{1,0:T(8,128)(2,1)S(1)}, u32[]{:S(2)}, u32[]{:S(2)}) collective-permute-start(bf16[64,1024]{1,0:T(8,128)(2,1)S(1)} %collective-permute-done.37.refs_2_), channel_id=1, source_target_pairs={{0,7},{1,2},{2,1},{3,4},{4,3},{5,6},{6,5},{7,0},{8,15},{9,10},{10,... | collective-permute-start | bytes 393224 | tf_op jit(solution)/shard_map/ppermute | solution.py:47
  128.0 6.1 %collective-permute-start.24 = (bf16[64,1024]{1,0:T(8,128)(2,1)S(1)}, bf16[64,1024]{1,0:T(8,128)(2,1)S(1)}, u32[]{:S(2)}, u32[]{:S(2)}) collective-permute-start(bf16[64,1024]{1,0:T(8,128)(2,1)S(1)} %collective-permute-done.21.refs_1_), channel_id=1, source_target_pairs={{0,7},{1,2},{2,1},{3,4},{4,3},{5,6},{6,5},{7,0},{8,15},{9,10},{10,... | collective-permute-start | bytes 393224 | tf_op jit(solution)/shard_map/ppermute | solution.py:50
  130.9 6.4 %collective-permute-start.26 = (bf16[64,1024]{1,0:T(8,128)(2,1)S(1)}, bf16[64,1024]{1,0:T(8,128)(2,1)S(1)}, u32[]{:S(2)}, u32[]{:S(2)}) collective-permute-start(bf16[64,1024]{1,0:T(8,128)(2,1)S(1)} %collective-permute-done.23.refs_2_), channel_id=1, source_target_pairs={{0,7},{1,2},{2,1},{3,4},{4,3},{5,6},{6,5},{7,0},{8,15},{9,10},{10,... | collective-permute-start | bytes 393224 | tf_op jit(solution)/shard_map/ppermute | solution.py:47
  132.2 5.1 %collective-permute-start.39 = (bf16[64,1024]{1,0:T(8,128)(2,1)S(1)}, bf16[64,1024]{1,0:T(8,128)(2,1)S(1)}, u32[]{:S(2)}, u32[]{:S(2)}) collective-permute-start(bf16[64,1024]{1,0:T(8,128)(2,1)S(1)} %collective-permute-done.38.refs_6_), channel_id=1, source_target_pairs={{0,1},{1,0},{2,3},{3,2},{4,5},{5,4},{6,7},{7,6},{8,9},{9,8},{10,11... | collective-permute-start | bytes 393224 | tf_op jit(solution)/shard_map/ppermute | solution.py:50
  132.2 5.5 %collective-permute-start.41 = (bf16[64,1024]{1,0:T(8,128)(2,1)S(1)}, bf16[64,1024]{1,0:T(8,128)(2,1)S(1)}, u32[]{:S(2)}, u32[]{:S(2)}) collective-permute-start(bf16[64,1024]{1,0:T(8,128)(2,1)S(1)} %collective-permute-done.40.refs_5_), channel_id=1, source_target_pairs={{0,1},{1,0},{2,3},{3,2},{4,5},{5,4},{6,7},{7,6},{8,9},{9,8},{10,11... | collective-permute-start | bytes 393224 | tf_op jit(solution)/shard_map/ppermute | solution.py:47
  134.1 5.2 %collective-permute-start.25 = (bf16[64,1024]{1,0:T(8,128)(2,1)S(1)}, bf16[64,1024]{1,0:T(8,128)(2,1)S(1)}, u32[]{:S(2)}, u32[]{:S(2)}) collective-permute-start(bf16[64,1024]{1,0:T(8,128)(2,1)S(1)} %collective-permute-done.24.refs_6_), channel_id=1, source_target_pairs={{0,1},{1,0},{2,3},{3,2},{4,5},{5,4},{6,7},{7,6},{8,9},{9,8},{10,11... | collective-permute-start | bytes 393224 | tf_op jit(solution)/shard_map/ppermute | solution.py:50
  137.2 5.4 %collective-permute-start.27 = (bf16[64,1024]{1,0:T(8,128)(2,1)S(1)}, bf16[64,1024]{1,0:T(8,128)(2,1)S(1)}, u32[]{:S(2)}, u32[]{:S(2)}) collective-permute-start(bf16[64,1024]{1,0:T(8,128)(2,1)S(1)} %collective-permute-done.26.refs_5_), channel_id=1, source_target_pairs={{0,1},{1,0},{2,3},{3,2},{4,5},{5,4},{6,7},{7,6},{8,9},{9,8},{10,11... | collective-permute-start | bytes 393224 | tf_op jit(solution)/shard_map/ppermute | solution.py:47
  144.4 21.9 %copy-start.5 = (bf16[1024,512]{1,0:T(8,128)(2,1)S(1)}, bf16[1024,512]{1,0:T(8,128)(2,1)}, u32[]{:S(2)}) copy-start(bf16[1024,512]{1,0:T(8,128)(2,1)} %refs_8_.1) | copy-start | bytes 3145732
  144.4 35.6 %all-to-all-start.1 = ((bf16[16,64,512]{2,1,0:T(8,128)(2,1)}), bf16[16,64,512]{2,1,0:T(8,128)(2,1)S(1)}, u32[]{:S(2)}, u32[]{:S(2)}) async-start(bf16[16,64,512]{2,1,0:T(8,128)(2,1)} %bitcast.7), calls=%async_computation.1 | async-start | bytes 2097152 | tf_op jit(solution)/shard_map/all_to_all | solution.py:178
  151.8 4.0 %collective-permute-start.8 = (bf16[16,1024]{1,0:T(8,128)(2,1)S(1)}, bf16[16,1024]{1,0:T(8,128)(2,1)S(1)}, u32[]{:S(2)}, u32[]{:S(2)}) collective-permute-start(bf16[16,1024]{1,0:T(8,128)(2,1)S(1)} %fusion.14.refs_0_), channel_id=1, source_target_pairs={{0,7},{1,2},{2,1},{3,4},{4,3},{5,6},{6,5},{7,0},{8,15},{9,10},{10,... | collective-permute-start | bytes 98312 | tf_op jit(solution)/shard_map/ppermute | solution.py:47
  153.2 2.8 %collective-permute-start.7 = (bf16[16,1024]{1,0:T(8,128)(2,1)S(1)}, bf16[16,1024]{1,0:T(8,128)(2,1)S(1)}, u32[]{:S(2)}, u32[]{:S(2)}) collective-permute-start(bf16[16,1024]{1,0:T(8,128)(2,1)S(1)} %fusion.14.refs_0_), channel_id=1, source_target_pairs={{0,1},{1,0},{2,3},{3,2},{4,5},{5,4},{6,7},{7,6},{8,9},{9,8},{10,11... | collective-permute-start | bytes 98312 | tf_op jit(solution)/shard_map/ppermute | solution.py:50
  155.8 3.1 %collective-permute-start.9 = (bf16[16,1024]{1,0:T(8,128)(2,1)S(1)}, bf16[16,1024]{1,0:T(8,128)(2,1)S(1)}, u32[]{:S(2)}, u32[]{:S(2)}) collective-permute-start(bf16[16,1024]{1,0:T(8,128)(2,1)S(1)} %collective-permute-done.8.refs_7_), channel_id=1, source_target_pairs={{0,1},{1,0},{2,3},{3,2},{4,5},{5,4},{6,7},{7,6},{8,9},{9,8},{10,11... | collective-permute-start | bytes 98312 | tf_op jit(solution)/shard_map/ppermute | solution.py:47
  156.0 4.5 %collective-permute-start.10 = (bf16[16,1024]{1,0:T(8,128)(2,1)S(1)}, bf16[16,1024]{1,0:T(8,128)(2,1)S(1)}, u32[]{:S(2)}, u32[]{:S(2)}) collective-permute-start(bf16[16,1024]{1,0:T(8,128)(2,1)S(1)} %collective-permute-done.7.refs_1_), channel_id=1, source_target_pairs={{0,7},{1,2},{2,1},{3,4},{4,3},{5,6},{6,5},{7,0},{8,15},{9,10},{10,... | collective-permute-start | bytes 98312 | tf_op jit(solution)/shard_map/ppermute | solution.py:50
  158.9 4.4 %collective-permute-start.12 = (bf16[16,1024]{1,0:T(8,128)(2,1)S(1)}, bf16[16,1024]{1,0:T(8,128)(2,1)S(1)}, u32[]{:S(2)}, u32[]{:S(2)}) collective-permute-start(bf16[16,1024]{1,0:T(8,128)(2,1)S(1)} %collective-permute-done.9.refs_2_), channel_id=1, source_target_pairs={{0,7},{1,2},{2,1},{3,4},{4,3},{5,6},{6,5},{7,0},{8,15},{9,10},{10,... | collective-permute-start | bytes 98312 | tf_op jit(solution)/shard_map/ppermute | solution.py:47
  160.5 3.2 %collective-permute-start.11 = (bf16[16,1024]{1,0:T(8,128)(2,1)S(1)}, bf16[16,1024]{1,0:T(8,128)(2,1)S(1)}, u32[]{:S(2)}, u32[]{:S(2)}) collective-permute-start(bf16[16,1024]{1,0:T(8,128)(2,1)S(1)} %collective-permute-done.10.refs_6_), channel_id=1, source_target_pairs={{0,1},{1,0},{2,3},{3,2},{4,5},{5,4},{6,7},{7,6},{8,9},{9,8},{10,11... | collective-permute-start | bytes 98312 | tf_op jit(solution)/shard_map/ppermute | solution.py:50
  163.3 3.1 %collective-permute-start.13 = (bf16[16,1024]{1,0:T(8,128)(2,1)S(1)}, bf16[16,1024]{1,0:T(8,128)(2,1)S(1)}, u32[]{:S(2)}, u32[]{:S(2)}) collective-permute-start(bf16[16,1024]{1,0:T(8,128)(2,1)S(1)} %collective-permute-done.12.refs_5_), channel_id=1, source_target_pairs={{0,1},{1,0},{2,3},{3,2},{4,5},{5,4},{6,7},{7,6},{8,9},{9,8},{10,11... | collective-permute-start | bytes 98312 | tf_op jit(solution)/shard_map/ppermute | solution.py:47
  (8 other events, 43.2 us)

commit v8 on v6

--- a/solution.py
+++ b/solution.py
@@ -53,7 +53,7 @@
 
 
 LANES = 128
-TILE = 256
+TILE = 512
 IN_VMEM = pl.BlockSpec()
 IN_SMEM = pl.BlockSpec(memory_space=pltpu.SMEM)
 
@@ -98,36 +98,36 @@
     )(me, gain, rows, gate, up)
 
 
-def lower_down(me, blocks, flip, matrix, kind, above=()):
+def lower_down(me, blocks, flip, matrix, kind, below=()):
     size = len(blocks)
     count, units = blocks[0].shape
     height = size * count
     width = matrix.shape[1]
-    first = sum(v.shape[0] for v in above)
+    rest = sum(v.shape[0] for v in below)
 
     def body(me_ref, *refs):
-        ins, matrix_ref, above_refs, (out_ref, rows_ref) = refs[:size], refs[size], refs[size + 1 : -2], refs[-2:]
+        ins, matrix_ref, below_refs, (out_ref, rows_ref) = refs[:size], refs[size], refs[size + 1 : -2], refs[-2:]
         for d in range(size):
             rows_ref[pl.ds(block_row(me_ref[0], d, size, count, flip), count), :] = ins[d][...]
-        for ref in above_refs:
-            out_ref[:first, :] = ref[...]
+        for ref in below_refs:
+            out_ref[height:, :] = ref[...]
 
         def columns(n, _):
             at = pl.multiple_of(n * TILE, TILE)
-            out_ref[first:, pl.ds(at, TILE)] = dot(rows_ref[...], matrix_ref[:, pl.ds(at, TILE)]).astype(kind)
+            out_ref[:height, pl.ds(at, TILE)] = dot(rows_ref[...], matrix_ref[:, pl.ds(at, TILE)]).astype(kind)
             return 0
 
         lax.fori_loop(0, width // TILE, columns, 0)
 
     return pl.pallas_call(
         body,
-        out_shape=jax.ShapeDtypeStruct((first + height, width), kind),
-        in_specs=[IN_SMEM] + [IN_VMEM] * (size + 1 + len(above)),
+        out_shape=jax.ShapeDtypeStruct((height + rest, width), kind),
+        in_specs=[IN_SMEM] + [IN_VMEM] * (size + 1 + len(below)),
         out_specs=IN_VMEM,
         scratch_shapes=[pltpu.VMEM((height, units), bf16)],
         compiler_params=pltpu.CompilerParams(vmem_limit_bytes=12 << 20),
         name="lower_down",
-    )(me, *blocks, matrix, *above)
+    )(me, *blocks, matrix, *below)
 
 
 def layer(
@@ -199,8 +199,8 @@
     total_b = reduce_scatter(pieces_b, tp, True, "tp")
     blocks_a = all_gather(hidden_of(total_a), tp, False, "tp")
     blocks_b = all_gather(hidden_of(total_b), tp, False, "tp")
-    down_a = lower_down(me, blocks_a, False, down_matrix, bf16)
-    down = lower_down(me, blocks_b, False, down_matrix, bf16, above=(down_a,))
+    down_b = lower_down(me, blocks_b, False, down_matrix, bf16)
+    down = lower_down(me, blocks_a, False, down_matrix, bf16, below=(down_b,))
     came = swapped(down)
     blocks_s = all_gather(hidden_s, tp, False, "tp")
     shared_out = lower_down(me, blocks_s, False, shared_down, f32)

time: 193 us -> 192 us (level)
  starting transfers between devices: 61.7 us -> 65.1 us
  waiting for transfers between devices: 100 us -> 97.6 us
    ppermute x9, starting transfers between devices: 4.54 us -> 6.83 us  [all_gather(): y = lax.ppermute(y, axis, one if d % 2 else two)]
  transfers between devices with their start and end apart: 44 -> 44, of which waited for: 32 -> 30; matrix products, arithmetic and copies ran while one was open for 3% -> 3% of each run, Pallas kernels for 2% -> 1%
where the time goes in v8:
time: 192 us; the launch traced here: 191 us
  waiting for transfers between devices  97.6 us (51%)
  starting transfers between devices  65.1 us (34%)
  blocking collectives  8.97 us (5%)
  Pallas kernels  7.55 us (4%)
  other arithmetic  4.46 us (2%)
  local copies, waits for them, and re-layouts  4.17 us (2%)
  matrix products  2.9 us (2%)
    all_to_all x2, starting transfers between devices, swapped(): lax.all_to_all(rows.reshape(experts, capacity, width), 'ep', 0, 0, tiled=...  31.7 us
    all_to_all x2, waiting for transfers between devices, swapped(): lax.all_to_all(rows.reshape(experts, capacity, width), 'ep', 0, 0, tiled=...  26.9 us
    ppermute x9, waiting for transfers between devices, reduce_scatter(): x = lax.ppermute(x_next, axis, two if (half - d) % 2 else one)  25.9 us
    ppermute x12, waiting for transfers between devices, all_gather(): x = lax.ppermute(x, axis, two if d % 2 else one)  21.4 us
    ppermute x9, waiting for transfers between devices, reduce_scatter(): y = lax.ppermute(y_next, axis, one if (half - d) % 2 else two)  17.6 us
    ppermute x12, starting transfers between devices, all_gather(): x = lax.ppermute(x, axis, two if d % 2 else one)  10.8 us
    ppermute x9, starting transfers between devices, reduce_scatter(): y = lax.ppermute(y_next, axis, one if (half - d) % 2 else two)  9.44 us
    all_to_all x1, blocking collectives, layer(): square_sum = lax.all_to_all(copies, 'tp', 0, 0, tiled=True).sum(axis=0)  8.97 us
  transfers between devices with their start and end apart: 44, of which 30 were waited for; matrix products, arithmetic and copies ran while one was open for 3% of the time, Pallas kernels for 1%

profile of v8, /device:TPU:513, one launch (start us, length us, event | category | flops | bytes accessed | tf_op | source)
XLA Modules:
  0.0 191.2 jit_solution(9435712913773338101)
XLA Ops:
  4.1 1.4 project.3
  5.5 2.2 %collective-permute-start = (bf16[16,2176]{1,0:T(8,128)(2,1)}, bf16[16,2176]{1,0:T(8,128)(2,1)}, u32[]{:S(2)}, u32[]{:S(2)}) collective-permute-start(bf16[16,2176]{1,0:T(8,128)(2,1)} %get-tuple-element.35), channel_id=1, source_target_pairs={{0,1},{1,0},{2,3},{3,2},{4,5},{5,4},{6,7},{7,6},{8,9},{9,8},{10,11... | collective-permute-start | bytes 208904 | tf_op jit(solution)/shard_map/ppermute | solution.py:30
  8.2 1.5 convolution_convert_fusion
  9.7 23.8 %all-to-all-start = ((bf16[16,64,512]{2,1,0:T(8,128)(2,1)}), bf16[16,64,512]{2,1,0:T(8,128)(2,1)S(1)}, u32[]{:S(2)}, u32[]{:S(2)}) async-start(bf16[16,64,512]{2,1,0:T(8,128)(2,1)} %bitcast.1), calls=%async_computation | async-start | bytes 2097152 | tf_op jit(solution)/shard_map/all_to_all | solution.py:178
  35.6 2.8 %collective-permute-start.5 = (bf16[16,2176]{1,0:T(8,128)(2,1)S(1)}, bf16[16,2176]{1,0:T(8,128)(2,1)S(1)}, u32[]{:S(2)}, u32[]{:S(2)}) collective-permute-start(bf16[16,2176]{1,0:T(8,128)(2,1)S(1)} %add_convert_fusion.11), channel_id=1, source_target_pairs={{0,7},{1,2},{2,1},{3,4},{4,3},{5,6},{6,5},{7,0},{8,15},{9,10},{10,... | collective-permute-start | bytes 208904 | tf_op jit(solution)/shard_map/ppermute | solution.py:37
  39.5 1.6 collective-permute-done.5
  41.3 1.7 collective-permute-done.2
  43.4 1.3 collective-permute-done.6
  44.7 3.0 %collective-permute-done.3 = bf16[16,2176]{1,0:T(8,128)(2,1)S(1)} collective-permute-done((bf16[16,2176]{1,0:T(8,128)(2,1)S(1)}, bf16[16,2176]{1,0:T(8,128)(2,1)S(1)}, u32[]{:S(2)}, u32[]{:S(2)}) %collective-permute-start.3) | collective-permute-done | bytes 69664 | tf_op jit(solution)/shard_map/ppermute | solution.py:36
  48.0 13.6 %all-to-all-done = bf16[16,64,512]{2,1,0:T(8,128)(2,1)S(1)} async-done(((bf16[16,64,512]{2,1,0:T(8,128)(2,1)}), bf16[16,64,512]{2,1,0:T(8,128)(2,1)S(1)}, u32[]{:S(2)}, u32[]{:S(2)}) %all-to-all-start) | async-done | bytes 1048608 | tf_op jit(solution)/shard_map/all_to_all | solution.py:178
  61.6 1.7 project.5
  63.5 1.7 project.4
  65.1 2.8 %collective-permute-start.32 = (bf16[64,2176]{1,0:T(8,128)(2,1)S(1)}, bf16[64,2176]{1,0:T(8,128)(2,1)S(1)}, u32[]{:S(2)}, u32[]{:S(2)}) collective-permute-start(bf16[64,2176]{1,0:T(8,128)(2,1)S(1)} %get-tuple-element.56), channel_id=1, source_target_pairs={{0,7},{1,2},{2,1},{3,4},{4,3},{5,6},{6,5},{7,0},{8,15},{9,10},{10,... | collective-permute-start | bytes 835592 | tf_op jit(solution)/shard_map/ppermute | solution.py:37
  67.9 1.5 collective-permute-start.18
  69.4 3.9 %collective-permute-done.28 = bf16[64,2176]{1,0:T(8,128)(2,1)S(1)} collective-permute-done((bf16[64,2176]{1,0:T(8,128)(2,1)S(1)}, bf16[64,2176]{1,0:T(8,128)(2,1)S(1)}, u32[]{:S(2)}, u32[]{:S(2)}) %collective-permute-start.28) | collective-permute-done | bytes 278560 | tf_op jit(solution)/shard_map/ppermute | solution.py:30
  73.5 4.7 %collective-permute-done.32 = bf16[64,2176]{1,0:T(8,128)(2,1)S(1)} collective-permute-done((bf16[64,2176]{1,0:T(8,128)(2,1)S(1)}, bf16[64,2176]{1,0:T(8,128)(2,1)S(1)}, u32[]{:S(2)}, u32[]{:S(2)}) %collective-permute-start.32) | collective-permute-done | bytes 278560 | tf_op jit(solution)/shard_map/ppermute | solution.py:37
  78.7 3.9 %collective-permute-done.18 = bf16[64,2176]{1,0:T(8,128)(2,1)S(1)} collective-permute-done((bf16[64,2176]{1,0:T(8,128)(2,1)S(1)}, bf16[64,2176]{1,0:T(8,128)(2,1)S(1)}, u32[]{:S(2)}, u32[]{:S(2)}) %collective-permute-start.18) | collective-permute-done | bytes 278560 | tf_op jit(solution)/shard_map/ppermute | solution.py:37
  83.1 5.4 %collective-permute-done.29 = bf16[64,2176]{1,0:T(8,128)(2,1)S(1)} collective-permute-done((bf16[64,2176]{1,0:T(8,128)(2,1)S(1)}, bf16[64,2176]{1,0:T(8,128)(2,1)S(1)}, u32[]{:S(2)}, u32[]{:S(2)}) %collective-permute-start.29) | collective-permute-done | bytes 278560 | tf_op jit(solution)/shard_map/ppermute | solution.py:36
  88.9 5.4 %collective-permute-done.33 = bf16[64,2176]{1,0:T(8,128)(2,1)S(1)} collective-permute-done((bf16[64,2176]{1,0:T(8,128)(2,1)S(1)}, bf16[64,2176]{1,0:T(8,128)(2,1)S(1)}, u32[]{:S(2)}, u32[]{:S(2)}) %collective-permute-start.33) | collective-permute-done | bytes 278560 | tf_op jit(solution)/shard_map/ppermute | solution.py:37
  94.8 1.5 collective-permute-start.20
  96.4 3.7 %collective-permute-done.30 = bf16[64,2176]{1,0:T(8,128)(2,1)S(1)} collective-permute-done((bf16[64,2176]{1,0:T(8,128)(2,1)S(1)}, bf16[64,2176]{1,0:T(8,128)(2,1)S(1)}, u32[]{:S(2)}, u32[]{:S(2)}) %collective-permute-start.30) | collective-permute-done | bytes 278560 | tf_op jit(solution)/shard_map/ppermute | solution.py:36
  100.3 2.4 %collective-permute-done.16 = bf16[64,2176]{1,0:T(8,128)(2,1)S(1)} collective-permute-done((bf16[64,2176]{1,0:T(8,128)(2,1)S(1)}, bf16[64,2176]{1,0:T(8,128)(2,1)S(1)}, u32[]{:S(2)}, u32[]{:S(2)}) %collective-permute-start.16) | collective-permute-done | bytes 278560 | tf_op jit(solution)/shard_map/ppermute | solution.py:36
  102.8 2.5 %collective-permute-start.17 = (bf16[64,2176]{1,0:T(8,128)(2,1)S(1)}, bf16[64,2176]{1,0:T(8,128)(2,1)S(1)}, u32[]{:S(2)}, u32[]{:S(2)}) collective-permute-start(bf16[64,2176]{1,0:T(8,128)(2,1)S(1)} %add_convert_fusion.7), channel_id=1, source_target_pairs={{0,7},{1,2},{2,1},{3,4},{4,3},{5,6},{6,5},{7,0},{8,15},{9,10},{10,... | collective-permute-start | bytes 835592 | tf_op jit(solution)/shard_map/ppermute | solution.py:36
  106.1 8.6 %collective-permute-done.31 = bf16[64,2176]{1,0:T(8,128)(2,1)S(1)} collective-permute-done((bf16[64,2176]{1,0:T(8,128)(2,1)S(1)}, bf16[64,2176]{1,0:T(8,128)(2,1)S(1)}, u32[]{:S(2)}, u32[]{:S(2)}) %collective-permute-start.31) | collective-permute-done | bytes 278560 | tf_op jit(solution)/shard_map/ppermute | solution.py:36
  115.1 2.5 %collective-permute-start.36 = (bf16[64,1024]{1,0:T(8,128)(2,1)S(1)}, bf16[64,1024]{1,0:T(8,128)(2,1)S(1)}, u32[]{:S(2)}, u32[]{:S(2)}) collective-permute-start(bf16[64,1024]{1,0:T(8,128)(2,1)S(1)} %fusion.7.refs_0_), channel_id=1, source_target_pairs={{0,7},{1,2},{2,1},{3,4},{4,3},{5,6},{6,5},{7,0},{8,15},{9,10},{10,... | collective-permute-start | bytes 393224 | tf_op jit(solution)/shard_map/ppermute | solution.py:47
  118.4 1.8 collective-permute-done.36.refs_7_
  120.2 1.5 collective-permute-start.21
  121.7 1.4 collective-permute-done.22.refs_7_
  123.1 2.2 %collective-permute-start.38 = (bf16[64,1024]{1,0:T(8,128)(2,1)S(1)}, bf16[64,1024]{1,0:T(8,128)(2,1)S(1)}, u32[]{:S(2)}, u32[]{:S(2)}) collective-permute-start(bf16[64,1024]{1,0:T(8,128)(2,1)S(1)} %collective-permute-done.35.refs_1_), channel_id=1, source_target_pairs={{0,7},{1,2},{2,1},{3,4},{4,3},{5,6},{6,5},{7,0},{8,15},{9,10},{10,... | collective-permute-start | bytes 393224 | tf_op jit(solution)/shard_map/ppermute | solution.py:50
  125.5 2.1 %collective-permute-start.40 = (bf16[64,1024]{1,0:T(8,128)(2,1)S(1)}, bf16[64,1024]{1,0:T(8,128)(2,1)S(1)}, u32[]{:S(2)}, u32[]{:S(2)}) collective-permute-start(bf16[64,1024]{1,0:T(8,128)(2,1)S(1)} %collective-permute-done.37.refs_2_), channel_id=1, source_target_pairs={{0,7},{1,2},{2,1},{3,4},{4,3},{5,6},{6,5},{7,0},{8,15},{9,10},{10,... | collective-permute-start | bytes 393224 | tf_op jit(solution)/shard_map/ppermute | solution.py:47
  128.3 1.4 collective-permute-start.24
  129.8 1.4 collective-permute-done.23.refs_2_
  131.2 1.4 collective-permute-start.26
  132.6 1.5 collective-permute-start.41
  134.2 2.2 %collective-permute-done.26.refs_5_ = bf16[64,1024]{1,0:T(8,128)(2,1)S(1)} collective-permute-done((bf16[64,1024]{1,0:T(8,128)(2,1)S(1)}, bf16[64,1024]{1,0:T(8,128)(2,1)S(1)}, u32[]{:S(2)}, u32[]{:S(2)}) %collective-permute-start.26) | collective-permute-done | bytes 131104 | tf_op jit(solution)/shard_map/ppermute | solution.py:47
  136.7 1.4 collective-permute-done.41.refs_4_
  139.8 2.8 %collective-permute-done.27.refs_4_ = bf16[64,1024]{1,0:T(8,128)(2,1)S(1)} collective-permute-done((bf16[64,1024]{1,0:T(8,128)(2,1)S(1)}, bf16[64,1024]{1,0:T(8,128)(2,1)S(1)}, u32[]{:S(2)}, u32[]{:S(2)}) %collective-permute-start.27) | collective-permute-done | bytes 131104 | tf_op jit(solution)/shard_map/ppermute | solution.py:47
  142.6 1.8 lower_down.5
  144.4 7.8 %all-to-all-start.1 = ((bf16[16,64,512]{2,1,0:T(8,128)(2,1)}), bf16[16,64,512]{2,1,0:T(8,128)(2,1)S(1)}, u32[]{:S(2)}, u32[]{:S(2)}) async-start(bf16[16,64,512]{2,1,0:T(8,128)(2,1)} %bitcast.7), calls=%async_computation.1 | async-start | bytes 2097152 | tf_op jit(solution)/shard_map/all_to_all | solution.py:178
  152.3 1.4 collective-permute-start.8
  153.7 2.7 %collective-permute-done.8.refs_7_ = bf16[16,1024]{1,0:T(8,128)(2,1)S(1)} collective-permute-done((bf16[16,1024]{1,0:T(8,128)(2,1)S(1)}, bf16[16,1024]{1,0:T(8,128)(2,1)S(1)}, u32[]{:S(2)}, u32[]{:S(2)}) %collective-permute-start.8) | collective-permute-done | bytes 32800 | tf_op jit(solution)/shard_map/ppermute | solution.py:47
  156.4 1.4 collective-permute-start.10
  157.8 1.6 collective-permute-done.9.refs_2_
  159.4 1.3 collective-permute-start.12
  160.9 2.8 %collective-permute-done.12.refs_5_ = bf16[16,1024]{1,0:T(8,128)(2,1)S(1)} collective-permute-done((bf16[16,1024]{1,0:T(8,128)(2,1)S(1)}, bf16[16,1024]{1,0:T(8,128)(2,1)S(1)}, u32[]{:S(2)}, u32[]{:S(2)}) %collective-permute-start.12) | collective-permute-done | bytes 32800 | tf_op jit(solution)/shard_map/ppermute | solution.py:47
  163.8 3.0 %collective-permute-done.13.refs_4_ = bf16[16,1024]{1,0:T(8,128)(2,1)S(1)} collective-permute-done((bf16[16,1024]{1,0:T(8,128)(2,1)S(1)}, bf16[16,1024]{1,0:T(8,128)(2,1)S(1)}, u32[]{:S(2)}, u32[]{:S(2)}) %collective-permute-start.13) | collective-permute-done | bytes 32800 | tf_op jit(solution)/shard_map/ppermute | solution.py:47
  167.1 13.3 %all-to-all-done.1 = bf16[16,64,512]{2,1,0:T(8,128)(2,1)S(1)} async-done(((bf16[16,64,512]{2,1,0:T(8,128)(2,1)}), bf16[16,64,512]{2,1,0:T(8,128)(2,1)S(1)}, u32[]{:S(2)}, u32[]{:S(2)}) %all-to-all-start.1) | async-done | bytes 1048608 | tf_op jit(solution)/shard_map/all_to_all | solution.py:178
  181.4 9.0 %all_to_all.15 = f32[8,128,1]{1,2,0:T(1,128)S(1)} all-to-all(f32[8,128,1]{1,2,0:T(1,128)S(1)} %broadcast_in_dim.34), channel_id=1, replica_groups=mesh['grp'=2,'ep'=16,'tp'=8] {'tp'}, dimensions={0} | all-to-all | bytes 8192 | tf_op jit(solution)/shard_map/all_to_all | solution.py:211
  (113 shorter events, 18.6 us)
Async XLA Ops:
  5.5 28.0 %collective-permute-start = (bf16[16,2176]{1,0:T(8,128)(2,1)}, bf16[16,2176]{1,0:T(8,128)(2,1)}, u32[]{:S(2)}, u32[]{:S(2)}) collective-permute-start(bf16[16,2176]{1,0:T(8,128)(2,1)} %get-tuple-element.35), channel_id=1, source_target_pairs={{0,1},{1,0},{2,3},{3,2},{4,5},{5,4},{6,7},{7,6},{8,9},{9,8},{10,11... | collective-permute-start | bytes 208904 | tf_op jit(solution)/shard_map/ppermute | solution.py:30
  7.7 27.0 %collective-permute-start.4 = (bf16[16,2176]{1,0:T(8,128)(2,1)}, bf16[16,2176]{1,0:T(8,128)(2,1)}, u32[]{:S(2)}, u32[]{:S(2)}) collective-permute-start(bf16[16,2176]{1,0:T(8,128)(2,1)} %get-tuple-element.38), channel_id=1, source_target_pairs={{0,1},{1,0},{2,3},{3,2},{4,5},{5,4},{6,7},{7,6},{8,9},{9,8},{10,11... | collective-permute-start | bytes 208904 | tf_op jit(solution)/shard_map/ppermute | solution.py:37
  9.7 52.0 %copy-start.1 = (bf16[1,512,1024]{2,1,0:T(8,128)(2,1)S(1)}, bf16[1,512,1024]{2,1,0:T(8,128)(2,1)}, u32[]{:S(2)}) copy-start(bf16[1,512,1024]{2,1,0:T(8,128)(2,1)} %param.16) | copy-start | bytes 3145732
  9.7 52.0 %all-to-all-start = ((bf16[16,64,512]{2,1,0:T(8,128)(2,1)}), bf16[16,64,512]{2,1,0:T(8,128)(2,1)S(1)}, u32[]{:S(2)}, u32[]{:S(2)}) async-start(bf16[16,64,512]{2,1,0:T(8,128)(2,1)} %bitcast.1), calls=%async_computation | async-start | bytes 2097152 | tf_op jit(solution)/shard_map/all_to_all | solution.py:178
  33.5 28.1 %copy-start = (bf16[1,512,1024]{2,1,0:T(8,128)(2,1)S(1)}, bf16[1,512,1024]{2,1,0:T(8,128)(2,1)}, u32[]{:S(2)}) copy-start(bf16[1,512,1024]{2,1,0:T(8,128)(2,1)} %param.15) | copy-start | bytes 3145732
  34.5 4.8 %collective-permute-start.1 = (bf16[16,2176]{1,0:T(8,128)(2,1)S(1)}, bf16[16,2176]{1,0:T(8,128)(2,1)S(1)}, u32[]{:S(2)}, u32[]{:S(2)}) collective-permute-start(bf16[16,2176]{1,0:T(8,128)(2,1)S(1)} %add_convert_fusion.14), channel_id=1, source_target_pairs={{0,7},{1,2},{2,1},{3,4},{4,3},{5,6},{6,5},{7,0},{8,15},{9,10},{10,... | collective-permute-start | bytes 208904 | tf_op jit(solution)/shard_map/ppermute | solution.py:36
  35.6 5.5 %collective-permute-start.5 = (bf16[16,2176]{1,0:T(8,128)(2,1)S(1)}, bf16[16,2176]{1,0:T(8,128)(2,1)S(1)}, u32[]{:S(2)}, u32[]{:S(2)}) collective-permute-start(bf16[16,2176]{1,0:T(8,128)(2,1)S(1)} %add_convert_fusion.11), channel_id=1, source_target_pairs={{0,7},{1,2},{2,1},{3,4},{4,3},{5,6},{6,5},{7,0},{8,15},{9,10},{10,... | collective-permute-start | bytes 208904 | tf_op jit(solution)/shard_map/ppermute | solution.py:37
  39.4 3.6 %collective-permute-start.2 = (bf16[16,2176]{1,0:T(8,128)(2,1)S(1)}, bf16[16,2176]{1,0:T(8,128)(2,1)S(1)}, u32[]{:S(2)}, u32[]{:S(2)}) collective-permute-start(bf16[16,2176]{1,0:T(8,128)(2,1)S(1)} %add_convert_fusion.13), channel_id=1, source_target_pairs={{0,1},{1,0},{2,3},{3,2},{4,5},{5,4},{6,7},{7,6},{8,9},{9,8},{10,11... | collective-permute-start | bytes 208904 | tf_op jit(solution)/shard_map/ppermute | solution.py:36
  41.1 3.6 %collective-permute-start.6 = (bf16[16,2176]{1,0:T(8,128)(2,1)S(1)}, bf16[16,2176]{1,0:T(8,128)(2,1)S(1)}, u32[]{:S(2)}, u32[]{:S(2)}) collective-permute-start(bf16[16,2176]{1,0:T(8,128)(2,1)S(1)} %add_convert_fusion.10), channel_id=1, source_target_pairs={{0,1},{1,0},{2,3},{3,2},{4,5},{5,4},{6,7},{7,6},{8,9},{9,8},{10,11... | collective-permute-start | bytes 208904 | tf_op jit(solution)/shard_map/ppermute | solution.py:37
  43.0 4.8 %collective-permute-start.3 = (bf16[16,2176]{1,0:T(8,128)(2,1)S(1)}, bf16[16,2176]{1,0:T(8,128)(2,1)S(1)}, u32[]{:S(2)}, u32[]{:S(2)}) collective-permute-start(bf16[16,2176]{1,0:T(8,128)(2,1)S(1)} %add_convert_fusion.12), channel_id=1, source_target_pairs={{0,7},{1,2},{2,1},{3,4},{4,3},{5,6},{6,5},{7,0},{8,15},{9,10},{10,... | collective-permute-start | bytes 208904 | tf_op jit(solution)/shard_map/ppermute | solution.py:36
  63.3 10.0 %collective-permute-start.28 = (bf16[64,2176]{1,0:T(8,128)(2,1)S(1)}, bf16[64,2176]{1,0:T(8,128)(2,1)S(1)}, u32[]{:S(2)}, u32[]{:S(2)}) collective-permute-start(bf16[64,2176]{1,0:T(8,128)(2,1)S(1)} %get-tuple-element.53), channel_id=1, source_target_pairs={{0,7},{1,2},{2,1},{3,4},{4,3},{5,6},{6,5},{7,0},{8,15},{9,10},{10,... | collective-permute-start | bytes 835592 | tf_op jit(solution)/shard_map/ppermute | solution.py:30
  65.1 13.1 %collective-permute-start.32 = (bf16[64,2176]{1,0:T(8,128)(2,1)S(1)}, bf16[64,2176]{1,0:T(8,128)(2,1)S(1)}, u32[]{:S(2)}, u32[]{:S(2)}) collective-permute-start(bf16[64,2176]{1,0:T(8,128)(2,1)S(1)} %get-tuple-element.56), channel_id=1, source_target_pairs={{0,7},{1,2},{2,1},{3,4},{4,3},{5,6},{6,5},{7,0},{8,15},{9,10},{10,... | collective-permute-start | bytes 835592 | tf_op jit(solution)/shard_map/ppermute | solution.py:37
  67.9 10.5 %collective-permute-start.14 = (bf16[64,2176]{1,0:T(8,128)(2,1)S(1)}, bf16[64,2176]{1,0:T(8,128)(2,1)S(1)}, u32[]{:S(2)}, u32[]{:S(2)}) collective-permute-start(bf16[64,2176]{1,0:T(8,128)(2,1)S(1)} %get-tuple-element.45), channel_id=1, source_target_pairs={{0,1},{1,0},{2,3},{3,2},{4,5},{5,4},{6,7},{7,6},{8,9},{9,8},{10,11... | collective-permute-start | bytes 835592 | tf_op jit(solution)/shard_map/ppermute | solution.py:30
  67.9 14.6 %collective-permute-start.18 = (bf16[64,2176]{1,0:T(8,128)(2,1)S(1)}, bf16[64,2176]{1,0:T(8,128)(2,1)S(1)}, u32[]{:S(2)}, u32[]{:S(2)}) collective-permute-start(bf16[64,2176]{1,0:T(8,128)(2,1)S(1)} %get-tuple-element.48), channel_id=1, source_target_pairs={{0,1},{1,0},{2,3},{3,2},{4,5},{5,4},{6,7},{7,6},{8,9},{9,8},{10,11... | collective-permute-start | bytes 835592 | tf_op jit(solution)/shard_map/ppermute | solution.py:37
  73.4 15.1 %collective-permute-start.29 = (bf16[64,2176]{1,0:T(8,128)(2,1)S(1)}, bf16[64,2176]{1,0:T(8,128)(2,1)S(1)}, u32[]{:S(2)}, u32[]{:S(2)}) collective-permute-start(bf16[64,2176]{1,0:T(8,128)(2,1)S(1)} %add_convert_fusion.4), channel_id=1, source_target_pairs={{0,1},{1,0},{2,3},{3,2},{4,5},{5,4},{6,7},{7,6},{8,9},{9,8},{10,11... | collective-permute-start | bytes 835592 | tf_op jit(solution)/shard_map/ppermute | solution.py:36
  78.3 16.0 %collective-permute-start.33 = (bf16[64,2176]{1,0:T(8,128)(2,1)S(1)}, bf16[64,2176]{1,0:T(8,128)(2,1)S(1)}, u32[]{:S(2)}, u32[]{:S(2)}) collective-permute-start(bf16[64,2176]{1,0:T(8,128)(2,1)S(1)} %add_convert_fusion.1), channel_id=1, source_target_pairs={{0,1},{1,0},{2,3},{3,2},{4,5},{5,4},{6,7},{7,6},{8,9},{9,8},{10,11... | collective-permute-start | bytes 835592 | tf_op jit(solution)/shard_map/ppermute | solution.py:37
  78.5 16.0 %collective-permute-start.15 = (bf16[64,2176]{1,0:T(8,128)(2,1)S(1)}, bf16[64,2176]{1,0:T(8,128)(2,1)S(1)}, u32[]{:S(2)}, u32[]{:S(2)}) collective-permute-start(bf16[64,2176]{1,0:T(8,128)(2,1)S(1)} %add_convert_fusion.9), channel_id=1, source_target_pairs={{0,7},{1,2},{2,1},{3,4},{4,3},{5,6},{6,5},{7,0},{8,15},{9,10},{10,... | collective-permute-start | bytes 835592 | tf_op jit(solution)/shard_map/ppermute | solution.py:36
  82.6 12.1 %collective-permute-start.19 = (bf16[64,2176]{1,0:T(8,128)(2,1)S(1)}, bf16[64,2176]{1,0:T(8,128)(2,1)S(1)}, u32[]{:S(2)}, u32[]{:S(2)}) collective-permute-start(bf16[64,2176]{1,0:T(8,128)(2,1)S(1)} %add_convert_fusion.6), channel_id=1, source_target_pairs={{0,7},{1,2},{2,1},{3,4},{4,3},{5,6},{6,5},{7,0},{8,15},{9,10},{10,... | collective-permute-start | bytes 835592 | tf_op jit(solution)/shard_map/ppermute | solution.py:37
  88.6 11.5 %collective-permute-start.30 = (bf16[64,2176]{1,0:T(8,128)(2,1)S(1)}, bf16[64,2176]{1,0:T(8,128)(2,1)S(1)}, u32[]{:S(2)}, u32[]{:S(2)}) collective-permute-start(bf16[64,2176]{1,0:T(8,128)(2,1)S(1)} %add_convert_fusion.3), channel_id=1, source_target_pairs={{0,7},{1,2},{2,1},{3,4},{4,3},{5,6},{6,5},{7,0},{8,15},{9,10},{10,... | collective-permute-start | bytes 835592 | tf_op jit(solution)/shard_map/ppermute | solution.py:36
  94.3 11.7 %collective-permute-start.34 = (bf16[64,2176]{1,0:T(8,128)(2,1)S(1)}, bf16[64,2176]{1,0:T(8,128)(2,1)S(1)}, u32[]{:S(2)}, u32[]{:S(2)}) collective-permute-start(bf16[64,2176]{1,0:T(8,128)(2,1)S(1)} %add_convert_fusion), channel_id=1, source_target_pairs={{0,7},{1,2},{2,1},{3,4},{4,3},{5,6},{6,5},{7,0},{8,15},{9,10},{10,... | collective-permute-start | bytes 835592 | tf_op jit(solution)/shard_map/ppermute | solution.py:37
  94.6 8.2 %collective-permute-start.16 = (bf16[64,2176]{1,0:T(8,128)(2,1)S(1)}, bf16[64,2176]{1,0:T(8,128)(2,1)S(1)}, u32[]{:S(2)}, u32[]{:S(2)}) collective-permute-start(bf16[64,2176]{1,0:T(8,128)(2,1)S(1)} %add_convert_fusion.8), channel_id=1, source_target_pairs={{0,1},{1,0},{2,3},{3,2},{4,5},{5,4},{6,7},{7,6},{8,9},{9,8},{10,11... | collective-permute-start | bytes 835592 | tf_op jit(solution)/shard_map/ppermute | solution.py:36
  94.8 22.8 %collective-permute-start.20 = (bf16[64,2176]{1,0:T(8,128)(2,1)S(1)}, bf16[64,2176]{1,0:T(8,128)(2,1)S(1)}, u32[]{:S(2)}, u32[]{:S(2)}) collective-permute-start(bf16[64,2176]{1,0:T(8,128)(2,1)S(1)} %add_convert_fusion.5), channel_id=1, source_target_pairs={{0,1},{1,0},{2,3},{3,2},{4,5},{5,4},{6,7},{7,6},{8,9},{9,8},{10,11... | collective-permute-start | bytes 835592 | tf_op jit(solution)/shard_map/ppermute | solution.py:37
  100.2 14.5 %collective-permute-start.31 = (bf16[64,2176]{1,0:T(8,128)(2,1)S(1)}, bf16[64,2176]{1,0:T(8,128)(2,1)S(1)}, u32[]{:S(2)}, u32[]{:S(2)}) collective-permute-start(bf16[64,2176]{1,0:T(8,128)(2,1)S(1)} %add_convert_fusion.2), channel_id=1, source_target_pairs={{0,1},{1,0},{2,3},{3,2},{4,5},{5,4},{6,7},{7,6},{8,9},{9,8},{10,11... | collective-permute-start | bytes 835592 | tf_op jit(solution)/shard_map/ppermute | solution.py:36
  102.8 14.7 %collective-permute-start.17 = (bf16[64,2176]{1,0:T(8,128)(2,1)S(1)}, bf16[64,2176]{1,0:T(8,128)(2,1)S(1)}, u32[]{:S(2)}, u32[]{:S(2)}) collective-permute-start(bf16[64,2176]{1,0:T(8,128)(2,1)S(1)} %add_convert_fusion.7), channel_id=1, source_target_pairs={{0,7},{1,2},{2,1},{3,4},{4,3},{5,6},{6,5},{7,0},{8,15},{9,10},{10,... | collective-permute-start | bytes 835592 | tf_op jit(solution)/shard_map/ppermute | solution.py:36
  115.1 23.0 %copy-start.2 = (bf16[1,1024,512]{2,1,0:T(8,128)(2,1)S(1)}, bf16[1,1024,512]{2,1,0:T(8,128)(2,1)}, u32[]{:S(2)}) copy-start(bf16[1,1024,512]{2,1,0:T(8,128)(2,1)} %param.17) | copy-start | bytes 3145732
  115.1 5.2 %collective-permute-start.36 = (bf16[64,1024]{1,0:T(8,128)(2,1)S(1)}, bf16[64,1024]{1,0:T(8,128)(2,1)S(1)}, u32[]{:S(2)}, u32[]{:S(2)}) collective-permute-start(bf16[64,1024]{1,0:T(8,128)(2,1)S(1)} %fusion.7.refs_0_), channel_id=1, source_target_pairs={{0,7},{1,2},{2,1},{3,4},{4,3},{5,6},{6,5},{7,0},{8,15},{9,10},{10,... | collective-permute-start | bytes 393224 | tf_op jit(solution)/shard_map/ppermute | solution.py:47
  117.9 5.2 %collective-permute-start.22 = (bf16[64,1024]{1,0:T(8,128)(2,1)S(1)}, bf16[64,1024]{1,0:T(8,128)(2,1)S(1)}, u32[]{:S(2)}, u32[]{:S(2)}) collective-permute-start(bf16[64,1024]{1,0:T(8,128)(2,1)S(1)} %fusion.9.refs_0_), channel_id=1, source_target_pairs={{0,7},{1,2},{2,1},{3,4},{4,3},{5,6},{6,5},{7,0},{8,15},{9,10},{10,... | collective-permute-start | bytes 393224 | tf_op jit(solution)/shard_map/ppermute | solution.py:47
  118.4 4.7 %collective-permute-start.35 = (bf16[64,1024]{1,0:T(8,128)(2,1)S(1)}, bf16[64,1024]{1,0:T(8,128)(2,1)S(1)}, u32[]{:S(2)}, u32[]{:S(2)}) collective-permute-start(bf16[64,1024]{1,0:T(8,128)(2,1)S(1)} %fusion.7.refs_0_), channel_id=1, source_target_pairs={{0,1},{1,0},{2,3},{3,2},{4,5},{5,4},{6,7},{7,6},{8,9},{9,8},{10,11... | collective-permute-start | bytes 393224 | tf_op jit(solution)/shard_map/ppermute | solution.py:50
  120.2 5.3 %collective-permute-start.37 = (bf16[64,1024]{1,0:T(8,128)(2,1)S(1)}, bf16[64,1024]{1,0:T(8,128)(2,1)S(1)}, u32[]{:S(2)}, u32[]{:S(2)}) collective-permute-start(bf16[64,1024]{1,0:T(8,128)(2,1)S(1)} %collective-permute-done.36.refs_7_), channel_id=1, source_target_pairs={{0,1},{1,0},{2,3},{3,2},{4,5},{5,4},{6,7},{7,6},{8,9},{9,8},{10,11... | collective-permute-start | bytes 393224 | tf_op jit(solution)/shard_map/ppermute | solution.py:47
  120.2 8.1 %collective-permute-start.21 = (bf16[64,1024]{1,0:T(8,128)(2,1)S(1)}, bf16[64,1024]{1,0:T(8,128)(2,1)S(1)}, u32[]{:S(2)}, u32[]{:S(2)}) collective-permute-start(bf16[64,1024]{1,0:T(8,128)(2,1)S(1)} %fusion.9.refs_0_), channel_id=1, source_target_pairs={{0,1},{1,0},{2,3},{3,2},{4,5},{5,4},{6,7},{7,6},{8,9},{9,8},{10,11... | collective-permute-start | bytes 393224 | tf_op jit(solution)/shard_map/ppermute | solution.py:50
  123.1 8.0 %collective-permute-start.23 = (bf16[64,1024]{1,0:T(8,128)(2,1)S(1)}, bf16[64,1024]{1,0:T(8,128)(2,1)S(1)}, u32[]{:S(2)}, u32[]{:S(2)}) collective-permute-start(bf16[64,1024]{1,0:T(8,128)(2,1)S(1)} %collective-permute-done.22.refs_7_), channel_id=1, source_target_pairs={{0,1},{1,0},{2,3},{3,2},{4,5},{5,4},{6,7},{7,6},{8,9},{9,8},{10,11... | collective-permute-start | bytes 393224 | tf_op jit(solution)/shard_map/ppermute | solution.py:47
  123.1 9.5 %collective-permute-start.38 = (bf16[64,1024]{1,0:T(8,128)(2,1)S(1)}, bf16[64,1024]{1,0:T(8,128)(2,1)S(1)}, u32[]{:S(2)}, u32[]{:S(2)}) collective-permute-start(bf16[64,1024]{1,0:T(8,128)(2,1)S(1)} %collective-permute-done.35.refs_1_), channel_id=1, source_target_pairs={{0,7},{1,2},{2,1},{3,4},{4,3},{5,6},{6,5},{7,0},{8,15},{9,10},{10,... | collective-permute-start | bytes 393224 | tf_op jit(solution)/shard_map/ppermute | solution.py:50
  125.5 7.0 %collective-permute-start.40 = (bf16[64,1024]{1,0:T(8,128)(2,1)S(1)}, bf16[64,1024]{1,0:T(8,128)(2,1)S(1)}, u32[]{:S(2)}, u32[]{:S(2)}) collective-permute-start(bf16[64,1024]{1,0:T(8,128)(2,1)S(1)} %collective-permute-done.37.refs_2_), channel_id=1, source_target_pairs={{0,7},{1,2},{2,1},{3,4},{4,3},{5,6},{6,5},{7,0},{8,15},{9,10},{10,... | collective-permute-start | bytes 393224 | tf_op jit(solution)/shard_map/ppermute | solution.py:47
  128.3 5.7 %collective-permute-start.24 = (bf16[64,1024]{1,0:T(8,128)(2,1)S(1)}, bf16[64,1024]{1,0:T(8,128)(2,1)S(1)}, u32[]{:S(2)}, u32[]{:S(2)}) collective-permute-start(bf16[64,1024]{1,0:T(8,128)(2,1)S(1)} %collective-permute-done.21.refs_1_), channel_id=1, source_target_pairs={{0,7},{1,2},{2,1},{3,4},{4,3},{5,6},{6,5},{7,0},{8,15},{9,10},{10,... | collective-permute-start | bytes 393224 | tf_op jit(solution)/shard_map/ppermute | solution.py:50
  131.2 5.2 %collective-permute-start.26 = (bf16[64,1024]{1,0:T(8,128)(2,1)S(1)}, bf16[64,1024]{1,0:T(8,128)(2,1)S(1)}, u32[]{:S(2)}, u32[]{:S(2)}) collective-permute-start(bf16[64,1024]{1,0:T(8,128)(2,1)S(1)} %collective-permute-done.23.refs_2_), channel_id=1, source_target_pairs={{0,7},{1,2},{2,1},{3,4},{4,3},{5,6},{6,5},{7,0},{8,15},{9,10},{10,... | collective-permute-start | bytes 393224 | tf_op jit(solution)/shard_map/ppermute | solution.py:47
  132.6 4.1 %collective-permute-start.39 = (bf16[64,1024]{1,0:T(8,128)(2,1)S(1)}, bf16[64,1024]{1,0:T(8,128)(2,1)S(1)}, u32[]{:S(2)}, u32[]{:S(2)}) collective-permute-start(bf16[64,1024]{1,0:T(8,128)(2,1)S(1)} %collective-permute-done.38.refs_6_), channel_id=1, source_target_pairs={{0,1},{1,0},{2,3},{3,2},{4,5},{5,4},{6,7},{7,6},{8,9},{9,8},{10,11... | collective-permute-start | bytes 393224 | tf_op jit(solution)/shard_map/ppermute | solution.py:50
  132.6 5.5 %collective-permute-start.41 = (bf16[64,1024]{1,0:T(8,128)(2,1)S(1)}, bf16[64,1024]{1,0:T(8,128)(2,1)S(1)}, u32[]{:S(2)}, u32[]{:S(2)}) collective-permute-start(bf16[64,1024]{1,0:T(8,128)(2,1)S(1)} %collective-permute-done.40.refs_5_), channel_id=1, source_target_pairs={{0,1},{1,0},{2,3},{3,2},{4,5},{5,4},{6,7},{7,6},{8,9},{9,8},{10,11... | collective-permute-start | bytes 393224 | tf_op jit(solution)/shard_map/ppermute | solution.py:47
  134.0 5.8 %collective-permute-start.25 = (bf16[64,1024]{1,0:T(8,128)(2,1)S(1)}, bf16[64,1024]{1,0:T(8,128)(2,1)S(1)}, u32[]{:S(2)}, u32[]{:S(2)}) collective-permute-start(bf16[64,1024]{1,0:T(8,128)(2,1)S(1)} %collective-permute-done.24.refs_6_), channel_id=1, source_target_pairs={{0,1},{1,0},{2,3},{3,2},{4,5},{5,4},{6,7},{7,6},{8,9},{9,8},{10,11... | collective-permute-start | bytes 393224 | tf_op jit(solution)/shard_map/ppermute | solution.py:50
  136.4 6.2 %collective-permute-start.27 = (bf16[64,1024]{1,0:T(8,128)(2,1)S(1)}, bf16[64,1024]{1,0:T(8,128)(2,1)S(1)}, u32[]{:S(2)}, u32[]{:S(2)}) collective-permute-start(bf16[64,1024]{1,0:T(8,128)(2,1)S(1)} %collective-permute-done.26.refs_5_), channel_id=1, source_target_pairs={{0,1},{1,0},{2,3},{3,2},{4,5},{5,4},{6,7},{7,6},{8,9},{9,8},{10,11... | collective-permute-start | bytes 393224 | tf_op jit(solution)/shard_map/ppermute | solution.py:47
  144.4 36.0 %all-to-all-start.1 = ((bf16[16,64,512]{2,1,0:T(8,128)(2,1)}), bf16[16,64,512]{2,1,0:T(8,128)(2,1)S(1)}, u32[]{:S(2)}, u32[]{:S(2)}) async-start(bf16[16,64,512]{2,1,0:T(8,128)(2,1)} %bitcast.7), calls=%async_computation.1 | async-start | bytes 2097152 | tf_op jit(solution)/shard_map/all_to_all | solution.py:178
  152.3 28.1 %copy-start.10 = (pred[128,1024]{1,0:T(32,128)(4,1)S(1)}, pred[128,1024]{1,0:T(32,128)(4,1)}, u32[]{:S(2)}) copy-start(pred[128,1024]{1,0:T(32,128)(4,1)} %copy-done.9) | copy-start | bytes 393220
  152.3 4.1 %collective-permute-start.8 = (bf16[16,1024]{1,0:T(8,128)(2,1)S(1)}, bf16[16,1024]{1,0:T(8,128)(2,1)S(1)}, u32[]{:S(2)}, u32[]{:S(2)}) collective-permute-start(bf16[16,1024]{1,0:T(8,128)(2,1)S(1)} %fusion.13.refs_0_), channel_id=1, source_target_pairs={{0,7},{1,2},{2,1},{3,4},{4,3},{5,6},{6,5},{7,0},{8,15},{9,10},{10,... | collective-permute-start | bytes 98312 | tf_op jit(solution)/shard_map/ppermute | solution.py:47
  153.7 2.8 %collective-permute-start.7 = (bf16[16,1024]{1,0:T(8,128)(2,1)S(1)}, bf16[16,1024]{1,0:T(8,128)(2,1)S(1)}, u32[]{:S(2)}, u32[]{:S(2)}) collective-permute-start(bf16[16,1024]{1,0:T(8,128)(2,1)S(1)} %fusion.13.refs_0_), channel_id=1, source_target_pairs={{0,1},{1,0},{2,3},{3,2},{4,5},{5,4},{6,7},{7,6},{8,9},{9,8},{10,11... | collective-permute-start | bytes 98312 | tf_op jit(solution)/shard_map/ppermute | solution.py:50
  156.4 3.1 %collective-permute-start.9 = (bf16[16,1024]{1,0:T(8,128)(2,1)S(1)}, bf16[16,1024]{1,0:T(8,128)(2,1)S(1)}, u32[]{:S(2)}, u32[]{:S(2)}) collective-permute-start(bf16[16,1024]{1,0:T(8,128)(2,1)S(1)} %collective-permute-done.8.refs_7_), channel_id=1, source_target_pairs={{0,1},{1,0},{2,3},{3,2},{4,5},{5,4},{6,7},{7,6},{8,9},{9,8},{10,11... | collective-permute-start | bytes 98312 | tf_op jit(solution)/shard_map/ppermute | solution.py:47
  156.4 4.3 %collective-permute-start.10 = (bf16[16,1024]{1,0:T(8,128)(2,1)S(1)}, bf16[16,1024]{1,0:T(8,128)(2,1)S(1)}, u32[]{:S(2)}, u32[]{:S(2)}) collective-permute-start(bf16[16,1024]{1,0:T(8,128)(2,1)S(1)} %collective-permute-done.7.refs_1_), channel_id=1, source_target_pairs={{0,7},{1,2},{2,1},{3,4},{4,3},{5,6},{6,5},{7,0},{8,15},{9,10},{10,... | collective-permute-start | bytes 98312 | tf_op jit(solution)/shard_map/ppermute | solution.py:50
  159.4 4.3 %collective-permute-start.12 = (bf16[16,1024]{1,0:T(8,128)(2,1)S(1)}, bf16[16,1024]{1,0:T(8,128)(2,1)S(1)}, u32[]{:S(2)}, u32[]{:S(2)}) collective-permute-start(bf16[16,1024]{1,0:T(8,128)(2,1)S(1)} %collective-permute-done.9.refs_2_), channel_id=1, source_target_pairs={{0,7},{1,2},{2,1},{3,4},{4,3},{5,6},{6,5},{7,0},{8,15},{9,10},{10,... | collective-permute-start | bytes 98312 | tf_op jit(solution)/shard_map/ppermute | solution.py:47
  160.7 3.1 %collective-permute-start.11 = (bf16[16,1024]{1,0:T(8,128)(2,1)S(1)}, bf16[16,1024]{1,0:T(8,128)(2,1)S(1)}, u32[]{:S(2)}, u32[]{:S(2)}) collective-permute-start(bf16[16,1024]{1,0:T(8,128)(2,1)S(1)} %collective-permute-done.10.refs_6_), channel_id=1, source_target_pairs={{0,1},{1,0},{2,3},{3,2},{4,5},{5,4},{6,7},{7,6},{8,9},{9,8},{10,11... | collective-permute-start | bytes 98312 | tf_op jit(solution)/shard_map/ppermute | solution.py:50
  163.7 3.1 %collective-permute-start.13 = (bf16[16,1024]{1,0:T(8,128)(2,1)S(1)}, bf16[16,1024]{1,0:T(8,128)(2,1)S(1)}, u32[]{:S(2)}, u32[]{:S(2)}) collective-permute-start(bf16[16,1024]{1,0:T(8,128)(2,1)S(1)} %collective-permute-done.12.refs_5_), channel_id=1, source_target_pairs={{0,1},{1,0},{2,3},{3,2},{4,5},{5,4},{6,7},{7,6},{8,9},{9,8},{10,11... | collective-permute-start | bytes 98312 | tf_op jit(solution)/shard_map/ppermute | solution.py:47
  (10 other events, 67.8 us)
